TPU v7x, 32 devices: a whole 2x2x4 slice. The times are simulated.
32 devices in a mesh: grp: 2 (over y), sp: 4 (over z), tp: 4 (over x, core).
Axes of the slice: x: 2, y: 2, z: 4, core: 2. Of those that a mesh axis runs over, the one named last changes fastest.
Arguments:
- hidden_in: bfloat16 [2048, 2048], P(('grp', 'sp'), 'tp'), parts along dimension 0, may hold values from -40 to 40
- norm_gain: float32 [3, 2048], replicated, may hold values from 0.1 to 1.9
- query_weight: bfloat16 [3, 1024, 2048], P(None, 'tp'), may hold values from -6 to 6
- key_weight: bfloat16 [3, 1024, 2048], P(None, 'tp'), may hold values from -6 to 6
- value_weight: bfloat16 [3, 1024, 2048], P(None, 'tp'), may hold values from -0.125 to 0.125
- output_weight: bfloat16 [3, 1024, 2048], P(None, None, 'tp'), may hold values from -0.75 to 0.75
- offset_bias: float32 [3, 16, 15, 31], P(None, 'tp'), may hold values from -4 to 4
Outputs:
- hidden_out: bfloat16 [2048, 2048], P(('grp', 'sp'), 'tp'), parts along dimension 0
There are 2 independent parts, one for each index of `grp`. A program takes and returns all parts, laid end to end along the dimension named above; an argument that names none is the same for every part. Nothing has to cross between parts.
All inputs are finite; a program needn't handle non-finite values.
Results may differ from a plain program's by a relative error of at most 0.028.
Values may be sent and summed in bfloat16 or wider, within the bound.
No kernel may reach another device: no remote copies, remote signals or barrier semaphores. Data moves between devices by JAX's collectives and lax.ppermute only.
A program may use at most 64 MiB of HBM per device.

v0:
```python
from functools import partial

import jax
import jax.numpy as jnp
import numpy as np
from jax import lax
from jax.experimental import pallas as pl
from jax.experimental.pallas import tpu as pltpu
from jax.sharding import PartitionSpec as P

HEAD_DIM = 64
GRID_W = 64
ROW_SPAN = 8
COL_SPAN = 16
LAYERS = 3
HALF = ROW_SPAN // 2

EPS = 1e-06
NEG = -1e30
LANES = 128
F32 = jnp.float32
BF16 = jnp.bfloat16

VMEM = pl.BlockSpec(memory_space=pltpu.VMEM)
SMEM = pl.BlockSpec(memory_space=pltpu.SMEM)


def nt_dot(left, right):
    return lax.dot_general(left, right, (((1,), (1,)), ((), ())), preferred_element_type=F32)


def cost(flops, bytes_accessed, transcendentals=0):
    return pl.CostEstimate(
        flops=int(flops), bytes_accessed=int(bytes_accessed), transcendentals=int(transcendentals)
    )


def project_kernel(parts_n, first, last, full_width, where, *refs):
    sources = refs[:parts_n]
    refs = refs[parts_n:]
    gains, refs = refs[:parts_n], refs[parts_n:]
    weights, refs = refs[: 3 * parts_n], refs[3 * parts_n :]
    if not first:
        (acc_in, sq_in), refs = refs[:2], refs[2:]
    totals = [None, None, None]
    squares = None
    for at in range(parts_n):
        wide = sources[at][...].astype(F32)
        square = jnp.sum(wide * wide, axis=1, keepdims=True)
        squares = square if squares is None else squares + square
        scaled = (wide * gains[at][0]).astype(BF16)
        for kind in range(3):
            product = nt_dot(scaled, weights[3 * at + kind][0])
            totals[kind] = product if totals[kind] is None else totals[kind] + product
    if not first:
        squares = squares + sq_in[:, :1]
        totals = [totals[kind] + acc_in[kind] for kind in range(3)]
    if last:
        query_ref, pair_ref = refs
        row_scale = lax.rsqrt(squares * (1.0 / full_width) + EPS)
        query_ref[...] = (totals[0] * (row_scale * HEAD_DIM ** (-0.5))).astype(BF16)
        pair_ref[0] = (totals[1] * row_scale).astype(BF16)
        pair_ref[1] = (totals[2] * row_scale).astype(BF16)
    else:
        acc_out, sq_out = refs
        for kind in range(3):
            acc_out[kind] = totals[kind]
        sq_out[...] = jnp.broadcast_to(squares, sq_out.shape)


def project(parts, places, carried, last, layer, gain, weights):
    tok = parts[0].shape[0]
    width = parts[0].shape[1]
    channels = weights[0].shape[1]
    full = weights[0].shape[2]
    parts_n = len(parts)
    first = carried is None
    whole = lambda shape: pl.BlockSpec(shape, lambda i, s: (0,) * len(shape))
    in_specs = [whole(part.shape) for part in parts]
    in_specs += [
        pl.BlockSpec((1, 1, width), lambda i, s, at=at: (layer, 0, s[at])) for at in range(parts_n)
    ]
    operands = list(parts) + [gain] * parts_n
    for at in range(parts_n):
        for weight in weights:
            in_specs.append(
                pl.BlockSpec((1, channels, width), lambda i, s, at=at: (layer, 0, s[at]))
            )
            operands.append(weight)
    if not first:
        in_specs += [whole(part.shape) for part in carried]
        operands += list(carried)
    if last:
        out_shape = (
            jax.ShapeDtypeStruct((tok, channels), BF16),
            jax.ShapeDtypeStruct((2, tok, channels), BF16),
        )
    else:
        out_shape = (
            jax.ShapeDtypeStruct((3, tok, channels), F32),
            jax.ShapeDtypeStruct((tok, LANES), F32),
        )
    flops = 2 * tok * width * channels * 3 * parts_n
    return pl.pallas_call(
        partial(project_kernel, parts_n, first, last, full),
        out_shape=out_shape,
        grid_spec=pltpu.PrefetchScalarGridSpec(
            num_scalar_prefetch=1,
            grid=(1,),
            in_specs=in_specs,
            out_specs=[whole(shape.shape) for shape in out_shape],
        ),
        cost_estimate=cost(flops, parts_n * width * (channels * 6 + tok * 2) + 4 * tok * channels),
        name=f"project_{layer}_{parts_n}_{int(last)}",
    )(places, *operands)


def emit_kernel(parts_n, where, *refs):
    sources, refs = refs[:parts_n], refs[parts_n:]
    weights, refs = refs[:parts_n], refs[parts_n:]
    base_ref, out_ref = refs
    total = base_ref[...].astype(F32)
    for at in range(parts_n):
        total = total + jnp.dot(sources[at][...], weights[at][0], preferred_element_type=F32)
    out_ref[...] = total.astype(out_ref.dtype)


def emit(parts, places, base, out_type, layer, weight):
    tok, width = parts[0].shape
    cols = weight.shape[2]
    parts_n = len(parts)
    whole = lambda shape: pl.BlockSpec(shape, lambda i, s: (0,) * len(shape))
    in_specs = [whole(part.shape) for part in parts]
    in_specs += [
        pl.BlockSpec((1, width, cols), lambda i, s, at=at: (layer, s[at], 0)) for at in range(parts_n)
    ]
    in_specs.append(whole(base.shape))
    return pl.pallas_call(
        partial(emit_kernel, parts_n),
        out_shape=jax.ShapeDtypeStruct((tok, cols), out_type),
        grid_spec=pltpu.PrefetchScalarGridSpec(
            num_scalar_prefetch=1,
            grid=(1,),
            in_specs=in_specs,
            out_specs=whole((tok, cols)),
        ),
        cost_estimate=cost(
            2 * tok * width * cols * parts_n, parts_n * width * (cols + tok) * 2 + tok * cols * 6
        ),
        name=f"emit_{layer}_{parts_n}",
    )(places, *parts, *([weight] * parts_n), base)


def bias_kernel(rows_ref, out_ref):
    heads_n, spans = out_ref.shape[:2]
    shape = (GRID_W, LANES)
    query_col = lax.broadcasted_iota(jnp.int32, shape, 0)
    key_col = lax.broadcasted_iota(jnp.int32, shape, 1) % GRID_W
    first_col = jnp.clip(query_col - COL_SPAN // 2, 0, GRID_W - COL_SPAN)
    inside = (key_col >= first_col) & (key_col < first_col + COL_SPAN)
    for head in range(heads_n):
        for span in range(spans):
            row = jnp.broadcast_to(rows_ref[head, span : span + 1, :], shape)
            turned = pltpu.roll(row, LANES - (COL_SPAN - 1), axis=1, stride=1, stride_axis=0)
            out_ref[head, span] = jnp.where(inside, turned, NEG)


def expand_bias(table):
    heads_n, offsets, cols = table.shape
    padded = jnp.pad(table, ((0, 0), (0, 0), (0, GRID_W - cols)))
    rows = jnp.concatenate([padded[:, :-1], padded[:, 1:]], axis=2)
    spans = offsets - 1
    return pl.pallas_call(
        bias_kernel,
        out_shape=jax.ShapeDtypeStruct((heads_n, spans, GRID_W, LANES), F32),
        in_specs=[VMEM],
        out_specs=VMEM,
        cost_estimate=cost(heads_n * spans * GRID_W * LANES * 40, heads_n * spans * GRID_W * LANES * 4),
        name="expand_bias",
    )(rows)


def attend_kernel(
    rows_dev, where_ref, query_ref, own_ref, even_ref, odd_ref, bias_ref, out_ref, keys, values
):
    channels = query_ref.shape[1]
    group = min(LANES, channels)
    heads_in = group // HEAD_DIM
    span = ROW_SPAN * GRID_W
    low_slot, high_slot = 0, HALF + rows_dev
    even_slot = pl.multiple_of(where_ref[0] * GRID_W, GRID_W)
    odd_slot = pl.multiple_of(where_ref[1] * GRID_W, GRID_W)
    halo = HALF * GRID_W
    for scratch, kind in ((keys, 0), (values, 1)):
        scratch[HALF * GRID_W : (HALF + rows_dev) * GRID_W, :] = own_ref[kind]
        scratch[pl.ds(even_slot, halo), :] = even_ref[kind]
        scratch[pl.ds(odd_slot, halo), :] = odd_ref[kind]
    lane = lax.broadcasted_iota(jnp.int32, (GRID_W, group), 1)
    ones = jnp.ones((span, group), BF16)
    for row in range(rows_dev):
        first = pl.multiple_of(where_ref[2 + row] * GRID_W, GRID_W)
        offset = where_ref[2 + rows_dev + row]
        for pair in range(channels // group):
            cols = slice(pair * group, (pair + 1) * group)
            query = query_ref[row * GRID_W : (row + 1) * GRID_W, cols]
            if heads_in > 1:
                zero = jnp.zeros_like(query)
                query = jnp.concatenate(
                    [
                        jnp.where(lane // HEAD_DIM == head, query, zero)
                        for head in range(heads_in)
                    ],
                    axis=0,
                )
            scores = nt_dot(query, keys[pl.ds(first, span), cols])
            pieces = []
            for at in range(span // LANES):
                bias = jnp.concatenate(
                    [
                        bias_ref[pair * heads_in + head, offset + (LANES // GRID_W) * at]
                        for head in range(heads_in)
                    ],
                    axis=0,
                )
                pieces.append(scores[:, at * LANES : (at + 1) * LANES] + bias)
            peak = pieces[0]
            for piece in pieces[1:]:
                peak = jnp.maximum(peak, piece)
            peak = jnp.max(peak, axis=1, keepdims=True)
            lifted = jnp.concatenate([jnp.exp(piece - peak).astype(BF16) for piece in pieces], axis=1)
            mixed = jnp.dot(lifted, values[pl.ds(first, span), cols], preferred_element_type=F32)
            weight = jnp.dot(lifted, ones, preferred_element_type=F32)
            mixed = mixed / weight
            result = mixed[:GRID_W]
            for head in range(1, heads_in):
                result = jnp.where(
                    lane // HEAD_DIM == head, mixed[head * GRID_W : (head + 1) * GRID_W], result
                )
            out_ref[row * GRID_W : (row + 1) * GRID_W, cols] = result.astype(BF16)


def attend(where, query, own, even, odd, bias, rows_dev):
    tok, channels = query.shape
    padded = (rows_dev + 2 * HALF) * GRID_W
    scores = tok * (channels // HEAD_DIM) * ROW_SPAN * GRID_W
    return pl.pallas_call(
        partial(attend_kernel, rows_dev),
        out_shape=jax.ShapeDtypeStruct((tok, channels), BF16),
        in_specs=[SMEM] + [VMEM] * 5,
        out_specs=VMEM,
        scratch_shapes=[pltpu.VMEM((padded, channels), BF16)] * 2,
        cost_estimate=cost(scores * HEAD_DIM * 6, bias.size * 4 + tok * channels * 16, scores),
        name="attend",
    )(where, query, own, even, odd, bias)


def exchange(block, axis, pairs):
    return lax.ppermute(block, axis, [pair for one, two in pairs for pair in ((one, two), (two, one))])


def flip(block, axis, bit):
    count = lax.axis_size(axis)
    return lax.ppermute(block, axis, [(at, at ^ bit) for at in range(count)])


def body(hidden_in, norm_gain, query_weight, key_weight, value_weight, output_weight, offset_bias):
    tok_dev, width_local = hidden_in.shape
    rows_dev = tok_dev // GRID_W
    tp = lax.axis_size("tp")
    sp = lax.axis_size("sp")
    me = lax.axis_index("tp")
    mine = lax.axis_index("sp")
    all_rows = rows_dev * sp
    first_row = mine * rows_dev
    query_rows = first_row + jnp.arange(rows_dev, dtype=jnp.int32)
    window_first = jnp.clip(query_rows - HALF, 0, all_rows - ROW_SPAN)
    local_first = window_first - first_row + HALF
    offsets = window_first - query_rows + ROW_SPAN - 1
    is_odd = mine % 2
    high = HALF + rows_dev
    slots = jnp.stack([high * (1 - is_odd), high * is_odd])
    where = jnp.concatenate([slots, local_first, offsets]).astype(jnp.int32)
    gain = norm_gain[:, None, :]
    weights = (query_weight, key_weight, value_weight)
    near = jnp.stack([me, me ^ 1]).astype(jnp.int32)
    far = jnp.stack([me ^ 2]).astype(jnp.int32)
    last = jnp.stack([me ^ 3]).astype(jnp.int32)
    zero = jnp.zeros((1,), jnp.int32)
    even_pairs = [(at, at + 1) for at in range(0, sp - 1, 2)]
    odd_pairs = [(at, at + 1) for at in range(1, sp - 1, 2)]
    stream = hidden_in
    biases = [expand_bias(offset_bias[layer]) for layer in range(LAYERS)]
    for layer in range(LAYERS):
        step = partial(project, layer=layer, gain=gain, weights=weights)
        if tp == 4:
            across = flip(stream, "tp", 2)
            beside = flip(stream, "tp", 1)
            corner = flip(across, "tp", 1)
            carried = step([stream, beside], near, None, False)
            carried = step([across], far, carried, False)
            query, pair = step([corner], last, carried, True)
        else:
            gathered = lax.all_gather(stream, "tp", axis=1, tiled=True)
            query, pair = step([gathered], zero, None, True)
        if rows_dev == HALF:
            to_even = to_odd = pair
        else:
            low, top = pair[:, : HALF * GRID_W], pair[:, (rows_dev - HALF) * GRID_W :]
            to_even = jnp.where(is_odd == 0, top, low)
            to_odd = jnp.where(is_odd == 0, low, top)
        even = exchange(to_even, "sp", even_pairs)
        odd = exchange(to_odd, "sp", odd_pairs)
        attended = attend(where, query, pair, even, odd, biases[layer], rows_dev)
        if tp == 4:
            across = flip(attended, "tp", 2)
            beside = flip(attended, "tp", 1)
            corner = flip(across, "tp", 1)
            partly = emit([attended, beside], near, stream, F32, layer, output_weight)
            partly = emit([across], far, partly, F32, layer, output_weight)
            stream = emit([corner], last, partly, BF16, layer, output_weight)
        else:
            gathered = lax.all_gather(attended, "tp", axis=1, tiled=True)
            stream = emit([gathered], zero, stream, BF16, layer, output_weight)
    return stream


def solution(mesh):
    return jax.shard_map(
        body,
        mesh=mesh,
        in_specs=(
            P(("grp", "sp"), "tp"),
            P(),
            P(None, "tp", None),
            P(None, "tp", None),
            P(None, "tp", None),
            P(None, None, "tp"),
            P(None, "tp", None, None),
        ),
        out_specs=P(("grp", "sp"), "tp"),
        check_vma=False,
    )
```

profile of v0, /device:TPU:19, one launch (start us, length us, event | category | flops | bytes accessed | tf_op | source)
XLA Modules:
  0.0 151.8 jit_solution(7520203266807598643)
XLA Ops:
  2.0 1.4 broadcast_in_dim.3.refs_2_.refs_3_.refs_1_
  3.4 4.0 %collective-permute-done.refs_0_ = bf16[256,512]{1,0:T(8,128)(2,1)S(1)} collective-permute-done((bf16[256,512]{1,0:T(8,128)(2,1)}, bf16[256,512]{1,0:T(8,128)(2,1)S(1)}, u32[]{:S(2)}, u32[]{:S(2)}) %collective-permute-start) | collective-permute-done | bytes 262176 | tf_op jit(solution)/shard_map/ppermute | solution.py:263
  7.4 1.5 %collective-permute-start.1 = (bf16[256,512]{1,0:T(8,128)(2,1)S(1)}, bf16[256,512]{1,0:T(8,128)(2,1)S(1)}, u32[]{:S(2)}, u32[]{:S(2)}) collective-permute-start(bf16[256,512]{1,0:T(8,128)(2,1)S(1)} %collective-permute-done.refs_0_), channel_id=1, source_target_pairs={{0,1},{1,0},{2,3},{3,2},{4,5},{5,4},{6,7},{7,6},{8,9},{9,8},{10,11... | collective-permute-start | bytes 786440 | tf_op jit(solution)/shard_map/ppermute | solution.py:263
  10.3 3.7 %project_0_2_0.1 = (f32[3,256,256]{2,1,0:T(8,128)}, f32[256,128]{1,0:T(8,128)}) custom-call(s32[2]{0:T(128)} %pad_add_fusion.1.where, bf16[256,512]{1,0:T(8,128)(2,1)} %refs_4_.13, bf16[256,512]{1,0:T(8,128)(2,1)} %copy-done, f32[3,1,2048]{2,1,0:T(1,128)} %broadcast_in_dim.3.refs_2_.refs_3_.refs_1_, f32[3,1,2048]{2,1,0:T(1,128)} %broadcast_in_dim.3.refs_2_.refs_3_.refs_1_, ...), custom_call_target="tpu_custom_call" | custom-call | flops 402653184 | bytes 2359296 | tf_op jit(solution)/shard_map/project_0_2_0/pallas_call | solution.py:104
  14.0 2.9 %project_0_1_0.1 = (f32[3,256,256]{2,1,0:T(8,128)}, f32[256,128]{1,0:T(8,128)}) custom-call(s32[1]{0:T(128)} %bitcast.3.where, bf16[256,512]{1,0:T(8,128)(2,1)} %copy-done.5, f32[3,1,2048]{2,1,0:T(1,128)} %broadcast_in_dim.3.refs_2_.refs_3_.refs_1_, bf16[3,256,2048]{2,1,0:T(8,128)(2,1)} %refs_2_.16, bf16[3,256,2048]{2,1,0:T(8,128)(2,1)} %refs_3_.16, ...), custom_call_target="tpu_custom_call" | custom-call | flops 201326592 | bytes 1310720 | tf_op jit(solution)/shard_map/project_0_1_0/pallas_call | solution.py:104
  17.6 2.6 %project_0_1_1.1 = (bf16[256,256]{1,0:T(8,128)(2,1)}, bf16[2,256,256]{2,1,0:T(8,128)(2,1)}) custom-call(s32[1]{0:T(128)} %bitcast.where, bf16[256,512]{1,0:T(8,128)(2,1)} %copy-done.7, f32[3,1,2048]{2,1,0:T(1,128)} %broadcast_in_dim.3.refs_2_.refs_3_.refs_1_, bf16[3,256,2048]{2,1,0:T(8,128)(2,1)} %refs_2_.16, bf16[3,256,2048]{2,1,0:T(8,128)(2,1)} %refs_3_.16, ...), custom_call_target="tpu_custom_call" | custom-call | flops 201326592 | bytes 1310720 | tf_op jit(solution)/shard_map/project_0_1_1/pallas_call | solution.py:104
  20.2 1.3 collective-permute-start.3
  21.5 1.9 %collective-permute-start.4 = (bf16[2,256,256]{2,1,0:T(8,128)(2,1)}, bf16[2,256,256]{2,1,0:T(8,128)(2,1)S(1)}, u32[]{:S(2)}, u32[]{:S(2)}) collective-permute-start(bf16[2,256,256]{2,1,0:T(8,128)(2,1)} %get-tuple-element.28.own_ref), channel_id=1, source_target_pairs={{4,8},{8,4},{5,9},{9,5},{6,10},{10,6},{7,11},{11,7},{20,24},{24,20... | collective-permute-start | bytes 786440 | tf_op jit(solution)/shard_map/ppermute | solution.py:258
  24.1 2.6 %expand_bias.3.bias_ref = f32[4,14,64,128]{3,2,1,0:T(8,128)} custom-call(f32[4,14,128]{2,1,0:T(8,128)} %pad_maximum_fusion.rows_ref), custom_call_target="tpu_custom_call" | custom-call | flops 18350080 | bytes 1835008 | tf_op jit(solution)/shard_map/expand_bias/pallas_call | solution.py:173
  27.3 1.0 collective-permute-done.3.even_ref
  28.3 2.9 %collective-permute-done.4.odd_ref = bf16[2,256,256]{2,1,0:T(8,128)(2,1)S(1)} collective-permute-done((bf16[2,256,256]{2,1,0:T(8,128)(2,1)}, bf16[2,256,256]{2,1,0:T(8,128)(2,1)S(1)}, u32[]{:S(2)}, u32[]{:S(2)}) %collective-permute-start.4) | collective-permute-done | bytes 262176 | tf_op jit(solution)/shard_map/ppermute | solution.py:258
  31.9 5.0 %attend.3.refs_0_ = bf16[256,256]{1,0:T(8,128)(2,1)} custom-call(s32[10]{0:T(128)} %pad_add_fusion.where_ref, bf16[256,256]{1,0:T(8,128)(2,1)} %get-tuple-element.27.query_ref, bf16[2,256,256]{2,1,0:T(8,128)(2,1)} %get-tuple-element.28.own_ref, bf16[2,256,256]{2,1,0:T(8,128)(2,1)} %copy-done.3, bf16[2,256,256]{2,1,0:T(8,128)(2,1)} %copy-done.4, ...), custom_call_target="tpu_custom_call" | custom-call | flops 201326592 | bytes 2883584 | tf_op jit(solution)/shard_map/attend/pallas_call | solution.py:246
  37.1 1.4 collective-permute-start.7
  38.6 2.3 %collective-permute-done.5.refs_0_ = bf16[256,256]{1,0:T(8,128)(2,1)S(1)} collective-permute-done((bf16[256,256]{1,0:T(8,128)(2,1)}, bf16[256,256]{1,0:T(8,128)(2,1)S(1)}, u32[]{:S(2)}, u32[]{:S(2)}) %collective-permute-start.5) | collective-permute-done | bytes 131104 | tf_op jit(solution)/shard_map/ppermute | solution.py:263
  40.9 2.3 %collective-permute-start.6 = (bf16[256,256]{1,0:T(8,128)(2,1)S(1)}, bf16[256,256]{1,0:T(8,128)(2,1)S(1)}, u32[]{:S(2)}, u32[]{:S(2)}) collective-permute-start(bf16[256,256]{1,0:T(8,128)(2,1)S(1)} %collective-permute-done.5.refs_0_), channel_id=1, source_target_pairs={{0,1},{1,0},{2,3},{3,2},{4,5},{5,4},{6,7},{7,6},{8,9},{9,8},{10,11... | collective-permute-start | bytes 393224 | tf_op jit(solution)/shard_map/ppermute | solution.py:263
  43.9 3.0 %emit_0_2.1.refs_2_ = f32[256,512]{1,0:T(8,128)} custom-call(s32[2]{0:T(128)} %pad_add_fusion.1.where, bf16[256,256]{1,0:T(8,128)(2,1)} %attend.3.refs_0_, bf16[256,256]{1,0:T(8,128)(2,1)} %copy-done.23, bf16[3,1024,512]{2,1,0:T(8,128)(2,1)} %refs_1_.11, bf16[3,1024,512]{2,1,0:T(8,128)(2,1)} %refs_1_.11, bf16[256,512]{1,0:T(8,128)(2,1)} %refs_4_.13), custom_call_target="tpu_custom_call" | custom-call | flops 134217728 | bytes 1572864 | tf_op jit(solution)/shard_map/emit_0_2/pallas_call | solution.py:138
  46.9 2.2 %emit_0_1.2.refs_2_ = f32[256,512]{1,0:T(8,128)} custom-call(s32[1]{0:T(128)} %bitcast.3.where, bf16[256,256]{1,0:T(8,128)(2,1)} %copy-done.17, bf16[3,1024,512]{2,1,0:T(8,128)(2,1)} %refs_1_.11, f32[256,512]{1,0:T(8,128)} %emit_0_2.1.refs_2_), custom_call_target="tpu_custom_call" | custom-call | flops 67108864 | bytes 1179648 | tf_op jit(solution)/shard_map/emit_0_1/pallas_call | solution.py:138
  49.8 2.1 %emit_0_1.3.refs_0_.refs_4_ = bf16[256,512]{1,0:T(8,128)(2,1)} custom-call(s32[1]{0:T(128)} %bitcast.where, bf16[256,256]{1,0:T(8,128)(2,1)} %copy-done.20, bf16[3,1024,512]{2,1,0:T(8,128)(2,1)} %refs_1_.11, f32[256,512]{1,0:T(8,128)} %emit_0_1.2.refs_2_), custom_call_target="tpu_custom_call" | custom-call | flops 67108864 | bytes 1179648 | tf_op jit(solution)/shard_map/emit_0_1/pallas_call | solution.py:138
  52.4 7.5 %collective-permute-done.8.refs_0_ = bf16[256,512]{1,0:T(8,128)(2,1)S(1)} collective-permute-done((bf16[256,512]{1,0:T(8,128)(2,1)}, bf16[256,512]{1,0:T(8,128)(2,1)S(1)}, u32[]{:S(2)}, u32[]{:S(2)}) %collective-permute-start.8) | collective-permute-done | bytes 262176 | tf_op jit(solution)/shard_map/ppermute | solution.py:263
  61.5 3.7 %project_1_2_0.1 = (f32[3,256,256]{2,1,0:T(8,128)}, f32[256,128]{1,0:T(8,128)}) custom-call(s32[2]{0:T(128)} %pad_add_fusion.1.where, bf16[256,512]{1,0:T(8,128)(2,1)} %emit_0_1.3.refs_0_.refs_4_, bf16[256,512]{1,0:T(8,128)(2,1)} %copy-done.1, f32[3,1,2048]{2,1,0:T(1,128)} %broadcast_in_dim.3.refs_2_.refs_3_.refs_1_, ...), custom_call_target="tpu_custom_call" | custom-call | flops 402653184 | bytes 2359296 | tf_op jit(solution)/shard_map/project_1_2_0/pallas_call | solution.py:104
  65.2 2.9 %project_1_1_0.1 = (f32[3,256,256]{2,1,0:T(8,128)}, f32[256,128]{1,0:T(8,128)}) custom-call(s32[1]{0:T(128)} %bitcast.3.where, bf16[256,512]{1,0:T(8,128)(2,1)} %copy-done.10, f32[3,1,2048]{2,1,0:T(1,128)} %broadcast_in_dim.3.refs_2_.refs_3_.refs_1_, bf16[3,256,2048]{2,1,0:T(8,128)(2,1)} %refs_2_.16, bf16[3,256,2048]{2,1,0:T(8,128)(2,1)} %refs_3_.16, ...), custom_call_target="tpu_custom_call" | custom-call | flops 201326592 | bytes 1310720 | tf_op jit(solution)/shard_map/project_1_1_0/pallas_call | solution.py:104
  68.8 2.6 %project_1_1_1.1 = (bf16[256,256]{1,0:T(8,128)(2,1)}, bf16[2,256,256]{2,1,0:T(8,128)(2,1)}) custom-call(s32[1]{0:T(128)} %bitcast.where, bf16[256,512]{1,0:T(8,128)(2,1)} %copy-done.14, f32[3,1,2048]{2,1,0:T(1,128)} %broadcast_in_dim.3.refs_2_.refs_3_.refs_1_, bf16[3,256,2048]{2,1,0:T(8,128)(2,1)} %refs_2_.16, bf16[3,256,2048]{2,1,0:T(8,128)(2,1)} %refs_3_.16, ...), custom_call_target="tpu_custom_call" | custom-call | flops 201326592 | bytes 1310720 | tf_op jit(solution)/shard_map/project_1_1_1/pallas_call | solution.py:104
  71.5 2.0 %collective-permute-start.12 = (bf16[2,256,256]{2,1,0:T(8,128)(2,1)}, bf16[2,256,256]{2,1,0:T(8,128)(2,1)S(1)}, u32[]{:S(2)}, u32[]{:S(2)}) collective-permute-start(bf16[2,256,256]{2,1,0:T(8,128)(2,1)} %get-tuple-element.34.own_ref), channel_id=1, source_target_pairs={{4,8},{8,4},{5,9},{9,5},{6,10},{10,6},{7,11},{11,7},{20,24},{24,20... | collective-permute-start | bytes 786440 | tf_op jit(solution)/shard_map/ppermute | solution.py:258
  74.2 2.6 %expand_bias.4.bias_ref = f32[4,14,64,128]{3,2,1,0:T(8,128)} custom-call(f32[4,14,128]{2,1,0:T(8,128)} %pad_maximum_fusion.1.rows_ref), custom_call_target="tpu_custom_call" | custom-call | flops 18350080 | bytes 1835008 | tf_op jit(solution)/shard_map/expand_bias/pallas_call | solution.py:173
  76.7 2.8 %collective-permute-done.11.even_ref = bf16[2,256,256]{2,1,0:T(8,128)(2,1)S(1)} collective-permute-done((bf16[2,256,256]{2,1,0:T(8,128)(2,1)}, bf16[2,256,256]{2,1,0:T(8,128)(2,1)S(1)}, u32[]{:S(2)}, u32[]{:S(2)}) %collective-permute-start.11) | collective-permute-done | bytes 262176 | tf_op jit(solution)/shard_map/ppermute | solution.py:258
  79.5 1.9 %collective-permute-done.12.odd_ref = bf16[2,256,256]{2,1,0:T(8,128)(2,1)S(1)} collective-permute-done((bf16[2,256,256]{2,1,0:T(8,128)(2,1)}, bf16[2,256,256]{2,1,0:T(8,128)(2,1)S(1)}, u32[]{:S(2)}, u32[]{:S(2)}) %collective-permute-start.12) | collective-permute-done | bytes 262176 | tf_op jit(solution)/shard_map/ppermute | solution.py:258
  82.1 5.0 %attend.4.refs_0_ = bf16[256,256]{1,0:T(8,128)(2,1)} custom-call(s32[10]{0:T(128)} %pad_add_fusion.where_ref, bf16[256,256]{1,0:T(8,128)(2,1)} %get-tuple-element.33.query_ref, bf16[2,256,256]{2,1,0:T(8,128)(2,1)} %get-tuple-element.34.own_ref, bf16[2,256,256]{2,1,0:T(8,128)(2,1)} %copy-done.6, bf16[2,256,256]{2,1,0:T(8,128)(2,1)} %copy-done.8, ...), custom_call_target="tpu_custom_call" | custom-call | flops 201326592 | bytes 2883584 | tf_op jit(solution)/shard_map/attend/pallas_call | solution.py:246
  87.3 1.2 collective-permute-start.15
  88.5 3.0 %collective-permute-done.13.refs_0_ = bf16[256,256]{1,0:T(8,128)(2,1)S(1)} collective-permute-done((bf16[256,256]{1,0:T(8,128)(2,1)}, bf16[256,256]{1,0:T(8,128)(2,1)S(1)}, u32[]{:S(2)}, u32[]{:S(2)}) %collective-permute-start.13) | collective-permute-done | bytes 131104 | tf_op jit(solution)/shard_map/ppermute | solution.py:263
  91.4 1.7 %collective-permute-start.14 = (bf16[256,256]{1,0:T(8,128)(2,1)S(1)}, bf16[256,256]{1,0:T(8,128)(2,1)S(1)}, u32[]{:S(2)}, u32[]{:S(2)}) collective-permute-start(bf16[256,256]{1,0:T(8,128)(2,1)S(1)} %collective-permute-done.13.refs_0_), channel_id=1, source_target_pairs={{0,1},{1,0},{2,3},{3,2},{4,5},{5,4},{6,7},{7,6},{8,9},{9,8},{10,11... | collective-permute-start | bytes 393224 | tf_op jit(solution)/shard_map/ppermute | solution.py:263
  93.9 3.0 %emit_1_2.1.refs_2_ = f32[256,512]{1,0:T(8,128)} custom-call(s32[2]{0:T(128)} %pad_add_fusion.1.where, bf16[256,256]{1,0:T(8,128)(2,1)} %attend.4.refs_0_, bf16[256,256]{1,0:T(8,128)(2,1)} %copy-done.22, bf16[3,1024,512]{2,1,0:T(8,128)(2,1)} %refs_1_.11, bf16[3,1024,512]{2,1,0:T(8,128)(2,1)} %refs_1_.11, bf16[256,512]{1,0:T(8,128)(2,1)} %emit_0_1.3.refs_0_.refs_4_), custom_call_target="tpu_custom_call" | custom-call | flops 134217728 | bytes 1572864 | tf_op jit(solution)/shard_map/emit_1_2/pallas_call | solution.py:138
  96.9 2.2 %emit_1_1.2.refs_2_ = f32[256,512]{1,0:T(8,128)} custom-call(s32[1]{0:T(128)} %bitcast.3.where, bf16[256,256]{1,0:T(8,128)(2,1)} %copy-done.16, bf16[3,1024,512]{2,1,0:T(8,128)(2,1)} %refs_1_.11, f32[256,512]{1,0:T(8,128)} %emit_1_2.1.refs_2_), custom_call_target="tpu_custom_call" | custom-call | flops 67108864 | bytes 1179648 | tf_op jit(solution)/shard_map/emit_1_1/pallas_call | solution.py:138
  99.8 2.1 %emit_1_1.3.refs_0_.refs_4_ = bf16[256,512]{1,0:T(8,128)(2,1)} custom-call(s32[1]{0:T(128)} %bitcast.where, bf16[256,256]{1,0:T(8,128)(2,1)} %copy-done.19, bf16[3,1024,512]{2,1,0:T(8,128)(2,1)} %refs_1_.11, f32[256,512]{1,0:T(8,128)} %emit_1_1.2.refs_2_), custom_call_target="tpu_custom_call" | custom-call | flops 67108864 | bytes 1179648 | tf_op jit(solution)/shard_map/emit_1_1/pallas_call | solution.py:138
  102.4 7.5 %collective-permute-done.16.refs_0_ = bf16[256,512]{1,0:T(8,128)(2,1)S(1)} collective-permute-done((bf16[256,512]{1,0:T(8,128)(2,1)}, bf16[256,512]{1,0:T(8,128)(2,1)S(1)}, u32[]{:S(2)}, u32[]{:S(2)}) %collective-permute-start.16) | collective-permute-done | bytes 262176 | tf_op jit(solution)/shard_map/ppermute | solution.py:263
  111.5 3.7 %project_2_2_0.1 = (f32[3,256,256]{2,1,0:T(8,128)}, f32[256,128]{1,0:T(8,128)}) custom-call(s32[2]{0:T(128)} %pad_add_fusion.1.where, bf16[256,512]{1,0:T(8,128)(2,1)} %emit_1_1.3.refs_0_.refs_4_, bf16[256,512]{1,0:T(8,128)(2,1)} %copy-done.2, f32[3,1,2048]{2,1,0:T(1,128)} %broadcast_in_dim.3.refs_2_.refs_3_.refs_1_, ...), custom_call_target="tpu_custom_call" | custom-call | flops 402653184 | bytes 2359296 | tf_op jit(solution)/shard_map/project_2_2_0/pallas_call | solution.py:104
  115.2 2.9 %project_2_1_0.1 = (f32[3,256,256]{2,1,0:T(8,128)}, f32[256,128]{1,0:T(8,128)}) custom-call(s32[1]{0:T(128)} %bitcast.3.where, bf16[256,512]{1,0:T(8,128)(2,1)} %copy-done.11, f32[3,1,2048]{2,1,0:T(1,128)} %broadcast_in_dim.3.refs_2_.refs_3_.refs_1_, bf16[3,256,2048]{2,1,0:T(8,128)(2,1)} %refs_2_.16, bf16[3,256,2048]{2,1,0:T(8,128)(2,1)} %refs_3_.16, ...), custom_call_target="tpu_custom_call" | custom-call | flops 201326592 | bytes 1310720 | tf_op jit(solution)/shard_map/project_2_1_0/pallas_call | solution.py:104
  118.8 2.6 %project_2_1_1.1 = (bf16[256,256]{1,0:T(8,128)(2,1)}, bf16[2,256,256]{2,1,0:T(8,128)(2,1)}) custom-call(s32[1]{0:T(128)} %bitcast.where, bf16[256,512]{1,0:T(8,128)(2,1)} %copy-done.13, f32[3,1,2048]{2,1,0:T(1,128)} %broadcast_in_dim.3.refs_2_.refs_3_.refs_1_, bf16[3,256,2048]{2,1,0:T(8,128)(2,1)} %refs_2_.16, bf16[3,256,2048]{2,1,0:T(8,128)(2,1)} %refs_3_.16, ...), custom_call_target="tpu_custom_call" | custom-call | flops 201326592 | bytes 1310720 | tf_op jit(solution)/shard_map/project_2_1_1/pallas_call | solution.py:104
  121.4 2.1 %collective-permute-start.20 = (bf16[2,256,256]{2,1,0:T(8,128)(2,1)}, bf16[2,256,256]{2,1,0:T(8,128)(2,1)S(1)}, u32[]{:S(2)}, u32[]{:S(2)}) collective-permute-start(bf16[2,256,256]{2,1,0:T(8,128)(2,1)} %get-tuple-element.40.own_ref), channel_id=1, source_target_pairs={{4,8},{8,4},{5,9},{9,5},{6,10},{10,6},{7,11},{11,7},{20,24},{24,20... | collective-permute-start | bytes 786440 | tf_op jit(solution)/shard_map/ppermute | solution.py:258
  124.3 2.6 %expand_bias.5.bias_ref = f32[4,14,64,128]{3,2,1,0:T(8,128)} custom-call(f32[4,14,128]{2,1,0:T(8,128)} %pad_maximum_fusion.2.rows_ref), custom_call_target="tpu_custom_call" | custom-call | flops 18350080 | bytes 1835008 | tf_op jit(solution)/shard_map/expand_bias/pallas_call | solution.py:173
  126.8 2.6 %collective-permute-done.19.even_ref = bf16[2,256,256]{2,1,0:T(8,128)(2,1)S(1)} collective-permute-done((bf16[2,256,256]{2,1,0:T(8,128)(2,1)}, bf16[2,256,256]{2,1,0:T(8,128)(2,1)S(1)}, u32[]{:S(2)}, u32[]{:S(2)}) %collective-permute-start.19) | collective-permute-done | bytes 262176 | tf_op jit(solution)/shard_map/ppermute | solution.py:258
  129.5 1.9 %collective-permute-done.20.odd_ref = bf16[2,256,256]{2,1,0:T(8,128)(2,1)S(1)} collective-permute-done((bf16[2,256,256]{2,1,0:T(8,128)(2,1)}, bf16[2,256,256]{2,1,0:T(8,128)(2,1)S(1)}, u32[]{:S(2)}, u32[]{:S(2)}) %collective-permute-start.20) | collective-permute-done | bytes 262176 | tf_op jit(solution)/shard_map/ppermute | solution.py:258
  132.0 5.0 %attend.5.refs_0_ = bf16[256,256]{1,0:T(8,128)(2,1)} custom-call(s32[10]{0:T(128)} %pad_add_fusion.where_ref, bf16[256,256]{1,0:T(8,128)(2,1)} %get-tuple-element.39.query_ref, bf16[2,256,256]{2,1,0:T(8,128)(2,1)} %get-tuple-element.40.own_ref, bf16[2,256,256]{2,1,0:T(8,128)(2,1)} %copy-done.9, bf16[2,256,256]{2,1,0:T(8,128)(2,1)} %copy-done.12, ...), custom_call_target="tpu_custom_call" | custom-call | flops 201326592 | bytes 2883584 | tf_op jit(solution)/shard_map/attend/pallas_call | solution.py:246
  137.3 1.2 collective-permute-start.23
  138.5 2.9 %collective-permute-done.21.refs_0_ = bf16[256,256]{1,0:T(8,128)(2,1)S(1)} collective-permute-done((bf16[256,256]{1,0:T(8,128)(2,1)}, bf16[256,256]{1,0:T(8,128)(2,1)S(1)}, u32[]{:S(2)}, u32[]{:S(2)}) %collective-permute-start.21) | collective-permute-done | bytes 131104 | tf_op jit(solution)/shard_map/ppermute | solution.py:263
  141.4 1.8 %collective-permute-start.22 = (bf16[256,256]{1,0:T(8,128)(2,1)S(1)}, bf16[256,256]{1,0:T(8,128)(2,1)S(1)}, u32[]{:S(2)}, u32[]{:S(2)}) collective-permute-start(bf16[256,256]{1,0:T(8,128)(2,1)S(1)} %collective-permute-done.21.refs_0_), channel_id=1, source_target_pairs={{0,1},{1,0},{2,3},{3,2},{4,5},{5,4},{6,7},{7,6},{8,9},{9,8},{10,11... | collective-permute-start | bytes 393224 | tf_op jit(solution)/shard_map/ppermute | solution.py:263
  143.8 3.0 %emit_2_2.1.refs_2_ = f32[256,512]{1,0:T(8,128)} custom-call(s32[2]{0:T(128)} %pad_add_fusion.1.where, bf16[256,256]{1,0:T(8,128)(2,1)} %attend.5.refs_0_, bf16[256,256]{1,0:T(8,128)(2,1)} %copy-done.21, bf16[3,1024,512]{2,1,0:T(8,128)(2,1)} %refs_1_.11, bf16[3,1024,512]{2,1,0:T(8,128)(2,1)} %refs_1_.11, bf16[256,512]{1,0:T(8,128)(2,1)} %emit_1_1.3.refs_0_.refs_4_), custom_call_target="tpu_custom_call" | custom-call | flops 134217728 | bytes 1572864 | tf_op jit(solution)/shard_map/emit_2_2/pallas_call | solution.py:138
  146.8 2.2 %emit_2_1.2.refs_2_ = f32[256,512]{1,0:T(8,128)} custom-call(s32[1]{0:T(128)} %bitcast.3.where, bf16[256,256]{1,0:T(8,128)(2,1)} %copy-done.15, bf16[3,1024,512]{2,1,0:T(8,128)(2,1)} %refs_1_.11, f32[256,512]{1,0:T(8,128)} %emit_2_2.1.refs_2_), custom_call_target="tpu_custom_call" | custom-call | flops 67108864 | bytes 1179648 | tf_op jit(solution)/shard_map/emit_2_1/pallas_call | solution.py:138
  149.7 2.1 %emit_2_1.3 = bf16[256,512]{1,0:T(8,128)(2,1)} custom-call(s32[1]{0:T(128)} %bitcast.where, bf16[256,256]{1,0:T(8,128)(2,1)} %copy-done.18, bf16[3,1024,512]{2,1,0:T(8,128)(2,1)} %refs_1_.11, f32[256,512]{1,0:T(8,128)} %emit_2_1.2.refs_2_), custom_call_target="tpu_custom_call" | custom-call | flops 67108864 | bytes 1179648 | tf_op jit(solution)/shard_map/emit_2_1/pallas_call | solution.py:138
  (85 shorter events, 19.3 us)
Async XLA Ops:
  0.0 7.4 %collective-permute-start = (bf16[256,512]{1,0:T(8,128)(2,1)}, bf16[256,512]{1,0:T(8,128)(2,1)S(1)}, u32[]{:S(2)}, u32[]{:S(2)}) collective-permute-start(bf16[256,512]{1,0:T(8,128)(2,1)} %refs_4_.13), channel_id=1, source_target_pairs={{0,2},{1,3},{2,0},{3,1},{4,6},{5,7},{6,4},{7,5},{8,10},{9,11},{10,... | collective-permute-start | bytes 786440 | tf_op jit(solution)/shard_map/ppermute | solution.py:263
  0.3 9.3 %collective-permute-start.2 = (bf16[256,512]{1,0:T(8,128)(2,1)}, bf16[256,512]{1,0:T(8,128)(2,1)S(1)}, u32[]{:S(2)}, u32[]{:S(2)}) collective-permute-start(bf16[256,512]{1,0:T(8,128)(2,1)} %refs_4_.13), channel_id=1, source_target_pairs={{0,1},{1,0},{2,3},{3,2},{4,5},{5,4},{6,7},{7,6},{8,9},{9,8},{10,11... | collective-permute-start | bytes 786440 | tf_op jit(solution)/shard_map/ppermute | solution.py:263
  7.4 6.6 %copy-start.5 = (bf16[256,512]{1,0:T(8,128)(2,1)}, bf16[256,512]{1,0:T(8,128)(2,1)S(1)}, u32[]{:S(2)}) copy-start(bf16[256,512]{1,0:T(8,128)(2,1)S(1)} %collective-permute-done.refs_0_) | copy-start | bytes 786436
  7.4 9.5 %collective-permute-start.1 = (bf16[256,512]{1,0:T(8,128)(2,1)S(1)}, bf16[256,512]{1,0:T(8,128)(2,1)S(1)}, u32[]{:S(2)}, u32[]{:S(2)}) collective-permute-start(bf16[256,512]{1,0:T(8,128)(2,1)S(1)} %collective-permute-done.refs_0_), channel_id=1, source_target_pairs={{0,1},{1,0},{2,3},{3,2},{4,5},{5,4},{6,7},{7,6},{8,9},{9,8},{10,11... | collective-permute-start | bytes 786440 | tf_op jit(solution)/shard_map/ppermute | solution.py:263
  9.6 0.7 copy-start
  16.9 0.7 copy-start.7
  20.2 8.1 %collective-permute-start.3 = (bf16[2,256,256]{2,1,0:T(8,128)(2,1)}, bf16[2,256,256]{2,1,0:T(8,128)(2,1)S(1)}, u32[]{:S(2)}, u32[]{:S(2)}) collective-permute-start(bf16[2,256,256]{2,1,0:T(8,128)(2,1)} %get-tuple-element.28.own_ref), channel_id=1, source_target_pairs={{0,4},{4,0},{8,12},{12,8},{1,5},{5,1},{9,13},{13,9},{2,6},{6,2},{1... | collective-permute-start | bytes 786440 | tf_op jit(solution)/shard_map/ppermute | solution.py:258
  21.5 9.7 %collective-permute-start.4 = (bf16[2,256,256]{2,1,0:T(8,128)(2,1)}, bf16[2,256,256]{2,1,0:T(8,128)(2,1)S(1)}, u32[]{:S(2)}, u32[]{:S(2)}) collective-permute-start(bf16[2,256,256]{2,1,0:T(8,128)(2,1)} %get-tuple-element.28.own_ref), channel_id=1, source_target_pairs={{4,8},{8,4},{5,9},{9,5},{6,10},{10,6},{7,11},{11,7},{20,24},{24,20... | collective-permute-start | bytes 786440 | tf_op jit(solution)/shard_map/ppermute | solution.py:258
  28.3 2.9 %copy-start.3 = (bf16[2,256,256]{2,1,0:T(8,128)(2,1)}, bf16[2,256,256]{2,1,0:T(8,128)(2,1)S(1)}, u32[]{:S(2)}) copy-start(bf16[2,256,256]{2,1,0:T(8,128)(2,1)S(1)} %collective-permute-done.3.even_ref) | copy-start | bytes 786436
  31.2 0.7 copy-start.4
  36.9 4.0 %collective-permute-start.5 = (bf16[256,256]{1,0:T(8,128)(2,1)}, bf16[256,256]{1,0:T(8,128)(2,1)S(1)}, u32[]{:S(2)}, u32[]{:S(2)}) collective-permute-start(bf16[256,256]{1,0:T(8,128)(2,1)} %attend.3.refs_0_), channel_id=1, source_target_pairs={{0,2},{1,3},{2,0},{3,1},{4,6},{5,7},{6,4},{7,5},{8,10},{9,11},{10,... | collective-permute-start | bytes 393224 | tf_op jit(solution)/shard_map/ppermute | solution.py:263
  37.1 6.1 %collective-permute-start.7 = (bf16[256,256]{1,0:T(8,128)(2,1)}, bf16[256,256]{1,0:T(8,128)(2,1)S(1)}, u32[]{:S(2)}, u32[]{:S(2)}) collective-permute-start(bf16[256,256]{1,0:T(8,128)(2,1)} %attend.3.refs_0_), channel_id=1, source_target_pairs={{0,1},{1,0},{2,3},{3,2},{4,5},{5,4},{6,7},{7,6},{8,9},{9,8},{10,11... | collective-permute-start | bytes 393224 | tf_op jit(solution)/shard_map/ppermute | solution.py:263
  40.9 6.0 %copy-start.17 = (bf16[256,256]{1,0:T(8,128)(2,1)}, bf16[256,256]{1,0:T(8,128)(2,1)S(1)}, u32[]{:S(2)}) copy-start(bf16[256,256]{1,0:T(8,128)(2,1)S(1)} %collective-permute-done.5.refs_0_) | copy-start | bytes 393220
  40.9 8.2 %collective-permute-start.6 = (bf16[256,256]{1,0:T(8,128)(2,1)S(1)}, bf16[256,256]{1,0:T(8,128)(2,1)S(1)}, u32[]{:S(2)}, u32[]{:S(2)}) collective-permute-start(bf16[256,256]{1,0:T(8,128)(2,1)S(1)} %collective-permute-done.5.refs_0_), channel_id=1, source_target_pairs={{0,1},{1,0},{2,3},{3,2},{4,5},{5,4},{6,7},{7,6},{8,9},{9,8},{10,11... | collective-permute-start | bytes 393224 | tf_op jit(solution)/shard_map/ppermute | solution.py:263
  43.2 0.7 copy-start.23
  49.1 0.6 copy-start.20
  51.9 8.0 %collective-permute-start.8 = (bf16[256,512]{1,0:T(8,128)(2,1)}, bf16[256,512]{1,0:T(8,128)(2,1)S(1)}, u32[]{:S(2)}, u32[]{:S(2)}) collective-permute-start(bf16[256,512]{1,0:T(8,128)(2,1)} %emit_0_1.3.refs_0_.refs_4_), channel_id=1, source_target_pairs={{0,2},{1,3},{2,0},{3,1},{4,6},{5,7},{6,4},{7,5},{8,10},{9,11},{10,... | collective-permute-start | bytes 786440 | tf_op jit(solution)/shard_map/ppermute | solution.py:263
  52.1 8.7 %collective-permute-start.10 = (bf16[256,512]{1,0:T(8,128)(2,1)}, bf16[256,512]{1,0:T(8,128)(2,1)S(1)}, u32[]{:S(2)}, u32[]{:S(2)}) collective-permute-start(bf16[256,512]{1,0:T(8,128)(2,1)} %emit_0_1.3.refs_0_.refs_4_), channel_id=1, source_target_pairs={{0,1},{1,0},{2,3},{3,2},{4,5},{5,4},{6,7},{7,6},{8,9},{9,8},{10,11... | collective-permute-start | bytes 786440 | tf_op jit(solution)/shard_map/ppermute | solution.py:263
  59.9 5.3 %copy-start.10 = (bf16[256,512]{1,0:T(8,128)(2,1)}, bf16[256,512]{1,0:T(8,128)(2,1)S(1)}, u32[]{:S(2)}) copy-start(bf16[256,512]{1,0:T(8,128)(2,1)S(1)} %collective-permute-done.8.refs_0_) | copy-start | bytes 786436
  59.9 8.2 %collective-permute-start.9 = (bf16[256,512]{1,0:T(8,128)(2,1)S(1)}, bf16[256,512]{1,0:T(8,128)(2,1)S(1)}, u32[]{:S(2)}, u32[]{:S(2)}) collective-permute-start(bf16[256,512]{1,0:T(8,128)(2,1)S(1)} %collective-permute-done.8.refs_0_), channel_id=1, source_target_pairs={{0,1},{1,0},{2,3},{3,2},{4,5},{5,4},{6,7},{7,6},{8,9},{9,8},{10,11... | collective-permute-start | bytes 786440 | tf_op jit(solution)/shard_map/ppermute | solution.py:263
  60.8 0.7 copy-start.1
  68.1 0.7 copy-start.14
  71.5 8.0 %collective-permute-start.11 = (bf16[2,256,256]{2,1,0:T(8,128)(2,1)}, bf16[2,256,256]{2,1,0:T(8,128)(2,1)S(1)}, u32[]{:S(2)}, u32[]{:S(2)}) collective-permute-start(bf16[2,256,256]{2,1,0:T(8,128)(2,1)} %get-tuple-element.34.own_ref), channel_id=1, source_target_pairs={{0,4},{4,0},{8,12},{12,8},{1,5},{5,1},{9,13},{13,9},{2,6},{6,2},{1... | collective-permute-start | bytes 786440 | tf_op jit(solution)/shard_map/ppermute | solution.py:258
  71.5 9.9 %collective-permute-start.12 = (bf16[2,256,256]{2,1,0:T(8,128)(2,1)}, bf16[2,256,256]{2,1,0:T(8,128)(2,1)S(1)}, u32[]{:S(2)}, u32[]{:S(2)}) collective-permute-start(bf16[2,256,256]{2,1,0:T(8,128)(2,1)} %get-tuple-element.34.own_ref), channel_id=1, source_target_pairs={{4,8},{8,4},{5,9},{9,5},{6,10},{10,6},{7,11},{11,7},{20,24},{24,20... | collective-permute-start | bytes 786440 | tf_op jit(solution)/shard_map/ppermute | solution.py:258
  79.5 1.9 %copy-start.6 = (bf16[2,256,256]{2,1,0:T(8,128)(2,1)}, bf16[2,256,256]{2,1,0:T(8,128)(2,1)S(1)}, u32[]{:S(2)}) copy-start(bf16[2,256,256]{2,1,0:T(8,128)(2,1)S(1)} %collective-permute-done.11.even_ref) | copy-start | bytes 786436
  81.4 0.7 copy-start.8
  87.1 4.4 %collective-permute-start.13 = (bf16[256,256]{1,0:T(8,128)(2,1)}, bf16[256,256]{1,0:T(8,128)(2,1)S(1)}, u32[]{:S(2)}, u32[]{:S(2)}) collective-permute-start(bf16[256,256]{1,0:T(8,128)(2,1)} %attend.4.refs_0_), channel_id=1, source_target_pairs={{0,2},{1,3},{2,0},{3,1},{4,6},{5,7},{6,4},{7,5},{8,10},{9,11},{10,... | collective-permute-start | bytes 393224 | tf_op jit(solution)/shard_map/ppermute | solution.py:263
  87.3 5.9 %collective-permute-start.15 = (bf16[256,256]{1,0:T(8,128)(2,1)}, bf16[256,256]{1,0:T(8,128)(2,1)S(1)}, u32[]{:S(2)}, u32[]{:S(2)}) collective-permute-start(bf16[256,256]{1,0:T(8,128)(2,1)} %attend.4.refs_0_), channel_id=1, source_target_pairs={{0,1},{1,0},{2,3},{3,2},{4,5},{5,4},{6,7},{7,6},{8,9},{9,8},{10,11... | collective-permute-start | bytes 393224 | tf_op jit(solution)/shard_map/ppermute | solution.py:263
  91.4 5.4 %copy-start.16 = (bf16[256,256]{1,0:T(8,128)(2,1)}, bf16[256,256]{1,0:T(8,128)(2,1)S(1)}, u32[]{:S(2)}) copy-start(bf16[256,256]{1,0:T(8,128)(2,1)S(1)} %collective-permute-done.13.refs_0_) | copy-start | bytes 393220
  91.4 7.7 %collective-permute-start.14 = (bf16[256,256]{1,0:T(8,128)(2,1)S(1)}, bf16[256,256]{1,0:T(8,128)(2,1)S(1)}, u32[]{:S(2)}, u32[]{:S(2)}) collective-permute-start(bf16[256,256]{1,0:T(8,128)(2,1)S(1)} %collective-permute-done.13.refs_0_), channel_id=1, source_target_pairs={{0,1},{1,0},{2,3},{3,2},{4,5},{5,4},{6,7},{7,6},{8,9},{9,8},{10,11... | collective-permute-start | bytes 393224 | tf_op jit(solution)/shard_map/ppermute | solution.py:263
  93.2 0.7 copy-start.22
  99.1 0.6 copy-start.19
  101.9 8.0 %collective-permute-start.16 = (bf16[256,512]{1,0:T(8,128)(2,1)}, bf16[256,512]{1,0:T(8,128)(2,1)S(1)}, u32[]{:S(2)}, u32[]{:S(2)}) collective-permute-start(bf16[256,512]{1,0:T(8,128)(2,1)} %emit_1_1.3.refs_0_.refs_4_), channel_id=1, source_target_pairs={{0,2},{1,3},{2,0},{3,1},{4,6},{5,7},{6,4},{7,5},{8,10},{9,11},{10,... | collective-permute-start | bytes 786440 | tf_op jit(solution)/shard_map/ppermute | solution.py:263
  102.1 8.7 %collective-permute-start.18 = (bf16[256,512]{1,0:T(8,128)(2,1)}, bf16[256,512]{1,0:T(8,128)(2,1)S(1)}, u32[]{:S(2)}, u32[]{:S(2)}) collective-permute-start(bf16[256,512]{1,0:T(8,128)(2,1)} %emit_1_1.3.refs_0_.refs_4_), channel_id=1, source_target_pairs={{0,1},{1,0},{2,3},{3,2},{4,5},{5,4},{6,7},{7,6},{8,9},{9,8},{10,11... | collective-permute-start | bytes 786440 | tf_op jit(solution)/shard_map/ppermute | solution.py:263
  109.9 5.3 %copy-start.11 = (bf16[256,512]{1,0:T(8,128)(2,1)}, bf16[256,512]{1,0:T(8,128)(2,1)S(1)}, u32[]{:S(2)}) copy-start(bf16[256,512]{1,0:T(8,128)(2,1)S(1)} %collective-permute-done.16.refs_0_) | copy-start | bytes 786436
  109.9 8.2 %collective-permute-start.17 = (bf16[256,512]{1,0:T(8,128)(2,1)S(1)}, bf16[256,512]{1,0:T(8,128)(2,1)S(1)}, u32[]{:S(2)}, u32[]{:S(2)}) collective-permute-start(bf16[256,512]{1,0:T(8,128)(2,1)S(1)} %collective-permute-done.16.refs_0_), channel_id=1, source_target_pairs={{0,1},{1,0},{2,3},{3,2},{4,5},{5,4},{6,7},{7,6},{8,9},{9,8},{10,11... | collective-permute-start | bytes 786440 | tf_op jit(solution)/shard_map/ppermute | solution.py:263
  110.8 0.7 copy-start.2
  118.1 0.7 copy-start.13
  121.4 8.0 %collective-permute-start.19 = (bf16[2,256,256]{2,1,0:T(8,128)(2,1)}, bf16[2,256,256]{2,1,0:T(8,128)(2,1)S(1)}, u32[]{:S(2)}, u32[]{:S(2)}) collective-permute-start(bf16[2,256,256]{2,1,0:T(8,128)(2,1)} %get-tuple-element.40.own_ref), channel_id=1, source_target_pairs={{0,4},{4,0},{8,12},{12,8},{1,5},{5,1},{9,13},{13,9},{2,6},{6,2},{1... | collective-permute-start | bytes 786440 | tf_op jit(solution)/shard_map/ppermute | solution.py:258
  121.4 9.9 %collective-permute-start.20 = (bf16[2,256,256]{2,1,0:T(8,128)(2,1)}, bf16[2,256,256]{2,1,0:T(8,128)(2,1)S(1)}, u32[]{:S(2)}, u32[]{:S(2)}) collective-permute-start(bf16[2,256,256]{2,1,0:T(8,128)(2,1)} %get-tuple-element.40.own_ref), channel_id=1, source_target_pairs={{4,8},{8,4},{5,9},{9,5},{6,10},{10,6},{7,11},{11,7},{20,24},{24,20... | collective-permute-start | bytes 786440 | tf_op jit(solution)/shard_map/ppermute | solution.py:258
  129.5 1.9 %copy-start.9 = (bf16[2,256,256]{2,1,0:T(8,128)(2,1)}, bf16[2,256,256]{2,1,0:T(8,128)(2,1)S(1)}, u32[]{:S(2)}) copy-start(bf16[2,256,256]{2,1,0:T(8,128)(2,1)S(1)} %collective-permute-done.19.even_ref) | copy-start | bytes 786436
  131.3 0.7 copy-start.12
  137.0 4.4 %collective-permute-start.21 = (bf16[256,256]{1,0:T(8,128)(2,1)}, bf16[256,256]{1,0:T(8,128)(2,1)S(1)}, u32[]{:S(2)}, u32[]{:S(2)}) collective-permute-start(bf16[256,256]{1,0:T(8,128)(2,1)} %attend.5.refs_0_), channel_id=1, source_target_pairs={{0,2},{1,3},{2,0},{3,1},{4,6},{5,7},{6,4},{7,5},{8,10},{9,11},{10,... | collective-permute-start | bytes 393224 | tf_op jit(solution)/shard_map/ppermute | solution.py:263
  137.3 5.9 %collective-permute-start.23 = (bf16[256,256]{1,0:T(8,128)(2,1)}, bf16[256,256]{1,0:T(8,128)(2,1)S(1)}, u32[]{:S(2)}, u32[]{:S(2)}) collective-permute-start(bf16[256,256]{1,0:T(8,128)(2,1)} %attend.5.refs_0_), channel_id=1, source_target_pairs={{0,1},{1,0},{2,3},{3,2},{4,5},{5,4},{6,7},{7,6},{8,9},{9,8},{10,11... | collective-permute-start | bytes 393224 | tf_op jit(solution)/shard_map/ppermute | solution.py:263
  141.4 5.4 %copy-start.15 = (bf16[256,256]{1,0:T(8,128)(2,1)}, bf16[256,256]{1,0:T(8,128)(2,1)S(1)}, u32[]{:S(2)}) copy-start(bf16[256,256]{1,0:T(8,128)(2,1)S(1)} %collective-permute-done.21.refs_0_) | copy-start | bytes 393220
  141.4 7.7 %collective-permute-start.22 = (bf16[256,256]{1,0:T(8,128)(2,1)S(1)}, bf16[256,256]{1,0:T(8,128)(2,1)S(1)}, u32[]{:S(2)}, u32[]{:S(2)}) collective-permute-start(bf16[256,256]{1,0:T(8,128)(2,1)S(1)} %collective-permute-done.21.refs_0_), channel_id=1, source_target_pairs={{0,1},{1,0},{2,3},{3,2},{4,5},{5,4},{6,7},{7,6},{8,9},{9,8},{10,11... | collective-permute-start | bytes 393224 | tf_op jit(solution)/shard_map/ppermute | solution.py:263
  143.2 0.7 copy-start.21
  149.1 0.6 copy-start.18
where the time goes:
time: 153 us; the launch traced here: 152 us
  Pallas kernels  72.3 us (47%)
  waiting for transfers between devices  40.3 us (26%)
  starting transfers between devices  23.2 us (15%)
  local copies, waits for them, and re-layouts  12.5 us (8%)
  other arithmetic  3.3 us (2%)
    pallas_call x9, Pallas kernels, project(): pl.pallas_call(partial(project_kernel, parts_n, first, last, full), out_s...  27.5 us
    ppermute x18, waiting for transfers between devices, flip(): return lax.ppermute(block, axis, [(at, at ^ bit) for at in range(count)])  27.3 us
    pallas_call x9, Pallas kernels, emit(): pl.pallas_call(partial(emit_kernel, parts_n), out_shape=jax.ShapeDtypeStr...  22.1 us
    ppermute x18, starting transfers between devices, flip(): return lax.ppermute(block, axis, [(at, at ^ bit) for at in range(count)])  15.9 us
    pallas_call x3, Pallas kernels, attend(): pl.pallas_call(partial(attend_kernel, rows_dev), out_shape=jax.ShapeDtype...  15 us
    ppermute x6, waiting for transfers between devices, exchange(): lax.ppermute(block, axis, [pair for one, two in pairs for pair in ((one,...  13.1 us
    unnamed x49, local copies, waits for them, and re-layouts  10.3 us
    pallas_call x3, Pallas kernels, expand_bias(): pl.pallas_call(bias_kernel, out_shape=jax.ShapeDtypeStruct((heads_n, span...  7.66 us
  transfers between devices with their start and end apart: 24, of which 12 were waited for; matrix products, arithmetic and copies ran while one was open for 4% of the time, Pallas kernels for 28%

commit v1 on v0

v1 whole, which is shorter than its diff:
```python
from functools import partial

import jax
import jax.numpy as jnp
from jax import lax
from jax.experimental import pallas as pl
from jax.experimental.pallas import tpu as pltpu
from jax.sharding import PartitionSpec as P


HEAD_DIM = 64
GRID_W = 64
ROW_SPAN = 8
COL_SPAN = 16
LAYERS = 3
HALF = ROW_SPAN // 2

EPS = 1e-06
NEG = -1e30
LANES = 128
F32 = jnp.float32
BF16 = jnp.bfloat16

PARAMS = pltpu.CompilerParams(vmem_limit_bytes=8 * 2**20)
VMEM = pl.BlockSpec(memory_space=pltpu.VMEM)
HBM = pl.BlockSpec(memory_space=pltpu.HBM)
SMEM = pl.BlockSpec(memory_space=pltpu.SMEM)


def nt_dot(left, right):
    return lax.dot_general(left, right, (((1,), (1,)), ((), ())), preferred_element_type=F32)


def cost(flops, bytes_accessed, transcendentals=0):
    return pl.CostEstimate(
        flops=int(flops), bytes_accessed=int(bytes_accessed), transcendentals=int(transcendentals)
    )


def project_kernel(parts_n, first, last, layer, where_ref, *refs):
    sources, refs = refs[:parts_n], refs[parts_n:]
    gain_ref, refs = refs[0], refs[1:]
    if first:
        stored, refs = refs[:3], refs[3:]
        *refs, held_ref, sems = refs
        copies = [
            pltpu.make_async_copy(stored[kind].at[layer], held_ref.at[kind], sems.at[kind])
            for kind in range(3)
        ]
        for copy in copies:
            copy.start()
    else:
        (held_ref, acc_in, sq_in), refs = refs[:3], refs[3:]
    full = gain_ref.shape[2]
    totals = [None, None, None]
    squares = None
    for at in range(parts_n):
        wide = sources[at][...].astype(F32)
        width = wide.shape[1]
        cols = pl.ds(pl.multiple_of(where_ref[at] * width, LANES), width)
        square = jnp.sum(wide * wide, axis=1, keepdims=True)
        squares = square if squares is None else squares + square
        scaled = (wide * gain_ref[layer, :, cols]).astype(BF16)
        for kind in range(3):
            if first and at == 0:
                copies[kind].wait()
            product = nt_dot(scaled, held_ref[kind, :, cols])
            totals[kind] = product if totals[kind] is None else totals[kind] + product
    if not first:
        squares = squares + sq_in[:, :1]
        totals = [totals[kind] + acc_in[kind] for kind in range(3)]
    if last:
        query_ref, pair_ref = refs
        row_scale = lax.rsqrt(squares * (1.0 / full) + EPS)
        query_ref[...] = (totals[0] * (row_scale * HEAD_DIM ** (-0.5))).astype(BF16)
        pair_ref[0] = (totals[1] * row_scale).astype(BF16)
        pair_ref[1] = (totals[2] * row_scale).astype(BF16)
    else:
        acc_out, sq_out = refs
        for kind in range(3):
            acc_out[kind] = totals[kind]
        sq_out[...] = jnp.broadcast_to(squares, sq_out.shape)


def project(parts, places, weights, carried, last, layer, gain):
    tok, width = parts[0].shape
    parts_n = len(parts)
    first = carried is None
    operands = [places, *parts, gain]
    specs = [SMEM] + [VMEM] * (parts_n + 1)
    if first:
        _, channels, full = weights[0].shape
        operands += weights
        specs += [HBM] * 3
    else:
        _, channels, full = weights.shape
        operands += [weights, *carried]
        specs += [VMEM] * 3
    if last:
        out_shape = [pltpu.VMEM((tok, channels), BF16), pltpu.VMEM((2, tok, channels), BF16)]
    else:
        out_shape = [pltpu.VMEM((3, tok, channels), F32), pltpu.VMEM((tok, LANES), F32)]
    scratch = []
    if first:
        out_shape.append(pltpu.VMEM((3, channels, full), BF16))
        scratch.append(pltpu.SemaphoreType.DMA((3,)))
    flops = 2 * tok * width * channels * 3 * parts_n
    return pl.pallas_call(
        partial(project_kernel, parts_n, first, last, layer),
        out_shape=out_shape,
        in_specs=specs,
        out_specs=[VMEM] * len(out_shape),
        scratch_shapes=scratch,
        cost_estimate=cost(flops, parts_n * width * (channels * 6 + tok * 2) + 4 * tok * channels),
        compiler_params=PARAMS,
    )(*operands)


def emit_kernel(parts_n, first, layer, where_ref, *refs):
    sources, refs = refs[:parts_n], refs[parts_n:]
    if first:
        stored_ref, base_ref, out_ref, held_ref, sem = refs
        copy = pltpu.make_async_copy(stored_ref.at[layer], held_ref, sem)
        copy.start()
    else:
        held_ref, base_ref, out_ref = refs
    total = base_ref[...].astype(F32)
    if first:
        copy.wait()
    for at in range(parts_n):
        width = sources[at].shape[1]
        rows = pl.ds(pl.multiple_of(where_ref[at] * width, HEAD_DIM), width)
        total = total + jnp.dot(sources[at][...], held_ref[rows, :], preferred_element_type=F32)
    out_ref[...] = total.astype(out_ref.dtype)


def emit(parts, places, weight, base, out_type, first, layer):
    tok, width = parts[0].shape
    cols = base.shape[1]
    parts_n = len(parts)
    out_shape = [pltpu.VMEM((tok, cols), out_type)]
    if out_type == BF16 and layer == LAYERS - 1:
        out_shape = [jax.ShapeDtypeStruct((tok, cols), out_type)]
    scratch = []
    if first:
        out_shape.append(pltpu.VMEM(weight.shape[1:], BF16))
        scratch.append(pltpu.SemaphoreType.DMA)
    return pl.pallas_call(
        partial(emit_kernel, parts_n, first, layer),
        out_shape=out_shape,
        in_specs=[SMEM] + [VMEM] * parts_n + [HBM if first else VMEM, VMEM],
        out_specs=[VMEM] * len(out_shape),
        scratch_shapes=scratch,
        cost_estimate=cost(
            2 * tok * width * cols * parts_n, parts_n * width * (cols + tok) * 2 + tok * cols * 6
        ),
        compiler_params=PARAMS,
    )(places, *parts, weight, base)


def bias_kernel(rows_ref, out_ref):
    heads_n, spans = out_ref.shape[:2]
    shape = (GRID_W, LANES)
    query_col = lax.broadcasted_iota(jnp.int32, shape, 0)
    key_col = lax.broadcasted_iota(jnp.int32, shape, 1) % GRID_W
    first_col = jnp.clip(query_col - COL_SPAN // 2, 0, GRID_W - COL_SPAN)
    inside = (key_col >= first_col) & (key_col < first_col + COL_SPAN)
    for head in range(heads_n):
        for span in range(spans):
            row = jnp.broadcast_to(rows_ref[head, span : span + 1, :], shape)
            turned = pltpu.roll(row, LANES - (COL_SPAN - 1), axis=1, stride=1, stride_axis=0)
            out_ref[head, span] = jnp.where(inside, turned, NEG)


def expand_bias(table):
    heads_n, offsets, cols = table.shape
    padded = jnp.pad(table, ((0, 0), (0, 0), (0, GRID_W - cols)))
    rows = jnp.concatenate([padded[:, :-1], padded[:, 1:]], axis=2)
    spans = offsets - 1
    return pl.pallas_call(
        bias_kernel,
        out_shape=pltpu.VMEM((heads_n, spans, GRID_W, LANES), F32),
        in_specs=[VMEM],
        out_specs=VMEM,
        cost_estimate=cost(heads_n * spans * GRID_W * LANES * 40, heads_n * spans * GRID_W * LANES * 4),
        compiler_params=PARAMS,
        name="expand_bias",
    )(rows)


def attend_kernel(
    rows_dev, where_ref, query_ref, own_ref, even_ref, odd_ref, bias_ref, out_ref, keys, values
):
    channels = query_ref.shape[1]
    group = min(LANES, channels)
    heads_in = group // HEAD_DIM
    span = ROW_SPAN * GRID_W
    even_slot = pl.multiple_of(where_ref[0] * GRID_W, GRID_W)
    odd_slot = pl.multiple_of(where_ref[1] * GRID_W, GRID_W)
    halo = HALF * GRID_W
    for scratch, kind in ((keys, 0), (values, 1)):
        scratch[HALF * GRID_W : (HALF + rows_dev) * GRID_W, :] = own_ref[kind]
        scratch[pl.ds(even_slot, halo), :] = even_ref[kind]
        scratch[pl.ds(odd_slot, halo), :] = odd_ref[kind]
    lane = lax.broadcasted_iota(jnp.int32, (GRID_W, group), 1)
    ones = jnp.ones((span, group), BF16)
    for row in range(rows_dev):
        first = pl.multiple_of(where_ref[2 + row] * GRID_W, GRID_W)
        offset = where_ref[2 + rows_dev + row]
        for pair in range(channels // group):
            cols = slice(pair * group, (pair + 1) * group)
            query = query_ref[row * GRID_W : (row + 1) * GRID_W, cols]
            if heads_in > 1:
                zero = jnp.zeros_like(query)
                query = jnp.concatenate(
                    [
                        jnp.where(lane // HEAD_DIM == head, query, zero)
                        for head in range(heads_in)
                    ],
                    axis=0,
                )
            scores = nt_dot(query, keys[pl.ds(first, span), cols])
            pieces = []
            for at in range(span // LANES):
                bias = jnp.concatenate(
                    [
                        bias_ref[pair * heads_in + head, offset + (LANES // GRID_W) * at]
                        for head in range(heads_in)
                    ],
                    axis=0,
                )
                pieces.append(scores[:, at * LANES : (at + 1) * LANES] + bias)
            peak = pieces[0]
            for piece in pieces[1:]:
                peak = jnp.maximum(peak, piece)
            peak = jnp.max(peak, axis=1, keepdims=True)
            lifted = jnp.concatenate([jnp.exp(piece - peak).astype(BF16) for piece in pieces], axis=1)
            mixed = jnp.dot(lifted, values[pl.ds(first, span), cols], preferred_element_type=F32)
            weight = jnp.dot(lifted, ones, preferred_element_type=F32)
            mixed = mixed / weight
            result = mixed[:GRID_W]
            for head in range(1, heads_in):
                result = jnp.where(
                    lane // HEAD_DIM == head, mixed[head * GRID_W : (head + 1) * GRID_W], result
                )
            out_ref[row * GRID_W : (row + 1) * GRID_W, cols] = result.astype(BF16)


def attend(where, query, own, even, odd, bias, rows_dev):
    tok, channels = query.shape
    padded = (rows_dev + 2 * HALF) * GRID_W
    scores = tok * (channels // HEAD_DIM) * ROW_SPAN * GRID_W
    return pl.pallas_call(
        partial(attend_kernel, rows_dev),
        out_shape=pltpu.VMEM((tok, channels), BF16),
        in_specs=[SMEM] + [VMEM] * 5,
        out_specs=VMEM,
        scratch_shapes=[pltpu.VMEM((padded, channels), BF16)] * 2,
        cost_estimate=cost(scores * HEAD_DIM * 6, bias.size * 4 + tok * channels * 16, scores),
        compiler_params=PARAMS,
        name="attend",
    )(where, query, own, even, odd, bias)


def exchange(block, pairs):
    sp, tp = lax.axis_size("sp"), lax.axis_size("tp")
    partner = {}
    for one, two in pairs:
        partner[one], partner[two] = two, one
    moves = []
    for row in range(sp):
        for col in range(tp):
            if row in partner:
                moves.append((row * tp + col, partner[row] * tp + col))
            elif tp % 2 == 0:
                moves.append((row * tp + col, row * tp + (col ^ 1)))
    return lax.ppermute(block, ("sp", "tp"), moves)


def flip(block, axis, bit):
    count = lax.axis_size(axis)
    return lax.ppermute(block, axis, [(at, at ^ bit) for at in range(count)])


def body(hidden_in, norm_gain, query_weight, key_weight, value_weight, output_weight, offset_bias):
    tok_dev, _ = hidden_in.shape
    rows_dev = tok_dev // GRID_W
    tp = lax.axis_size("tp")
    sp = lax.axis_size("sp")
    me = lax.axis_index("tp")
    mine = lax.axis_index("sp")
    all_rows = rows_dev * sp
    first_row = mine * rows_dev
    query_rows = first_row + jnp.arange(rows_dev, dtype=jnp.int32)
    window_first = jnp.clip(query_rows - HALF, 0, all_rows - ROW_SPAN)
    local_first = window_first - first_row + HALF
    offsets = window_first - query_rows + ROW_SPAN - 1
    is_odd = mine % 2
    high = HALF + rows_dev
    slots = jnp.stack([high * (1 - is_odd), high * is_odd])
    where = jnp.concatenate([slots, local_first, offsets]).astype(jnp.int32)
    gain = norm_gain[:, None, :]
    in_hbm = partial(pltpu.with_memory_space_constraint, memory_space=pltpu.HBM)
    weights = [in_hbm(weight) for weight in (query_weight, key_weight, value_weight)]
    output_weight = in_hbm(output_weight)
    near = jnp.stack([me]).astype(jnp.int32)
    far = jnp.stack([me ^ 1, me ^ 2]).astype(jnp.int32)
    last = jnp.stack([me ^ 3]).astype(jnp.int32)
    zero = jnp.zeros((1,), jnp.int32)
    even_pairs = [(at, at + 1) for at in range(0, sp - 1, 2)]
    odd_pairs = [(at, at + 1) for at in range(1, sp - 1, 2)]
    stream = hidden_in
    for layer in range(LAYERS):
        step = partial(project, layer=layer, gain=gain)
        if tp == 4:
            across = flip(stream, "tp", 2)
            beside = flip(stream, "tp", 1)
            corner = flip(across, "tp", 1)
            *carried, held = step([stream], near, weights, None, False)
            carried = step([beside, across], far, held, carried, False)
            query, pair = step([corner], last, held, carried, True)
        else:
            gathered = lax.all_gather(stream, "tp", axis=1, tiled=True)
            query, pair, _ = step([gathered], zero, weights, None, True)
        if rows_dev == HALF:
            to_even = to_odd = pair
        else:
            low, top = pair[:, : HALF * GRID_W], pair[:, (rows_dev - HALF) * GRID_W :]
            to_even = jnp.where(is_odd == 0, top, low)
            to_odd = jnp.where(is_odd == 0, low, top)
        even = exchange(to_even, even_pairs)
        odd = exchange(to_odd, odd_pairs)
        bias = expand_bias(offset_bias[layer])
        attended = attend(where, query, pair, even, odd, bias, rows_dev)
        step = partial(emit, layer=layer)
        if tp == 4:
            across = flip(attended, "tp", 2)
            beside = flip(attended, "tp", 1)
            corner = flip(across, "tp", 1)
            partly, held = step([attended], near, output_weight, stream, F32, True)
            (partly,) = step([beside, across], far, held, partly, F32, False)
            (stream,) = step([corner], last, held, partly, BF16, False)
        else:
            gathered = lax.all_gather(attended, "tp", axis=1, tiled=True)
            stream, _ = step([gathered], zero, output_weight, stream, BF16, True)
    return stream


def solution(mesh):
    return jax.shard_map(
        body,
        mesh=mesh,
        in_specs=(
            P(("grp", "sp"), "tp"),
            P(),
            P(None, "tp", None),
            P(None, "tp", None),
            P(None, "tp", None),
            P(None, None, "tp"),
            P(None, "tp", None, None),
        ),
        out_specs=P(("grp", "sp"), "tp"),
        check_vma=False,
    )
```

time: 153 us -> 98.1 us (0.64)
  Pallas kernels: 72.3 us -> 30.9 us
  local copies, waits for them, and re-layouts: 12.5 us -> 2.56 us
  starting transfers between devices: 23.2 us -> 19.2 us
  waiting for transfers between devices: 40.3 us -> 43.5 us
  other arithmetic: 3.3 us -> 0.4 us
    pallas_call x24, Pallas kernels: 72.3 us -> 30.9 us  [the longest x9 11.8 us: project(): pl.pallas_call(partial(project_kernel, parts_n, first, last, layer), out_...]
    unnamed x49 -> x5, local copies, waits for them, and re-layouts: 10.3 us -> 0.96 us
    ppermute x6, waiting for transfers between devices: 13.1 us -> 20.7 us  [exchange(): return lax.ppermute(block, ('sp', 'tp'), moves)]
    ppermute x6, starting transfers between devices: 7.3 us -> 1.87 us  [exchange(): return lax.ppermute(block, ('sp', 'tp'), moves)]
    ppermute x18, waiting for transfers between devices: 27.3 us -> 22.7 us  [flip(): return lax.ppermute(block, axis, [(at, at ^ bit) for at in range(count)])]
    concatenate x3, other arithmetic: 2.08 us -> 0.24 us  [expand_bias(): rows = jnp.concatenate([padded[:, :-1], padded[:, 1:]], axis=2)]
  transfers between devices with their start and end apart: 24 -> 24, of which waited for: 12 -> 10; matrix products, arithmetic and copies ran while one was open for 4% -> 2% of each run, Pallas kernels for 28% -> 20%
where the time goes in v1:
time: 98.1 us; the launch traced here: 96.9 us
  waiting for transfers between devices  43.5 us (44%)
  Pallas kernels  30.9 us (31%)
  starting transfers between devices  19.2 us (20%)
  local copies, waits for them, and re-layouts  2.56 us (3%)
    ppermute x18, waiting for transfers between devices, flip(): return lax.ppermute(block, axis, [(at, at ^ bit) for at in range(count)])  22.7 us
    ppermute x6, waiting for transfers between devices, exchange(): return lax.ppermute(block, ('sp', 'tp'), moves)  20.7 us
    ppermute x18, starting transfers between devices, flip(): return lax.ppermute(block, axis, [(at, at ^ bit) for at in range(count)])  17.3 us
    pallas_call x9, Pallas kernels, project(): pl.pallas_call(partial(project_kernel, parts_n, first, last, layer), out_...  11.8 us
    pallas_call x3, Pallas kernels, attend(): pl.pallas_call(partial(attend_kernel, rows_dev), out_shape=pltpu.VMEM((to...  9.21 us
    pallas_call x9, Pallas kernels, emit(): pl.pallas_call(partial(emit_kernel, parts_n, first, layer), out_shape=out...  8.31 us
  transfers between devices with their start and end apart: 24, of which 10 were waited for; matrix products, arithmetic and copies ran while one was open for 2% of the time, Pallas kernels for 20%

profile of v1, /device:TPU:19, one launch (start us, length us, event | category | flops | bytes accessed | tf_op | source)
XLA Modules:
  0.0 96.9 jit_solution(15576335913390036701)
XLA Ops:
  0.3 1.0 collective-permute-start.2
  1.2 0.8 fusion
  2.0 0.8 broadcast_in_dim.3.refs_1_.refs_2_
  2.8 0.9 copy-done
  3.8 2.2 %shard_map.73 = (f32[3,256,256]{2,1,0:T(8,128)S(1)}, f32[256,128]{1,0:T(8,128)S(1)}, bf16[3,256,2048]{2,1,0:T(8,128)(2,1)S(1)}) custom-call(s32[1]{0:T(128)} %bitcast.3.where_ref, bf16[256,512]{1,0:T(8,128)(2,1)S(1)} %copy-done, f32[3,1,2048]{2,1,0:T(1,128)S(1)} %broadcast_in_dim.3.refs_1_.refs_2_, bf16[3,256,2048]{2,1,0:T(8,128)(2,1)} %refs_2_.7, ...), custom_call_target="tpu_custom_call" | custom-call | flops 201326592 | bytes 1310720 | tf_op jit(solution)/shard_map/pallas_call | solution.py:108
  6.0 1.4 %collective-permute-done.refs_1_ = bf16[256,512]{1,0:T(8,128)(2,1)S(1)} collective-permute-done((bf16[256,512]{1,0:T(8,128)(2,1)}, bf16[256,512]{1,0:T(8,128)(2,1)S(1)}, u32[]{:S(2)}, u32[]{:S(2)}) %collective-permute-start) | collective-permute-done | bytes 262176 | tf_op jit(solution)/shard_map/ppermute | solution.py:282
  7.4 1.5 %collective-permute-start.1 = (bf16[256,512]{1,0:T(8,128)(2,1)S(1)}, bf16[256,512]{1,0:T(8,128)(2,1)S(1)}, u32[]{:S(2)}, u32[]{:S(2)}) collective-permute-start(bf16[256,512]{1,0:T(8,128)(2,1)S(1)} %collective-permute-done.refs_1_), channel_id=1, source_target_pairs={{0,1},{1,0},{2,3},{3,2},{4,5},{5,4},{6,7},{7,6},{8,9},{9,8},{10,11... | collective-permute-start | bytes 786440 | tf_op jit(solution)/shard_map/ppermute | solution.py:282
  9.0 1.2 %shard_map.74 = (f32[3,256,256]{2,1,0:T(8,128)S(1)}, f32[256,128]{1,0:T(8,128)S(1)}) custom-call(s32[2]{0:T(128)S(1)} %pad_add_fusion.1.where_ref, bf16[256,512]{1,0:T(8,128)(2,1)S(1)} %collective-permute-done.2.refs_0_, bf16[256,512]{1,0:T(8,128)(2,1)S(1)} %collective-permute-done.refs_1_, f32[3,1,2048]{2,1,0:T(1,128)S(1)} %broadcast_in_dim.3.refs_1_.refs_2_, ...), custom_call_target="tpu_custom_call" | custom-call | flops 402653184 | bytes 2359296 | tf_op jit(solution)/shard_map/pallas_call | solution.py:108
  10.3 0.5 shard_map.75
  10.8 1.4 %collective-permute-start.3 = (bf16[2,256,256]{2,1,0:T(8,128)(2,1)S(1)}, bf16[2,256,256]{2,1,0:T(8,128)(2,1)S(1)}, u32[]{:S(2)}, u32[]{:S(2)}) collective-permute-start(bf16[2,256,256]{2,1,0:T(8,128)(2,1)S(1)} %get-tuple-element.38.own_ref), channel_id=1, source_target_pairs={{0,4},{1,5},{2,6},{3,7},{4,0},{5,1},{6,2},{7,3},{8,12},{9,13},{10,... | collective-permute-start | bytes 786440 | tf_op jit(solution)/shard_map/ppermute | solution.py:277
  12.2 0.5 expand_bias.3.bias_ref
  12.9 5.7 %collective-permute-done.3.even_ref = bf16[2,256,256]{2,1,0:T(8,128)(2,1)S(1)} collective-permute-done((bf16[2,256,256]{2,1,0:T(8,128)(2,1)S(1)}, bf16[2,256,256]{2,1,0:T(8,128)(2,1)S(1)}, u32[]{:S(2)}, u32[]{:S(2)}) %collective-permute-start.3) | collective-permute-done | bytes 262176 | tf_op jit(solution)/shard_map/ppermute | solution.py:277
  18.5 1.0 %collective-permute-done.4.odd_ref = bf16[2,256,256]{2,1,0:T(8,128)(2,1)S(1)} collective-permute-done((bf16[2,256,256]{2,1,0:T(8,128)(2,1)S(1)}, bf16[2,256,256]{2,1,0:T(8,128)(2,1)S(1)}, u32[]{:S(2)}, u32[]{:S(2)}) %collective-permute-start.4) | collective-permute-done | bytes 262176 | tf_op jit(solution)/shard_map/ppermute | solution.py:277
  19.6 3.1 %attend.3.refs_0_ = bf16[256,256]{1,0:T(8,128)(2,1)S(1)} custom-call(s32[10]{0:T(128)S(1)} %pad_add_fusion.where_ref, bf16[256,256]{1,0:T(8,128)(2,1)S(1)} %get-tuple-element.37.query_ref, bf16[2,256,256]{2,1,0:T(8,128)(2,1)S(1)} %get-tuple-element.38.own_ref, bf16[2,256,256]{2,1,0:T(8,128)(2,1)S(1)} %collective-permute-done.3.even_ref, ...), custom_call_target="tpu_custom_call" | custom-call | flops 201326592 | bytes 2883584 | tf_op jit(solution)/shard_map/attend/pallas_call | solution.py:253
  23.0 1.6 %collective-permute-start.7 = (bf16[256,256]{1,0:T(8,128)(2,1)S(1)}, bf16[256,256]{1,0:T(8,128)(2,1)S(1)}, u32[]{:S(2)}, u32[]{:S(2)}) collective-permute-start(bf16[256,256]{1,0:T(8,128)(2,1)S(1)} %attend.3.refs_0_), channel_id=1, source_target_pairs={{0,1},{1,0},{2,3},{3,2},{4,5},{5,4},{6,7},{7,6},{8,9},{9,8},{10,11... | collective-permute-start | bytes 393224 | tf_op jit(solution)/shard_map/ppermute | solution.py:282
  24.5 2.0 %collective-permute-done.5.refs_1_ = bf16[256,256]{1,0:T(8,128)(2,1)S(1)} collective-permute-done((bf16[256,256]{1,0:T(8,128)(2,1)S(1)}, bf16[256,256]{1,0:T(8,128)(2,1)S(1)}, u32[]{:S(2)}, u32[]{:S(2)}) %collective-permute-start.5) | collective-permute-done | bytes 131104 | tf_op jit(solution)/shard_map/ppermute | solution.py:282
  26.5 2.4 %collective-permute-start.6 = (bf16[256,256]{1,0:T(8,128)(2,1)S(1)}, bf16[256,256]{1,0:T(8,128)(2,1)S(1)}, u32[]{:S(2)}, u32[]{:S(2)}) collective-permute-start(bf16[256,256]{1,0:T(8,128)(2,1)S(1)} %collective-permute-done.5.refs_1_), channel_id=1, source_target_pairs={{0,1},{1,0},{2,3},{3,2},{4,5},{5,4},{6,7},{7,6},{8,9},{9,8},{10,11... | collective-permute-start | bytes 393224 | tf_op jit(solution)/shard_map/ppermute | solution.py:282
  29.0 1.5 %shard_map.76 = (f32[256,512]{1,0:T(8,128)S(1)}, bf16[1024,512]{1,0:T(8,128)(2,1)S(1)}) custom-call(s32[1]{0:T(128)} %bitcast.3.where_ref, bf16[256,256]{1,0:T(8,128)(2,1)S(1)} %attend.3.refs_0_, bf16[3,1024,512]{2,1,0:T(8,128)(2,1)} %refs_1_.5, bf16[256,512]{1,0:T(8,128)(2,1)S(1)} %copy-done.1), custom_call_target="tpu_custom_call" | custom-call | flops 67108864 | bytes 1179648 | tf_op jit(solution)/shard_map/pallas_call | solution.py:148
  30.4 0.8 shard_map.77.refs_2_
  32.2 7.3 %collective-permute-done.8.refs_1_ = bf16[256,512]{1,0:T(8,128)(2,1)S(1)} collective-permute-done((bf16[256,512]{1,0:T(8,128)(2,1)S(1)}, bf16[256,512]{1,0:T(8,128)(2,1)S(1)}, u32[]{:S(2)}, u32[]{:S(2)}) %collective-permute-start.8) | collective-permute-done | bytes 262176 | tf_op jit(solution)/shard_map/ppermute | solution.py:282
  39.5 0.9 collective-permute-start.9
  40.3 2.2 %shard_map.79 = (f32[3,256,256]{2,1,0:T(8,128)S(1)}, f32[256,128]{1,0:T(8,128)S(1)}, bf16[3,256,2048]{2,1,0:T(8,128)(2,1)S(1)}) custom-call(s32[1]{0:T(128)} %bitcast.3.where_ref, bf16[256,512]{1,0:T(8,128)(2,1)S(1)} %shard_map.78.refs_0_.refs_2_, f32[3,1,2048]{2,1,0:T(1,128)S(1)} %broadcast_in_dim.3.refs_1_.refs_2_, bf16[3,256,2048]{2,1,0:T(8,128)(2,1)} %refs_2_.7, ...), custom_call_target="tpu_custom_call" | custom-call | flops 201326592 | bytes 1310720 | tf_op jit(solution)/shard_map/pallas_call | solution.py:108
  42.6 1.2 %shard_map.80 = (f32[3,256,256]{2,1,0:T(8,128)S(1)}, f32[256,128]{1,0:T(8,128)S(1)}) custom-call(s32[2]{0:T(128)S(1)} %pad_add_fusion.1.where_ref, bf16[256,512]{1,0:T(8,128)(2,1)S(1)} %collective-permute-done.10.refs_0_, bf16[256,512]{1,0:T(8,128)(2,1)S(1)} %collective-permute-done.8.refs_1_, f32[3,1,2048]{2,1,0:T(1,128)S(1)} %broadcast_in_dim.3.refs_1_.refs_2_, ...), custom_call_target="tpu_custom_call" | custom-call | flops 402653184 | bytes 2359296 | tf_op jit(solution)/shard_map/pallas_call | solution.py:108
  43.8 0.5 shard_map.81
  44.6 0.5 expand_bias.4.bias_ref
  45.1 7.1 %collective-permute-done.11.even_ref = bf16[2,256,256]{2,1,0:T(8,128)(2,1)S(1)} collective-permute-done((bf16[2,256,256]{2,1,0:T(8,128)(2,1)S(1)}, bf16[2,256,256]{2,1,0:T(8,128)(2,1)S(1)}, u32[]{:S(2)}, u32[]{:S(2)}) %collective-permute-start.11) | collective-permute-done | bytes 262176 | tf_op jit(solution)/shard_map/ppermute | solution.py:277
  52.2 3.1 %attend.4.refs_0_ = bf16[256,256]{1,0:T(8,128)(2,1)S(1)} custom-call(s32[10]{0:T(128)S(1)} %pad_add_fusion.where_ref, bf16[256,256]{1,0:T(8,128)(2,1)S(1)} %get-tuple-element.46.query_ref, bf16[2,256,256]{2,1,0:T(8,128)(2,1)S(1)} %get-tuple-element.47.own_ref, bf16[2,256,256]{2,1,0:T(8,128)(2,1)S(1)} %collective-permute-done.11.even_ref, ...), custom_call_target="tpu_custom_call" | custom-call | flops 201326592 | bytes 2883584 | tf_op jit(solution)/shard_map/attend/pallas_call | solution.py:253
  55.3 0.3 collective-permute-start.13
  55.6 1.2 %collective-permute-start.15 = (bf16[256,256]{1,0:T(8,128)(2,1)S(1)}, bf16[256,256]{1,0:T(8,128)(2,1)S(1)}, u32[]{:S(2)}, u32[]{:S(2)}) collective-permute-start(bf16[256,256]{1,0:T(8,128)(2,1)S(1)} %attend.4.refs_0_), channel_id=1, source_target_pairs={{0,1},{1,0},{2,3},{3,2},{4,5},{5,4},{6,7},{7,6},{8,9},{9,8},{10,11... | collective-permute-start | bytes 393224 | tf_op jit(solution)/shard_map/ppermute | solution.py:282
  56.8 2.3 %collective-permute-done.13.refs_1_ = bf16[256,256]{1,0:T(8,128)(2,1)S(1)} collective-permute-done((bf16[256,256]{1,0:T(8,128)(2,1)S(1)}, bf16[256,256]{1,0:T(8,128)(2,1)S(1)}, u32[]{:S(2)}, u32[]{:S(2)}) %collective-permute-start.13) | collective-permute-done | bytes 131104 | tf_op jit(solution)/shard_map/ppermute | solution.py:282
  59.2 2.1 %collective-permute-start.14 = (bf16[256,256]{1,0:T(8,128)(2,1)S(1)}, bf16[256,256]{1,0:T(8,128)(2,1)S(1)}, u32[]{:S(2)}, u32[]{:S(2)}) collective-permute-start(bf16[256,256]{1,0:T(8,128)(2,1)S(1)} %collective-permute-done.13.refs_1_), channel_id=1, source_target_pairs={{0,1},{1,0},{2,3},{3,2},{4,5},{5,4},{6,7},{7,6},{8,9},{9,8},{10,11... | collective-permute-start | bytes 393224 | tf_op jit(solution)/shard_map/ppermute | solution.py:282
  61.3 1.5 %shard_map.82 = (f32[256,512]{1,0:T(8,128)S(1)}, bf16[1024,512]{1,0:T(8,128)(2,1)S(1)}) custom-call(s32[1]{0:T(128)} %bitcast.3.where_ref, bf16[256,256]{1,0:T(8,128)(2,1)S(1)} %attend.4.refs_0_, bf16[3,1024,512]{2,1,0:T(8,128)(2,1)} %refs_1_.5, bf16[256,512]{1,0:T(8,128)(2,1)S(1)} %shard_map.78.refs_0_.refs_2_), custom_call_target="tpu_custom_call" | custom-call | flops 67108864 | bytes 1179648 | tf_op jit(solution)/shard_map/pallas_call | solution.py:148
  62.8 0.8 shard_map.83.refs_2_
  64.5 7.3 %collective-permute-done.16.refs_1_ = bf16[256,512]{1,0:T(8,128)(2,1)S(1)} collective-permute-done((bf16[256,512]{1,0:T(8,128)(2,1)S(1)}, bf16[256,512]{1,0:T(8,128)(2,1)S(1)}, u32[]{:S(2)}, u32[]{:S(2)}) %collective-permute-start.16) | collective-permute-done | bytes 262176 | tf_op jit(solution)/shard_map/ppermute | solution.py:282
  71.8 0.8 collective-permute-start.17
  72.6 2.2 %shard_map.85 = (f32[3,256,256]{2,1,0:T(8,128)S(1)}, f32[256,128]{1,0:T(8,128)S(1)}, bf16[3,256,2048]{2,1,0:T(8,128)(2,1)S(1)}) custom-call(s32[1]{0:T(128)} %bitcast.3.where_ref, bf16[256,512]{1,0:T(8,128)(2,1)S(1)} %shard_map.84.refs_0_.refs_2_, f32[3,1,2048]{2,1,0:T(1,128)S(1)} %broadcast_in_dim.3.refs_1_.refs_2_, bf16[3,256,2048]{2,1,0:T(8,128)(2,1)} %refs_2_.7, ...), custom_call_target="tpu_custom_call" | custom-call | flops 201326592 | bytes 1310720 | tf_op jit(solution)/shard_map/pallas_call | solution.py:108
  74.9 1.2 %shard_map.86 = (f32[3,256,256]{2,1,0:T(8,128)S(1)}, f32[256,128]{1,0:T(8,128)S(1)}) custom-call(s32[2]{0:T(128)S(1)} %pad_add_fusion.1.where_ref, bf16[256,512]{1,0:T(8,128)(2,1)S(1)} %collective-permute-done.18.refs_0_, bf16[256,512]{1,0:T(8,128)(2,1)S(1)} %collective-permute-done.16.refs_1_, f32[3,1,2048]{2,1,0:T(1,128)S(1)} %broadcast_in_dim.3.refs_1_.refs_2_, ...), custom_call_target="tpu_custom_call" | custom-call | flops 402653184 | bytes 2359296 | tf_op jit(solution)/shard_map/pallas_call | solution.py:108
  76.1 0.5 shard_map.87
  77.1 0.5 expand_bias.5.bias_ref
  77.6 6.9 %collective-permute-done.19.even_ref = bf16[2,256,256]{2,1,0:T(8,128)(2,1)S(1)} collective-permute-done((bf16[2,256,256]{2,1,0:T(8,128)(2,1)S(1)}, bf16[2,256,256]{2,1,0:T(8,128)(2,1)S(1)}, u32[]{:S(2)}, u32[]{:S(2)}) %collective-permute-start.19) | collective-permute-done | bytes 262176 | tf_op jit(solution)/shard_map/ppermute | solution.py:277
  84.5 3.1 %attend.5.refs_0_ = bf16[256,256]{1,0:T(8,128)(2,1)S(1)} custom-call(s32[10]{0:T(128)S(1)} %pad_add_fusion.where_ref, bf16[256,256]{1,0:T(8,128)(2,1)S(1)} %get-tuple-element.55.query_ref, bf16[2,256,256]{2,1,0:T(8,128)(2,1)S(1)} %get-tuple-element.56.own_ref, bf16[2,256,256]{2,1,0:T(8,128)(2,1)S(1)} %collective-permute-done.19.even_ref, ...), custom_call_target="tpu_custom_call" | custom-call | flops 201326592 | bytes 2883584 | tf_op jit(solution)/shard_map/attend/pallas_call | solution.py:253
  87.6 0.3 collective-permute-start.21
  87.9 1.2 %collective-permute-start.23 = (bf16[256,256]{1,0:T(8,128)(2,1)S(1)}, bf16[256,256]{1,0:T(8,128)(2,1)S(1)}, u32[]{:S(2)}, u32[]{:S(2)}) collective-permute-start(bf16[256,256]{1,0:T(8,128)(2,1)S(1)} %attend.5.refs_0_), channel_id=1, source_target_pairs={{0,1},{1,0},{2,3},{3,2},{4,5},{5,4},{6,7},{7,6},{8,9},{9,8},{10,11... | collective-permute-start | bytes 393224 | tf_op jit(solution)/shard_map/ppermute | solution.py:282
  89.2 2.3 %collective-permute-done.21.refs_1_ = bf16[256,256]{1,0:T(8,128)(2,1)S(1)} collective-permute-done((bf16[256,256]{1,0:T(8,128)(2,1)S(1)}, bf16[256,256]{1,0:T(8,128)(2,1)S(1)}, u32[]{:S(2)}, u32[]{:S(2)}) %collective-permute-start.21) | collective-permute-done | bytes 131104 | tf_op jit(solution)/shard_map/ppermute | solution.py:282
  91.5 2.1 %collective-permute-start.22 = (bf16[256,256]{1,0:T(8,128)(2,1)S(1)}, bf16[256,256]{1,0:T(8,128)(2,1)S(1)}, u32[]{:S(2)}, u32[]{:S(2)}) collective-permute-start(bf16[256,256]{1,0:T(8,128)(2,1)S(1)} %collective-permute-done.21.refs_1_), channel_id=1, source_target_pairs={{0,1},{1,0},{2,3},{3,2},{4,5},{5,4},{6,7},{7,6},{8,9},{9,8},{10,11... | collective-permute-start | bytes 393224 | tf_op jit(solution)/shard_map/ppermute | solution.py:282
  93.6 1.5 %shard_map.88 = (f32[256,512]{1,0:T(8,128)S(1)}, bf16[1024,512]{1,0:T(8,128)(2,1)S(1)}) custom-call(s32[1]{0:T(128)} %bitcast.3.where_ref, bf16[256,256]{1,0:T(8,128)(2,1)S(1)} %attend.5.refs_0_, bf16[3,1024,512]{2,1,0:T(8,128)(2,1)} %refs_1_.5, bf16[256,512]{1,0:T(8,128)(2,1)S(1)} %shard_map.84.refs_0_.refs_2_), custom_call_target="tpu_custom_call" | custom-call | flops 67108864 | bytes 1179648 | tf_op jit(solution)/shard_map/pallas_call | solution.py:148
  95.1 0.8 shard_map.89.refs_2_
  95.9 0.9 shard_map.90
  (41 shorter events, 3.3 us)
Async XLA Ops:
  0.0 7.4 %collective-permute-start = (bf16[256,512]{1,0:T(8,128)(2,1)}, bf16[256,512]{1,0:T(8,128)(2,1)S(1)}, u32[]{:S(2)}, u32[]{:S(2)}) collective-permute-start(bf16[256,512]{1,0:T(8,128)(2,1)} %refs_2_.5), channel_id=1, source_target_pairs={{0,2},{1,3},{2,0},{3,1},{4,6},{5,7},{6,4},{7,5},{8,10},{9,11},{10,... | collective-permute-start | bytes 786440 | tf_op jit(solution)/shard_map/ppermute | solution.py:282
  0.3 8.8 %collective-permute-start.2 = (bf16[256,512]{1,0:T(8,128)(2,1)}, bf16[256,512]{1,0:T(8,128)(2,1)S(1)}, u32[]{:S(2)}, u32[]{:S(2)}) collective-permute-start(bf16[256,512]{1,0:T(8,128)(2,1)} %refs_2_.5), channel_id=1, source_target_pairs={{0,1},{1,0},{2,3},{3,2},{4,5},{5,4},{6,7},{7,6},{8,9},{9,8},{10,11... | collective-permute-start | bytes 786440 | tf_op jit(solution)/shard_map/ppermute | solution.py:282
  2.8 1.0 copy-start
  7.4 2.9 %collective-permute-start.1 = (bf16[256,512]{1,0:T(8,128)(2,1)S(1)}, bf16[256,512]{1,0:T(8,128)(2,1)S(1)}, u32[]{:S(2)}, u32[]{:S(2)}) collective-permute-start(bf16[256,512]{1,0:T(8,128)(2,1)S(1)} %collective-permute-done.refs_1_), channel_id=1, source_target_pairs={{0,1},{1,0},{2,3},{3,2},{4,5},{5,4},{6,7},{7,6},{8,9},{9,8},{10,11... | collective-permute-start | bytes 786440 | tf_op jit(solution)/shard_map/ppermute | solution.py:282
  10.8 18.2 %copy-start.1 = (bf16[256,512]{1,0:T(8,128)(2,1)S(1)}, bf16[256,512]{1,0:T(8,128)(2,1)}, u32[]{:S(2)}) copy-start(bf16[256,512]{1,0:T(8,128)(2,1)} %refs_2_.5) | copy-start | bytes 786436
  10.8 7.8 %collective-permute-start.3 = (bf16[2,256,256]{2,1,0:T(8,128)(2,1)S(1)}, bf16[2,256,256]{2,1,0:T(8,128)(2,1)S(1)}, u32[]{:S(2)}, u32[]{:S(2)}) collective-permute-start(bf16[2,256,256]{2,1,0:T(8,128)(2,1)S(1)} %get-tuple-element.38.own_ref), channel_id=1, source_target_pairs={{0,4},{1,5},{2,6},{3,7},{4,0},{5,1},{6,2},{7,3},{8,12},{9,13},{10,... | collective-permute-start | bytes 786440 | tf_op jit(solution)/shard_map/ppermute | solution.py:277
  12.1 7.4 %collective-permute-start.4 = (bf16[2,256,256]{2,1,0:T(8,128)(2,1)S(1)}, bf16[2,256,256]{2,1,0:T(8,128)(2,1)S(1)}, u32[]{:S(2)}, u32[]{:S(2)}) collective-permute-start(bf16[2,256,256]{2,1,0:T(8,128)(2,1)S(1)} %get-tuple-element.38.own_ref), channel_id=1, source_target_pairs={{0,1},{1,0},{2,3},{3,2},{4,8},{5,9},{6,10},{7,11},{8,4},{9,5},{10,... | collective-permute-start | bytes 786440 | tf_op jit(solution)/shard_map/ppermute | solution.py:277
  22.6 3.9 %collective-permute-start.5 = (bf16[256,256]{1,0:T(8,128)(2,1)S(1)}, bf16[256,256]{1,0:T(8,128)(2,1)S(1)}, u32[]{:S(2)}, u32[]{:S(2)}) collective-permute-start(bf16[256,256]{1,0:T(8,128)(2,1)S(1)} %attend.3.refs_0_), channel_id=1, source_target_pairs={{0,2},{1,3},{2,0},{3,1},{4,6},{5,7},{6,4},{7,5},{8,10},{9,11},{10,... | collective-permute-start | bytes 393224 | tf_op jit(solution)/shard_map/ppermute | solution.py:282
  23.0 7.5 %collective-permute-start.7 = (bf16[256,256]{1,0:T(8,128)(2,1)S(1)}, bf16[256,256]{1,0:T(8,128)(2,1)S(1)}, u32[]{:S(2)}, u32[]{:S(2)}) collective-permute-start(bf16[256,256]{1,0:T(8,128)(2,1)S(1)} %attend.3.refs_0_), channel_id=1, source_target_pairs={{0,1},{1,0},{2,3},{3,2},{4,5},{5,4},{6,7},{7,6},{8,9},{9,8},{10,11... | collective-permute-start | bytes 393224 | tf_op jit(solution)/shard_map/ppermute | solution.py:282
  26.5 4.8 %collective-permute-start.6 = (bf16[256,256]{1,0:T(8,128)(2,1)S(1)}, bf16[256,256]{1,0:T(8,128)(2,1)S(1)}, u32[]{:S(2)}, u32[]{:S(2)}) collective-permute-start(bf16[256,256]{1,0:T(8,128)(2,1)S(1)} %collective-permute-done.5.refs_1_), channel_id=1, source_target_pairs={{0,1},{1,0},{2,3},{3,2},{4,5},{5,4},{6,7},{7,6},{8,9},{9,8},{10,11... | collective-permute-start | bytes 393224 | tf_op jit(solution)/shard_map/ppermute | solution.py:282
  31.5 7.9 %collective-permute-start.8 = (bf16[256,512]{1,0:T(8,128)(2,1)S(1)}, bf16[256,512]{1,0:T(8,128)(2,1)S(1)}, u32[]{:S(2)}, u32[]{:S(2)}) collective-permute-start(bf16[256,512]{1,0:T(8,128)(2,1)S(1)} %shard_map.78.refs_0_.refs_2_), channel_id=1, source_target_pairs={{0,2},{1,3},{2,0},{3,1},{4,6},{5,7},{6,4},{7,5},{8,10},{9,11},{10,... | collective-permute-start | bytes 786440 | tf_op jit(solution)/shard_map/ppermute | solution.py:282
  31.9 10.7 %collective-permute-start.10 = (bf16[256,512]{1,0:T(8,128)(2,1)S(1)}, bf16[256,512]{1,0:T(8,128)(2,1)S(1)}, u32[]{:S(2)}, u32[]{:S(2)}) collective-permute-start(bf16[256,512]{1,0:T(8,128)(2,1)S(1)} %shard_map.78.refs_0_.refs_2_), channel_id=1, source_target_pairs={{0,1},{1,0},{2,3},{3,2},{4,5},{5,4},{6,7},{7,6},{8,9},{9,8},{10,11... | collective-permute-start | bytes 786440 | tf_op jit(solution)/shard_map/ppermute | solution.py:282
  39.5 4.4 %collective-permute-start.9 = (bf16[256,512]{1,0:T(8,128)(2,1)S(1)}, bf16[256,512]{1,0:T(8,128)(2,1)S(1)}, u32[]{:S(2)}, u32[]{:S(2)}) collective-permute-start(bf16[256,512]{1,0:T(8,128)(2,1)S(1)} %collective-permute-done.8.refs_1_), channel_id=1, source_target_pairs={{0,1},{1,0},{2,3},{3,2},{4,5},{5,4},{6,7},{7,6},{8,9},{9,8},{10,11... | collective-permute-start | bytes 786440 | tf_op jit(solution)/shard_map/ppermute | solution.py:282
  44.3 7.9 %collective-permute-start.11 = (bf16[2,256,256]{2,1,0:T(8,128)(2,1)S(1)}, bf16[2,256,256]{2,1,0:T(8,128)(2,1)S(1)}, u32[]{:S(2)}, u32[]{:S(2)}) collective-permute-start(bf16[2,256,256]{2,1,0:T(8,128)(2,1)S(1)} %get-tuple-element.47.own_ref), channel_id=1, source_target_pairs={{0,4},{1,5},{2,6},{3,7},{4,0},{5,1},{6,2},{7,3},{8,12},{9,13},{10,... | collective-permute-start | bytes 786440 | tf_op jit(solution)/shard_map/ppermute | solution.py:277
  44.4 7.8 %collective-permute-start.12 = (bf16[2,256,256]{2,1,0:T(8,128)(2,1)S(1)}, bf16[2,256,256]{2,1,0:T(8,128)(2,1)S(1)}, u32[]{:S(2)}, u32[]{:S(2)}) collective-permute-start(bf16[2,256,256]{2,1,0:T(8,128)(2,1)S(1)} %get-tuple-element.47.own_ref), channel_id=1, source_target_pairs={{0,1},{1,0},{2,3},{3,2},{4,8},{5,9},{6,10},{7,11},{8,4},{9,5},{10,... | collective-permute-start | bytes 786440 | tf_op jit(solution)/shard_map/ppermute | solution.py:277
  55.3 3.9 %collective-permute-start.13 = (bf16[256,256]{1,0:T(8,128)(2,1)S(1)}, bf16[256,256]{1,0:T(8,128)(2,1)S(1)}, u32[]{:S(2)}, u32[]{:S(2)}) collective-permute-start(bf16[256,256]{1,0:T(8,128)(2,1)S(1)} %attend.4.refs_0_), channel_id=1, source_target_pairs={{0,2},{1,3},{2,0},{3,1},{4,6},{5,7},{6,4},{7,5},{8,10},{9,11},{10,... | collective-permute-start | bytes 393224 | tf_op jit(solution)/shard_map/ppermute | solution.py:282
  55.6 7.1 %collective-permute-start.15 = (bf16[256,256]{1,0:T(8,128)(2,1)S(1)}, bf16[256,256]{1,0:T(8,128)(2,1)S(1)}, u32[]{:S(2)}, u32[]{:S(2)}) collective-permute-start(bf16[256,256]{1,0:T(8,128)(2,1)S(1)} %attend.4.refs_0_), channel_id=1, source_target_pairs={{0,1},{1,0},{2,3},{3,2},{4,5},{5,4},{6,7},{7,6},{8,9},{9,8},{10,11... | collective-permute-start | bytes 393224 | tf_op jit(solution)/shard_map/ppermute | solution.py:282
  59.2 4.4 %collective-permute-start.14 = (bf16[256,256]{1,0:T(8,128)(2,1)S(1)}, bf16[256,256]{1,0:T(8,128)(2,1)S(1)}, u32[]{:S(2)}, u32[]{:S(2)}) collective-permute-start(bf16[256,256]{1,0:T(8,128)(2,1)S(1)} %collective-permute-done.13.refs_1_), channel_id=1, source_target_pairs={{0,1},{1,0},{2,3},{3,2},{4,5},{5,4},{6,7},{7,6},{8,9},{9,8},{10,11... | collective-permute-start | bytes 393224 | tf_op jit(solution)/shard_map/ppermute | solution.py:282
  63.8 7.9 %collective-permute-start.16 = (bf16[256,512]{1,0:T(8,128)(2,1)S(1)}, bf16[256,512]{1,0:T(8,128)(2,1)S(1)}, u32[]{:S(2)}, u32[]{:S(2)}) collective-permute-start(bf16[256,512]{1,0:T(8,128)(2,1)S(1)} %shard_map.84.refs_0_.refs_2_), channel_id=1, source_target_pairs={{0,2},{1,3},{2,0},{3,1},{4,6},{5,7},{6,4},{7,5},{8,10},{9,11},{10,... | collective-permute-start | bytes 786440 | tf_op jit(solution)/shard_map/ppermute | solution.py:282
  64.2 10.7 %collective-permute-start.18 = (bf16[256,512]{1,0:T(8,128)(2,1)S(1)}, bf16[256,512]{1,0:T(8,128)(2,1)S(1)}, u32[]{:S(2)}, u32[]{:S(2)}) collective-permute-start(bf16[256,512]{1,0:T(8,128)(2,1)S(1)} %shard_map.84.refs_0_.refs_2_), channel_id=1, source_target_pairs={{0,1},{1,0},{2,3},{3,2},{4,5},{5,4},{6,7},{7,6},{8,9},{9,8},{10,11... | collective-permute-start | bytes 786440 | tf_op jit(solution)/shard_map/ppermute | solution.py:282
  71.8 4.4 %collective-permute-start.17 = (bf16[256,512]{1,0:T(8,128)(2,1)S(1)}, bf16[256,512]{1,0:T(8,128)(2,1)S(1)}, u32[]{:S(2)}, u32[]{:S(2)}) collective-permute-start(bf16[256,512]{1,0:T(8,128)(2,1)S(1)} %collective-permute-done.16.refs_1_), channel_id=1, source_target_pairs={{0,1},{1,0},{2,3},{3,2},{4,5},{5,4},{6,7},{7,6},{8,9},{9,8},{10,11... | collective-permute-start | bytes 786440 | tf_op jit(solution)/shard_map/ppermute | solution.py:282
  76.6 7.9 %collective-permute-start.19 = (bf16[2,256,256]{2,1,0:T(8,128)(2,1)S(1)}, bf16[2,256,256]{2,1,0:T(8,128)(2,1)S(1)}, u32[]{:S(2)}, u32[]{:S(2)}) collective-permute-start(bf16[2,256,256]{2,1,0:T(8,128)(2,1)S(1)} %get-tuple-element.56.own_ref), channel_id=1, source_target_pairs={{0,4},{1,5},{2,6},{3,7},{4,0},{5,1},{6,2},{7,3},{8,12},{9,13},{10,... | collective-permute-start | bytes 786440 | tf_op jit(solution)/shard_map/ppermute | solution.py:277
  76.7 7.8 %collective-permute-start.20 = (bf16[2,256,256]{2,1,0:T(8,128)(2,1)S(1)}, bf16[2,256,256]{2,1,0:T(8,128)(2,1)S(1)}, u32[]{:S(2)}, u32[]{:S(2)}) collective-permute-start(bf16[2,256,256]{2,1,0:T(8,128)(2,1)S(1)} %get-tuple-element.56.own_ref), channel_id=1, source_target_pairs={{0,1},{1,0},{2,3},{3,2},{4,8},{5,9},{6,10},{7,11},{8,4},{9,5},{10,... | collective-permute-start | bytes 786440 | tf_op jit(solution)/shard_map/ppermute | solution.py:277
  87.6 3.9 %collective-permute-start.21 = (bf16[256,256]{1,0:T(8,128)(2,1)S(1)}, bf16[256,256]{1,0:T(8,128)(2,1)S(1)}, u32[]{:S(2)}, u32[]{:S(2)}) collective-permute-start(bf16[256,256]{1,0:T(8,128)(2,1)S(1)} %attend.5.refs_0_), channel_id=1, source_target_pairs={{0,2},{1,3},{2,0},{3,1},{4,6},{5,7},{6,4},{7,5},{8,10},{9,11},{10,... | collective-permute-start | bytes 393224 | tf_op jit(solution)/shard_map/ppermute | solution.py:282
  87.9 7.1 %collective-permute-start.23 = (bf16[256,256]{1,0:T(8,128)(2,1)S(1)}, bf16[256,256]{1,0:T(8,128)(2,1)S(1)}, u32[]{:S(2)}, u32[]{:S(2)}) collective-permute-start(bf16[256,256]{1,0:T(8,128)(2,1)S(1)} %attend.5.refs_0_), channel_id=1, source_target_pairs={{0,1},{1,0},{2,3},{3,2},{4,5},{5,4},{6,7},{7,6},{8,9},{9,8},{10,11... | collective-permute-start | bytes 393224 | tf_op jit(solution)/shard_map/ppermute | solution.py:282
  91.5 4.4 %collective-permute-start.22 = (bf16[256,256]{1,0:T(8,128)(2,1)S(1)}, bf16[256,256]{1,0:T(8,128)(2,1)S(1)}, u32[]{:S(2)}, u32[]{:S(2)}) collective-permute-start(bf16[256,256]{1,0:T(8,128)(2,1)S(1)} %collective-permute-done.21.refs_1_), channel_id=1, source_target_pairs={{0,1},{1,0},{2,3},{3,2},{4,5},{5,4},{6,7},{7,6},{8,9},{9,8},{10,11... | collective-permute-start | bytes 393224 | tf_op jit(solution)/shard_map/ppermute | solution.py:282

commit v2 on v1

v2 whole, which is shorter than its diff:
```python
from functools import partial

import jax
import jax.numpy as jnp
from jax import lax
from jax.experimental import pallas as pl
from jax.experimental.pallas import tpu as pltpu
from jax.sharding import PartitionSpec as P


HEAD_DIM = 64
GRID_W = 64
ROW_SPAN = 8
COL_SPAN = 16
LAYERS = 3
HALF = ROW_SPAN // 2

EPS = 1e-06
NEG = -1e30
LANES = 128
F32 = jnp.float32
BF16 = jnp.bfloat16

PARAMS = pltpu.CompilerParams(vmem_limit_bytes=8 * 2**20)
VMEM = pl.BlockSpec(memory_space=pltpu.VMEM)
HBM = pl.BlockSpec(memory_space=pltpu.HBM)


def nt_dot(left, right):
    return lax.dot_general(left, right, (((1,), (1,)), ((), ())), preferred_element_type=F32)


def in_vmem(array):
    return pltpu.with_memory_space_constraint(array, memory_space=pltpu.VMEM)


def in_hbm(array):
    return pltpu.with_memory_space_constraint(array, memory_space=pltpu.HBM)


def cost(flops, bytes_accessed, transcendentals=0):
    return pl.CostEstimate(
        flops=int(flops), bytes_accessed=int(bytes_accessed), transcendentals=int(transcendentals)
    )


def block_at(bit, width, unit):
    if bit is None:
        return slice(None)
    return pl.ds(pl.multiple_of((lax.axis_index("tp") ^ bit) * width, unit), width)


def window_at(row, rows_dev, sp):
    first_row = lax.axis_index("sp") * rows_dev
    first = jnp.minimum(jnp.maximum(first_row + row - HALF, 0), rows_dev * sp - ROW_SPAN)
    return first - first_row + HALF


def halo_slots(high):
    odd = lax.axis_index("sp") % 2
    return (
        pl.multiple_of((1 - odd) * (high * GRID_W), GRID_W),
        pl.multiple_of(odd * (high * GRID_W), GRID_W),
    )


def project_kernel(bits, first, kinds, layer, *refs):
    sources, refs = refs[: len(bits)], refs[len(bits) :]
    gain_ref, refs = refs[0], refs[1:]
    if first:
        stored, refs = refs[:3], refs[3:]
        *refs, held_ref, sems = refs
        copies = [
            pltpu.make_async_copy(stored[kind].at[layer], held_ref.at[kind], sems.at[kind])
            for kind in range(3)
        ]
        for copy in copies:
            copy.start()
    else:
        (held_ref, acc_in, sq_in), refs = refs[:3], refs[3:]
    full = gain_ref.shape[1]
    totals = [None, None, None]
    squares = None
    for at, bit in enumerate(bits):
        wide = sources[at][...].astype(F32)
        width = wide.shape[1]
        cols = block_at(bit, width, LANES)
        square = jnp.sum(wide * wide, axis=1, keepdims=True)
        squares = square if squares is None else squares + square
        scaled = (wide * gain_ref[layer : layer + 1, cols]).astype(BF16)
        for kind in kinds or range(3):
            if first and at == 0:
                copies[kind].wait()
            product = nt_dot(scaled, held_ref[kind, :, cols])
            totals[kind] = product if totals[kind] is None else totals[kind] + product
    if not first:
        squares = squares + sq_in[:, :1]
        for kind in kinds or range(3):
            totals[kind] = totals[kind] + acc_in[kind]
    if kinds:
        row_scale = lax.rsqrt(squares * (1.0 / full) + EPS)
        for at, kind in enumerate(kinds):
            scale = row_scale * HEAD_DIM ** (-0.5) if kind == 0 else row_scale
            refs[0][at] = (totals[kind] * scale).astype(BF16)
    else:
        acc_out, sq_out = refs
        for kind in range(3):
            acc_out[kind] = totals[kind]
        sq_out[...] = jnp.broadcast_to(squares, sq_out.shape)


def project(parts, bits, weights, carried, kinds, layer, gain):
    tok, width = parts[0].shape
    parts_n = len(parts)
    first = carried is None
    operands = [*parts, gain]
    specs = [VMEM] * (parts_n + 1)
    if first:
        _, channels, full = weights[0].shape
        operands += weights
        specs += [HBM] * 3
    else:
        _, channels, full = weights.shape
        operands += [in_vmem(weights), *map(in_vmem, carried)]
        specs += [VMEM] * 3
    if kinds:
        out_shape = [pltpu.VMEM((len(kinds), tok, channels), BF16)]
    else:
        out_shape = [pltpu.VMEM((3, tok, channels), F32), pltpu.VMEM((tok, LANES), F32)]
    scratch = []
    if first:
        out_shape.append(pltpu.VMEM((3, channels, full), BF16))
        scratch.append(pltpu.SemaphoreType.DMA((3,)))
    flops = 2 * tok * width * channels * len(kinds or range(3)) * parts_n
    return pl.pallas_call(
        partial(project_kernel, bits, first, kinds, layer),
        out_shape=out_shape,
        in_specs=specs,
        out_specs=[VMEM] * len(out_shape),
        scratch_shapes=scratch,
        cost_estimate=cost(flops, parts_n * width * (channels * 6 + tok * 2) + 4 * tok * channels),
        compiler_params=PARAMS,
    )(*operands)


def emit_kernel(bits, first, layer, *refs):
    sources, refs = refs[: len(bits)], refs[len(bits) :]
    if first:
        stored_ref, base_ref, out_ref, held_ref, sem = refs
        copy = pltpu.make_async_copy(stored_ref.at[layer], held_ref, sem)
        copy.start()
    else:
        held_ref, base_ref, out_ref = refs
    total = base_ref[...].astype(F32)
    if first:
        copy.wait()
    for at, bit in enumerate(bits):
        rows = block_at(bit, sources[at].shape[1], HEAD_DIM)
        total = total + jnp.dot(sources[at][...], held_ref[rows, :], preferred_element_type=F32)
    out_ref[...] = total.astype(out_ref.dtype)


def emit(parts, bits, weight, base, out_type, first, layer):
    tok, width = parts[0].shape
    cols = base.shape[1]
    parts_n = len(parts)
    out_shape = [pltpu.VMEM((tok, cols), out_type)]
    if out_type == BF16 and layer == LAYERS - 1:
        out_shape = [jax.ShapeDtypeStruct((tok, cols), out_type)]
    scratch = []
    if first:
        out_shape.append(pltpu.VMEM(weight.shape[1:], BF16))
        scratch.append(pltpu.SemaphoreType.DMA)
    return pl.pallas_call(
        partial(emit_kernel, bits, first, layer),
        out_shape=out_shape,
        in_specs=[VMEM] * parts_n + [HBM if first else VMEM, VMEM],
        out_specs=[VMEM] * len(out_shape),
        scratch_shapes=scratch,
        cost_estimate=cost(
            2 * tok * width * cols * parts_n, parts_n * width * (cols + tok) * 2 + tok * cols * 6
        ),
        compiler_params=PARAMS,
    )(*parts, weight if first else in_vmem(weight), base if first else in_vmem(base))


def bias_kernel(layer, sp, table_ref, out_ref, *refs):
    *halo_refs, rows_ref = refs
    heads_n, spans = out_ref.shape[:2]
    offsets, cols = table_ref.shape[2:]
    rows_ref[...] = jnp.zeros_like(rows_ref)
    for head in range(heads_n):
        rows_ref[head, :offsets, :cols] = table_ref[layer, head]
    shape = (GRID_W, LANES)
    query_col = lax.broadcasted_iota(jnp.int32, shape, 0)
    lane = lax.broadcasted_iota(jnp.int32, shape, 1)
    key_col = lane % GRID_W
    first_col = jnp.clip(query_col - COL_SPAN // 2, 0, GRID_W - COL_SPAN)
    inside = (key_col >= first_col) & (key_col < first_col + COL_SPAN)
    for head in range(heads_n):
        plain = rows_ref[head]
        after = pltpu.roll(pltpu.roll(plain, GRID_W, axis=1), rows_ref.shape[1] - 1, axis=0)
        at_lane = lax.broadcasted_iota(jnp.int32, plain.shape, 1)
        both = jnp.where(at_lane < GRID_W, plain, after)
        for span in range(spans):
            row = jnp.broadcast_to(both[span : span + 1, :], shape)
            turned = pltpu.roll(row, LANES - (COL_SPAN - 1), axis=1, stride=1, stride_axis=0)
            out_ref[head, span] = jnp.where(inside, turned, NEG)
    for halo_ref in halo_refs:
        for row in range(halo_ref.shape[0]):
            for at in range(halo_ref.shape[2]):
                one = window_at(row, halo_ref.shape[0], sp) + 2 * at
                low = one + jnp.where(one < HALF, HALF - 1, ROW_SPAN - 1) - row
                high = one + jnp.where(one + 1 < HALF, HALF - 1, ROW_SPAN - 1) - row
                for head in range(heads_n):
                    halo_ref[row, head, at] = jnp.where(
                        lane < GRID_W, out_ref[head, low], out_ref[head, high]
                    )


def expand_bias(table, layer, halo_rows):
    _, heads_n, offsets, _ = table.shape
    spans = offsets - 1
    out_shape = [pltpu.VMEM((heads_n, spans, GRID_W, LANES), F32)]
    if halo_rows:
        out_shape.append(pltpu.VMEM((halo_rows, heads_n, HALF // 2, GRID_W, LANES), F32))
    return pl.pallas_call(
        partial(bias_kernel, layer, lax.axis_size("sp")),
        out_shape=out_shape,
        in_specs=[VMEM],
        out_specs=[VMEM] * len(out_shape),
        scratch_shapes=[pltpu.VMEM((heads_n, 2 * ROW_SPAN, LANES), F32)],
        cost_estimate=cost(heads_n * spans * GRID_W * LANES * 40, heads_n * spans * GRID_W * LANES * 4),
        compiler_params=PARAMS,
        name="expand_bias",
    )(table)


def stacked_query(query, lane, heads_in):
    if heads_in == 1:
        return query
    zero = jnp.zeros_like(query)
    return jnp.concatenate(
        [jnp.where(lane // HEAD_DIM == head, query, zero) for head in range(heads_in)], axis=0
    )


def own_kernel(rows_dev, query_ref, pair_ref, bias_ref, mixed_ref, peak_ref):
    channels = query_ref.shape[2]
    group = min(LANES, channels)
    heads_in = group // HEAD_DIM
    tok = rows_dev * GRID_W
    stack = heads_in * GRID_W
    lane = lax.broadcasted_iota(jnp.int32, (GRID_W, group), 1)
    ones = jnp.ones((tok, LANES), BF16)
    for pair in range(channels // group):
        cols = slice(pair * group, (pair + 1) * group)
        query = jnp.concatenate(
            [
                stacked_query(query_ref[0, row * GRID_W : (row + 1) * GRID_W, cols], lane, heads_in)
                for row in range(rows_dev)
            ],
            axis=0,
        )
        scores = nt_dot(query, pair_ref[0, :, cols])
        values = jnp.concatenate([pair_ref[1, :, cols], ones], axis=1)
        for row in range(rows_dev):
            here = slice(row * stack, (row + 1) * stack)
            pieces = []
            for at in range(tok // LANES):
                offset = (LANES // GRID_W) * at - row + ROW_SPAN - 1
                bias = jnp.concatenate(
                    [bias_ref[pair * heads_in + head, offset] for head in range(heads_in)], axis=0
                )
                pieces.append(scores[here, at * LANES : (at + 1) * LANES] + bias)
            peak = pieces[0]
            for piece in pieces[1:]:
                peak = jnp.maximum(peak, piece)
            peak = jnp.max(peak, axis=1, keepdims=True)
            lifted = jnp.concatenate([jnp.exp(piece - peak).astype(BF16) for piece in pieces], axis=1)
            mixed_ref[pair, here, :] = jnp.dot(lifted, values, preferred_element_type=F32)
            peak_ref[pair, here, :] = jnp.broadcast_to(peak, (stack, LANES))


def attend_own(query, pair, bias, rows_dev):
    _, tok, channels = query.shape
    group = min(LANES, channels)
    pairs, rows = channels // group, tok * (group // HEAD_DIM)
    return pl.pallas_call(
        partial(own_kernel, rows_dev),
        out_shape=[
            pltpu.VMEM((pairs, rows, group + LANES), F32),
            pltpu.VMEM((pairs, rows, LANES), F32),
        ],
        in_specs=[VMEM] * 3,
        out_specs=[VMEM] * 2,
        cost_estimate=cost(pairs * rows * tok * 800, bias.size * 4, pairs * rows * tok),
        compiler_params=PARAMS,
        name="attend_own",
    )(*map(in_vmem, (query, pair, bias)))


def halo_kernel(
    rows_dev, sp, query_ref, even_ref, odd_ref, bias_ref, mixed_ref, peak_ref, out_ref, keys, values
):
    channels = query_ref.shape[2]
    group = min(LANES, channels)
    heads_in = group // HEAD_DIM
    span = HALF * GRID_W
    stack = heads_in * GRID_W
    even_slot, odd_slot = halo_slots(HALF)
    for scratch, kind in ((keys, 0), (values, 1)):
        scratch[pl.ds(even_slot, span), :] = even_ref[kind]
        scratch[pl.ds(odd_slot, span), :] = odd_ref[kind]
    lane = lax.broadcasted_iota(jnp.int32, (GRID_W, group), 1)
    ones = jnp.ones((span, LANES), BF16)
    for row in range(rows_dev):
        first = pl.multiple_of(window_at(row, rows_dev, sp) * GRID_W, GRID_W)
        here = slice(row * stack, (row + 1) * stack)
        for pair in range(channels // group):
            cols = slice(pair * group, (pair + 1) * group)
            query = stacked_query(query_ref[0, row * GRID_W : (row + 1) * GRID_W, cols], lane, heads_in)
            scores = nt_dot(query, keys[pl.ds(first, span), cols])
            pieces = []
            for at in range(span // LANES):
                bias = jnp.concatenate(
                    [bias_ref[row, pair * heads_in + head, at] for head in range(heads_in)], axis=0
                )
                pieces.append(scores[:, at * LANES : (at + 1) * LANES] + bias)
            peak = pieces[0]
            for piece in pieces[1:]:
                peak = jnp.maximum(peak, piece)
            before = peak_ref[pair, here, :]
            peak = jnp.maximum(jnp.max(peak, axis=1, keepdims=True), before)
            lifted = jnp.concatenate([jnp.exp(piece - peak).astype(BF16) for piece in pieces], axis=1)
            wide = jnp.concatenate([values[pl.ds(first, span), cols], ones], axis=1)
            mixed = jnp.dot(lifted, wide, preferred_element_type=F32)
            fade = jnp.exp(before - peak)
            top = mixed_ref[pair, here, :group] * fade[:, :group] + mixed[:, :group]
            weight = mixed_ref[pair, here, group:] * fade + mixed[:, group:]
            result, total = top[:GRID_W], weight[:GRID_W, :group]
            for head in range(1, heads_in):
                mine = lane // HEAD_DIM == head
                below = slice(head * GRID_W, (head + 1) * GRID_W)
                result = jnp.where(mine, top[below], result)
                total = jnp.where(mine, weight[below, :group], total)
            out_ref[row * GRID_W : (row + 1) * GRID_W, cols] = (result / total).astype(BF16)


def attend_halo(query, even, odd, bias, mixed, peak, rows_dev):
    _, tok, channels = query.shape
    scores = tok * (channels // HEAD_DIM) * HALF * GRID_W
    return pl.pallas_call(
        partial(halo_kernel, rows_dev, lax.axis_size("sp")),
        out_shape=pltpu.VMEM((tok, channels), BF16),
        in_specs=[VMEM] * 6,
        out_specs=VMEM,
        scratch_shapes=[pltpu.VMEM((ROW_SPAN * GRID_W, channels), BF16)] * 2,
        cost_estimate=cost(scores * HEAD_DIM * 6, bias.size * 4 + tok * channels * 16, scores),
        compiler_params=PARAMS,
        name="attend_halo",
    )(*map(in_vmem, (query, even, odd, bias, mixed, peak)))


def attend_kernel(
    rows_dev, sp, query_ref, own_ref, even_ref, odd_ref, bias_ref, out_ref, keys, values
):
    channels = query_ref.shape[2]
    group = min(LANES, channels)
    heads_in = group // HEAD_DIM
    span = ROW_SPAN * GRID_W
    even_slot, odd_slot = halo_slots(HALF + rows_dev)
    halo = HALF * GRID_W
    for scratch, kind in ((keys, 0), (values, 1)):
        scratch[HALF * GRID_W : (HALF + rows_dev) * GRID_W, :] = own_ref[kind]
        scratch[pl.ds(even_slot, halo), :] = even_ref[kind]
        scratch[pl.ds(odd_slot, halo), :] = odd_ref[kind]
    lane = lax.broadcasted_iota(jnp.int32, (GRID_W, group), 1)
    ones = jnp.ones((span, group), BF16)
    for row in range(rows_dev):
        window = window_at(row, rows_dev, sp)
        first = pl.multiple_of(window * GRID_W, GRID_W)
        offset = window - row + HALF - 1
        for pair in range(channels // group):
            cols = slice(pair * group, (pair + 1) * group)
            query = query_ref[0, row * GRID_W : (row + 1) * GRID_W, cols]
            query = stacked_query(query, lane, heads_in)
            scores = nt_dot(query, keys[pl.ds(first, span), cols])
            pieces = []
            for at in range(span // LANES):
                bias = jnp.concatenate(
                    [
                        bias_ref[pair * heads_in + head, offset + (LANES // GRID_W) * at]
                        for head in range(heads_in)
                    ],
                    axis=0,
                )
                pieces.append(scores[:, at * LANES : (at + 1) * LANES] + bias)
            peak = pieces[0]
            for piece in pieces[1:]:
                peak = jnp.maximum(peak, piece)
            peak = jnp.max(peak, axis=1, keepdims=True)
            lifted = jnp.concatenate([jnp.exp(piece - peak).astype(BF16) for piece in pieces], axis=1)
            mixed = jnp.dot(lifted, values[pl.ds(first, span), cols], preferred_element_type=F32)
            weight = jnp.dot(lifted, ones, preferred_element_type=F32)
            mixed = mixed / weight
            result = mixed[:GRID_W]
            for head in range(1, heads_in):
                result = jnp.where(
                    lane // HEAD_DIM == head, mixed[head * GRID_W : (head + 1) * GRID_W], result
                )
            out_ref[row * GRID_W : (row + 1) * GRID_W, cols] = result.astype(BF16)


def attend(query, own, even, odd, bias, rows_dev):
    _, tok, channels = query.shape
    padded = (rows_dev + 2 * HALF) * GRID_W
    scores = tok * (channels // HEAD_DIM) * ROW_SPAN * GRID_W
    return pl.pallas_call(
        partial(attend_kernel, rows_dev, lax.axis_size("sp")),
        out_shape=pltpu.VMEM((tok, channels), BF16),
        in_specs=[VMEM] * 5,
        out_specs=VMEM,
        scratch_shapes=[pltpu.VMEM((padded, channels), BF16)] * 2,
        cost_estimate=cost(scores * HEAD_DIM * 6, bias.size * 4 + tok * channels * 16, scores),
        compiler_params=PARAMS,
        name="attend",
    )(query, own, even, odd, bias)


def exchange(block, pairs):
    sp, tp = lax.axis_size("sp"), lax.axis_size("tp")
    partner = {}
    for one, two in pairs:
        partner[one], partner[two] = two, one
    moves = []
    for row in range(sp):
        for col in range(tp):
            if row in partner:
                moves.append((row * tp + col, partner[row] * tp + col))
            elif tp % 2 == 0:
                moves.append((row * tp + col, row * tp + (col ^ 1)))
    return lax.ppermute(block, ("sp", "tp"), moves)


def flip(block, axis, bit):
    count = lax.axis_size(axis)
    return lax.ppermute(block, axis, [(at, at ^ bit) for at in range(count)])


def body(hidden_in, norm_gain, query_weight, key_weight, value_weight, output_weight, offset_bias):
    tok_dev, _ = hidden_in.shape
    rows_dev = tok_dev // GRID_W
    tp = lax.axis_size("tp")
    sp = lax.axis_size("sp")
    is_odd = lax.axis_index("sp") % 2
    split = rows_dev == HALF
    weights = [in_hbm(weight) for weight in (query_weight, key_weight, value_weight)]
    output_weight = in_hbm(output_weight)
    even_pairs = [(at, at + 1) for at in range(0, sp - 1, 2)]
    odd_pairs = [(at, at + 1) for at in range(1, sp - 1, 2)]
    stream = hidden_in
    for layer in range(LAYERS):
        step = partial(project, layer=layer, gain=norm_gain)
        if tp == 4:
            across = flip(stream, "tp", 2)
            beside = flip(stream, "tp", 1)
            corner = flip(across, "tp", 1)
            *carried, held = step([stream], (0,), weights, None, None)
            carried = step([beside], (1,), held, carried, None)
            carried = step([across], (2,), held, carried, None)
            (pair,) = step([corner], (3,), held, carried, (1, 2))
            (query,) = step([corner], (3,), held, carried, (0,))
        else:
            gathered = lax.all_gather(stream, "tp", axis=1, tiled=True)
            *carried, held = step([gathered], (None,), weights, None, (0, 1, 2))
            query, pair = carried[0][:1], carried[0][1:]
        if split:
            to_even = to_odd = pair
        else:
            low, top = pair[:, : HALF * GRID_W], pair[:, (rows_dev - HALF) * GRID_W :]
            to_even = jnp.where(is_odd == 0, top, low)
            to_odd = jnp.where(is_odd == 0, low, top)
        even = exchange(to_even, even_pairs)
        odd = exchange(to_odd, odd_pairs)
        bias, *halo_bias = expand_bias(offset_bias, layer, rows_dev if split else 0)
        if split:
            mixed, peak = attend_own(query, pair, bias, rows_dev)
            attended = attend_halo(
                query, even, odd, halo_bias[0], mixed, peak, rows_dev
            )
        else:
            attended = attend(query, pair, even, odd, bias, rows_dev)
        step = partial(emit, layer=layer)
        if tp == 4:
            across = flip(attended, "tp", 2)
            beside = flip(attended, "tp", 1)
            corner = flip(across, "tp", 1)
            partly, held = step([attended], (0,), output_weight, stream, F32, True)
            (partly,) = step([beside], (1,), held, partly, F32, False)
            (partly,) = step([across], (2,), held, partly, F32, False)
            (stream,) = step([corner], (3,), held, partly, BF16, False)
        else:
            gathered = lax.all_gather(attended, "tp", axis=1, tiled=True)
            stream, _ = step([gathered], (None,), output_weight, stream, BF16, True)
    return stream


def solution(mesh):
    return jax.shard_map(
        body,
        mesh=mesh,
        in_specs=(
            P(("grp", "sp"), "tp"),
            P(),
            P(None, "tp", None),
            P(None, "tp", None),
            P(None, "tp", None),
            P(None, None, "tp"),
            P(None, "tp", None, None),
        ),
        out_specs=P(("grp", "sp"), "tp"),
        check_vma=False,
    )
```

time: 98.1 us -> 92.6 us (0.944)
  Pallas kernels: 30.9 us -> 25.5 us
  waiting for transfers between devices: 43.5 us -> 44.7 us
    pallas_call x24 -> x36, Pallas kernels: 30.9 us -> 25.5 us  [the longest x15 11.6 us: project(): pl.pallas_call(partial(project_kernel, bits, first, kinds, layer), out_sh...]
    ppermute x18, waiting for transfers between devices: 22.7 us -> 27.7 us  [flip(): return lax.ppermute(block, axis, [(at, at ^ bit) for at in range(count)])]
    ppermute x6, waiting for transfers between devices: 20.7 us -> 17.1 us  [exchange(): return lax.ppermute(block, ('sp', 'tp'), moves)]
  transfers between devices with their start and end apart: 24 -> 24, of which waited for: 10 -> 10; matrix products, arithmetic and copies ran while one was open for 2% -> 0% of each run, Pallas kernels for 20% -> 23%
where the time goes in v2:
time: 92.6 us; the launch traced here: 91.4 us
  waiting for transfers between devices  44.7 us (48%)
  Pallas kernels  25.5 us (28%)
  starting transfers between devices  19 us (21%)
  local copies, waits for them, and re-layouts  1.73 us (2%)
    ppermute x18, waiting for transfers between devices, flip(): return lax.ppermute(block, axis, [(at, at ^ bit) for at in range(count)])  27.7 us
    ppermute x6, waiting for transfers between devices, exchange(): return lax.ppermute(block, ('sp', 'tp'), moves)  17.1 us
    ppermute x18, starting transfers between devices, flip(): return lax.ppermute(block, axis, [(at, at ^ bit) for at in range(count)])  17 us
    pallas_call x15, Pallas kernels, project(): pl.pallas_call(partial(project_kernel, bits, first, kinds, layer), out_sh...  11.6 us
    pallas_call x12, Pallas kernels, emit(): pl.pallas_call(partial(emit_kernel, bits, first, layer), out_shape=out_sh...  7.18 us
    pallas_call x3, Pallas kernels, expand_bias(): pl.pallas_call(partial(bias_kernel, layer, lax.axis_size('sp')), out_shap...  2.82 us
    pallas_call x3, Pallas kernels, attend_halo(): pl.pallas_call(partial(halo_kernel, rows_dev, lax.axis_size('sp')), out_s...  2.07 us
    ppermute x6, starting transfers between devices, exchange(): return lax.ppermute(block, ('sp', 'tp'), moves)  1.98 us
  transfers between devices with their start and end apart: 24, of which 10 were waited for; matrix products, arithmetic and copies ran while one was open for 0% of the time, Pallas kernels for 23%

profile of v2, /device:TPU:19, one launch (start us, length us, event | category | flops | bytes accessed | tf_op | source)
XLA Modules:
  0.0 91.4 jit_solution(4159264792887870884)
XLA Ops:
  0.3 1.0 %collective-permute-start.2 = (bf16[256,512]{1,0:T(8,128)(2,1)}, bf16[256,512]{1,0:T(8,128)(2,1)S(1)}, u32[]{:S(2)}, u32[]{:S(2)}) collective-permute-start(bf16[256,512]{1,0:T(8,128)(2,1)} %refs_2_.5), channel_id=1, source_target_pairs={{0,1},{1,0},{2,3},{3,2},{4,5},{5,4},{6,7},{7,6},{8,9},{9,8},{10,11... | collective-permute-start | bytes 786440 | tf_op jit(solution)/shard_map/ppermute | solution.py:448
  1.2 6.2 %collective-permute-done.refs_0_ = bf16[256,512]{1,0:T(8,128)(2,1)S(1)} collective-permute-done((bf16[256,512]{1,0:T(8,128)(2,1)}, bf16[256,512]{1,0:T(8,128)(2,1)S(1)}, u32[]{:S(2)}, u32[]{:S(2)}) %collective-permute-start) | collective-permute-done | bytes 262176 | tf_op jit(solution)/shard_map/ppermute | solution.py:448
  7.4 1.5 %collective-permute-start.1 = (bf16[256,512]{1,0:T(8,128)(2,1)S(1)}, bf16[256,512]{1,0:T(8,128)(2,1)S(1)}, u32[]{:S(2)}, u32[]{:S(2)}) collective-permute-start(bf16[256,512]{1,0:T(8,128)(2,1)S(1)} %collective-permute-done.refs_0_), channel_id=1, source_target_pairs={{0,1},{1,0},{2,3},{3,2},{4,5},{5,4},{6,7},{7,6},{8,9},{9,8},{10,11... | collective-permute-start | bytes 786440 | tf_op jit(solution)/shard_map/ppermute | solution.py:448
  8.9 0.8 copy-done
  9.7 0.9 %copy-done.2 = bf16[256,512]{1,0:T(8,128)(2,1)S(1)} copy-done((bf16[256,512]{1,0:T(8,128)(2,1)S(1)}, bf16[256,512]{1,0:T(8,128)(2,1)}, u32[]{:S(2)}) %copy-start.2) | copy-done | bytes 262168
  10.6 2.2 %shard_map.73 = (f32[3,256,256]{2,1,0:T(8,128)S(1)}, f32[256,128]{1,0:T(8,128)S(1)}, bf16[3,256,2048]{2,1,0:T(8,128)(2,1)S(1)}) custom-call(bf16[256,512]{1,0:T(8,128)(2,1)S(1)} %copy-done.2, f32[3,2048]{1,0:T(4,128)S(1)} %copy-done, bf16[3,256,2048]{2,1,0:T(8,128)(2,1)} %refs_2_.7, bf16[3,256,2048]{2,1,0:T(8,128)(2,1)} %refs_3_.5, bf16[3,256,2048]{2,1,0:T(8,128)(2,1)} %refs_4_.5), custom_call_target="tpu_custom_call" | custom-call | flops 201326592 | bytes 1310720 | tf_op jit(solution)/shard_map/pallas_call | solution.py:135
  12.9 0.5 shard_map.74
  13.4 0.5 shard_map.75
  13.9 0.4 shard_map.77.pair_ref
  14.3 1.4 %collective-permute-start.3 = (bf16[2,256,256]{2,1,0:T(8,128)(2,1)S(1)}, bf16[2,256,256]{2,1,0:T(8,128)(2,1)S(1)}, u32[]{:S(2)}, u32[]{:S(2)}) collective-permute-start(bf16[2,256,256]{2,1,0:T(8,128)(2,1)S(1)} %shard_map.77.pair_ref), channel_id=1, source_target_pairs={{0,4},{1,5},{2,6},{3,7},{4,0},{5,1},{6,2},{7,3},{8,12},{9,13},{10,... | collective-permute-start | bytes 786440 | tf_op jit(solution)/shard_map/ppermute | solution.py:443
  15.6 0.9 %expand_bias.3 = (f32[4,14,64,128]{3,2,1,0:T(8,128)S(1)}, f32[4,4,2,64,128]{4,3,2,1,0:T(8,128)S(1)}) custom-call(f32[3,4,15,31]{3,2,1,0:T(8,128)S(1)} %copy.8.table_ref), custom_call_target="tpu_custom_call" | custom-call | flops 18350080 | bytes 1835008 | tf_op jit(solution)/shard_map/expand_bias/pallas_call | solution.py:227
  16.9 0.6 attend_own.3
  17.6 4.6 %collective-permute-done.3.even_ref = bf16[2,256,256]{2,1,0:T(8,128)(2,1)S(1)} collective-permute-done((bf16[2,256,256]{2,1,0:T(8,128)(2,1)S(1)}, bf16[2,256,256]{2,1,0:T(8,128)(2,1)S(1)}, u32[]{:S(2)}, u32[]{:S(2)}) %collective-permute-start.3) | collective-permute-done | bytes 262176 | tf_op jit(solution)/shard_map/ppermute | solution.py:443
  22.2 1.0 %collective-permute-done.4.odd_ref = bf16[2,256,256]{2,1,0:T(8,128)(2,1)S(1)} collective-permute-done((bf16[2,256,256]{2,1,0:T(8,128)(2,1)S(1)}, bf16[2,256,256]{2,1,0:T(8,128)(2,1)S(1)}, u32[]{:S(2)}, u32[]{:S(2)}) %collective-permute-start.4) | collective-permute-done | bytes 262176 | tf_op jit(solution)/shard_map/ppermute | solution.py:443
  23.2 0.7 attend_halo.3.refs_0_
  24.2 1.4 %collective-permute-start.7 = (bf16[256,256]{1,0:T(8,128)(2,1)S(1)}, bf16[256,256]{1,0:T(8,128)(2,1)S(1)}, u32[]{:S(2)}, u32[]{:S(2)}) collective-permute-start(bf16[256,256]{1,0:T(8,128)(2,1)S(1)} %attend_halo.3.refs_0_), channel_id=1, source_target_pairs={{0,1},{1,0},{2,3},{3,2},{4,5},{5,4},{6,7},{7,6},{8,9},{9,8},{10,11... | collective-permute-start | bytes 393224 | tf_op jit(solution)/shard_map/ppermute | solution.py:448
  25.6 2.1 %collective-permute-done.5.refs_0_ = bf16[256,256]{1,0:T(8,128)(2,1)S(1)} collective-permute-done((bf16[256,256]{1,0:T(8,128)(2,1)S(1)}, bf16[256,256]{1,0:T(8,128)(2,1)S(1)}, u32[]{:S(2)}, u32[]{:S(2)}) %collective-permute-start.5) | collective-permute-done | bytes 131104 | tf_op jit(solution)/shard_map/ppermute | solution.py:448
  27.8 2.3 %collective-permute-start.6 = (bf16[256,256]{1,0:T(8,128)(2,1)S(1)}, bf16[256,256]{1,0:T(8,128)(2,1)S(1)}, u32[]{:S(2)}, u32[]{:S(2)}) collective-permute-start(bf16[256,256]{1,0:T(8,128)(2,1)S(1)} %collective-permute-done.5.refs_0_), channel_id=1, source_target_pairs={{0,1},{1,0},{2,3},{3,2},{4,5},{5,4},{6,7},{7,6},{8,9},{9,8},{10,11... | collective-permute-start | bytes 393224 | tf_op jit(solution)/shard_map/ppermute | solution.py:448
  30.1 1.5 %shard_map.78 = (f32[256,512]{1,0:T(8,128)S(1)}, bf16[1024,512]{1,0:T(8,128)(2,1)S(1)}) custom-call(bf16[256,256]{1,0:T(8,128)(2,1)S(1)} %attend_halo.3.refs_0_, bf16[3,1024,512]{2,1,0:T(8,128)(2,1)} %refs_1_.35, bf16[256,512]{1,0:T(8,128)(2,1)S(1)} %copy-done.3), custom_call_target="tpu_custom_call" | custom-call | flops 67108864 | bytes 1179648 | tf_op jit(solution)/shard_map/pallas_call | solution.py:174
  32.9 7.3 %collective-permute-done.8.refs_0_ = bf16[256,512]{1,0:T(8,128)(2,1)S(1)} collective-permute-done((bf16[256,512]{1,0:T(8,128)(2,1)S(1)}, bf16[256,512]{1,0:T(8,128)(2,1)S(1)}, u32[]{:S(2)}, u32[]{:S(2)}) %collective-permute-start.8) | collective-permute-done | bytes 262176 | tf_op jit(solution)/shard_map/ppermute | solution.py:448
  40.2 0.9 collective-permute-start.9
  41.1 2.2 %shard_map.82 = (f32[3,256,256]{2,1,0:T(8,128)S(1)}, f32[256,128]{1,0:T(8,128)S(1)}, bf16[3,256,2048]{2,1,0:T(8,128)(2,1)S(1)}) custom-call(bf16[256,512]{1,0:T(8,128)(2,1)S(1)} %shard_map.81.refs_0_.refs_2_, f32[3,2048]{1,0:T(4,128)S(1)} %copy-done.1, bf16[3,256,2048]{2,1,0:T(8,128)(2,1)} %refs_2_.7, bf16[3,256,2048]{2,1,0:T(8,128)(2,1)} %refs_3_.5, ...), custom_call_target="tpu_custom_call" | custom-call | flops 201326592 | bytes 1310720 | tf_op jit(solution)/shard_map/pallas_call | solution.py:135
  43.3 0.5 shard_map.83
  43.8 0.5 shard_map.84
  44.3 0.4 shard_map.86.pair_ref
  44.9 0.9 %expand_bias.4 = (f32[4,14,64,128]{3,2,1,0:T(8,128)S(1)}, f32[4,4,2,64,128]{4,3,2,1,0:T(8,128)S(1)}) custom-call(f32[3,4,15,31]{3,2,1,0:T(8,128)S(1)} %copy.8.table_ref), custom_call_target="tpu_custom_call" | custom-call | flops 18350080 | bytes 1835008 | tf_op jit(solution)/shard_map/expand_bias/pallas_call | solution.py:227
  46.1 0.6 attend_own.4
  46.8 5.8 %collective-permute-done.11.even_ref = bf16[2,256,256]{2,1,0:T(8,128)(2,1)S(1)} collective-permute-done((bf16[2,256,256]{2,1,0:T(8,128)(2,1)S(1)}, bf16[2,256,256]{2,1,0:T(8,128)(2,1)S(1)}, u32[]{:S(2)}, u32[]{:S(2)}) %collective-permute-start.11) | collective-permute-done | bytes 262176 | tf_op jit(solution)/shard_map/ppermute | solution.py:443
  52.6 0.7 attend_halo.4.refs_0_
  53.6 1.2 %collective-permute-start.15 = (bf16[256,256]{1,0:T(8,128)(2,1)S(1)}, bf16[256,256]{1,0:T(8,128)(2,1)S(1)}, u32[]{:S(2)}, u32[]{:S(2)}) collective-permute-start(bf16[256,256]{1,0:T(8,128)(2,1)S(1)} %attend_halo.4.refs_0_), channel_id=1, source_target_pairs={{0,1},{1,0},{2,3},{3,2},{4,5},{5,4},{6,7},{7,6},{8,9},{9,8},{10,11... | collective-permute-start | bytes 393224 | tf_op jit(solution)/shard_map/ppermute | solution.py:448
  54.8 2.3 %collective-permute-done.13.refs_0_ = bf16[256,256]{1,0:T(8,128)(2,1)S(1)} collective-permute-done((bf16[256,256]{1,0:T(8,128)(2,1)S(1)}, bf16[256,256]{1,0:T(8,128)(2,1)S(1)}, u32[]{:S(2)}, u32[]{:S(2)}) %collective-permute-start.13) | collective-permute-done | bytes 131104 | tf_op jit(solution)/shard_map/ppermute | solution.py:448
  57.2 2.1 %collective-permute-start.14 = (bf16[256,256]{1,0:T(8,128)(2,1)S(1)}, bf16[256,256]{1,0:T(8,128)(2,1)S(1)}, u32[]{:S(2)}, u32[]{:S(2)}) collective-permute-start(bf16[256,256]{1,0:T(8,128)(2,1)S(1)} %collective-permute-done.13.refs_0_), channel_id=1, source_target_pairs={{0,1},{1,0},{2,3},{3,2},{4,5},{5,4},{6,7},{7,6},{8,9},{9,8},{10,11... | collective-permute-start | bytes 393224 | tf_op jit(solution)/shard_map/ppermute | solution.py:448
  59.3 1.5 %shard_map.87 = (f32[256,512]{1,0:T(8,128)S(1)}, bf16[1024,512]{1,0:T(8,128)(2,1)S(1)}) custom-call(bf16[256,256]{1,0:T(8,128)(2,1)S(1)} %attend_halo.4.refs_0_, bf16[3,1024,512]{2,1,0:T(8,128)(2,1)} %refs_1_.35, bf16[256,512]{1,0:T(8,128)(2,1)S(1)} %shard_map.81.refs_0_.refs_2_), custom_call_target="tpu_custom_call" | custom-call | flops 67108864 | bytes 1179648 | tf_op jit(solution)/shard_map/pallas_call | solution.py:174
  62.1 7.3 %collective-permute-done.16.refs_0_ = bf16[256,512]{1,0:T(8,128)(2,1)S(1)} collective-permute-done((bf16[256,512]{1,0:T(8,128)(2,1)S(1)}, bf16[256,512]{1,0:T(8,128)(2,1)S(1)}, u32[]{:S(2)}, u32[]{:S(2)}) %collective-permute-start.16) | collective-permute-done | bytes 262176 | tf_op jit(solution)/shard_map/ppermute | solution.py:448
  69.4 0.8 collective-permute-start.17
  70.3 2.2 %shard_map.91 = (f32[3,256,256]{2,1,0:T(8,128)S(1)}, f32[256,128]{1,0:T(8,128)S(1)}, bf16[3,256,2048]{2,1,0:T(8,128)(2,1)S(1)}) custom-call(bf16[256,512]{1,0:T(8,128)(2,1)S(1)} %shard_map.90.refs_0_.refs_2_, f32[3,2048]{1,0:T(4,128)S(1)} %copy-done.1, bf16[3,256,2048]{2,1,0:T(8,128)(2,1)} %refs_2_.7, bf16[3,256,2048]{2,1,0:T(8,128)(2,1)} %refs_3_.5, ...), custom_call_target="tpu_custom_call" | custom-call | flops 201326592 | bytes 1310720 | tf_op jit(solution)/shard_map/pallas_call | solution.py:135
  72.5 0.5 shard_map.92
  73.0 0.5 shard_map.93
  73.5 0.4 shard_map.95.pair_ref
  74.3 0.9 %expand_bias.5 = (f32[4,14,64,128]{3,2,1,0:T(8,128)S(1)}, f32[4,4,2,64,128]{4,3,2,1,0:T(8,128)S(1)}) custom-call(f32[3,4,15,31]{3,2,1,0:T(8,128)S(1)} %copy.8.table_ref), custom_call_target="tpu_custom_call" | custom-call | flops 18350080 | bytes 1835008 | tf_op jit(solution)/shard_map/expand_bias/pallas_call | solution.py:227
  75.5 0.6 attend_own.5
  76.2 5.6 %collective-permute-done.19.even_ref = bf16[2,256,256]{2,1,0:T(8,128)(2,1)S(1)} collective-permute-done((bf16[2,256,256]{2,1,0:T(8,128)(2,1)S(1)}, bf16[2,256,256]{2,1,0:T(8,128)(2,1)S(1)}, u32[]{:S(2)}, u32[]{:S(2)}) %collective-permute-start.19) | collective-permute-done | bytes 262176 | tf_op jit(solution)/shard_map/ppermute | solution.py:443
  81.8 0.7 attend_halo.5.refs_0_
  82.8 1.2 %collective-permute-start.23 = (bf16[256,256]{1,0:T(8,128)(2,1)S(1)}, bf16[256,256]{1,0:T(8,128)(2,1)S(1)}, u32[]{:S(2)}, u32[]{:S(2)}) collective-permute-start(bf16[256,256]{1,0:T(8,128)(2,1)S(1)} %attend_halo.5.refs_0_), channel_id=1, source_target_pairs={{0,1},{1,0},{2,3},{3,2},{4,5},{5,4},{6,7},{7,6},{8,9},{9,8},{10,11... | collective-permute-start | bytes 393224 | tf_op jit(solution)/shard_map/ppermute | solution.py:448
  84.0 2.3 %collective-permute-done.21.refs_0_ = bf16[256,256]{1,0:T(8,128)(2,1)S(1)} collective-permute-done((bf16[256,256]{1,0:T(8,128)(2,1)S(1)}, bf16[256,256]{1,0:T(8,128)(2,1)S(1)}, u32[]{:S(2)}, u32[]{:S(2)}) %collective-permute-start.21) | collective-permute-done | bytes 131104 | tf_op jit(solution)/shard_map/ppermute | solution.py:448
  86.4 2.1 %collective-permute-start.22 = (bf16[256,256]{1,0:T(8,128)(2,1)S(1)}, bf16[256,256]{1,0:T(8,128)(2,1)S(1)}, u32[]{:S(2)}, u32[]{:S(2)}) collective-permute-start(bf16[256,256]{1,0:T(8,128)(2,1)S(1)} %collective-permute-done.21.refs_0_), channel_id=1, source_target_pairs={{0,1},{1,0},{2,3},{3,2},{4,5},{5,4},{6,7},{7,6},{8,9},{9,8},{10,11... | collective-permute-start | bytes 393224 | tf_op jit(solution)/shard_map/ppermute | solution.py:448
  88.5 1.5 %shard_map.96 = (f32[256,512]{1,0:T(8,128)S(1)}, bf16[1024,512]{1,0:T(8,128)(2,1)S(1)}) custom-call(bf16[256,256]{1,0:T(8,128)(2,1)S(1)} %attend_halo.5.refs_0_, bf16[3,1024,512]{2,1,0:T(8,128)(2,1)} %refs_1_.35, bf16[256,512]{1,0:T(8,128)(2,1)S(1)} %shard_map.90.refs_0_.refs_2_), custom_call_target="tpu_custom_call" | custom-call | flops 67108864 | bytes 1179648 | tf_op jit(solution)/shard_map/pallas_call | solution.py:174
  90.4 0.9 %shard_map.99 = bf16[256,512]{1,0:T(8,128)(2,1)} custom-call(bf16[256,256]{1,0:T(8,128)(2,1)S(1)} %collective-permute-done.22.refs_0_, bf16[1024,512]{1,0:T(8,128)(2,1)S(1)} %get-tuple-element.81.refs_1_, f32[256,512]{1,0:T(8,128)S(1)} %shard_map.98.refs_2_), custom_call_target="tpu_custom_call" | custom-call | flops 67108864 | bytes 1179648 | tf_op jit(solution)/shard_map/pallas_call | solution.py:174
  (47 shorter events, 5.9 us)
Async XLA Ops:
  0.0 7.4 %collective-permute-start = (bf16[256,512]{1,0:T(8,128)(2,1)}, bf16[256,512]{1,0:T(8,128)(2,1)S(1)}, u32[]{:S(2)}, u32[]{:S(2)}) collective-permute-start(bf16[256,512]{1,0:T(8,128)(2,1)} %refs_2_.5), channel_id=1, source_target_pairs={{0,2},{1,3},{2,0},{3,1},{4,6},{5,7},{6,4},{7,5},{8,10},{9,11},{10,... | collective-permute-start | bytes 786440 | tf_op jit(solution)/shard_map/ppermute | solution.py:448
  0.3 12.6 %collective-permute-start.2 = (bf16[256,512]{1,0:T(8,128)(2,1)}, bf16[256,512]{1,0:T(8,128)(2,1)S(1)}, u32[]{:S(2)}, u32[]{:S(2)}) collective-permute-start(bf16[256,512]{1,0:T(8,128)(2,1)} %refs_2_.5), channel_id=1, source_target_pairs={{0,1},{1,0},{2,3},{3,2},{4,5},{5,4},{6,7},{7,6},{8,9},{9,8},{10,11... | collective-permute-start | bytes 786440 | tf_op jit(solution)/shard_map/ppermute | solution.py:448
  7.4 6.5 %collective-permute-start.1 = (bf16[256,512]{1,0:T(8,128)(2,1)S(1)}, bf16[256,512]{1,0:T(8,128)(2,1)S(1)}, u32[]{:S(2)}, u32[]{:S(2)}) collective-permute-start(bf16[256,512]{1,0:T(8,128)(2,1)S(1)} %collective-permute-done.refs_0_), channel_id=1, source_target_pairs={{0,1},{1,0},{2,3},{3,2},{4,5},{5,4},{6,7},{7,6},{8,9},{9,8},{10,11... | collective-permute-start | bytes 786440 | tf_op jit(solution)/shard_map/ppermute | solution.py:448
  8.9 0.8 copy-start
  9.7 0.9 %copy-start.2 = (bf16[256,512]{1,0:T(8,128)(2,1)S(1)}, bf16[256,512]{1,0:T(8,128)(2,1)}, u32[]{:S(2)}) copy-start(bf16[256,512]{1,0:T(8,128)(2,1)} %refs_2_.5) | copy-start | bytes 786436
  10.6 2.3 %copy-start.1 = (f32[3,2048]{1,0:T(4,128)S(1)}, f32[3,2048]{1,0:T(4,128)}, u32[]{:S(2)}) copy-start(f32[3,2048]{1,0:T(4,128)} %refs_1_.34) | copy-start | bytes 73732
  13.9 1.8 %copy-start.4 = (f32[3,4,15,31]{3,1,2,0:T(4,128)S(1)}, f32[3,4,15,31]{3,1,2,0:T(4,128)}, u32[]{:S(2)}) copy-start(f32[3,4,15,31]{3,1,2,0:T(4,128)} %param.13) | copy-start | bytes 66964
  14.3 7.9 %collective-permute-start.3 = (bf16[2,256,256]{2,1,0:T(8,128)(2,1)S(1)}, bf16[2,256,256]{2,1,0:T(8,128)(2,1)S(1)}, u32[]{:S(2)}, u32[]{:S(2)}) collective-permute-start(bf16[2,256,256]{2,1,0:T(8,128)(2,1)S(1)} %shard_map.77.pair_ref), channel_id=1, source_target_pairs={{0,4},{1,5},{2,6},{3,7},{4,0},{5,1},{6,2},{7,3},{8,12},{9,13},{10,... | collective-permute-start | bytes 786440 | tf_op jit(solution)/shard_map/ppermute | solution.py:443
  15.6 7.6 %collective-permute-start.4 = (bf16[2,256,256]{2,1,0:T(8,128)(2,1)S(1)}, bf16[2,256,256]{2,1,0:T(8,128)(2,1)S(1)}, u32[]{:S(2)}, u32[]{:S(2)}) collective-permute-start(bf16[2,256,256]{2,1,0:T(8,128)(2,1)S(1)} %shard_map.77.pair_ref), channel_id=1, source_target_pairs={{0,1},{1,0},{2,3},{3,2},{4,8},{5,9},{6,10},{7,11},{8,4},{9,5},{10,... | collective-permute-start | bytes 786440 | tf_op jit(solution)/shard_map/ppermute | solution.py:443
  16.9 13.2 %copy-start.3 = (bf16[256,512]{1,0:T(8,128)(2,1)S(1)}, bf16[256,512]{1,0:T(8,128)(2,1)}, u32[]{:S(2)}) copy-start(bf16[256,512]{1,0:T(8,128)(2,1)} %refs_2_.5) | copy-start | bytes 786436
  23.9 3.9 %collective-permute-start.5 = (bf16[256,256]{1,0:T(8,128)(2,1)S(1)}, bf16[256,256]{1,0:T(8,128)(2,1)S(1)}, u32[]{:S(2)}, u32[]{:S(2)}) collective-permute-start(bf16[256,256]{1,0:T(8,128)(2,1)S(1)} %attend_halo.3.refs_0_), channel_id=1, source_target_pairs={{0,2},{1,3},{2,0},{3,1},{4,6},{5,7},{6,4},{7,5},{8,10},{9,11},{10,... | collective-permute-start | bytes 393224 | tf_op jit(solution)/shard_map/ppermute | solution.py:448
  24.2 7.3 %collective-permute-start.7 = (bf16[256,256]{1,0:T(8,128)(2,1)S(1)}, bf16[256,256]{1,0:T(8,128)(2,1)S(1)}, u32[]{:S(2)}, u32[]{:S(2)}) collective-permute-start(bf16[256,256]{1,0:T(8,128)(2,1)S(1)} %attend_halo.3.refs_0_), channel_id=1, source_target_pairs={{0,1},{1,0},{2,3},{3,2},{4,5},{5,4},{6,7},{7,6},{8,9},{9,8},{10,11... | collective-permute-start | bytes 393224 | tf_op jit(solution)/shard_map/ppermute | solution.py:448
  27.8 4.3 %collective-permute-start.6 = (bf16[256,256]{1,0:T(8,128)(2,1)S(1)}, bf16[256,256]{1,0:T(8,128)(2,1)S(1)}, u32[]{:S(2)}, u32[]{:S(2)}) collective-permute-start(bf16[256,256]{1,0:T(8,128)(2,1)S(1)} %collective-permute-done.5.refs_0_), channel_id=1, source_target_pairs={{0,1},{1,0},{2,3},{3,2},{4,5},{5,4},{6,7},{7,6},{8,9},{9,8},{10,11... | collective-permute-start | bytes 393224 | tf_op jit(solution)/shard_map/ppermute | solution.py:448
  32.3 7.9 %collective-permute-start.8 = (bf16[256,512]{1,0:T(8,128)(2,1)S(1)}, bf16[256,512]{1,0:T(8,128)(2,1)S(1)}, u32[]{:S(2)}, u32[]{:S(2)}) collective-permute-start(bf16[256,512]{1,0:T(8,128)(2,1)S(1)} %shard_map.81.refs_0_.refs_2_), channel_id=1, source_target_pairs={{0,2},{1,3},{2,0},{3,1},{4,6},{5,7},{6,4},{7,5},{8,10},{9,11},{10,... | collective-permute-start | bytes 786440 | tf_op jit(solution)/shard_map/ppermute | solution.py:448
  32.6 10.7 %collective-permute-start.10 = (bf16[256,512]{1,0:T(8,128)(2,1)S(1)}, bf16[256,512]{1,0:T(8,128)(2,1)S(1)}, u32[]{:S(2)}, u32[]{:S(2)}) collective-permute-start(bf16[256,512]{1,0:T(8,128)(2,1)S(1)} %shard_map.81.refs_0_.refs_2_), channel_id=1, source_target_pairs={{0,1},{1,0},{2,3},{3,2},{4,5},{5,4},{6,7},{7,6},{8,9},{9,8},{10,11... | collective-permute-start | bytes 786440 | tf_op jit(solution)/shard_map/ppermute | solution.py:448
  40.2 4.1 %collective-permute-start.9 = (bf16[256,512]{1,0:T(8,128)(2,1)S(1)}, bf16[256,512]{1,0:T(8,128)(2,1)S(1)}, u32[]{:S(2)}, u32[]{:S(2)}) collective-permute-start(bf16[256,512]{1,0:T(8,128)(2,1)S(1)} %collective-permute-done.8.refs_0_), channel_id=1, source_target_pairs={{0,1},{1,0},{2,3},{3,2},{4,5},{5,4},{6,7},{7,6},{8,9},{9,8},{10,11... | collective-permute-start | bytes 786440 | tf_op jit(solution)/shard_map/ppermute | solution.py:448
  44.7 7.9 %collective-permute-start.11 = (bf16[2,256,256]{2,1,0:T(8,128)(2,1)S(1)}, bf16[2,256,256]{2,1,0:T(8,128)(2,1)S(1)}, u32[]{:S(2)}, u32[]{:S(2)}) collective-permute-start(bf16[2,256,256]{2,1,0:T(8,128)(2,1)S(1)} %shard_map.86.pair_ref), channel_id=1, source_target_pairs={{0,4},{1,5},{2,6},{3,7},{4,0},{5,1},{6,2},{7,3},{8,12},{9,13},{10,... | collective-permute-start | bytes 786440 | tf_op jit(solution)/shard_map/ppermute | solution.py:443
  44.8 7.8 %collective-permute-start.12 = (bf16[2,256,256]{2,1,0:T(8,128)(2,1)S(1)}, bf16[2,256,256]{2,1,0:T(8,128)(2,1)S(1)}, u32[]{:S(2)}, u32[]{:S(2)}) collective-permute-start(bf16[2,256,256]{2,1,0:T(8,128)(2,1)S(1)} %shard_map.86.pair_ref), channel_id=1, source_target_pairs={{0,1},{1,0},{2,3},{3,2},{4,8},{5,9},{6,10},{7,11},{8,4},{9,5},{10,... | collective-permute-start | bytes 786440 | tf_op jit(solution)/shard_map/ppermute | solution.py:443
  53.3 3.9 %collective-permute-start.13 = (bf16[256,256]{1,0:T(8,128)(2,1)S(1)}, bf16[256,256]{1,0:T(8,128)(2,1)S(1)}, u32[]{:S(2)}, u32[]{:S(2)}) collective-permute-start(bf16[256,256]{1,0:T(8,128)(2,1)S(1)} %attend_halo.4.refs_0_), channel_id=1, source_target_pairs={{0,2},{1,3},{2,0},{3,1},{4,6},{5,7},{6,4},{7,5},{8,10},{9,11},{10,... | collective-permute-start | bytes 393224 | tf_op jit(solution)/shard_map/ppermute | solution.py:448
  53.6 7.1 %collective-permute-start.15 = (bf16[256,256]{1,0:T(8,128)(2,1)S(1)}, bf16[256,256]{1,0:T(8,128)(2,1)S(1)}, u32[]{:S(2)}, u32[]{:S(2)}) collective-permute-start(bf16[256,256]{1,0:T(8,128)(2,1)S(1)} %attend_halo.4.refs_0_), channel_id=1, source_target_pairs={{0,1},{1,0},{2,3},{3,2},{4,5},{5,4},{6,7},{7,6},{8,9},{9,8},{10,11... | collective-permute-start | bytes 393224 | tf_op jit(solution)/shard_map/ppermute | solution.py:448
  57.2 4.1 %collective-permute-start.14 = (bf16[256,256]{1,0:T(8,128)(2,1)S(1)}, bf16[256,256]{1,0:T(8,128)(2,1)S(1)}, u32[]{:S(2)}, u32[]{:S(2)}) collective-permute-start(bf16[256,256]{1,0:T(8,128)(2,1)S(1)} %collective-permute-done.13.refs_0_), channel_id=1, source_target_pairs={{0,1},{1,0},{2,3},{3,2},{4,5},{5,4},{6,7},{7,6},{8,9},{9,8},{10,11... | collective-permute-start | bytes 393224 | tf_op jit(solution)/shard_map/ppermute | solution.py:448
  61.5 7.9 %collective-permute-start.16 = (bf16[256,512]{1,0:T(8,128)(2,1)S(1)}, bf16[256,512]{1,0:T(8,128)(2,1)S(1)}, u32[]{:S(2)}, u32[]{:S(2)}) collective-permute-start(bf16[256,512]{1,0:T(8,128)(2,1)S(1)} %shard_map.90.refs_0_.refs_2_), channel_id=1, source_target_pairs={{0,2},{1,3},{2,0},{3,1},{4,6},{5,7},{6,4},{7,5},{8,10},{9,11},{10,... | collective-permute-start | bytes 786440 | tf_op jit(solution)/shard_map/ppermute | solution.py:448
  61.8 10.7 %collective-permute-start.18 = (bf16[256,512]{1,0:T(8,128)(2,1)S(1)}, bf16[256,512]{1,0:T(8,128)(2,1)S(1)}, u32[]{:S(2)}, u32[]{:S(2)}) collective-permute-start(bf16[256,512]{1,0:T(8,128)(2,1)S(1)} %shard_map.90.refs_0_.refs_2_), channel_id=1, source_target_pairs={{0,1},{1,0},{2,3},{3,2},{4,5},{5,4},{6,7},{7,6},{8,9},{9,8},{10,11... | collective-permute-start | bytes 786440 | tf_op jit(solution)/shard_map/ppermute | solution.py:448
  69.4 4.1 %collective-permute-start.17 = (bf16[256,512]{1,0:T(8,128)(2,1)S(1)}, bf16[256,512]{1,0:T(8,128)(2,1)S(1)}, u32[]{:S(2)}, u32[]{:S(2)}) collective-permute-start(bf16[256,512]{1,0:T(8,128)(2,1)S(1)} %collective-permute-done.16.refs_0_), channel_id=1, source_target_pairs={{0,1},{1,0},{2,3},{3,2},{4,5},{5,4},{6,7},{7,6},{8,9},{9,8},{10,11... | collective-permute-start | bytes 786440 | tf_op jit(solution)/shard_map/ppermute | solution.py:448
  73.9 7.9 %collective-permute-start.19 = (bf16[2,256,256]{2,1,0:T(8,128)(2,1)S(1)}, bf16[2,256,256]{2,1,0:T(8,128)(2,1)S(1)}, u32[]{:S(2)}, u32[]{:S(2)}) collective-permute-start(bf16[2,256,256]{2,1,0:T(8,128)(2,1)S(1)} %shard_map.95.pair_ref), channel_id=1, source_target_pairs={{0,4},{1,5},{2,6},{3,7},{4,0},{5,1},{6,2},{7,3},{8,12},{9,13},{10,... | collective-permute-start | bytes 786440 | tf_op jit(solution)/shard_map/ppermute | solution.py:443
  74.0 7.8 %collective-permute-start.20 = (bf16[2,256,256]{2,1,0:T(8,128)(2,1)S(1)}, bf16[2,256,256]{2,1,0:T(8,128)(2,1)S(1)}, u32[]{:S(2)}, u32[]{:S(2)}) collective-permute-start(bf16[2,256,256]{2,1,0:T(8,128)(2,1)S(1)} %shard_map.95.pair_ref), channel_id=1, source_target_pairs={{0,1},{1,0},{2,3},{3,2},{4,8},{5,9},{6,10},{7,11},{8,4},{9,5},{10,... | collective-permute-start | bytes 786440 | tf_op jit(solution)/shard_map/ppermute | solution.py:443
  82.5 3.9 %collective-permute-start.21 = (bf16[256,256]{1,0:T(8,128)(2,1)S(1)}, bf16[256,256]{1,0:T(8,128)(2,1)S(1)}, u32[]{:S(2)}, u32[]{:S(2)}) collective-permute-start(bf16[256,256]{1,0:T(8,128)(2,1)S(1)} %attend_halo.5.refs_0_), channel_id=1, source_target_pairs={{0,2},{1,3},{2,0},{3,1},{4,6},{5,7},{6,4},{7,5},{8,10},{9,11},{10,... | collective-permute-start | bytes 393224 | tf_op jit(solution)/shard_map/ppermute | solution.py:448
  82.8 7.1 %collective-permute-start.23 = (bf16[256,256]{1,0:T(8,128)(2,1)S(1)}, bf16[256,256]{1,0:T(8,128)(2,1)S(1)}, u32[]{:S(2)}, u32[]{:S(2)}) collective-permute-start(bf16[256,256]{1,0:T(8,128)(2,1)S(1)} %attend_halo.5.refs_0_), channel_id=1, source_target_pairs={{0,1},{1,0},{2,3},{3,2},{4,5},{5,4},{6,7},{7,6},{8,9},{9,8},{10,11... | collective-permute-start | bytes 393224 | tf_op jit(solution)/shard_map/ppermute | solution.py:448
  86.4 4.1 %collective-permute-start.22 = (bf16[256,256]{1,0:T(8,128)(2,1)S(1)}, bf16[256,256]{1,0:T(8,128)(2,1)S(1)}, u32[]{:S(2)}, u32[]{:S(2)}) collective-permute-start(bf16[256,256]{1,0:T(8,128)(2,1)S(1)} %collective-permute-done.21.refs_0_), channel_id=1, source_target_pairs={{0,1},{1,0},{2,3},{3,2},{4,5},{5,4},{6,7},{7,6},{8,9},{9,8},{10,11... | collective-permute-start | bytes 393224 | tf_op jit(solution)/shard_map/ppermute | solution.py:448

commit v3 on v2

--- a/solution.py
+++ b/solution.py
@@ -64,10 +64,10 @@
     )
 
 
-def project_kernel(bits, first, kinds, layer, *refs):
+def project_kernel(bits, load, first, kinds, layer, *refs):
     sources, refs = refs[: len(bits)], refs[len(bits) :]
     gain_ref, refs = refs[0], refs[1:]
-    if first:
+    if load:
         stored, refs = refs[:3], refs[3:]
         *refs, held_ref, sems = refs
         copies = [
@@ -77,7 +77,9 @@
         for copy in copies:
             copy.start()
     else:
-        (held_ref, acc_in, sq_in), refs = refs[:3], refs[3:]
+        held_ref, refs = refs[0], refs[1:]
+    if not first:
+        (acc_in, sq_in), refs = refs[:2], refs[2:]
     full = gain_ref.shape[1]
     totals = [None, None, None]
     squares = None
@@ -89,7 +91,7 @@
         squares = square if squares is None else squares + square
         scaled = (wide * gain_ref[layer : layer + 1, cols]).astype(BF16)
         for kind in kinds or range(3):
-            if first and at == 0:
+            if load and at == 0:
                 copies[kind].wait()
             product = nt_dot(scaled, held_ref[kind, :, cols])
             totals[kind] = product if totals[kind] is None else totals[kind] + product
@@ -115,25 +117,29 @@
     first = carried is None
     operands = [*parts, gain]
     specs = [VMEM] * (parts_n + 1)
-    if first:
+    load = isinstance(weights, list)
+    if load:
         _, channels, full = weights[0].shape
         operands += weights
         specs += [HBM] * 3
     else:
         _, channels, full = weights.shape
-        operands += [in_vmem(weights), *map(in_vmem, carried)]
-        specs += [VMEM] * 3
+        operands.append(in_vmem(weights))
+        specs.append(VMEM)
+    if not first:
+        operands += map(in_vmem, carried)
+        specs += [VMEM] * 2
     if kinds:
         out_shape = [pltpu.VMEM((len(kinds), tok, channels), BF16)]
     else:
         out_shape = [pltpu.VMEM((3, tok, channels), F32), pltpu.VMEM((tok, LANES), F32)]
     scratch = []
-    if first:
+    if load:
         out_shape.append(pltpu.VMEM((3, channels, full), BF16))
         scratch.append(pltpu.SemaphoreType.DMA((3,)))
     flops = 2 * tok * width * channels * len(kinds or range(3)) * parts_n
     return pl.pallas_call(
-        partial(project_kernel, bits, first, kinds, layer),
+        partial(project_kernel, bits, load, first, kinds, layer),
         out_shape=out_shape,
         in_specs=specs,
         out_specs=[VMEM] * len(out_shape),
@@ -182,6 +188,91 @@
         ),
         compiler_params=PARAMS,
     )(*parts, weight if first else in_vmem(weight), base if first else in_vmem(base))
+
+
+def fetch_kernel(pick, count, *refs):
+    sources, targets, sems = refs[:count], refs[count:-1], refs[-1]
+    copies = [
+        pltpu.make_async_copy(source, target, sems.at[at])
+        for at, (source, target) in enumerate(pick(sources, targets))
+    ]
+    for copy in copies:
+        copy.start()
+    for copy in copies:
+        copy.wait()
+
+
+def fetch(arrays, shapes, pick, copies):
+    return pl.pallas_call(
+        partial(fetch_kernel, pick, len(arrays)),
+        out_shape=[pltpu.VMEM(shape, BF16) for shape in shapes],
+        in_specs=[HBM] * len(arrays),
+        out_specs=[VMEM] * len(shapes),
+        scratch_shapes=[pltpu.SemaphoreType.DMA((copies,))],
+        cost_estimate=cost(10**6, 10**6),
+        compiler_params=PARAMS,
+    )(*arrays)
+
+
+def load_weights(weights, layer):
+    _, channels, full = weights[0].shape
+
+    def pick(sources, targets):
+        return [(source.at[layer], targets[0].at[kind]) for kind, source in enumerate(sources)]
+
+    return fetch(weights, [(3, channels, full)], pick, 3)[0]
+
+
+def cut_weight(weight, layer):
+    _, rows, cols = weight.shape
+    half = rows // 2
+    widths = (cols // 2, cols // 4, cols // 4)
+
+    def pick(sources, targets):
+        here = pl.ds(pl.multiple_of(lax.axis_index("grp") * half, half), half)
+        firsts = (0, cols // 2, 3 * cols // 4)
+        return [
+            (sources[0].at[layer, here, pl.ds(first, width)], target)
+            for first, width, target in zip(firsts, widths, targets)
+        ]
+
+    return fetch([weight], [(half, width) for width in widths], pick, 3)
+
+
+def far_kernel(pieces, own_ref, beside_ref, across_ref, corner_ref, base_ref, *refs):
+    near, side, out_ref = refs[:pieces], refs[pieces:-1], refs[-1]
+    me = lax.axis_index("tp")
+    even = me % 2 == 0
+    aligned = me // 2 == lax.axis_index("grp")
+    own, beside, across, corner = own_ref[...], beside_ref[...], across_ref[...], corner_ref[...]
+    mine = jnp.concatenate([jnp.where(even, own, beside), jnp.where(even, beside, own)], axis=1)
+    other = jnp.concatenate(
+        [jnp.where(even, across, corner), jnp.where(even, corner, across)], axis=1
+    )
+    with_near = jnp.where(aligned, mine, other)
+    with_side = jnp.where(aligned, other, mine)
+    done = 0
+    for at in range(pieces):
+        cols = slice(done, done + near[at].shape[1])
+        done = cols.stop
+        total = base_ref[:, cols].astype(F32)
+        total = total + jnp.dot(with_near, near[at][...], preferred_element_type=F32)
+        total = total + jnp.dot(with_side, side[at][...], preferred_element_type=F32)
+        out_ref[:, cols] = total.astype(BF16)
+
+
+def emit_far(parts, base, near, side):
+    tok, cols = base.shape
+    operands = [*parts, base, *near, *side]
+    return pl.pallas_call(
+        partial(far_kernel, len(near)),
+        out_shape=pltpu.VMEM((tok, cols), BF16),
+        in_specs=[VMEM] * len(operands),
+        out_specs=VMEM,
+        cost_estimate=cost(2 * tok * cols * 4 * parts[0].shape[1], 10**6),
+        compiler_params=PARAMS,
+        name="lent",
+    )(*map(in_vmem, operands))
 
 
 def bias_kernel(layer, sp, table_ref, out_ref, *refs):
@@ -448,6 +539,14 @@
     return lax.ppermute(block, axis, [(at, at ^ bit) for at in range(count)])
 
 
+def send_weight(weight, layer):
+    cuts = cut_weight(weight, layer)
+    near = []
+    for cut in cuts:
+        near.append(flip(cut, "tp", 2))
+    return near
+
+
 def body(hidden_in, norm_gain, query_weight, key_weight, value_weight, output_weight, offset_bias):
     tok_dev, _ = hidden_in.shape
     rows_dev = tok_dev // GRID_W
@@ -460,21 +559,41 @@
     even_pairs = [(at, at + 1) for at in range(0, sp - 1, 2)]
     odd_pairs = [(at, at + 1) for at in range(1, sp - 1, 2)]
     stream = hidden_in
+    lend = split and tp == 4 and lax.axis_size("grp") == 2
+    carry = None
     for layer in range(LAYERS):
         step = partial(project, layer=layer, gain=norm_gain)
-        if tp == 4:
+        if carry is not None:
+            parts, base, held = carry
+            beside = flip(stream, "tp", 1)
+            across = emit_far(parts, base, *last_lent)
+            corner = flip(across, "tp", 1)
+            carried = step([stream, across], (0, 2), held, None, None)
+            carried = step([beside], (1,), held, carried, None)
+        elif tp == 4:
             across = flip(stream, "tp", 2)
             beside = flip(stream, "tp", 1)
             corner = flip(across, "tp", 1)
             *carried, held = step([stream], (0,), weights, None, None)
             carried = step([beside], (1,), held, carried, None)
             carried = step([across], (2,), held, carried, None)
+        if tp == 4:
+            across_stream = across
             (pair,) = step([corner], (3,), held, carried, (1, 2))
             (query,) = step([corner], (3,), held, carried, (0,))
         else:
             gathered = lax.all_gather(stream, "tp", axis=1, tiled=True)
             *carried, held = step([gathered], (None,), weights, None, (0, 1, 2))
             query, pair = carried[0][:1], carried[0][1:]
+        if lend and layer < LAYERS - 1:
+            if layer == 0:
+                near = send_weight(output_weight, layer)
+            side = []
+            for piece in near:
+                side.append(flip(piece, "grp", 1))
+            lent = (near, side)
+        else:
+            lent = None
         if split:
             to_even = to_odd = pair
         else:
@@ -492,14 +611,23 @@
         else:
             attended = attend(query, pair, even, odd, bias, rows_dev)
         step = partial(emit, layer=layer)
+        carry = None
+        if lent:
+            last_lent = lent
+            carry = load_weights(weights, layer + 1)
         if tp == 4:
             across = flip(attended, "tp", 2)
             beside = flip(attended, "tp", 1)
             corner = flip(across, "tp", 1)
+            if lent and layer + 1 < LAYERS - 1:
+                near = send_weight(output_weight, layer + 1)
             partly, held = step([attended], (0,), output_weight, stream, F32, True)
             (partly,) = step([beside], (1,), held, partly, F32, False)
             (partly,) = step([across], (2,), held, partly, F32, False)
+            old = across_stream
             (stream,) = step([corner], (3,), held, partly, BF16, False)
+            if carry is not None:
+                carry = ([attended, beside, across, corner], old, carry)
         else:
             gathered = lax.all_gather(attended, "tp", axis=1, tiled=True)
             stream, _ = step([gathered], (None,), output_weight, stream, BF16, True)

time: 92.6 us -> 94.3 us (1.018)
  waiting for transfers between devices: 44.7 us -> 23.6 us
  starting transfers between devices: 19 us -> 38.5 us
  Pallas kernels: 25.5 us -> 28.6 us
    ppermute x18 -> x28, starting transfers between devices: 17 us -> 35.3 us  [flip(): return lax.ppermute(block, axis, [(at, at ^ bit) for at in range(count)])]
    ppermute x18 -> x28, waiting for transfers between devices: 27.7 us -> 9.98 us  [flip(): return lax.ppermute(block, axis, [(at, at ^ bit) for at in range(count)])]
    ppermute x6, waiting for transfers between devices: 17.1 us -> 13.6 us  [exchange(): return lax.ppermute(block, ('sp', 'tp'), moves)]
    pallas_call x15 -> x19, Pallas kernels: 11.6 us -> 14.6 us  [the longest x13 7.56 us: project(): pl.pallas_call(partial(project_kernel, bits, load, first, kinds, layer),...]
    ppermute x6, starting transfers between devices: 1.98 us -> 3.26 us  [exchange(): return lax.ppermute(block, ('sp', 'tp'), moves)]
  transfers between devices with their start and end apart: 24 -> 34, of which waited for: 10 -> 10; matrix products, arithmetic and copies ran while one was open for 0% -> 0% of each run, Pallas kernels for 23% -> 28%
where the time goes in v3:
time: 94.3 us; the launch traced here: 92.8 us
  starting transfers between devices  38.5 us (41%)
  Pallas kernels  28.6 us (30%)
  waiting for transfers between devices  23.6 us (25%)
  local copies, waits for them, and re-layouts  1.73 us (2%)
    ppermute x28, starting transfers between devices, flip(): return lax.ppermute(block, axis, [(at, at ^ bit) for at in range(count)])  35.3 us
    ppermute x6, waiting for transfers between devices, exchange(): return lax.ppermute(block, ('sp', 'tp'), moves)  13.6 us
    ppermute x28, waiting for transfers between devices, flip(): return lax.ppermute(block, axis, [(at, at ^ bit) for at in range(count)])  9.98 us
    pallas_call x13, Pallas kernels, project(): pl.pallas_call(partial(project_kernel, bits, load, first, kinds, layer),...  7.56 us
    pallas_call x12, Pallas kernels, emit(): pl.pallas_call(partial(emit_kernel, bits, first, layer), out_shape=out_sh...  7.19 us
    pallas_call x4, Pallas kernels, fetch(): pl.pallas_call(partial(fetch_kernel, pick, len(arrays)), out_shape=[pltpu...  5.91 us
    ppermute x6, starting transfers between devices, exchange(): return lax.ppermute(block, ('sp', 'tp'), moves)  3.26 us
    pallas_call x3, Pallas kernels, expand_bias(): pl.pallas_call(partial(bias_kernel, layer, lax.axis_size('sp')), out_shap...  2.82 us
  transfers between devices with their start and end apart: 34, of which 10 were waited for; matrix products, arithmetic and copies ran while one was open for 0% of the time, Pallas kernels for 28%

profile of v3, /device:TPU:19, one launch (start us, length us, event | category | flops | bytes accessed | tf_op | source)
XLA Modules:
  0.0 92.8 jit_solution(16375348568698277034)
XLA Ops:
  0.3 1.0 %collective-permute-start.2 = (bf16[256,512]{1,0:T(8,128)(2,1)}, bf16[256,512]{1,0:T(8,128)(2,1)S(1)}, u32[]{:S(2)}, u32[]{:S(2)}) collective-permute-start(bf16[256,512]{1,0:T(8,128)(2,1)} %refs_2_.8), channel_id=1, source_target_pairs={{0,1},{1,0},{2,3},{3,2},{4,5},{5,4},{6,7},{7,6},{8,9},{9,8},{10,11... | collective-permute-start | bytes 786440 | tf_op jit(solution)/shard_map/ppermute | solution.py:539
  1.2 6.2 %collective-permute-done.refs_0_.base_ref = bf16[256,512]{1,0:T(8,128)(2,1)S(1)} collective-permute-done((bf16[256,512]{1,0:T(8,128)(2,1)}, bf16[256,512]{1,0:T(8,128)(2,1)S(1)}, u32[]{:S(2)}, u32[]{:S(2)}) %collective-permute-start) | collective-permute-done | bytes 262176 | tf_op jit(solution)/shard_map/ppermute | solution.py:539
  7.4 1.5 %collective-permute-start.1 = (bf16[256,512]{1,0:T(8,128)(2,1)S(1)}, bf16[256,512]{1,0:T(8,128)(2,1)S(1)}, u32[]{:S(2)}, u32[]{:S(2)}) collective-permute-start(bf16[256,512]{1,0:T(8,128)(2,1)S(1)} %collective-permute-done.refs_0_.base_ref), channel_id=1, source_target_pairs={{0,1},{1,0},{2,3},{3,2},{4,5},{5,4},{6,7},{7,6},{8,9},{9,8},{10,11... | collective-permute-start | bytes 786440 | tf_op jit(solution)/shard_map/ppermute | solution.py:539
  8.9 0.8 copy-done
  9.7 0.9 %copy-done.2 = bf16[256,512]{1,0:T(8,128)(2,1)S(1)} copy-done((bf16[256,512]{1,0:T(8,128)(2,1)S(1)}, bf16[256,512]{1,0:T(8,128)(2,1)}, u32[]{:S(2)}) %copy-start.2) | copy-done | bytes 262168
  10.6 2.2 %shard_map.73 = (f32[3,256,256]{2,1,0:T(8,128)S(1)}, f32[256,128]{1,0:T(8,128)S(1)}, bf16[3,256,2048]{2,1,0:T(8,128)(2,1)S(1)}) custom-call(bf16[256,512]{1,0:T(8,128)(2,1)S(1)} %copy-done.2, f32[3,2048]{1,0:T(4,128)S(1)} %copy-done, bf16[3,256,2048]{2,1,0:T(8,128)(2,1)} %refs_0_.9, bf16[3,256,2048]{2,1,0:T(8,128)(2,1)} %refs_1_.26, ...), custom_call_target="tpu_custom_call" | custom-call | flops 201326592 | bytes 1310720 | tf_op jit(solution)/shard_map/pallas_call | solution.py:141
  14.3 1.4 %collective-permute-start.3 = (bf16[2,256,256]{2,1,0:T(8,128)(2,1)S(1)}, bf16[2,256,256]{2,1,0:T(8,128)(2,1)S(1)}, u32[]{:S(2)}, u32[]{:S(2)}) collective-permute-start(bf16[2,256,256]{2,1,0:T(8,128)(2,1)S(1)} %shard_map.77.pair_ref), channel_id=1, source_target_pairs={{0,4},{1,5},{2,6},{3,7},{4,0},{5,1},{6,2},{7,3},{8,12},{9,13},{10,... | collective-permute-start | bytes 786440 | tf_op jit(solution)/shard_map/ppermute | solution.py:534
  15.6 1.1 %shard_map.78 = (bf16[512,256]{1,0:T(8,128)(2,1)S(1)}, bf16[512,128]{1,0:T(8,128)(2,1)S(1)}, bf16[512,128]{1,0:T(8,128)(2,1)S(1)}) custom-call(bf16[3,1024,512]{2,1,0:T(8,128)(2,1)} %refs_1_.31), custom_call_target="tpu_custom_call" | custom-call | flops 1000000 | bytes 1000000 | tf_op jit(solution)/shard_map/pallas_call | solution.py:206
  17.0 0.9 %expand_bias.3 = (f32[4,14,64,128]{3,2,1,0:T(8,128)S(1)}, f32[4,4,2,64,128]{4,3,2,1,0:T(8,128)S(1)}) custom-call(f32[3,4,15,31]{3,2,1,0:T(8,128)S(1)} %copy.8.table_ref), custom_call_target="tpu_custom_call" | custom-call | flops 18350080 | bytes 1835008 | tf_op jit(solution)/shard_map/expand_bias/pallas_call | solution.py:318
  19.0 3.2 %collective-permute-done.3.even_ref = bf16[2,256,256]{2,1,0:T(8,128)(2,1)S(1)} collective-permute-done((bf16[2,256,256]{2,1,0:T(8,128)(2,1)S(1)}, bf16[2,256,256]{2,1,0:T(8,128)(2,1)S(1)}, u32[]{:S(2)}, u32[]{:S(2)}) %collective-permute-start.3) | collective-permute-done | bytes 262176 | tf_op jit(solution)/shard_map/ppermute | solution.py:534
  22.2 1.0 %collective-permute-done.4.odd_ref = bf16[2,256,256]{2,1,0:T(8,128)(2,1)S(1)} collective-permute-done((bf16[2,256,256]{2,1,0:T(8,128)(2,1)S(1)}, bf16[2,256,256]{2,1,0:T(8,128)(2,1)S(1)}, u32[]{:S(2)}, u32[]{:S(2)}) %collective-permute-start.4) | collective-permute-done | bytes 262176 | tf_op jit(solution)/shard_map/ppermute | solution.py:534
  23.2 0.7 attend_halo.3.own_ref.refs_0_
  24.2 1.2 %collective-permute-start.9 = (bf16[512,128]{1,0:T(8,128)(2,1)S(1)}, bf16[512,128]{1,0:T(8,128)(2,1)S(1)}, u32[]{:S(2)}, u32[]{:S(2)}) collective-permute-start(bf16[512,128]{1,0:T(8,128)(2,1)S(1)} %get-tuple-element.56), channel_id=1, source_target_pairs={{0,2},{1,3},{2,0},{3,1},{4,6},{5,7},{6,4},{7,5},{8,10},{9,11},{10,... | collective-permute-start | bytes 393224 | tf_op jit(solution)/shard_map/ppermute | solution.py:539
  25.7 1.2 %collective-permute-start.11 = (bf16[512,256]{1,0:T(8,128)(2,1)S(1)}, bf16[512,256]{1,0:T(8,128)(2,1)S(1)}, u32[]{:S(2)}, u32[]{:S(2)}) collective-permute-start(bf16[512,256]{1,0:T(8,128)(2,1)S(1)} %collective-permute-done.8.refs_0_), channel_id=1, source_target_pairs={{0,16},{16,0},{1,17},{17,1},{2,18},{18,2},{3,19},{19,3},{4,20},{20... | collective-permute-start | bytes 786440 | tf_op jit(solution)/shard_map/ppermute | solution.py:539
  26.9 2.3 %collective-permute-start.5 = (bf16[256,256]{1,0:T(8,128)(2,1)S(1)}, bf16[256,256]{1,0:T(8,128)(2,1)S(1)}, u32[]{:S(2)}, u32[]{:S(2)}) collective-permute-start(bf16[256,256]{1,0:T(8,128)(2,1)S(1)} %attend_halo.3.own_ref.refs_0_), channel_id=1, source_target_pairs={{0,1},{1,0},{2,3},{3,2},{4,5},{5,4},{6,7},{7,6},{8,9},{9,8},{10,11... | collective-permute-start | bytes 393224 | tf_op jit(solution)/shard_map/ppermute | solution.py:539
  29.2 2.3 %collective-permute-start.7 = (bf16[256,256]{1,0:T(8,128)(2,1)S(1)}, bf16[256,256]{1,0:T(8,128)(2,1)S(1)}, u32[]{:S(2)}, u32[]{:S(2)}) collective-permute-start(bf16[256,256]{1,0:T(8,128)(2,1)S(1)} %collective-permute-done.6.across_ref.refs_0_), channel_id=1, source_target_pairs={{0,1},{1,0},{2,3},{3,2},{4,5},{5,4},{6,7},{7,6},{8,9},{9,8},{10,11... | collective-permute-start | bytes 393224 | tf_op jit(solution)/shard_map/ppermute | solution.py:539
  31.5 1.2 %collective-permute-start.12 = (bf16[512,128]{1,0:T(8,128)(2,1)S(1)}, bf16[512,128]{1,0:T(8,128)(2,1)S(1)}, u32[]{:S(2)}, u32[]{:S(2)}) collective-permute-start(bf16[512,128]{1,0:T(8,128)(2,1)S(1)} %collective-permute-done.9.refs_1_), channel_id=1, source_target_pairs={{0,16},{16,0},{1,17},{17,1},{2,18},{18,2},{3,19},{19,3},{4,20},{20... | collective-permute-start | bytes 393224 | tf_op jit(solution)/shard_map/ppermute | solution.py:539
  32.7 0.8 collective-permute-done.10.refs_2_
  33.5 1.2 %collective-permute-start.13 = (bf16[512,128]{1,0:T(8,128)(2,1)S(1)}, bf16[512,128]{1,0:T(8,128)(2,1)S(1)}, u32[]{:S(2)}, u32[]{:S(2)}) collective-permute-start(bf16[512,128]{1,0:T(8,128)(2,1)S(1)} %collective-permute-done.10.refs_2_), channel_id=1, source_target_pairs={{0,16},{16,0},{1,17},{17,1},{2,18},{18,2},{3,19},{19,3},{4,20},{20... | collective-permute-start | bytes 393224 | tf_op jit(solution)/shard_map/ppermute | solution.py:539
  34.7 1.5 %shard_map.80 = (f32[256,512]{1,0:T(8,128)S(1)}, bf16[1024,512]{1,0:T(8,128)(2,1)S(1)}) custom-call(bf16[256,256]{1,0:T(8,128)(2,1)S(1)} %attend_halo.3.own_ref.refs_0_, bf16[3,1024,512]{2,1,0:T(8,128)(2,1)} %refs_1_.31, bf16[256,512]{1,0:T(8,128)(2,1)S(1)} %copy-done.3), custom_call_target="tpu_custom_call" | custom-call | flops 67108864 | bytes 1179648 | tf_op jit(solution)/shard_map/pallas_call | solution.py:180
  36.9 2.3 %collective-permute-start.15 = (bf16[256,512]{1,0:T(8,128)(2,1)S(1)}, bf16[256,512]{1,0:T(8,128)(2,1)S(1)}, u32[]{:S(2)}, u32[]{:S(2)}) collective-permute-start(bf16[256,512]{1,0:T(8,128)(2,1)S(1)} %shard_map.83.refs_0_.refs_2_), channel_id=1, source_target_pairs={{0,1},{1,0},{2,3},{3,2},{4,5},{5,4},{6,7},{7,6},{8,9},{9,8},{10,11... | collective-permute-start | bytes 786440 | tf_op jit(solution)/shard_map/ppermute | solution.py:539
  39.9 1.6 %collective-permute-start.14 = (bf16[256,512]{1,0:T(8,128)(2,1)S(1)}, bf16[256,512]{1,0:T(8,128)(2,1)S(1)}, u32[]{:S(2)}, u32[]{:S(2)}) collective-permute-start(bf16[256,512]{1,0:T(8,128)(2,1)S(1)} %lent.2.refs_1_.base_ref), channel_id=1, source_target_pairs={{0,1},{1,0},{2,3},{3,2},{4,5},{5,4},{6,7},{7,6},{8,9},{9,8},{10,11... | collective-permute-start | bytes 786440 | tf_op jit(solution)/shard_map/ppermute | solution.py:539
  41.5 1.9 %shard_map.79.refs_3_.refs_2_ = bf16[3,256,2048]{2,1,0:T(8,128)(2,1)S(1)} custom-call(bf16[3,256,2048]{2,1,0:T(8,128)(2,1)} %refs_0_.9, bf16[3,256,2048]{2,1,0:T(8,128)(2,1)} %refs_1_.26, bf16[3,256,2048]{2,1,0:T(8,128)(2,1)} %refs_2_.10), custom_call_target="tpu_custom_call" | custom-call | flops 1000000 | bytes 1000000 | tf_op jit(solution)/shard_map/pallas_call | solution.py:206
  43.4 0.6 shard_map.84
  45.6 1.1 %shard_map.88 = (bf16[512,256]{1,0:T(8,128)(2,1)S(1)}, bf16[512,128]{1,0:T(8,128)(2,1)S(1)}, bf16[512,128]{1,0:T(8,128)(2,1)S(1)}) custom-call(bf16[3,1024,512]{2,1,0:T(8,128)(2,1)} %refs_1_.31), custom_call_target="tpu_custom_call" | custom-call | flops 1000000 | bytes 1000000 | tf_op jit(solution)/shard_map/pallas_call | solution.py:206
  46.9 0.9 %expand_bias.4 = (f32[4,14,64,128]{3,2,1,0:T(8,128)S(1)}, f32[4,4,2,64,128]{4,3,2,1,0:T(8,128)S(1)}) custom-call(f32[3,4,15,31]{3,2,1,0:T(8,128)S(1)} %copy.8.table_ref), custom_call_target="tpu_custom_call" | custom-call | flops 18350080 | bytes 1835008 | tf_op jit(solution)/shard_map/expand_bias/pallas_call | solution.py:318
  48.8 3.9 %collective-permute-done.16.even_ref = bf16[2,256,256]{2,1,0:T(8,128)(2,1)S(1)} collective-permute-done((bf16[2,256,256]{2,1,0:T(8,128)(2,1)S(1)}, bf16[2,256,256]{2,1,0:T(8,128)(2,1)S(1)}, u32[]{:S(2)}, u32[]{:S(2)}) %collective-permute-start.16) | collective-permute-done | bytes 262176 | tf_op jit(solution)/shard_map/ppermute | solution.py:534
  53.1 0.7 attend_halo.4.own_ref.refs_0_
  54.0 1.3 %collective-permute-start.22 = (bf16[512,128]{1,0:T(8,128)(2,1)S(1)}, bf16[512,128]{1,0:T(8,128)(2,1)S(1)}, u32[]{:S(2)}, u32[]{:S(2)}) collective-permute-start(bf16[512,128]{1,0:T(8,128)(2,1)S(1)} %get-tuple-element.69), channel_id=1, source_target_pairs={{0,2},{1,3},{2,0},{3,1},{4,6},{5,7},{6,4},{7,5},{8,10},{9,11},{10,... | collective-permute-start | bytes 393224 | tf_op jit(solution)/shard_map/ppermute | solution.py:539
  55.5 1.2 %collective-permute-start.24 = (bf16[512,256]{1,0:T(8,128)(2,1)S(1)}, bf16[512,256]{1,0:T(8,128)(2,1)S(1)}, u32[]{:S(2)}, u32[]{:S(2)}) collective-permute-start(bf16[512,256]{1,0:T(8,128)(2,1)S(1)} %collective-permute-done.21.refs_0_), channel_id=1, source_target_pairs={{0,16},{16,0},{1,17},{17,1},{2,18},{18,2},{3,19},{19,3},{4,20},{20... | collective-permute-start | bytes 786440 | tf_op jit(solution)/shard_map/ppermute | solution.py:539
  56.7 2.3 %collective-permute-start.18 = (bf16[256,256]{1,0:T(8,128)(2,1)S(1)}, bf16[256,256]{1,0:T(8,128)(2,1)S(1)}, u32[]{:S(2)}, u32[]{:S(2)}) collective-permute-start(bf16[256,256]{1,0:T(8,128)(2,1)S(1)} %attend_halo.4.own_ref.refs_0_), channel_id=1, source_target_pairs={{0,1},{1,0},{2,3},{3,2},{4,5},{5,4},{6,7},{7,6},{8,9},{9,8},{10,11... | collective-permute-start | bytes 393224 | tf_op jit(solution)/shard_map/ppermute | solution.py:539
  59.0 2.3 %collective-permute-start.20 = (bf16[256,256]{1,0:T(8,128)(2,1)S(1)}, bf16[256,256]{1,0:T(8,128)(2,1)S(1)}, u32[]{:S(2)}, u32[]{:S(2)}) collective-permute-start(bf16[256,256]{1,0:T(8,128)(2,1)S(1)} %collective-permute-done.19.across_ref.refs_0_), channel_id=1, source_target_pairs={{0,1},{1,0},{2,3},{3,2},{4,5},{5,4},{6,7},{7,6},{8,9},{9,8},{10,11... | collective-permute-start | bytes 393224 | tf_op jit(solution)/shard_map/ppermute | solution.py:539
  61.3 1.2 %collective-permute-start.25 = (bf16[512,128]{1,0:T(8,128)(2,1)S(1)}, bf16[512,128]{1,0:T(8,128)(2,1)S(1)}, u32[]{:S(2)}, u32[]{:S(2)}) collective-permute-start(bf16[512,128]{1,0:T(8,128)(2,1)S(1)} %collective-permute-done.22.refs_1_), channel_id=1, source_target_pairs={{0,16},{16,0},{1,17},{17,1},{2,18},{18,2},{3,19},{19,3},{4,20},{20... | collective-permute-start | bytes 393224 | tf_op jit(solution)/shard_map/ppermute | solution.py:539
  62.6 0.8 collective-permute-done.23.refs_2_
  63.3 1.2 %collective-permute-start.26 = (bf16[512,128]{1,0:T(8,128)(2,1)S(1)}, bf16[512,128]{1,0:T(8,128)(2,1)S(1)}, u32[]{:S(2)}, u32[]{:S(2)}) collective-permute-start(bf16[512,128]{1,0:T(8,128)(2,1)S(1)} %collective-permute-done.23.refs_2_), channel_id=1, source_target_pairs={{0,16},{16,0},{1,17},{17,1},{2,18},{18,2},{3,19},{19,3},{4,20},{20... | collective-permute-start | bytes 393224 | tf_op jit(solution)/shard_map/ppermute | solution.py:539
  64.5 1.5 %shard_map.90 = (f32[256,512]{1,0:T(8,128)S(1)}, bf16[1024,512]{1,0:T(8,128)(2,1)S(1)}) custom-call(bf16[256,256]{1,0:T(8,128)(2,1)S(1)} %attend_halo.4.own_ref.refs_0_, bf16[3,1024,512]{2,1,0:T(8,128)(2,1)} %refs_1_.31, bf16[256,512]{1,0:T(8,128)(2,1)S(1)} %shard_map.83.refs_0_.refs_2_), custom_call_target="tpu_custom_call" | custom-call | flops 67108864 | bytes 1179648 | tf_op jit(solution)/shard_map/pallas_call | solution.py:180
  66.7 2.4 %collective-permute-start.28 = (bf16[256,512]{1,0:T(8,128)(2,1)S(1)}, bf16[256,512]{1,0:T(8,128)(2,1)S(1)}, u32[]{:S(2)}, u32[]{:S(2)}) collective-permute-start(bf16[256,512]{1,0:T(8,128)(2,1)S(1)} %shard_map.93.refs_0_.refs_2_), channel_id=1, source_target_pairs={{0,1},{1,0},{2,3},{3,2},{4,5},{5,4},{6,7},{7,6},{8,9},{9,8},{10,11... | collective-permute-start | bytes 786440 | tf_op jit(solution)/shard_map/ppermute | solution.py:539
  69.7 1.6 %collective-permute-start.27 = (bf16[256,512]{1,0:T(8,128)(2,1)S(1)}, bf16[256,512]{1,0:T(8,128)(2,1)S(1)}, u32[]{:S(2)}, u32[]{:S(2)}) collective-permute-start(bf16[256,512]{1,0:T(8,128)(2,1)S(1)} %lent.3.refs_1_), channel_id=1, source_target_pairs={{0,1},{1,0},{2,3},{3,2},{4,5},{5,4},{6,7},{7,6},{8,9},{9,8},{10,11... | collective-permute-start | bytes 786440 | tf_op jit(solution)/shard_map/ppermute | solution.py:539
  71.3 1.9 %shard_map.89.refs_3_.refs_2_ = bf16[3,256,2048]{2,1,0:T(8,128)(2,1)S(1)} custom-call(bf16[3,256,2048]{2,1,0:T(8,128)(2,1)} %refs_0_.9, bf16[3,256,2048]{2,1,0:T(8,128)(2,1)} %refs_1_.26, bf16[3,256,2048]{2,1,0:T(8,128)(2,1)} %refs_2_.10), custom_call_target="tpu_custom_call" | custom-call | flops 1000000 | bytes 1000000 | tf_op jit(solution)/shard_map/pallas_call | solution.py:206
  73.2 0.6 shard_map.94
  76.0 0.9 %expand_bias.5 = (f32[4,14,64,128]{3,2,1,0:T(8,128)S(1)}, f32[4,4,2,64,128]{4,3,2,1,0:T(8,128)S(1)}) custom-call(f32[3,4,15,31]{3,2,1,0:T(8,128)S(1)} %copy.8.table_ref), custom_call_target="tpu_custom_call" | custom-call | flops 18350080 | bytes 1835008 | tf_op jit(solution)/shard_map/expand_bias/pallas_call | solution.py:318
  77.9 4.8 %collective-permute-done.29.even_ref = bf16[2,256,256]{2,1,0:T(8,128)(2,1)S(1)} collective-permute-done((bf16[2,256,256]{2,1,0:T(8,128)(2,1)S(1)}, bf16[2,256,256]{2,1,0:T(8,128)(2,1)S(1)}, u32[]{:S(2)}, u32[]{:S(2)}) %collective-permute-start.29) | collective-permute-done | bytes 262176 | tf_op jit(solution)/shard_map/ppermute | solution.py:534
  83.0 0.7 attend_halo.5.refs_0_
  84.0 1.4 %collective-permute-start.33 = (bf16[256,256]{1,0:T(8,128)(2,1)S(1)}, bf16[256,256]{1,0:T(8,128)(2,1)S(1)}, u32[]{:S(2)}, u32[]{:S(2)}) collective-permute-start(bf16[256,256]{1,0:T(8,128)(2,1)S(1)} %attend_halo.5.refs_0_), channel_id=1, source_target_pairs={{0,1},{1,0},{2,3},{3,2},{4,5},{5,4},{6,7},{7,6},{8,9},{9,8},{10,11... | collective-permute-start | bytes 393224 | tf_op jit(solution)/shard_map/ppermute | solution.py:539
  85.4 2.2 %collective-permute-done.31.refs_0_ = bf16[256,256]{1,0:T(8,128)(2,1)S(1)} collective-permute-done((bf16[256,256]{1,0:T(8,128)(2,1)S(1)}, bf16[256,256]{1,0:T(8,128)(2,1)S(1)}, u32[]{:S(2)}, u32[]{:S(2)}) %collective-permute-start.31) | collective-permute-done | bytes 131104 | tf_op jit(solution)/shard_map/ppermute | solution.py:539
  87.6 2.3 %collective-permute-start.32 = (bf16[256,256]{1,0:T(8,128)(2,1)S(1)}, bf16[256,256]{1,0:T(8,128)(2,1)S(1)}, u32[]{:S(2)}, u32[]{:S(2)}) collective-permute-start(bf16[256,256]{1,0:T(8,128)(2,1)S(1)} %collective-permute-done.31.refs_0_), channel_id=1, source_target_pairs={{0,1},{1,0},{2,3},{3,2},{4,5},{5,4},{6,7},{7,6},{8,9},{9,8},{10,11... | collective-permute-start | bytes 393224 | tf_op jit(solution)/shard_map/ppermute | solution.py:539
  89.9 1.5 %shard_map.98 = (f32[256,512]{1,0:T(8,128)S(1)}, bf16[1024,512]{1,0:T(8,128)(2,1)S(1)}) custom-call(bf16[256,256]{1,0:T(8,128)(2,1)S(1)} %attend_halo.5.refs_0_, bf16[3,1024,512]{2,1,0:T(8,128)(2,1)} %refs_1_.31, bf16[256,512]{1,0:T(8,128)(2,1)S(1)} %shard_map.93.refs_0_.refs_2_), custom_call_target="tpu_custom_call" | custom-call | flops 67108864 | bytes 1179648 | tf_op jit(solution)/shard_map/pallas_call | solution.py:180
  91.9 0.9 %shard_map.101 = bf16[256,512]{1,0:T(8,128)(2,1)} custom-call(bf16[256,256]{1,0:T(8,128)(2,1)S(1)} %collective-permute-done.32.refs_0_, bf16[1024,512]{1,0:T(8,128)(2,1)S(1)} %get-tuple-element.81.refs_1_, f32[256,512]{1,0:T(8,128)S(1)} %shard_map.100.refs_2_), custom_call_target="tpu_custom_call" | custom-call | flops 67108864 | bytes 1179648 | tf_op jit(solution)/shard_map/pallas_call | solution.py:180
  (71 shorter events, 13.6 us)
Async XLA Ops:
  0.0 7.4 %collective-permute-start = (bf16[256,512]{1,0:T(8,128)(2,1)}, bf16[256,512]{1,0:T(8,128)(2,1)S(1)}, u32[]{:S(2)}, u32[]{:S(2)}) collective-permute-start(bf16[256,512]{1,0:T(8,128)(2,1)} %refs_2_.8), channel_id=1, source_target_pairs={{0,2},{1,3},{2,0},{3,1},{4,6},{5,7},{6,4},{7,5},{8,10},{9,11},{10,... | collective-permute-start | bytes 786440 | tf_op jit(solution)/shard_map/ppermute | solution.py:539
  0.3 12.6 %collective-permute-start.2 = (bf16[256,512]{1,0:T(8,128)(2,1)}, bf16[256,512]{1,0:T(8,128)(2,1)S(1)}, u32[]{:S(2)}, u32[]{:S(2)}) collective-permute-start(bf16[256,512]{1,0:T(8,128)(2,1)} %refs_2_.8), channel_id=1, source_target_pairs={{0,1},{1,0},{2,3},{3,2},{4,5},{5,4},{6,7},{7,6},{8,9},{9,8},{10,11... | collective-permute-start | bytes 786440 | tf_op jit(solution)/shard_map/ppermute | solution.py:539
  7.4 6.5 %collective-permute-start.1 = (bf16[256,512]{1,0:T(8,128)(2,1)S(1)}, bf16[256,512]{1,0:T(8,128)(2,1)S(1)}, u32[]{:S(2)}, u32[]{:S(2)}) collective-permute-start(bf16[256,512]{1,0:T(8,128)(2,1)S(1)} %collective-permute-done.refs_0_.base_ref), channel_id=1, source_target_pairs={{0,1},{1,0},{2,3},{3,2},{4,5},{5,4},{6,7},{7,6},{8,9},{9,8},{10,11... | collective-permute-start | bytes 786440 | tf_op jit(solution)/shard_map/ppermute | solution.py:539
  8.9 0.8 copy-start
  9.7 0.9 %copy-start.2 = (bf16[256,512]{1,0:T(8,128)(2,1)S(1)}, bf16[256,512]{1,0:T(8,128)(2,1)}, u32[]{:S(2)}) copy-start(bf16[256,512]{1,0:T(8,128)(2,1)} %refs_2_.8) | copy-start | bytes 786436
  10.6 2.3 %copy-start.1 = (f32[3,2048]{1,0:T(4,128)S(1)}, f32[3,2048]{1,0:T(4,128)}, u32[]{:S(2)}) copy-start(f32[3,2048]{1,0:T(4,128)} %refs_1_.30) | copy-start | bytes 73732
  13.9 3.1 %copy-start.4 = (f32[3,4,15,31]{3,1,2,0:T(4,128)S(1)}, f32[3,4,15,31]{3,1,2,0:T(4,128)}, u32[]{:S(2)}) copy-start(f32[3,4,15,31]{3,1,2,0:T(4,128)} %param.13) | copy-start | bytes 66964
  14.3 7.9 %collective-permute-start.3 = (bf16[2,256,256]{2,1,0:T(8,128)(2,1)S(1)}, bf16[2,256,256]{2,1,0:T(8,128)(2,1)S(1)}, u32[]{:S(2)}, u32[]{:S(2)}) collective-permute-start(bf16[2,256,256]{2,1,0:T(8,128)(2,1)S(1)} %shard_map.77.pair_ref), channel_id=1, source_target_pairs={{0,4},{1,5},{2,6},{3,7},{4,0},{5,1},{6,2},{7,3},{8,12},{9,13},{10,... | collective-permute-start | bytes 786440 | tf_op jit(solution)/shard_map/ppermute | solution.py:534
  15.6 7.6 %collective-permute-start.4 = (bf16[2,256,256]{2,1,0:T(8,128)(2,1)S(1)}, bf16[2,256,256]{2,1,0:T(8,128)(2,1)S(1)}, u32[]{:S(2)}, u32[]{:S(2)}) collective-permute-start(bf16[2,256,256]{2,1,0:T(8,128)(2,1)S(1)} %shard_map.77.pair_ref), channel_id=1, source_target_pairs={{0,1},{1,0},{2,3},{3,2},{4,8},{5,9},{6,10},{7,11},{8,4},{9,5},{10,... | collective-permute-start | bytes 786440 | tf_op jit(solution)/shard_map/ppermute | solution.py:534
  16.7 9.0 %collective-permute-start.8 = (bf16[512,256]{1,0:T(8,128)(2,1)S(1)}, bf16[512,256]{1,0:T(8,128)(2,1)S(1)}, u32[]{:S(2)}, u32[]{:S(2)}) collective-permute-start(bf16[512,256]{1,0:T(8,128)(2,1)S(1)} %get-tuple-element.55), channel_id=1, source_target_pairs={{0,2},{1,3},{2,0},{3,1},{4,6},{5,7},{6,4},{7,5},{8,10},{9,11},{10,... | collective-permute-start | bytes 786440 | tf_op jit(solution)/shard_map/ppermute | solution.py:539
  18.3 16.4 %copy-start.3 = (bf16[256,512]{1,0:T(8,128)(2,1)S(1)}, bf16[256,512]{1,0:T(8,128)(2,1)}, u32[]{:S(2)}) copy-start(bf16[256,512]{1,0:T(8,128)(2,1)} %refs_2_.8) | copy-start | bytes 786436
  23.9 5.3 %collective-permute-start.6 = (bf16[256,256]{1,0:T(8,128)(2,1)S(1)}, bf16[256,256]{1,0:T(8,128)(2,1)S(1)}, u32[]{:S(2)}, u32[]{:S(2)}) collective-permute-start(bf16[256,256]{1,0:T(8,128)(2,1)S(1)} %attend_halo.3.own_ref.refs_0_), channel_id=1, source_target_pairs={{0,2},{1,3},{2,0},{3,1},{4,6},{5,7},{6,4},{7,5},{8,10},{9,11},{10,... | collective-permute-start | bytes 393224 | tf_op jit(solution)/shard_map/ppermute | solution.py:539
  24.2 7.3 %collective-permute-start.9 = (bf16[512,128]{1,0:T(8,128)(2,1)S(1)}, bf16[512,128]{1,0:T(8,128)(2,1)S(1)}, u32[]{:S(2)}, u32[]{:S(2)}) collective-permute-start(bf16[512,128]{1,0:T(8,128)(2,1)S(1)} %get-tuple-element.56), channel_id=1, source_target_pairs={{0,2},{1,3},{2,0},{3,1},{4,6},{5,7},{6,4},{7,5},{8,10},{9,11},{10,... | collective-permute-start | bytes 393224 | tf_op jit(solution)/shard_map/ppermute | solution.py:539
  25.4 8.1 %collective-permute-start.10 = (bf16[512,128]{1,0:T(8,128)(2,1)S(1)}, bf16[512,128]{1,0:T(8,128)(2,1)S(1)}, u32[]{:S(2)}, u32[]{:S(2)}) collective-permute-start(bf16[512,128]{1,0:T(8,128)(2,1)S(1)} %get-tuple-element.57), channel_id=1, source_target_pairs={{0,2},{1,3},{2,0},{3,1},{4,6},{5,7},{6,4},{7,5},{8,10},{9,11},{10,... | collective-permute-start | bytes 393224 | tf_op jit(solution)/shard_map/ppermute | solution.py:539
  25.7 13.6 %collective-permute-start.11 = (bf16[512,256]{1,0:T(8,128)(2,1)S(1)}, bf16[512,256]{1,0:T(8,128)(2,1)S(1)}, u32[]{:S(2)}, u32[]{:S(2)}) collective-permute-start(bf16[512,256]{1,0:T(8,128)(2,1)S(1)} %collective-permute-done.8.refs_0_), channel_id=1, source_target_pairs={{0,16},{16,0},{1,17},{17,1},{2,18},{18,2},{3,19},{19,3},{4,20},{20... | collective-permute-start | bytes 786440 | tf_op jit(solution)/shard_map/ppermute | solution.py:539
  26.9 9.3 %collective-permute-start.5 = (bf16[256,256]{1,0:T(8,128)(2,1)S(1)}, bf16[256,256]{1,0:T(8,128)(2,1)S(1)}, u32[]{:S(2)}, u32[]{:S(2)}) collective-permute-start(bf16[256,256]{1,0:T(8,128)(2,1)S(1)} %attend_halo.3.own_ref.refs_0_), channel_id=1, source_target_pairs={{0,1},{1,0},{2,3},{3,2},{4,5},{5,4},{6,7},{7,6},{8,9},{9,8},{10,11... | collective-permute-start | bytes 393224 | tf_op jit(solution)/shard_map/ppermute | solution.py:539
  29.2 7.5 %collective-permute-start.7 = (bf16[256,256]{1,0:T(8,128)(2,1)S(1)}, bf16[256,256]{1,0:T(8,128)(2,1)S(1)}, u32[]{:S(2)}, u32[]{:S(2)}) collective-permute-start(bf16[256,256]{1,0:T(8,128)(2,1)S(1)} %collective-permute-done.6.across_ref.refs_0_), channel_id=1, source_target_pairs={{0,1},{1,0},{2,3},{3,2},{4,5},{5,4},{6,7},{7,6},{8,9},{9,8},{10,11... | collective-permute-start | bytes 393224 | tf_op jit(solution)/shard_map/ppermute | solution.py:539
  31.5 7.8 %collective-permute-start.12 = (bf16[512,128]{1,0:T(8,128)(2,1)S(1)}, bf16[512,128]{1,0:T(8,128)(2,1)S(1)}, u32[]{:S(2)}, u32[]{:S(2)}) collective-permute-start(bf16[512,128]{1,0:T(8,128)(2,1)S(1)} %collective-permute-done.9.refs_1_), channel_id=1, source_target_pairs={{0,16},{16,0},{1,17},{17,1},{2,18},{18,2},{3,19},{19,3},{4,20},{20... | collective-permute-start | bytes 393224 | tf_op jit(solution)/shard_map/ppermute | solution.py:539
  33.5 5.8 %collective-permute-start.13 = (bf16[512,128]{1,0:T(8,128)(2,1)S(1)}, bf16[512,128]{1,0:T(8,128)(2,1)S(1)}, u32[]{:S(2)}, u32[]{:S(2)}) collective-permute-start(bf16[512,128]{1,0:T(8,128)(2,1)S(1)} %collective-permute-done.10.refs_2_), channel_id=1, source_target_pairs={{0,16},{16,0},{1,17},{17,1},{2,18},{18,2},{3,19},{19,3},{4,20},{20... | collective-permute-start | bytes 393224 | tf_op jit(solution)/shard_map/ppermute | solution.py:539
  36.9 7.1 %collective-permute-start.15 = (bf16[256,512]{1,0:T(8,128)(2,1)S(1)}, bf16[256,512]{1,0:T(8,128)(2,1)S(1)}, u32[]{:S(2)}, u32[]{:S(2)}) collective-permute-start(bf16[256,512]{1,0:T(8,128)(2,1)S(1)} %shard_map.83.refs_0_.refs_2_), channel_id=1, source_target_pairs={{0,1},{1,0},{2,3},{3,2},{4,5},{5,4},{6,7},{7,6},{8,9},{9,8},{10,11... | collective-permute-start | bytes 786440 | tf_op jit(solution)/shard_map/ppermute | solution.py:539
  39.9 4.6 %collective-permute-start.14 = (bf16[256,512]{1,0:T(8,128)(2,1)S(1)}, bf16[256,512]{1,0:T(8,128)(2,1)S(1)}, u32[]{:S(2)}, u32[]{:S(2)}) collective-permute-start(bf16[256,512]{1,0:T(8,128)(2,1)S(1)} %lent.2.refs_1_.base_ref), channel_id=1, source_target_pairs={{0,1},{1,0},{2,3},{3,2},{4,5},{5,4},{6,7},{7,6},{8,9},{9,8},{10,11... | collective-permute-start | bytes 786440 | tf_op jit(solution)/shard_map/ppermute | solution.py:539
  44.9 7.9 %collective-permute-start.16 = (bf16[2,256,256]{2,1,0:T(8,128)(2,1)S(1)}, bf16[2,256,256]{2,1,0:T(8,128)(2,1)S(1)}, u32[]{:S(2)}, u32[]{:S(2)}) collective-permute-start(bf16[2,256,256]{2,1,0:T(8,128)(2,1)S(1)} %shard_map.87.pair_ref), channel_id=1, source_target_pairs={{0,4},{1,5},{2,6},{3,7},{4,0},{5,1},{6,2},{7,3},{8,12},{9,13},{10,... | collective-permute-start | bytes 786440 | tf_op jit(solution)/shard_map/ppermute | solution.py:534
  45.5 7.6 %collective-permute-start.17 = (bf16[2,256,256]{2,1,0:T(8,128)(2,1)S(1)}, bf16[2,256,256]{2,1,0:T(8,128)(2,1)S(1)}, u32[]{:S(2)}, u32[]{:S(2)}) collective-permute-start(bf16[2,256,256]{2,1,0:T(8,128)(2,1)S(1)} %shard_map.87.pair_ref), channel_id=1, source_target_pairs={{0,1},{1,0},{2,3},{3,2},{4,8},{5,9},{6,10},{7,11},{8,4},{9,5},{10,... | collective-permute-start | bytes 786440 | tf_op jit(solution)/shard_map/ppermute | solution.py:534
  46.7 8.8 %collective-permute-start.21 = (bf16[512,256]{1,0:T(8,128)(2,1)S(1)}, bf16[512,256]{1,0:T(8,128)(2,1)S(1)}, u32[]{:S(2)}, u32[]{:S(2)}) collective-permute-start(bf16[512,256]{1,0:T(8,128)(2,1)S(1)} %get-tuple-element.68), channel_id=1, source_target_pairs={{0,2},{1,3},{2,0},{3,1},{4,6},{5,7},{6,4},{7,5},{8,10},{9,11},{10,... | collective-permute-start | bytes 786440 | tf_op jit(solution)/shard_map/ppermute | solution.py:539
  53.8 5.3 %collective-permute-start.19 = (bf16[256,256]{1,0:T(8,128)(2,1)S(1)}, bf16[256,256]{1,0:T(8,128)(2,1)S(1)}, u32[]{:S(2)}, u32[]{:S(2)}) collective-permute-start(bf16[256,256]{1,0:T(8,128)(2,1)S(1)} %attend_halo.4.own_ref.refs_0_), channel_id=1, source_target_pairs={{0,2},{1,3},{2,0},{3,1},{4,6},{5,7},{6,4},{7,5},{8,10},{9,11},{10,... | collective-permute-start | bytes 393224 | tf_op jit(solution)/shard_map/ppermute | solution.py:539
  54.0 7.3 %collective-permute-start.22 = (bf16[512,128]{1,0:T(8,128)(2,1)S(1)}, bf16[512,128]{1,0:T(8,128)(2,1)S(1)}, u32[]{:S(2)}, u32[]{:S(2)}) collective-permute-start(bf16[512,128]{1,0:T(8,128)(2,1)S(1)} %get-tuple-element.69), channel_id=1, source_target_pairs={{0,2},{1,3},{2,0},{3,1},{4,6},{5,7},{6,4},{7,5},{8,10},{9,11},{10,... | collective-permute-start | bytes 393224 | tf_op jit(solution)/shard_map/ppermute | solution.py:539
  55.3 8.1 %collective-permute-start.23 = (bf16[512,128]{1,0:T(8,128)(2,1)S(1)}, bf16[512,128]{1,0:T(8,128)(2,1)S(1)}, u32[]{:S(2)}, u32[]{:S(2)}) collective-permute-start(bf16[512,128]{1,0:T(8,128)(2,1)S(1)} %get-tuple-element.70), channel_id=1, source_target_pairs={{0,2},{1,3},{2,0},{3,1},{4,6},{5,7},{6,4},{7,5},{8,10},{9,11},{10,... | collective-permute-start | bytes 393224 | tf_op jit(solution)/shard_map/ppermute | solution.py:539
  55.5 13.6 %collective-permute-start.24 = (bf16[512,256]{1,0:T(8,128)(2,1)S(1)}, bf16[512,256]{1,0:T(8,128)(2,1)S(1)}, u32[]{:S(2)}, u32[]{:S(2)}) collective-permute-start(bf16[512,256]{1,0:T(8,128)(2,1)S(1)} %collective-permute-done.21.refs_0_), channel_id=1, source_target_pairs={{0,16},{16,0},{1,17},{17,1},{2,18},{18,2},{3,19},{19,3},{4,20},{20... | collective-permute-start | bytes 786440 | tf_op jit(solution)/shard_map/ppermute | solution.py:539
  56.7 9.3 %collective-permute-start.18 = (bf16[256,256]{1,0:T(8,128)(2,1)S(1)}, bf16[256,256]{1,0:T(8,128)(2,1)S(1)}, u32[]{:S(2)}, u32[]{:S(2)}) collective-permute-start(bf16[256,256]{1,0:T(8,128)(2,1)S(1)} %attend_halo.4.own_ref.refs_0_), channel_id=1, source_target_pairs={{0,1},{1,0},{2,3},{3,2},{4,5},{5,4},{6,7},{7,6},{8,9},{9,8},{10,11... | collective-permute-start | bytes 393224 | tf_op jit(solution)/shard_map/ppermute | solution.py:539
  59.0 7.5 %collective-permute-start.20 = (bf16[256,256]{1,0:T(8,128)(2,1)S(1)}, bf16[256,256]{1,0:T(8,128)(2,1)S(1)}, u32[]{:S(2)}, u32[]{:S(2)}) collective-permute-start(bf16[256,256]{1,0:T(8,128)(2,1)S(1)} %collective-permute-done.19.across_ref.refs_0_), channel_id=1, source_target_pairs={{0,1},{1,0},{2,3},{3,2},{4,5},{5,4},{6,7},{7,6},{8,9},{9,8},{10,11... | collective-permute-start | bytes 393224 | tf_op jit(solution)/shard_map/ppermute | solution.py:539
  61.3 7.8 %collective-permute-start.25 = (bf16[512,128]{1,0:T(8,128)(2,1)S(1)}, bf16[512,128]{1,0:T(8,128)(2,1)S(1)}, u32[]{:S(2)}, u32[]{:S(2)}) collective-permute-start(bf16[512,128]{1,0:T(8,128)(2,1)S(1)} %collective-permute-done.22.refs_1_), channel_id=1, source_target_pairs={{0,16},{16,0},{1,17},{17,1},{2,18},{18,2},{3,19},{19,3},{4,20},{20... | collective-permute-start | bytes 393224 | tf_op jit(solution)/shard_map/ppermute | solution.py:539
  63.3 5.8 %collective-permute-start.26 = (bf16[512,128]{1,0:T(8,128)(2,1)S(1)}, bf16[512,128]{1,0:T(8,128)(2,1)S(1)}, u32[]{:S(2)}, u32[]{:S(2)}) collective-permute-start(bf16[512,128]{1,0:T(8,128)(2,1)S(1)} %collective-permute-done.23.refs_2_), channel_id=1, source_target_pairs={{0,16},{16,0},{1,17},{17,1},{2,18},{18,2},{3,19},{19,3},{4,20},{20... | collective-permute-start | bytes 393224 | tf_op jit(solution)/shard_map/ppermute | solution.py:539
  66.7 7.1 %collective-permute-start.28 = (bf16[256,512]{1,0:T(8,128)(2,1)S(1)}, bf16[256,512]{1,0:T(8,128)(2,1)S(1)}, u32[]{:S(2)}, u32[]{:S(2)}) collective-permute-start(bf16[256,512]{1,0:T(8,128)(2,1)S(1)} %shard_map.93.refs_0_.refs_2_), channel_id=1, source_target_pairs={{0,1},{1,0},{2,3},{3,2},{4,5},{5,4},{6,7},{7,6},{8,9},{9,8},{10,11... | collective-permute-start | bytes 786440 | tf_op jit(solution)/shard_map/ppermute | solution.py:539
  69.7 4.8 %collective-permute-start.27 = (bf16[256,512]{1,0:T(8,128)(2,1)S(1)}, bf16[256,512]{1,0:T(8,128)(2,1)S(1)}, u32[]{:S(2)}, u32[]{:S(2)}) collective-permute-start(bf16[256,512]{1,0:T(8,128)(2,1)S(1)} %lent.3.refs_1_), channel_id=1, source_target_pairs={{0,1},{1,0},{2,3},{3,2},{4,5},{5,4},{6,7},{7,6},{8,9},{9,8},{10,11... | collective-permute-start | bytes 786440 | tf_op jit(solution)/shard_map/ppermute | solution.py:539
  74.8 7.9 %collective-permute-start.29 = (bf16[2,256,256]{2,1,0:T(8,128)(2,1)S(1)}, bf16[2,256,256]{2,1,0:T(8,128)(2,1)S(1)}, u32[]{:S(2)}, u32[]{:S(2)}) collective-permute-start(bf16[2,256,256]{2,1,0:T(8,128)(2,1)S(1)} %shard_map.97.pair_ref), channel_id=1, source_target_pairs={{0,4},{1,5},{2,6},{3,7},{4,0},{5,1},{6,2},{7,3},{8,12},{9,13},{10,... | collective-permute-start | bytes 786440 | tf_op jit(solution)/shard_map/ppermute | solution.py:534
  75.5 7.6 %collective-permute-start.30 = (bf16[2,256,256]{2,1,0:T(8,128)(2,1)S(1)}, bf16[2,256,256]{2,1,0:T(8,128)(2,1)S(1)}, u32[]{:S(2)}, u32[]{:S(2)}) collective-permute-start(bf16[2,256,256]{2,1,0:T(8,128)(2,1)S(1)} %shard_map.97.pair_ref), channel_id=1, source_target_pairs={{0,1},{1,0},{2,3},{3,2},{4,8},{5,9},{6,10},{7,11},{8,4},{9,5},{10,... | collective-permute-start | bytes 786440 | tf_op jit(solution)/shard_map/ppermute | solution.py:534
  83.7 3.9 %collective-permute-start.31 = (bf16[256,256]{1,0:T(8,128)(2,1)S(1)}, bf16[256,256]{1,0:T(8,128)(2,1)S(1)}, u32[]{:S(2)}, u32[]{:S(2)}) collective-permute-start(bf16[256,256]{1,0:T(8,128)(2,1)S(1)} %attend_halo.5.refs_0_), channel_id=1, source_target_pairs={{0,2},{1,3},{2,0},{3,1},{4,6},{5,7},{6,4},{7,5},{8,10},{9,11},{10,... | collective-permute-start | bytes 393224 | tf_op jit(solution)/shard_map/ppermute | solution.py:539
  84.0 7.4 %collective-permute-start.33 = (bf16[256,256]{1,0:T(8,128)(2,1)S(1)}, bf16[256,256]{1,0:T(8,128)(2,1)S(1)}, u32[]{:S(2)}, u32[]{:S(2)}) collective-permute-start(bf16[256,256]{1,0:T(8,128)(2,1)S(1)} %attend_halo.5.refs_0_), channel_id=1, source_target_pairs={{0,1},{1,0},{2,3},{3,2},{4,5},{5,4},{6,7},{7,6},{8,9},{9,8},{10,11... | collective-permute-start | bytes 393224 | tf_op jit(solution)/shard_map/ppermute | solution.py:539
  87.6 4.3 %collective-permute-start.32 = (bf16[256,256]{1,0:T(8,128)(2,1)S(1)}, bf16[256,256]{1,0:T(8,128)(2,1)S(1)}, u32[]{:S(2)}, u32[]{:S(2)}) collective-permute-start(bf16[256,256]{1,0:T(8,128)(2,1)S(1)} %collective-permute-done.31.refs_0_), channel_id=1, source_target_pairs={{0,1},{1,0},{2,3},{3,2},{4,5},{5,4},{6,7},{7,6},{8,9},{9,8},{10,11... | collective-permute-start | bytes 393224 | tf_op jit(solution)/shard_map/ppermute | solution.py:539

commit v4 on v3

--- a/solution.py
+++ b/solution.py
@@ -14,6 +14,7 @@
 COL_SPAN = 16
 LAYERS = 3
 HALF = ROW_SPAN // 2
+PARTS = ((1, 2, 1), (2, 2))
 
 EPS = 1e-06
 NEG = -1e30
@@ -44,6 +45,37 @@
     )
 
 
+def call(kernel, operands, in_specs, out_shape, estimate, scratch=(), rider=None):
+    taken, given = len(operands), len(out_shape)
+    arrays, shapes, pick, count = rider or ((), (), None, 0)
+
+    def carrying(*refs):
+        ends = taken, taken + len(arrays), taken + len(arrays) + given
+        last = ends[2] + len(shapes)
+        copies = [
+            pltpu.make_async_copy(source, target, refs[-1].at[at])
+            for at, (source, target) in enumerate(
+                pick(refs[ends[0] : ends[1]], refs[ends[2] : last])
+            )
+        ]
+        for copy in copies:
+            copy.start()
+        kernel(*refs[: ends[0]], *refs[ends[1] : ends[2]], *refs[last:-1])
+        for copy in copies:
+            copy.wait()
+
+    sems = [pltpu.SemaphoreType.DMA((count,))] if rider else []
+    return pl.pallas_call(
+        carrying if rider else kernel,
+        out_shape=[*out_shape, *(pltpu.VMEM(shape, BF16) for shape in shapes)],
+        in_specs=[*in_specs, *[HBM] * len(arrays)],
+        out_specs=[VMEM] * (given + len(shapes)),
+        scratch_shapes=[*scratch, *sems],
+        cost_estimate=estimate,
+        compiler_params=PARAMS,
+    )(*operands, *arrays)
+
+
 def block_at(bit, width, unit):
     if bit is None:
         return slice(None)
@@ -64,7 +96,7 @@
     )
 
 
-def project_kernel(bits, load, first, kinds, layer, *refs):
+def project_kernel(bits, load, shared, first, kinds, layer, *refs):
     sources, refs = refs[: len(bits)], refs[len(bits) :]
     gain_ref, refs = refs[0], refs[1:]
     if load:
@@ -76,6 +108,8 @@
         ]
         for copy in copies:
             copy.start()
+    elif shared:
+        stored, refs = refs[:3], refs[3:]
     else:
         held_ref, refs = refs[0], refs[1:]
     if not first:
@@ -93,7 +127,8 @@
         for kind in kinds or range(3):
             if load and at == 0:
                 copies[kind].wait()
-            product = nt_dot(scaled, held_ref[kind, :, cols])
+            held = stored[kind][layer, :, cols] if shared else held_ref[kind, :, cols]
+            product = nt_dot(scaled, held)
             totals[kind] = product if totals[kind] is None else totals[kind] + product
     if not first:
         squares = squares + sq_in[:, :1]
@@ -117,11 +152,15 @@
     first = carried is None
     operands = [*parts, gain]
     specs = [VMEM] * (parts_n + 1)
-    load = isinstance(weights, list)
+    load, shared = isinstance(weights, list), isinstance(weights, tuple)
     if load:
         _, channels, full = weights[0].shape
         operands += weights
         specs += [HBM] * 3
+    elif shared:
+        _, channels, full = weights[0].shape
+        operands += weights
+        specs += [VMEM] * 3
     else:
         _, channels, full = weights.shape
         operands.append(in_vmem(weights))
@@ -138,105 +177,74 @@
         out_shape.append(pltpu.VMEM((3, channels, full), BF16))
         scratch.append(pltpu.SemaphoreType.DMA((3,)))
     flops = 2 * tok * width * channels * len(kinds or range(3)) * parts_n
-    return pl.pallas_call(
-        partial(project_kernel, bits, load, first, kinds, layer),
-        out_shape=out_shape,
-        in_specs=specs,
-        out_specs=[VMEM] * len(out_shape),
-        scratch_shapes=scratch,
-        cost_estimate=cost(flops, parts_n * width * (channels * 6 + tok * 2) + 4 * tok * channels),
-        compiler_params=PARAMS,
-    )(*operands)
-
-
-def emit_kernel(bits, first, layer, *refs):
+    return call(
+        partial(project_kernel, bits, load, shared, first, kinds, layer),
+        operands,
+        specs,
+        out_shape,
+        cost(flops, parts_n * width * (channels * 6 + tok * 2) + 4 * tok * channels),
+        scratch,
+    )
+
+
+def emit_kernel(bits, load, layer, *refs):
     sources, refs = refs[: len(bits)], refs[len(bits) :]
-    if first:
-        stored_ref, base_ref, out_ref, held_ref, sem = refs
+    held_ref, base_ref, out_ref, *rest = refs
+    if load:
+        stored_ref, (held_ref, sem) = held_ref, rest
         copy = pltpu.make_async_copy(stored_ref.at[layer], held_ref, sem)
         copy.start()
-    else:
-        held_ref, base_ref, out_ref = refs
     total = base_ref[...].astype(F32)
-    if first:
+    if load:
         copy.wait()
     for at, bit in enumerate(bits):
         rows = block_at(bit, sources[at].shape[1], HEAD_DIM)
-        total = total + jnp.dot(sources[at][...], held_ref[rows, :], preferred_element_type=F32)
+        held = held_ref[rows, :] if load else held_ref[layer, rows, :]
+        total = total + jnp.dot(sources[at][...], held, preferred_element_type=F32)
     out_ref[...] = total.astype(out_ref.dtype)
 
 
-def emit(parts, bits, weight, base, out_type, first, layer):
+def emit(parts, bits, weight, base, out_type, load, layer):
     tok, width = parts[0].shape
     cols = base.shape[1]
-    parts_n = len(parts)
     out_shape = [pltpu.VMEM((tok, cols), out_type)]
     if out_type == BF16 and layer == LAYERS - 1:
         out_shape = [jax.ShapeDtypeStruct((tok, cols), out_type)]
     scratch = []
-    if first:
-        out_shape.append(pltpu.VMEM(weight.shape[1:], BF16))
-        scratch.append(pltpu.SemaphoreType.DMA)
-    return pl.pallas_call(
-        partial(emit_kernel, bits, first, layer),
-        out_shape=out_shape,
-        in_specs=[VMEM] * parts_n + [HBM if first else VMEM, VMEM],
-        out_specs=[VMEM] * len(out_shape),
-        scratch_shapes=scratch,
-        cost_estimate=cost(
-            2 * tok * width * cols * parts_n, parts_n * width * (cols + tok) * 2 + tok * cols * 6
-        ),
-        compiler_params=PARAMS,
-    )(*parts, weight if first else in_vmem(weight), base if first else in_vmem(base))
-
-
-def fetch_kernel(pick, count, *refs):
-    sources, targets, sems = refs[:count], refs[count:-1], refs[-1]
-    copies = [
-        pltpu.make_async_copy(source, target, sems.at[at])
-        for at, (source, target) in enumerate(pick(sources, targets))
-    ]
-    for copy in copies:
-        copy.start()
-    for copy in copies:
-        copy.wait()
-
-
-def fetch(arrays, shapes, pick, copies):
-    return pl.pallas_call(
-        partial(fetch_kernel, pick, len(arrays)),
-        out_shape=[pltpu.VMEM(shape, BF16) for shape in shapes],
-        in_specs=[HBM] * len(arrays),
-        out_specs=[VMEM] * len(shapes),
-        scratch_shapes=[pltpu.SemaphoreType.DMA((copies,))],
-        cost_estimate=cost(10**6, 10**6),
-        compiler_params=PARAMS,
-    )(*arrays)
-
-
-def load_weights(weights, layer):
-    _, channels, full = weights[0].shape
-
-    def pick(sources, targets):
-        return [(source.at[layer], targets[0].at[kind]) for kind, source in enumerate(sources)]
-
-    return fetch(weights, [(3, channels, full)], pick, 3)[0]
-
-
-def cut_weight(weight, layer):
+    if load:
+        scratch = [pltpu.VMEM(weight.shape[1:], BF16), pltpu.SemaphoreType.DMA]
+    return call(
+        partial(emit_kernel, bits, load, layer),
+        [*parts, weight, base],
+        [VMEM] * len(parts) + [HBM if load else VMEM, VMEM],
+        out_shape,
+        cost(2 * tok * width * cols * len(bits), 10**6),
+        scratch,
+    )
+
+
+def cut_weight(weight):
     _, rows, cols = weight.shape
     half = rows // 2
-    widths = (cols // 2, cols // 4, cols // 4)
+    slabs = []
+    for layer, parts in enumerate(PARTS):
+        unit = cols // sum(parts)
+        for at, part in enumerate(parts):
+            slabs.append((layer, unit * sum(parts[:at]), unit * part))
 
     def pick(sources, targets):
         here = pl.ds(pl.multiple_of(lax.axis_index("grp") * half, half), half)
-        firsts = (0, cols // 2, 3 * cols // 4)
         return [
             (sources[0].at[layer, here, pl.ds(first, width)], target)
-            for first, width, target in zip(firsts, widths, targets)
+            for (layer, first, width), target in zip(slabs, targets)
         ]
 
-    return fetch([weight], [(half, width) for width in widths], pick, 3)
+    shapes = [(half, width) for _, _, width in slabs]
+    rider = [weight], shapes, pick, len(slabs)
+    cuts = call(lambda *refs: None, [], [], [], cost(10**6, 10**6), rider=rider)
+    return [
+        [cut for cut, slab in zip(cuts, slabs) if slab[0] == layer] for layer in range(len(PARTS))
+    ]
 
 
 def far_kernel(pieces, own_ref, beside_ref, across_ref, corner_ref, base_ref, *refs):
@@ -315,16 +323,14 @@
     out_shape = [pltpu.VMEM((heads_n, spans, GRID_W, LANES), F32)]
     if halo_rows:
         out_shape.append(pltpu.VMEM((halo_rows, heads_n, HALF // 2, GRID_W, LANES), F32))
-    return pl.pallas_call(
+    return call(
         partial(bias_kernel, layer, lax.axis_size("sp")),
-        out_shape=out_shape,
-        in_specs=[VMEM],
-        out_specs=[VMEM] * len(out_shape),
-        scratch_shapes=[pltpu.VMEM((heads_n, 2 * ROW_SPAN, LANES), F32)],
-        cost_estimate=cost(heads_n * spans * GRID_W * LANES * 40, heads_n * spans * GRID_W * LANES * 4),
-        compiler_params=PARAMS,
-        name="expand_bias",
-    )(table)
+        [table],
+        [VMEM],
+        out_shape,
+        cost(heads_n * spans * GRID_W * LANES * 40, heads_n * spans * GRID_W * LANES * 4),
+        [pltpu.VMEM((heads_n, 2 * ROW_SPAN, LANES), F32)],
+    )
 
 
 def stacked_query(query, lane, heads_in):
@@ -377,18 +383,16 @@
     _, tok, channels = query.shape
     group = min(LANES, channels)
     pairs, rows = channels // group, tok * (group // HEAD_DIM)
-    return pl.pallas_call(
+    return call(
         partial(own_kernel, rows_dev),
-        out_shape=[
+        [*map(in_vmem, (query, pair, bias))],
+        [VMEM] * 3,
+        [
             pltpu.VMEM((pairs, rows, group + LANES), F32),
             pltpu.VMEM((pairs, rows, LANES), F32),
         ],
-        in_specs=[VMEM] * 3,
-        out_specs=[VMEM] * 2,
-        cost_estimate=cost(pairs * rows * tok * 800, bias.size * 4, pairs * rows * tok),
-        compiler_params=PARAMS,
-        name="attend_own",
-    )(*map(in_vmem, (query, pair, bias)))
+        cost(pairs * rows * tok * 800, bias.size * 4, pairs * rows * tok),
+    )
 
 
 def halo_kernel(
@@ -449,7 +453,7 @@
         scratch_shapes=[pltpu.VMEM((ROW_SPAN * GRID_W, channels), BF16)] * 2,
         cost_estimate=cost(scores * HEAD_DIM * 6, bias.size * 4 + tok * channels * 16, scores),
         compiler_params=PARAMS,
-        name="attend_halo",
+        name="halo",
     )(*map(in_vmem, (query, even, odd, bias, mixed, peak)))
 
 
@@ -539,14 +543,6 @@
     return lax.ppermute(block, axis, [(at, at ^ bit) for at in range(count)])
 
 
-def send_weight(weight, layer):
-    cuts = cut_weight(weight, layer)
-    near = []
-    for cut in cuts:
-        near.append(flip(cut, "tp", 2))
-    return near
-
-
 def body(hidden_in, norm_gain, query_weight, key_weight, value_weight, output_weight, offset_bias):
     tok_dev, _ = hidden_in.shape
     rows_dev = tok_dev // GRID_W
@@ -555,18 +551,24 @@
     is_odd = lax.axis_index("sp") % 2
     split = rows_dev == HALF
     weights = [in_hbm(weight) for weight in (query_weight, key_weight, value_weight)]
-    output_weight = in_hbm(output_weight)
     even_pairs = [(at, at + 1) for at in range(0, sp - 1, 2)]
     odd_pairs = [(at, at + 1) for at in range(1, sp - 1, 2)]
     stream = hidden_in
-    lend = split and tp == 4 and lax.axis_size("grp") == 2
-    carry = None
+    lend = split and tp == 4 and lax.axis_size("grp") == 2 and len(PARTS) == LAYERS - 1
+    lent = None
+    near = {}
+    shared = query_weight, key_weight, value_weight
+
+    def send(cuts, layer, first, end):
+        for at in range(first, end):
+            near.setdefault(layer, []).append(flip(cuts[layer][at], "tp", 2))
+
     for layer in range(LAYERS):
         step = partial(project, layer=layer, gain=norm_gain)
-        if carry is not None:
+        if lent:
             parts, base, held = carry
             beside = flip(stream, "tp", 1)
-            across = emit_far(parts, base, *last_lent)
+            across = emit_far(parts, base, near[layer - 1], side)
             corner = flip(across, "tp", 1)
             carried = step([stream, across], (0, 2), held, None, None)
             carried = step([beside], (1,), held, carried, None)
@@ -576,24 +578,18 @@
             corner = flip(across, "tp", 1)
             *carried, held = step([stream], (0,), weights, None, None)
             carried = step([beside], (1,), held, carried, None)
+            if lend:
+                cuts = cut_weight(in_hbm(output_weight))
+                send(cuts, layer, 0, len(cuts[layer]))
             carried = step([across], (2,), held, carried, None)
         if tp == 4:
-            across_stream = across
+            old = across
             (pair,) = step([corner], (3,), held, carried, (1, 2))
-            (query,) = step([corner], (3,), held, carried, (0,))
+            (query,) = step([corner], (3,), shared if lend else held, carried, (0,))
         else:
             gathered = lax.all_gather(stream, "tp", axis=1, tiled=True)
             *carried, held = step([gathered], (None,), weights, None, (0, 1, 2))
             query, pair = carried[0][:1], carried[0][1:]
-        if lend and layer < LAYERS - 1:
-            if layer == 0:
-                near = send_weight(output_weight, layer)
-            side = []
-            for piece in near:
-                side.append(flip(piece, "grp", 1))
-            lent = (near, side)
-        else:
-            lent = None
         if split:
             to_even = to_odd = pair
         else:
@@ -602,7 +598,13 @@
             to_odd = jnp.where(is_odd == 0, low, top)
         even = exchange(to_even, even_pairs)
         odd = exchange(to_odd, odd_pairs)
+        lent = lend and layer < LAYERS - 1
+        more = lend and layer < LAYERS - 2
         bias, *halo_bias = expand_bias(offset_bias, layer, rows_dev if split else 0)
+        if lent:
+            side = []
+            for piece in near[layer]:
+                side.append(flip(piece, "grp", 1))
         if split:
             mixed, peak = attend_own(query, pair, bias, rows_dev)
             attended = attend_halo(
@@ -611,26 +613,21 @@
         else:
             attended = attend(query, pair, even, odd, bias, rows_dev)
         step = partial(emit, layer=layer)
-        carry = None
-        if lent:
-            last_lent = lent
-            carry = load_weights(weights, layer + 1)
         if tp == 4:
             across = flip(attended, "tp", 2)
             beside = flip(attended, "tp", 1)
             corner = flip(across, "tp", 1)
-            if lent and layer + 1 < LAYERS - 1:
-                near = send_weight(output_weight, layer + 1)
-            partly, held = step([attended], (0,), output_weight, stream, F32, True)
-            (partly,) = step([beside], (1,), held, partly, F32, False)
-            (partly,) = step([across], (2,), held, partly, F32, False)
-            old = across_stream
-            (stream,) = step([corner], (3,), held, partly, BF16, False)
-            if carry is not None:
-                carry = ([attended, beside, across, corner], old, carry)
+            (partly,) = step([attended], (0,), output_weight, stream, F32, False)
+            (partly,) = step([beside], (1,), output_weight, partly, F32, False)
+            (partly,) = step([across], (2,), output_weight, partly, F32, False)
+            if more:
+                send(cuts, layer + 1, 0, len(cuts[layer + 1]))
+            (stream,) = step([corner], (3,), output_weight, partly, BF16, False)
+            if lent:
+                carry = ([attended, beside, across, corner], old, shared)
         else:
             gathered = lax.all_gather(attended, "tp", axis=1, tiled=True)
-            stream, _ = step([gathered], (None,), output_weight, stream, BF16, True)
+            (stream,) = step([gathered], (None,), in_hbm(output_weight), stream, BF16, True)
     return stream
 
 

time: 94.3 us -> 87.5 us (0.928)
  Pallas kernels: 28.6 us -> 20.4 us
  waiting for transfers between devices: 23.6 us -> 25.8 us
  starting transfers between devices: 38.5 us -> 37.5 us
    pallas_call x35 -> x32, Pallas kernels: 25.3 us -> 17.3 us  [call(): pl.pallas_call(carrying if rider else kernel, out_shape=[*out_shape, *(pl...]
    ppermute x28 -> x26, waiting for transfers between devices: 9.98 us -> 13.8 us  [flip(): return lax.ppermute(block, axis, [(at, at ^ bit) for at in range(count)])]
    ppermute x28 -> x26, starting transfers between devices: 35.3 us -> 33.6 us  [flip(): return lax.ppermute(block, axis, [(at, at ^ bit) for at in range(count)])]
    ppermute x6, waiting for transfers between devices: 13.6 us -> 12 us  [exchange(): return lax.ppermute(block, ('sp', 'tp'), moves)]
  transfers between devices with their start and end apart: 34 -> 32, of which waited for: 10 -> 13; matrix products, arithmetic and copies ran while one was open for 0% -> 0% of each run, Pallas kernels for 28% -> 21%
where the time goes in v4:
time: 87.5 us; the launch traced here: 85.9 us
  starting transfers between devices  37.5 us (43%)
  waiting for transfers between devices  25.8 us (29%)
  Pallas kernels  20.4 us (23%)
  local copies, waits for them, and re-layouts  1.76 us (2%)
    ppermute x26, starting transfers between devices, flip(): return lax.ppermute(block, axis, [(at, at ^ bit) for at in range(count)])  33.6 us
    pallas_call x32, Pallas kernels, call(): pl.pallas_call(carrying if rider else kernel, out_shape=[*out_shape, *(pl...  17.3 us
    ppermute x26, waiting for transfers between devices, flip(): return lax.ppermute(block, axis, [(at, at ^ bit) for at in range(count)])  13.8 us
    ppermute x6, waiting for transfers between devices, exchange(): return lax.ppermute(block, ('sp', 'tp'), moves)  12 us
    ppermute x6, starting transfers between devices, exchange(): return lax.ppermute(block, ('sp', 'tp'), moves)  3.9 us
    pallas_call x3, Pallas kernels, attend_halo(): pl.pallas_call(partial(halo_kernel, rows_dev, lax.axis_size('sp')), out_s...  2.07 us
    unnamed x19, local copies, waits for them, and re-layouts  1.76 us
  transfers between devices with their start and end apart: 32, of which 13 were waited for; matrix products, arithmetic and copies ran while one was open for 0% of the time, Pallas kernels for 21%

profile of v4, /device:TPU:19, one launch (start us, length us, event | category | flops | bytes accessed | tf_op | source)
XLA Modules:
  0.0 85.9 jit_solution(3526924609112311958)
XLA Ops:
  0.3 1.0 %collective-permute-start.2 = (bf16[256,512]{1,0:T(8,128)(2,1)}, bf16[256,512]{1,0:T(8,128)(2,1)S(1)}, u32[]{:S(2)}, u32[]{:S(2)}) collective-permute-start(bf16[256,512]{1,0:T(8,128)(2,1)} %refs_2_.13), channel_id=1, source_target_pairs={{0,1},{1,0},{2,3},{3,2},{4,5},{5,4},{6,7},{7,6},{8,9},{9,8},{10,11... | collective-permute-start | bytes 786440 | tf_op jit(solution)/shard_map/ppermute | solution.py:543
  1.2 6.2 %collective-permute-done.refs_0_.base_ref = bf16[256,512]{1,0:T(8,128)(2,1)S(1)} collective-permute-done((bf16[256,512]{1,0:T(8,128)(2,1)}, bf16[256,512]{1,0:T(8,128)(2,1)S(1)}, u32[]{:S(2)}, u32[]{:S(2)}) %collective-permute-start) | collective-permute-done | bytes 262176 | tf_op jit(solution)/shard_map/ppermute | solution.py:543
  7.4 1.5 %collective-permute-start.1 = (bf16[256,512]{1,0:T(8,128)(2,1)S(1)}, bf16[256,512]{1,0:T(8,128)(2,1)S(1)}, u32[]{:S(2)}, u32[]{:S(2)}) collective-permute-start(bf16[256,512]{1,0:T(8,128)(2,1)S(1)} %collective-permute-done.refs_0_.base_ref), channel_id=1, source_target_pairs={{0,1},{1,0},{2,3},{3,2},{4,5},{5,4},{6,7},{7,6},{8,9},{9,8},{10,11... | collective-permute-start | bytes 786440 | tf_op jit(solution)/shard_map/ppermute | solution.py:543
  8.9 0.8 copy-done.4
  9.7 0.9 %copy-done.6 = bf16[256,512]{1,0:T(8,128)(2,1)S(1)} copy-done((bf16[256,512]{1,0:T(8,128)(2,1)S(1)}, bf16[256,512]{1,0:T(8,128)(2,1)}, u32[]{:S(2)}) %copy-start.6) | copy-done | bytes 262168
  10.6 2.2 %shard_map.73 = (f32[3,256,256]{2,1,0:T(8,128)S(1)}, f32[256,128]{1,0:T(8,128)S(1)}, bf16[3,256,2048]{2,1,0:T(8,128)(2,1)S(1)}) custom-call(bf16[256,512]{1,0:T(8,128)(2,1)S(1)} %copy-done.6, f32[3,2048]{1,0:T(4,128)S(1)} %copy-done.4, bf16[3,256,2048]{2,1,0:T(8,128)(2,1)} %refs_2_.21, bf16[3,256,2048]{2,1,0:T(8,128)(2,1)} %refs_3_.19, ...), custom_call_target="tpu_custom_call" | custom-call | flops 201326592 | bytes 1310720 | tf_op jit(solution)/shard_map/pallas_call | solution.py:68
  14.3 1.4 %collective-permute-start.3 = (bf16[2,256,256]{2,1,0:T(8,128)(2,1)S(1)}, bf16[2,256,256]{2,1,0:T(8,128)(2,1)S(1)}, u32[]{:S(2)}, u32[]{:S(2)}) collective-permute-start(bf16[2,256,256]{2,1,0:T(8,128)(2,1)S(1)} %shard_map.77.pair_ref), channel_id=1, source_target_pairs={{0,4},{1,5},{2,6},{3,7},{4,0},{5,1},{6,2},{7,3},{8,12},{9,13},{10,... | collective-permute-start | bytes 786440 | tf_op jit(solution)/shard_map/ppermute | solution.py:538
  15.7 1.8 %shard_map.80 = (bf16[512,128]{1,0:T(8,128)(2,1)S(1)}, bf16[512,256]{1,0:T(8,128)(2,1)S(1)}, bf16[512,128]{1,0:T(8,128)(2,1)S(1)}, bf16[512,256]{1,0:T(8,128)(2,1)S(1)}, bf16[512,256]{1,0:T(8,128)(2,1)S(1)}) custom-call(bf16[3,1024,512]{2,1,0:T(8,128)(2,1)} %refs_1_.45), custom_call_target="tpu_custom_call" | custom-call | flops 1000000 | bytes 1000000 | tf_op jit(solution)/shard_map/pallas_call | solution.py:68
  17.8 0.9 %shard_map.78 = (f32[4,14,64,128]{3,2,1,0:T(8,128)S(1)}, f32[4,4,2,64,128]{4,3,2,1,0:T(8,128)S(1)}) custom-call(f32[3,4,15,31]{3,2,1,0:T(8,128)S(1)} %copy.8.table_ref), custom_call_target="tpu_custom_call" | custom-call | flops 18350080 | bytes 1835008 | tf_op jit(solution)/shard_map/pallas_call | solution.py:68
  19.1 0.6 shard_map.79
  19.8 2.5 %collective-permute-done.3.even_ref = bf16[2,256,256]{2,1,0:T(8,128)(2,1)S(1)} collective-permute-done((bf16[2,256,256]{2,1,0:T(8,128)(2,1)S(1)}, bf16[2,256,256]{2,1,0:T(8,128)(2,1)S(1)}, u32[]{:S(2)}, u32[]{:S(2)}) %collective-permute-start.3) | collective-permute-done | bytes 262176 | tf_op jit(solution)/shard_map/ppermute | solution.py:538
  22.2 1.0 %collective-permute-done.4.odd_ref = bf16[2,256,256]{2,1,0:T(8,128)(2,1)S(1)} collective-permute-done((bf16[2,256,256]{2,1,0:T(8,128)(2,1)S(1)}, bf16[2,256,256]{2,1,0:T(8,128)(2,1)S(1)}, u32[]{:S(2)}, u32[]{:S(2)}) %collective-permute-start.4) | collective-permute-done | bytes 262176 | tf_op jit(solution)/shard_map/ppermute | solution.py:538
  23.2 0.7 halo.3.own_ref.refs_0_
  24.3 1.2 %collective-permute-start.8 = (bf16[512,128]{1,0:T(8,128)(2,1)S(1)}, bf16[512,128]{1,0:T(8,128)(2,1)S(1)}, u32[]{:S(2)}, u32[]{:S(2)}) collective-permute-start(bf16[512,128]{1,0:T(8,128)(2,1)S(1)} %get-tuple-element.48), channel_id=1, source_target_pairs={{0,2},{1,3},{2,0},{3,1},{4,6},{5,7},{6,4},{7,5},{8,10},{9,11},{10,... | collective-permute-start | bytes 393224 | tf_op jit(solution)/shard_map/ppermute | solution.py:543
  25.7 1.3 %collective-permute-start.12 = (bf16[512,256]{1,0:T(8,128)(2,1)S(1)}, bf16[512,256]{1,0:T(8,128)(2,1)S(1)}, u32[]{:S(2)}, u32[]{:S(2)}) collective-permute-start(bf16[512,256]{1,0:T(8,128)(2,1)S(1)} %collective-permute-done.9.refs_1_), channel_id=1, source_target_pairs={{0,16},{16,0},{1,17},{17,1},{2,18},{18,2},{3,19},{19,3},{4,20},{20... | collective-permute-start | bytes 786440 | tf_op jit(solution)/shard_map/ppermute | solution.py:543
  27.0 2.3 %collective-permute-start.5 = (bf16[256,256]{1,0:T(8,128)(2,1)S(1)}, bf16[256,256]{1,0:T(8,128)(2,1)S(1)}, u32[]{:S(2)}, u32[]{:S(2)}) collective-permute-start(bf16[256,256]{1,0:T(8,128)(2,1)S(1)} %halo.3.own_ref.refs_0_), channel_id=1, source_target_pairs={{0,1},{1,0},{2,3},{3,2},{4,5},{5,4},{6,7},{7,6},{8,9},{9,8},{10,11... | collective-permute-start | bytes 393224 | tf_op jit(solution)/shard_map/ppermute | solution.py:543
  29.2 2.3 %collective-permute-start.7 = (bf16[256,256]{1,0:T(8,128)(2,1)S(1)}, bf16[256,256]{1,0:T(8,128)(2,1)S(1)}, u32[]{:S(2)}, u32[]{:S(2)}) collective-permute-start(bf16[256,256]{1,0:T(8,128)(2,1)S(1)} %collective-permute-done.6.across_ref.refs_0_), channel_id=1, source_target_pairs={{0,1},{1,0},{2,3},{3,2},{4,5},{5,4},{6,7},{7,6},{8,9},{9,8},{10,11... | collective-permute-start | bytes 393224 | tf_op jit(solution)/shard_map/ppermute | solution.py:543
  31.5 1.2 %collective-permute-start.11 = (bf16[512,128]{1,0:T(8,128)(2,1)S(1)}, bf16[512,128]{1,0:T(8,128)(2,1)S(1)}, u32[]{:S(2)}, u32[]{:S(2)}) collective-permute-start(bf16[512,128]{1,0:T(8,128)(2,1)S(1)} %collective-permute-done.8.refs_0_), channel_id=1, source_target_pairs={{0,16},{16,0},{1,17},{17,1},{2,18},{18,2},{3,19},{19,3},{4,20},{20... | collective-permute-start | bytes 393224 | tf_op jit(solution)/shard_map/ppermute | solution.py:543
  32.8 0.8 collective-permute-done.10.refs_2_
  33.6 1.3 %collective-permute-start.13 = (bf16[512,128]{1,0:T(8,128)(2,1)S(1)}, bf16[512,128]{1,0:T(8,128)(2,1)S(1)}, u32[]{:S(2)}, u32[]{:S(2)}) collective-permute-start(bf16[512,128]{1,0:T(8,128)(2,1)S(1)} %collective-permute-done.10.refs_2_), channel_id=1, source_target_pairs={{0,16},{16,0},{1,17},{17,1},{2,18},{18,2},{3,19},{19,3},{4,20},{20... | collective-permute-start | bytes 393224 | tf_op jit(solution)/shard_map/ppermute | solution.py:543
  35.8 2.3 %collective-permute-start.15 = (bf16[256,512]{1,0:T(8,128)(2,1)S(1)}, bf16[256,512]{1,0:T(8,128)(2,1)S(1)}, u32[]{:S(2)}, u32[]{:S(2)}) collective-permute-start(bf16[256,512]{1,0:T(8,128)(2,1)S(1)} %shard_map.84.refs_0_.refs_2_), channel_id=1, source_target_pairs={{0,1},{1,0},{2,3},{3,2},{4,5},{5,4},{6,7},{7,6},{8,9},{9,8},{10,11... | collective-permute-start | bytes 786440 | tf_op jit(solution)/shard_map/ppermute | solution.py:543
  38.1 0.6 lent.2.refs_1_.base_ref
  38.7 2.8 %collective-permute-start.14 = (bf16[256,512]{1,0:T(8,128)(2,1)S(1)}, bf16[256,512]{1,0:T(8,128)(2,1)S(1)}, u32[]{:S(2)}, u32[]{:S(2)}) collective-permute-start(bf16[256,512]{1,0:T(8,128)(2,1)S(1)} %lent.2.refs_1_.base_ref), channel_id=1, source_target_pairs={{0,1},{1,0},{2,3},{3,2},{4,5},{5,4},{6,7},{7,6},{8,9},{9,8},{10,11... | collective-permute-start | bytes 786440 | tf_op jit(solution)/shard_map/ppermute | solution.py:543
  41.5 0.6 shard_map.85
  43.0 0.6 collective-permute-start.16
  44.0 1.2 %collective-permute-start.22 = (bf16[512,256]{1,0:T(8,128)(2,1)S(1)}, bf16[512,256]{1,0:T(8,128)(2,1)S(1)}, u32[]{:S(2)}, u32[]{:S(2)}) collective-permute-start(bf16[512,256]{1,0:T(8,128)(2,1)S(1)} %get-tuple-element.60), channel_id=1, source_target_pairs={{0,2},{1,3},{2,0},{3,1},{4,6},{5,7},{6,4},{7,5},{8,10},{9,11},{10,... | collective-permute-start | bytes 786440 | tf_op jit(solution)/shard_map/ppermute | solution.py:543
  45.2 0.9 %shard_map.89 = (f32[4,14,64,128]{3,2,1,0:T(8,128)S(1)}, f32[4,4,2,64,128]{4,3,2,1,0:T(8,128)S(1)}) custom-call(f32[3,4,15,31]{3,2,1,0:T(8,128)S(1)} %copy.8.table_ref), custom_call_target="tpu_custom_call" | custom-call | flops 18350080 | bytes 1835008 | tf_op jit(solution)/shard_map/pallas_call | solution.py:68
  46.5 0.6 shard_map.90
  47.1 3.5 %collective-permute-done.16.even_ref = bf16[2,256,256]{2,1,0:T(8,128)(2,1)S(1)} collective-permute-done((bf16[2,256,256]{2,1,0:T(8,128)(2,1)S(1)}, bf16[2,256,256]{2,1,0:T(8,128)(2,1)S(1)}, u32[]{:S(2)}, u32[]{:S(2)}) %collective-permute-start.16) | collective-permute-done | bytes 262176 | tf_op jit(solution)/shard_map/ppermute | solution.py:538
  50.9 0.7 halo.4.own_ref.refs_0_
  51.9 1.2 %collective-permute-start.23 = (bf16[512,256]{1,0:T(8,128)(2,1)S(1)}, bf16[512,256]{1,0:T(8,128)(2,1)S(1)}, u32[]{:S(2)}, u32[]{:S(2)}) collective-permute-start(bf16[512,256]{1,0:T(8,128)(2,1)S(1)} %collective-permute-done.21.refs_0_), channel_id=1, source_target_pairs={{0,16},{16,0},{1,17},{17,1},{2,18},{18,2},{3,19},{19,3},{4,20},{20... | collective-permute-start | bytes 786440 | tf_op jit(solution)/shard_map/ppermute | solution.py:543
  53.1 3.4 %collective-permute-done.22.refs_1_ = bf16[512,256]{1,0:T(8,128)(2,1)S(1)} collective-permute-done((bf16[512,256]{1,0:T(8,128)(2,1)S(1)}, bf16[512,256]{1,0:T(8,128)(2,1)S(1)}, u32[]{:S(2)}, u32[]{:S(2)}) %collective-permute-start.22) | collective-permute-done | bytes 262176 | tf_op jit(solution)/shard_map/ppermute | solution.py:543
  56.6 1.3 %collective-permute-start.24 = (bf16[512,256]{1,0:T(8,128)(2,1)S(1)}, bf16[512,256]{1,0:T(8,128)(2,1)S(1)}, u32[]{:S(2)}, u32[]{:S(2)}) collective-permute-start(bf16[512,256]{1,0:T(8,128)(2,1)S(1)} %collective-permute-done.22.refs_1_), channel_id=1, source_target_pairs={{0,16},{16,0},{1,17},{17,1},{2,18},{18,2},{3,19},{19,3},{4,20},{20... | collective-permute-start | bytes 786440 | tf_op jit(solution)/shard_map/ppermute | solution.py:543
  57.8 2.9 %collective-permute-start.18 = (bf16[256,256]{1,0:T(8,128)(2,1)S(1)}, bf16[256,256]{1,0:T(8,128)(2,1)S(1)}, u32[]{:S(2)}, u32[]{:S(2)}) collective-permute-start(bf16[256,256]{1,0:T(8,128)(2,1)S(1)} %halo.4.own_ref.refs_0_), channel_id=1, source_target_pairs={{0,1},{1,0},{2,3},{3,2},{4,5},{5,4},{6,7},{7,6},{8,9},{9,8},{10,11... | collective-permute-start | bytes 393224 | tf_op jit(solution)/shard_map/ppermute | solution.py:543
  61.1 0.6 collective-permute-done.18.beside_ref.refs_0_
  62.9 0.8 collective-permute-done.24.refs_3_
  64.1 2.6 %collective-permute-start.25 = (bf16[256,512]{1,0:T(8,128)(2,1)S(1)}, bf16[256,512]{1,0:T(8,128)(2,1)S(1)}, u32[]{:S(2)}, u32[]{:S(2)}) collective-permute-start(bf16[256,512]{1,0:T(8,128)(2,1)S(1)} %lent.3.refs_1_), channel_id=1, source_target_pairs={{0,1},{1,0},{2,3},{3,2},{4,5},{5,4},{6,7},{7,6},{8,9},{9,8},{10,11... | collective-permute-start | bytes 786440 | tf_op jit(solution)/shard_map/ppermute | solution.py:543
  66.7 0.6 shard_map.95
  68.2 1.3 %collective-permute-start.27 = (bf16[2,256,256]{2,1,0:T(8,128)(2,1)S(1)}, bf16[2,256,256]{2,1,0:T(8,128)(2,1)S(1)}, u32[]{:S(2)}, u32[]{:S(2)}) collective-permute-start(bf16[2,256,256]{2,1,0:T(8,128)(2,1)S(1)} %shard_map.98.pair_ref), channel_id=1, source_target_pairs={{0,4},{1,5},{2,6},{3,7},{4,0},{5,1},{6,2},{7,3},{8,12},{9,13},{10,... | collective-permute-start | bytes 786440 | tf_op jit(solution)/shard_map/ppermute | solution.py:538
  70.1 0.9 %shard_map.99 = (f32[4,14,64,128]{3,2,1,0:T(8,128)S(1)}, f32[4,4,2,64,128]{4,3,2,1,0:T(8,128)S(1)}) custom-call(f32[3,4,15,31]{3,2,1,0:T(8,128)S(1)} %copy.8.table_ref), custom_call_target="tpu_custom_call" | custom-call | flops 18350080 | bytes 1835008 | tf_op jit(solution)/shard_map/pallas_call | solution.py:68
  71.3 0.6 shard_map.100
  72.0 3.8 %collective-permute-done.27.even_ref = bf16[2,256,256]{2,1,0:T(8,128)(2,1)S(1)} collective-permute-done((bf16[2,256,256]{2,1,0:T(8,128)(2,1)S(1)}, bf16[2,256,256]{2,1,0:T(8,128)(2,1)S(1)}, u32[]{:S(2)}, u32[]{:S(2)}) %collective-permute-start.27) | collective-permute-done | bytes 262176 | tf_op jit(solution)/shard_map/ppermute | solution.py:538
  75.8 1.0 %collective-permute-done.28.odd_ref = bf16[2,256,256]{2,1,0:T(8,128)(2,1)S(1)} collective-permute-done((bf16[2,256,256]{2,1,0:T(8,128)(2,1)S(1)}, bf16[2,256,256]{2,1,0:T(8,128)(2,1)S(1)}, u32[]{:S(2)}, u32[]{:S(2)}) %collective-permute-start.28) | collective-permute-done | bytes 262176 | tf_op jit(solution)/shard_map/ppermute | solution.py:538
  76.7 0.7 halo.5.refs_0_
  77.9 1.8 %collective-permute-start.31 = (bf16[256,256]{1,0:T(8,128)(2,1)S(1)}, bf16[256,256]{1,0:T(8,128)(2,1)S(1)}, u32[]{:S(2)}, u32[]{:S(2)}) collective-permute-start(bf16[256,256]{1,0:T(8,128)(2,1)S(1)} %halo.5.refs_0_), channel_id=1, source_target_pairs={{0,1},{1,0},{2,3},{3,2},{4,5},{5,4},{6,7},{7,6},{8,9},{9,8},{10,11... | collective-permute-start | bytes 393224 | tf_op jit(solution)/shard_map/ppermute | solution.py:543
  79.7 1.6 %collective-permute-done.29.refs_0_ = bf16[256,256]{1,0:T(8,128)(2,1)S(1)} collective-permute-done((bf16[256,256]{1,0:T(8,128)(2,1)S(1)}, bf16[256,256]{1,0:T(8,128)(2,1)S(1)}, u32[]{:S(2)}, u32[]{:S(2)}) %collective-permute-start.29) | collective-permute-done | bytes 131104 | tf_op jit(solution)/shard_map/ppermute | solution.py:543
  81.3 2.7 %collective-permute-start.30 = (bf16[256,256]{1,0:T(8,128)(2,1)S(1)}, bf16[256,256]{1,0:T(8,128)(2,1)S(1)}, u32[]{:S(2)}, u32[]{:S(2)}) collective-permute-start(bf16[256,256]{1,0:T(8,128)(2,1)S(1)} %collective-permute-done.29.refs_0_), channel_id=1, source_target_pairs={{0,1},{1,0},{2,3},{3,2},{4,5},{5,4},{6,7},{7,6},{8,9},{9,8},{10,11... | collective-permute-start | bytes 393224 | tf_op jit(solution)/shard_map/ppermute | solution.py:543
  85.0 0.9 %shard_map.104 = bf16[256,512]{1,0:T(8,128)(2,1)} custom-call(bf16[256,256]{1,0:T(8,128)(2,1)S(1)} %collective-permute-done.30.refs_0_, bf16[3,1024,512]{2,1,0:T(8,128)(2,1)S(1)} %copy-done, f32[256,512]{1,0:T(8,128)S(1)} %shard_map.103.refs_2_), custom_call_target="tpu_custom_call" | custom-call | flops 67108864 | bytes 1000000 | tf_op jit(solution)/shard_map/pallas_call | solution.py:68
  (72 shorter events, 10.9 us)
Async XLA Ops:
  0.0 7.4 %collective-permute-start = (bf16[256,512]{1,0:T(8,128)(2,1)}, bf16[256,512]{1,0:T(8,128)(2,1)S(1)}, u32[]{:S(2)}, u32[]{:S(2)}) collective-permute-start(bf16[256,512]{1,0:T(8,128)(2,1)} %refs_2_.13), channel_id=1, source_target_pairs={{0,2},{1,3},{2,0},{3,1},{4,6},{5,7},{6,4},{7,5},{8,10},{9,11},{10,... | collective-permute-start | bytes 786440 | tf_op jit(solution)/shard_map/ppermute | solution.py:543
  0.3 12.6 %collective-permute-start.2 = (bf16[256,512]{1,0:T(8,128)(2,1)}, bf16[256,512]{1,0:T(8,128)(2,1)S(1)}, u32[]{:S(2)}, u32[]{:S(2)}) collective-permute-start(bf16[256,512]{1,0:T(8,128)(2,1)} %refs_2_.13), channel_id=1, source_target_pairs={{0,1},{1,0},{2,3},{3,2},{4,5},{5,4},{6,7},{7,6},{8,9},{9,8},{10,11... | collective-permute-start | bytes 786440 | tf_op jit(solution)/shard_map/ppermute | solution.py:543
  7.4 6.5 %collective-permute-start.1 = (bf16[256,512]{1,0:T(8,128)(2,1)S(1)}, bf16[256,512]{1,0:T(8,128)(2,1)S(1)}, u32[]{:S(2)}, u32[]{:S(2)}) collective-permute-start(bf16[256,512]{1,0:T(8,128)(2,1)S(1)} %collective-permute-done.refs_0_.base_ref), channel_id=1, source_target_pairs={{0,1},{1,0},{2,3},{3,2},{4,5},{5,4},{6,7},{7,6},{8,9},{9,8},{10,11... | collective-permute-start | bytes 786440 | tf_op jit(solution)/shard_map/ppermute | solution.py:543
  8.9 0.8 copy-start.4
  9.7 0.9 %copy-start.6 = (bf16[256,512]{1,0:T(8,128)(2,1)S(1)}, bf16[256,512]{1,0:T(8,128)(2,1)}, u32[]{:S(2)}) copy-start(bf16[256,512]{1,0:T(8,128)(2,1)} %refs_2_.13) | copy-start | bytes 786436
  10.6 2.3 %copy-start.5 = (f32[3,2048]{1,0:T(4,128)S(1)}, f32[3,2048]{1,0:T(4,128)}, u32[]{:S(2)}) copy-start(f32[3,2048]{1,0:T(4,128)} %refs_1_.41) | copy-start | bytes 73732
  13.4 5.4 %copy-start.3 = (bf16[3,256,2048]{2,1,0:T(8,128)(2,1)S(1)}, bf16[3,256,2048]{2,1,0:T(8,128)(2,1)}, u32[]{:S(2)}) copy-start(bf16[3,256,2048]{2,1,0:T(8,128)(2,1)} %refs_4_.19) | copy-start | bytes 9437188
  13.9 3.9 %copy-start.8 = (f32[3,4,15,31]{3,1,2,0:T(4,128)S(1)}, f32[3,4,15,31]{3,1,2,0:T(4,128)}, u32[]{:S(2)}) copy-start(f32[3,4,15,31]{3,1,2,0:T(4,128)} %param.13) | copy-start | bytes 66964
  13.9 4.9 %copy-start.1 = (bf16[3,256,2048]{2,1,0:T(8,128)(2,1)S(1)}, bf16[3,256,2048]{2,1,0:T(8,128)(2,1)}, u32[]{:S(2)}) copy-start(bf16[3,256,2048]{2,1,0:T(8,128)(2,1)} %refs_2_.21) | copy-start | bytes 9437188
  13.9 4.9 %copy-start.2 = (bf16[3,256,2048]{2,1,0:T(8,128)(2,1)S(1)}, bf16[3,256,2048]{2,1,0:T(8,128)(2,1)}, u32[]{:S(2)}) copy-start(bf16[3,256,2048]{2,1,0:T(8,128)(2,1)} %refs_3_.19) | copy-start | bytes 9437188
  14.3 7.9 %collective-permute-start.3 = (bf16[2,256,256]{2,1,0:T(8,128)(2,1)S(1)}, bf16[2,256,256]{2,1,0:T(8,128)(2,1)S(1)}, u32[]{:S(2)}, u32[]{:S(2)}) collective-permute-start(bf16[2,256,256]{2,1,0:T(8,128)(2,1)S(1)} %shard_map.77.pair_ref), channel_id=1, source_target_pairs={{0,4},{1,5},{2,6},{3,7},{4,0},{5,1},{6,2},{7,3},{8,12},{9,13},{10,... | collective-permute-start | bytes 786440 | tf_op jit(solution)/shard_map/ppermute | solution.py:538
  15.7 7.6 %collective-permute-start.4 = (bf16[2,256,256]{2,1,0:T(8,128)(2,1)S(1)}, bf16[2,256,256]{2,1,0:T(8,128)(2,1)S(1)}, u32[]{:S(2)}, u32[]{:S(2)}) collective-permute-start(bf16[2,256,256]{2,1,0:T(8,128)(2,1)S(1)} %shard_map.77.pair_ref), channel_id=1, source_target_pairs={{0,1},{1,0},{2,3},{3,2},{4,8},{5,9},{6,10},{7,11},{8,4},{9,5},{10,... | collective-permute-start | bytes 786440 | tf_op jit(solution)/shard_map/ppermute | solution.py:538
  17.5 8.2 %collective-permute-start.9 = (bf16[512,256]{1,0:T(8,128)(2,1)S(1)}, bf16[512,256]{1,0:T(8,128)(2,1)S(1)}, u32[]{:S(2)}, u32[]{:S(2)}) collective-permute-start(bf16[512,256]{1,0:T(8,128)(2,1)S(1)} %get-tuple-element.49), channel_id=1, source_target_pairs={{0,2},{1,3},{2,0},{3,1},{4,6},{5,7},{6,4},{7,5},{8,10},{9,11},{10,... | collective-permute-start | bytes 786440 | tf_op jit(solution)/shard_map/ppermute | solution.py:543
  19.1 15.7 %copy-start = (bf16[3,1024,512]{2,1,0:T(8,128)(2,1)S(1)}, bf16[3,1024,512]{2,1,0:T(8,128)(2,1)}, u32[]{:S(2)}) copy-start(bf16[3,1024,512]{2,1,0:T(8,128)(2,1)} %refs_1_.45) | copy-start | bytes 9437188
  19.1 15.7 %copy-start.7 = (bf16[256,512]{1,0:T(8,128)(2,1)S(1)}, bf16[256,512]{1,0:T(8,128)(2,1)}, u32[]{:S(2)}) copy-start(bf16[256,512]{1,0:T(8,128)(2,1)} %refs_2_.13) | copy-start | bytes 786436
  23.9 5.3 %collective-permute-start.6 = (bf16[256,256]{1,0:T(8,128)(2,1)S(1)}, bf16[256,256]{1,0:T(8,128)(2,1)S(1)}, u32[]{:S(2)}, u32[]{:S(2)}) collective-permute-start(bf16[256,256]{1,0:T(8,128)(2,1)S(1)} %halo.3.own_ref.refs_0_), channel_id=1, source_target_pairs={{0,2},{1,3},{2,0},{3,1},{4,6},{5,7},{6,4},{7,5},{8,10},{9,11},{10,... | collective-permute-start | bytes 393224 | tf_op jit(solution)/shard_map/ppermute | solution.py:543
  24.3 7.3 %collective-permute-start.8 = (bf16[512,128]{1,0:T(8,128)(2,1)S(1)}, bf16[512,128]{1,0:T(8,128)(2,1)S(1)}, u32[]{:S(2)}, u32[]{:S(2)}) collective-permute-start(bf16[512,128]{1,0:T(8,128)(2,1)S(1)} %get-tuple-element.48), channel_id=1, source_target_pairs={{0,2},{1,3},{2,0},{3,1},{4,6},{5,7},{6,4},{7,5},{8,10},{9,11},{10,... | collective-permute-start | bytes 393224 | tf_op jit(solution)/shard_map/ppermute | solution.py:543
  25.5 8.1 %collective-permute-start.10 = (bf16[512,128]{1,0:T(8,128)(2,1)S(1)}, bf16[512,128]{1,0:T(8,128)(2,1)S(1)}, u32[]{:S(2)}, u32[]{:S(2)}) collective-permute-start(bf16[512,128]{1,0:T(8,128)(2,1)S(1)} %get-tuple-element.50), channel_id=1, source_target_pairs={{0,2},{1,3},{2,0},{3,1},{4,6},{5,7},{6,4},{7,5},{8,10},{9,11},{10,... | collective-permute-start | bytes 393224 | tf_op jit(solution)/shard_map/ppermute | solution.py:543
  25.7 12.4 %collective-permute-start.12 = (bf16[512,256]{1,0:T(8,128)(2,1)S(1)}, bf16[512,256]{1,0:T(8,128)(2,1)S(1)}, u32[]{:S(2)}, u32[]{:S(2)}) collective-permute-start(bf16[512,256]{1,0:T(8,128)(2,1)S(1)} %collective-permute-done.9.refs_1_), channel_id=1, source_target_pairs={{0,16},{16,0},{1,17},{17,1},{2,18},{18,2},{3,19},{19,3},{4,20},{20... | collective-permute-start | bytes 786440 | tf_op jit(solution)/shard_map/ppermute | solution.py:543
  27.0 8.1 %collective-permute-start.5 = (bf16[256,256]{1,0:T(8,128)(2,1)S(1)}, bf16[256,256]{1,0:T(8,128)(2,1)S(1)}, u32[]{:S(2)}, u32[]{:S(2)}) collective-permute-start(bf16[256,256]{1,0:T(8,128)(2,1)S(1)} %halo.3.own_ref.refs_0_), channel_id=1, source_target_pairs={{0,1},{1,0},{2,3},{3,2},{4,5},{5,4},{6,7},{7,6},{8,9},{9,8},{10,11... | collective-permute-start | bytes 393224 | tf_op jit(solution)/shard_map/ppermute | solution.py:543
  29.2 6.3 %collective-permute-start.7 = (bf16[256,256]{1,0:T(8,128)(2,1)S(1)}, bf16[256,256]{1,0:T(8,128)(2,1)S(1)}, u32[]{:S(2)}, u32[]{:S(2)}) collective-permute-start(bf16[256,256]{1,0:T(8,128)(2,1)S(1)} %collective-permute-done.6.across_ref.refs_0_), channel_id=1, source_target_pairs={{0,1},{1,0},{2,3},{3,2},{4,5},{5,4},{6,7},{7,6},{8,9},{9,8},{10,11... | collective-permute-start | bytes 393224 | tf_op jit(solution)/shard_map/ppermute | solution.py:543
  31.5 6.6 %collective-permute-start.11 = (bf16[512,128]{1,0:T(8,128)(2,1)S(1)}, bf16[512,128]{1,0:T(8,128)(2,1)S(1)}, u32[]{:S(2)}, u32[]{:S(2)}) collective-permute-start(bf16[512,128]{1,0:T(8,128)(2,1)S(1)} %collective-permute-done.8.refs_0_), channel_id=1, source_target_pairs={{0,16},{16,0},{1,17},{17,1},{2,18},{18,2},{3,19},{19,3},{4,20},{20... | collective-permute-start | bytes 393224 | tf_op jit(solution)/shard_map/ppermute | solution.py:543
  33.6 4.6 %collective-permute-start.13 = (bf16[512,128]{1,0:T(8,128)(2,1)S(1)}, bf16[512,128]{1,0:T(8,128)(2,1)S(1)}, u32[]{:S(2)}, u32[]{:S(2)}) collective-permute-start(bf16[512,128]{1,0:T(8,128)(2,1)S(1)} %collective-permute-done.10.refs_2_), channel_id=1, source_target_pairs={{0,16},{16,0},{1,17},{17,1},{2,18},{18,2},{3,19},{19,3},{4,20},{20... | collective-permute-start | bytes 393224 | tf_op jit(solution)/shard_map/ppermute | solution.py:543
  35.8 6.4 %collective-permute-start.15 = (bf16[256,512]{1,0:T(8,128)(2,1)S(1)}, bf16[256,512]{1,0:T(8,128)(2,1)S(1)}, u32[]{:S(2)}, u32[]{:S(2)}) collective-permute-start(bf16[256,512]{1,0:T(8,128)(2,1)S(1)} %shard_map.84.refs_0_.refs_2_), channel_id=1, source_target_pairs={{0,1},{1,0},{2,3},{3,2},{4,5},{5,4},{6,7},{7,6},{8,9},{9,8},{10,11... | collective-permute-start | bytes 786440 | tf_op jit(solution)/shard_map/ppermute | solution.py:543
  38.7 4.0 %collective-permute-start.14 = (bf16[256,512]{1,0:T(8,128)(2,1)S(1)}, bf16[256,512]{1,0:T(8,128)(2,1)S(1)}, u32[]{:S(2)}, u32[]{:S(2)}) collective-permute-start(bf16[256,512]{1,0:T(8,128)(2,1)S(1)} %lent.2.refs_1_.base_ref), channel_id=1, source_target_pairs={{0,1},{1,0},{2,3},{3,2},{4,5},{5,4},{6,7},{7,6},{8,9},{9,8},{10,11... | collective-permute-start | bytes 786440 | tf_op jit(solution)/shard_map/ppermute | solution.py:543
  43.0 7.5 %collective-permute-start.16 = (bf16[2,256,256]{2,1,0:T(8,128)(2,1)S(1)}, bf16[2,256,256]{2,1,0:T(8,128)(2,1)S(1)}, u32[]{:S(2)}, u32[]{:S(2)}) collective-permute-start(bf16[2,256,256]{2,1,0:T(8,128)(2,1)S(1)} %shard_map.88.pair_ref), channel_id=1, source_target_pairs={{0,4},{1,5},{2,6},{3,7},{4,0},{5,1},{6,2},{7,3},{8,12},{9,13},{10,... | collective-permute-start | bytes 786440 | tf_op jit(solution)/shard_map/ppermute | solution.py:538
  43.7 7.2 %collective-permute-start.17 = (bf16[2,256,256]{2,1,0:T(8,128)(2,1)S(1)}, bf16[2,256,256]{2,1,0:T(8,128)(2,1)S(1)}, u32[]{:S(2)}, u32[]{:S(2)}) collective-permute-start(bf16[2,256,256]{2,1,0:T(8,128)(2,1)S(1)} %shard_map.88.pair_ref), channel_id=1, source_target_pairs={{0,1},{1,0},{2,3},{3,2},{4,8},{5,9},{6,10},{7,11},{8,4},{9,5},{10,... | collective-permute-start | bytes 786440 | tf_op jit(solution)/shard_map/ppermute | solution.py:538
  43.7 8.1 %collective-permute-start.21 = (bf16[512,256]{1,0:T(8,128)(2,1)S(1)}, bf16[512,256]{1,0:T(8,128)(2,1)S(1)}, u32[]{:S(2)}, u32[]{:S(2)}) collective-permute-start(bf16[512,256]{1,0:T(8,128)(2,1)S(1)} %get-tuple-element.59), channel_id=1, source_target_pairs={{0,2},{1,3},{2,0},{3,1},{4,6},{5,7},{6,4},{7,5},{8,10},{9,11},{10,... | collective-permute-start | bytes 786440 | tf_op jit(solution)/shard_map/ppermute | solution.py:543
  44.0 12.6 %collective-permute-start.22 = (bf16[512,256]{1,0:T(8,128)(2,1)S(1)}, bf16[512,256]{1,0:T(8,128)(2,1)S(1)}, u32[]{:S(2)}, u32[]{:S(2)}) collective-permute-start(bf16[512,256]{1,0:T(8,128)(2,1)S(1)} %get-tuple-element.60), channel_id=1, source_target_pairs={{0,2},{1,3},{2,0},{3,1},{4,6},{5,7},{6,4},{7,5},{8,10},{9,11},{10,... | collective-permute-start | bytes 786440 | tf_op jit(solution)/shard_map/ppermute | solution.py:543
  51.6 9.2 %collective-permute-start.19 = (bf16[256,256]{1,0:T(8,128)(2,1)S(1)}, bf16[256,256]{1,0:T(8,128)(2,1)S(1)}, u32[]{:S(2)}, u32[]{:S(2)}) collective-permute-start(bf16[256,256]{1,0:T(8,128)(2,1)S(1)} %halo.4.own_ref.refs_0_), channel_id=1, source_target_pairs={{0,2},{1,3},{2,0},{3,1},{4,6},{5,7},{6,4},{7,5},{8,10},{9,11},{10,... | collective-permute-start | bytes 393224 | tf_op jit(solution)/shard_map/ppermute | solution.py:543
  51.9 11.0 %collective-permute-start.23 = (bf16[512,256]{1,0:T(8,128)(2,1)S(1)}, bf16[512,256]{1,0:T(8,128)(2,1)S(1)}, u32[]{:S(2)}, u32[]{:S(2)}) collective-permute-start(bf16[512,256]{1,0:T(8,128)(2,1)S(1)} %collective-permute-done.21.refs_0_), channel_id=1, source_target_pairs={{0,16},{16,0},{1,17},{17,1},{2,18},{18,2},{3,19},{19,3},{4,20},{20... | collective-permute-start | bytes 786440 | tf_op jit(solution)/shard_map/ppermute | solution.py:543
  56.6 7.1 %collective-permute-start.24 = (bf16[512,256]{1,0:T(8,128)(2,1)S(1)}, bf16[512,256]{1,0:T(8,128)(2,1)S(1)}, u32[]{:S(2)}, u32[]{:S(2)}) collective-permute-start(bf16[512,256]{1,0:T(8,128)(2,1)S(1)} %collective-permute-done.22.refs_1_), channel_id=1, source_target_pairs={{0,16},{16,0},{1,17},{17,1},{2,18},{18,2},{3,19},{19,3},{4,20},{20... | collective-permute-start | bytes 786440 | tf_op jit(solution)/shard_map/ppermute | solution.py:543
  57.8 3.9 %collective-permute-start.18 = (bf16[256,256]{1,0:T(8,128)(2,1)S(1)}, bf16[256,256]{1,0:T(8,128)(2,1)S(1)}, u32[]{:S(2)}, u32[]{:S(2)}) collective-permute-start(bf16[256,256]{1,0:T(8,128)(2,1)S(1)} %halo.4.own_ref.refs_0_), channel_id=1, source_target_pairs={{0,1},{1,0},{2,3},{3,2},{4,5},{5,4},{6,7},{7,6},{8,9},{9,8},{10,11... | collective-permute-start | bytes 393224 | tf_op jit(solution)/shard_map/ppermute | solution.py:543
  60.7 1.4 %collective-permute-start.20 = (bf16[256,256]{1,0:T(8,128)(2,1)S(1)}, bf16[256,256]{1,0:T(8,128)(2,1)S(1)}, u32[]{:S(2)}, u32[]{:S(2)}) collective-permute-start(bf16[256,256]{1,0:T(8,128)(2,1)S(1)} %collective-permute-done.19.across_ref.refs_0_), channel_id=1, source_target_pairs={{0,1},{1,0},{2,3},{3,2},{4,5},{5,4},{6,7},{7,6},{8,9},{9,8},{10,11... | collective-permute-start | bytes 393224 | tf_op jit(solution)/shard_map/ppermute | solution.py:543
  62.4 4.9 %collective-permute-start.26 = (bf16[256,512]{1,0:T(8,128)(2,1)S(1)}, bf16[256,512]{1,0:T(8,128)(2,1)S(1)}, u32[]{:S(2)}, u32[]{:S(2)}) collective-permute-start(bf16[256,512]{1,0:T(8,128)(2,1)S(1)} %shard_map.94.refs_0_.refs_2_), channel_id=1, source_target_pairs={{0,1},{1,0},{2,3},{3,2},{4,5},{5,4},{6,7},{7,6},{8,9},{9,8},{10,11... | collective-permute-start | bytes 786440 | tf_op jit(solution)/shard_map/ppermute | solution.py:543
  64.1 3.8 %collective-permute-start.25 = (bf16[256,512]{1,0:T(8,128)(2,1)S(1)}, bf16[256,512]{1,0:T(8,128)(2,1)S(1)}, u32[]{:S(2)}, u32[]{:S(2)}) collective-permute-start(bf16[256,512]{1,0:T(8,128)(2,1)S(1)} %lent.3.refs_1_), channel_id=1, source_target_pairs={{0,1},{1,0},{2,3},{3,2},{4,5},{5,4},{6,7},{7,6},{8,9},{9,8},{10,11... | collective-permute-start | bytes 786440 | tf_op jit(solution)/shard_map/ppermute | solution.py:543
  68.2 7.5 %collective-permute-start.27 = (bf16[2,256,256]{2,1,0:T(8,128)(2,1)S(1)}, bf16[2,256,256]{2,1,0:T(8,128)(2,1)S(1)}, u32[]{:S(2)}, u32[]{:S(2)}) collective-permute-start(bf16[2,256,256]{2,1,0:T(8,128)(2,1)S(1)} %shard_map.98.pair_ref), channel_id=1, source_target_pairs={{0,4},{1,5},{2,6},{3,7},{4,0},{5,1},{6,2},{7,3},{8,12},{9,13},{10,... | collective-permute-start | bytes 786440 | tf_op jit(solution)/shard_map/ppermute | solution.py:538
  69.5 7.2 %collective-permute-start.28 = (bf16[2,256,256]{2,1,0:T(8,128)(2,1)S(1)}, bf16[2,256,256]{2,1,0:T(8,128)(2,1)S(1)}, u32[]{:S(2)}, u32[]{:S(2)}) collective-permute-start(bf16[2,256,256]{2,1,0:T(8,128)(2,1)S(1)} %shard_map.98.pair_ref), channel_id=1, source_target_pairs={{0,1},{1,0},{2,3},{3,2},{4,8},{5,9},{6,10},{7,11},{8,4},{9,5},{10,... | collective-permute-start | bytes 786440 | tf_op jit(solution)/shard_map/ppermute | solution.py:538
  77.4 3.9 %collective-permute-start.29 = (bf16[256,256]{1,0:T(8,128)(2,1)S(1)}, bf16[256,256]{1,0:T(8,128)(2,1)S(1)}, u32[]{:S(2)}, u32[]{:S(2)}) collective-permute-start(bf16[256,256]{1,0:T(8,128)(2,1)S(1)} %halo.5.refs_0_), channel_id=1, source_target_pairs={{0,2},{1,3},{2,0},{3,1},{4,6},{5,7},{6,4},{7,5},{8,10},{9,11},{10,... | collective-permute-start | bytes 393224 | tf_op jit(solution)/shard_map/ppermute | solution.py:543
  77.9 6.3 %collective-permute-start.31 = (bf16[256,256]{1,0:T(8,128)(2,1)S(1)}, bf16[256,256]{1,0:T(8,128)(2,1)S(1)}, u32[]{:S(2)}, u32[]{:S(2)}) collective-permute-start(bf16[256,256]{1,0:T(8,128)(2,1)S(1)} %halo.5.refs_0_), channel_id=1, source_target_pairs={{0,1},{1,0},{2,3},{3,2},{4,5},{5,4},{6,7},{7,6},{8,9},{9,8},{10,11... | collective-permute-start | bytes 393224 | tf_op jit(solution)/shard_map/ppermute | solution.py:543
  81.3 3.7 %collective-permute-start.30 = (bf16[256,256]{1,0:T(8,128)(2,1)S(1)}, bf16[256,256]{1,0:T(8,128)(2,1)S(1)}, u32[]{:S(2)}, u32[]{:S(2)}) collective-permute-start(bf16[256,256]{1,0:T(8,128)(2,1)S(1)} %collective-permute-done.29.refs_0_), channel_id=1, source_target_pairs={{0,1},{1,0},{2,3},{3,2},{4,5},{5,4},{6,7},{7,6},{8,9},{9,8},{10,11... | collective-permute-start | bytes 393224 | tf_op jit(solution)/shard_map/ppermute | solution.py:543

commit v5 on v4

--- a/solution.py
+++ b/solution.py
@@ -76,10 +76,11 @@
     )(*operands, *arrays)
 
 
-def block_at(bit, width, unit):
+def block_at(bit, width, unit, sub=0, subs=1):
     if bit is None:
         return slice(None)
-    return pl.ds(pl.multiple_of((lax.axis_index("tp") ^ bit) * width, unit), width)
+    first = (lax.axis_index("tp") ^ bit) * (width * subs) + sub * width
+    return pl.ds(pl.multiple_of(first, unit), width)
 
 
 def window_at(row, rows_dev, sp):
@@ -138,7 +139,10 @@
         row_scale = lax.rsqrt(squares * (1.0 / full) + EPS)
         for at, kind in enumerate(kinds):
             scale = row_scale * HEAD_DIM ** (-0.5) if kind == 0 else row_scale
-            refs[0][at] = (totals[kind] * scale).astype(BF16)
+            made = (totals[kind] * scale).astype(BF16)
+            for group, out_ref in enumerate(refs):
+                width = out_ref.shape[2]
+                out_ref[at] = made[:, group * width : (group + 1) * width]
     else:
         acc_out, sq_out = refs
         for kind in range(3):
@@ -146,7 +150,7 @@
         sq_out[...] = jnp.broadcast_to(squares, sq_out.shape)
 
 
-def project(parts, bits, weights, carried, kinds, layer, gain):
+def project(parts, bits, weights, carried, kinds, layer, gain, groups=1):
     tok, width = parts[0].shape
     parts_n = len(parts)
     first = carried is None
@@ -169,7 +173,7 @@
         operands += map(in_vmem, carried)
         specs += [VMEM] * 2
     if kinds:
-        out_shape = [pltpu.VMEM((len(kinds), tok, channels), BF16)]
+        out_shape = [pltpu.VMEM((len(kinds), tok, channels // groups), BF16)] * groups
     else:
         out_shape = [pltpu.VMEM((3, tok, channels), F32), pltpu.VMEM((tok, LANES), F32)]
     scratch = []
@@ -187,7 +191,7 @@
     )
 
 
-def emit_kernel(bits, load, layer, *refs):
+def emit_kernel(bits, load, layer, sub, subs, *refs):
     sources, refs = refs[: len(bits)], refs[len(bits) :]
     held_ref, base_ref, out_ref, *rest = refs
     if load:
@@ -198,13 +202,13 @@
     if load:
         copy.wait()
     for at, bit in enumerate(bits):
-        rows = block_at(bit, sources[at].shape[1], HEAD_DIM)
+        rows = block_at(bit, sources[at].shape[1], HEAD_DIM, sub, subs)
         held = held_ref[rows, :] if load else held_ref[layer, rows, :]
         total = total + jnp.dot(sources[at][...], held, preferred_element_type=F32)
     out_ref[...] = total.astype(out_ref.dtype)
 
 
-def emit(parts, bits, weight, base, out_type, load, layer):
+def emit(parts, bits, weight, base, out_type, load, layer, sub=0, subs=1):
     tok, width = parts[0].shape
     cols = base.shape[1]
     out_shape = [pltpu.VMEM((tok, cols), out_type)]
@@ -214,7 +218,7 @@
     if load:
         scratch = [pltpu.VMEM(weight.shape[1:], BF16), pltpu.SemaphoreType.DMA]
     return call(
-        partial(emit_kernel, bits, load, layer),
+        partial(emit_kernel, bits, load, layer, sub, subs),
         [*parts, weight, base],
         [VMEM] * len(parts) + [HBM if load else VMEM, VMEM],
         out_shape,
@@ -342,7 +346,7 @@
     )
 
 
-def own_kernel(rows_dev, query_ref, pair_ref, bias_ref, mixed_ref, peak_ref):
+def own_kernel(rows_dev, head0, query_ref, pair_ref, bias_ref, mixed_ref, peak_ref):
     channels = query_ref.shape[2]
     group = min(LANES, channels)
     heads_in = group // HEAD_DIM
@@ -367,7 +371,8 @@
             for at in range(tok // LANES):
                 offset = (LANES // GRID_W) * at - row + ROW_SPAN - 1
                 bias = jnp.concatenate(
-                    [bias_ref[pair * heads_in + head, offset] for head in range(heads_in)], axis=0
+                    [bias_ref[head0 + pair * heads_in + head, offset] for head in range(heads_in)],
+                    axis=0,
                 )
                 pieces.append(scores[here, at * LANES : (at + 1) * LANES] + bias)
             peak = pieces[0]
@@ -379,12 +384,12 @@
             peak_ref[pair, here, :] = jnp.broadcast_to(peak, (stack, LANES))
 
 
-def attend_own(query, pair, bias, rows_dev):
+def attend_own(query, pair, bias, rows_dev, head0=0):
     _, tok, channels = query.shape
     group = min(LANES, channels)
     pairs, rows = channels // group, tok * (group // HEAD_DIM)
     return call(
-        partial(own_kernel, rows_dev),
+        partial(own_kernel, rows_dev, head0),
         [*map(in_vmem, (query, pair, bias))],
         [VMEM] * 3,
         [
@@ -396,7 +401,7 @@
 
 
 def halo_kernel(
-    rows_dev, sp, query_ref, even_ref, odd_ref, bias_ref, mixed_ref, peak_ref, out_ref, keys, values
+    rows_dev, sp, head0, query_ref, even_ref, odd_ref, bias_ref, mixed_ref, peak_ref, out_ref, keys, values
 ):
     channels = query_ref.shape[2]
     group = min(LANES, channels)
@@ -419,7 +424,8 @@
             pieces = []
             for at in range(span // LANES):
                 bias = jnp.concatenate(
-                    [bias_ref[row, pair * heads_in + head, at] for head in range(heads_in)], axis=0
+                    [bias_ref[row, head0 + pair * heads_in + head, at] for head in range(heads_in)],
+                    axis=0,
                 )
                 pieces.append(scores[:, at * LANES : (at + 1) * LANES] + bias)
             peak = pieces[0]
@@ -442,11 +448,11 @@
             out_ref[row * GRID_W : (row + 1) * GRID_W, cols] = (result / total).astype(BF16)
 
 
-def attend_halo(query, even, odd, bias, mixed, peak, rows_dev):
+def attend_halo(query, even, odd, bias, mixed, peak, rows_dev, head0=0):
     _, tok, channels = query.shape
     scores = tok * (channels // HEAD_DIM) * HALF * GRID_W
     return pl.pallas_call(
-        partial(halo_kernel, rows_dev, lax.axis_size("sp")),
+        partial(halo_kernel, rows_dev, lax.axis_size("sp"), head0),
         out_shape=pltpu.VMEM((tok, channels), BF16),
         in_specs=[VMEM] * 6,
         out_specs=VMEM,
@@ -582,6 +588,41 @@
                 cuts = cut_weight(in_hbm(output_weight))
                 send(cuts, layer, 0, len(cuts[layer]))
             carried = step([across], (2,), held, carried, None)
+        groups = query_weight.shape[1] // LANES
+        if lend and layer == LAYERS - 1 and groups == 2:
+            pairs, queries, swaps, attended = [], [], [], []
+            pairs = step([corner], (3,), held, carried, (1, 2), groups=groups)
+            queries = step([corner], (3,), held, carried, (0,), groups=groups)
+            for pair in pairs:
+                swaps.append(exchange(pair, even_pairs))
+                swaps.append(exchange(pair, odd_pairs))
+            bias, halo_bias = expand_bias(offset_bias, layer, rows_dev)
+            beside, across, corner = [], [], []
+            for group in range(groups):
+                head0 = group * (LANES // HEAD_DIM)
+                mixed, peak = attend_own(queries[group], pairs[group], bias, rows_dev, head0)
+                halo = swaps[2 * group : 2 * group + 2]
+                done = attend_halo(queries[group], *halo, halo_bias, mixed, peak, rows_dev, head0)
+                attended.append(done)
+                across.append(flip(done, "tp", 2))
+                beside.append(flip(done, "tp", 1))
+                corner.append(flip(across[-1], "tp", 1))
+            turns = [(attended, 0), (beside, 1), (across, 2), (corner, 3)]
+            for group in range(groups):
+                for part, bit in turns:
+                    final = group == groups - 1 and bit == 3
+                    (stream,) = emit(
+                        [part[group]],
+                        (bit,),
+                        output_weight,
+                        stream,
+                        BF16 if final else F32,
+                        False,
+                        layer,
+                        group,
+                        groups,
+                    )
+            return stream
         if tp == 4:
             old = across
             (pair,) = step([corner], (3,), held, carried, (1, 2))

time: 87.5 us -> 87.5 us (level)
  the two profiles are of different devices: /device:TPU:19 before, /device:TPU:1 now
where the time goes in v5:
time: 87.5 us; the launch traced here: 87.3 us
  starting transfers between devices  46.4 us (53%)
  Pallas kernels  21.4 us (24%)
  waiting for transfers between devices  17.2 us (20%)
  local copies, waits for them, and re-layouts  1.76 us (2%)
    ppermute x29, starting transfers between devices, flip(): return lax.ppermute(block, axis, [(at, at ^ bit) for at in range(count)])  37.6 us
    pallas_call x37, Pallas kernels, call(): pl.pallas_call(carrying if rider else kernel, out_shape=[*out_shape, *(pl...  18 us
    ppermute x29, waiting for transfers between devices, flip(): return lax.ppermute(block, axis, [(at, at ^ bit) for at in range(count)])  13.5 us
    ppermute x8, starting transfers between devices, exchange(): return lax.ppermute(block, ('sp', 'tp'), moves)  8.76 us
    ppermute x8, waiting for transfers between devices, exchange(): return lax.ppermute(block, ('sp', 'tp'), moves)  3.75 us
    pallas_call x4, Pallas kernels, attend_halo(): pl.pallas_call(partial(halo_kernel, rows_dev, lax.axis_size('sp'), head0)...  2.43 us
    unnamed x19, local copies, waits for them, and re-layouts  1.76 us
  transfers between devices with their start and end apart: 37, of which 9 were waited for; matrix products, arithmetic and copies ran while one was open for 0% of the time, Pallas kernels for 22%

profile of v5, /device:TPU:1, one launch (start us, length us, event | category | flops | bytes accessed | tf_op | source)
XLA Modules:
  0.0 87.3 jit_solution(8372175303881118613)
XLA Ops:
  0.0 2.0 %collective-permute-start = (bf16[256,512]{1,0:T(8,128)(2,1)}, bf16[256,512]{1,0:T(8,128)(2,1)S(1)}, u32[]{:S(2)}, u32[]{:S(2)}) collective-permute-start(bf16[256,512]{1,0:T(8,128)(2,1)} %refs_2_.13), channel_id=1, source_target_pairs={{0,2},{1,3},{2,0},{3,1},{4,6},{5,7},{6,4},{7,5},{8,10},{9,11},{10,... | collective-permute-start | bytes 786440 | tf_op jit(solution)/shard_map/ppermute | solution.py:549
  2.0 1.0 %collective-permute-start.2 = (bf16[256,512]{1,0:T(8,128)(2,1)}, bf16[256,512]{1,0:T(8,128)(2,1)S(1)}, u32[]{:S(2)}, u32[]{:S(2)}) collective-permute-start(bf16[256,512]{1,0:T(8,128)(2,1)} %refs_2_.13), channel_id=1, source_target_pairs={{0,1},{1,0},{2,3},{3,2},{4,5},{5,4},{6,7},{7,6},{8,9},{9,8},{10,11... | collective-permute-start | bytes 786440 | tf_op jit(solution)/shard_map/ppermute | solution.py:549
  3.0 5.3 %collective-permute-done.refs_0_.base_ref = bf16[256,512]{1,0:T(8,128)(2,1)S(1)} collective-permute-done((bf16[256,512]{1,0:T(8,128)(2,1)}, bf16[256,512]{1,0:T(8,128)(2,1)S(1)}, u32[]{:S(2)}, u32[]{:S(2)}) %collective-permute-start) | collective-permute-done | bytes 262176 | tf_op jit(solution)/shard_map/ppermute | solution.py:549
  8.2 1.3 %collective-permute-start.1 = (bf16[256,512]{1,0:T(8,128)(2,1)S(1)}, bf16[256,512]{1,0:T(8,128)(2,1)S(1)}, u32[]{:S(2)}, u32[]{:S(2)}) collective-permute-start(bf16[256,512]{1,0:T(8,128)(2,1)S(1)} %collective-permute-done.refs_0_.base_ref), channel_id=1, source_target_pairs={{0,1},{1,0},{2,3},{3,2},{4,5},{5,4},{6,7},{7,6},{8,9},{9,8},{10,11... | collective-permute-start | bytes 786440 | tf_op jit(solution)/shard_map/ppermute | solution.py:549
  9.5 0.8 copy-done.4
  10.3 0.9 %copy-done.6 = bf16[256,512]{1,0:T(8,128)(2,1)S(1)} copy-done((bf16[256,512]{1,0:T(8,128)(2,1)S(1)}, bf16[256,512]{1,0:T(8,128)(2,1)}, u32[]{:S(2)}) %copy-start.6) | copy-done | bytes 262168
  11.2 2.2 %shard_map.73 = (f32[3,256,256]{2,1,0:T(8,128)S(1)}, f32[256,128]{1,0:T(8,128)S(1)}, bf16[3,256,2048]{2,1,0:T(8,128)(2,1)S(1)}) custom-call(bf16[256,512]{1,0:T(8,128)(2,1)S(1)} %copy-done.6, f32[3,2048]{1,0:T(4,128)S(1)} %copy-done.4, bf16[3,256,2048]{2,1,0:T(8,128)(2,1)} %refs_2_.21, bf16[3,256,2048]{2,1,0:T(8,128)(2,1)} %refs_3_.19, ...), custom_call_target="tpu_custom_call" | custom-call | flops 201326592 | bytes 1310720 | tf_op jit(solution)/shard_map/pallas_call | solution.py:68
  14.9 1.6 %collective-permute-start.3 = (bf16[2,256,256]{2,1,0:T(8,128)(2,1)S(1)}, bf16[2,256,256]{2,1,0:T(8,128)(2,1)S(1)}, u32[]{:S(2)}, u32[]{:S(2)}) collective-permute-start(bf16[2,256,256]{2,1,0:T(8,128)(2,1)S(1)} %shard_map.77.pair_ref), channel_id=1, source_target_pairs={{0,4},{1,5},{2,6},{3,7},{4,0},{5,1},{6,2},{7,3},{8,12},{9,13},{10,... | collective-permute-start | bytes 786440 | tf_op jit(solution)/shard_map/ppermute | solution.py:544
  16.8 1.3 %shard_map.80 = (bf16[512,128]{1,0:T(8,128)(2,1)S(1)}, bf16[512,256]{1,0:T(8,128)(2,1)S(1)}, bf16[512,128]{1,0:T(8,128)(2,1)S(1)}, bf16[512,256]{1,0:T(8,128)(2,1)S(1)}, bf16[512,256]{1,0:T(8,128)(2,1)S(1)}) custom-call(bf16[3,1024,512]{2,1,0:T(8,128)(2,1)} %refs_1_.53), custom_call_target="tpu_custom_call" | custom-call | flops 1000000 | bytes 1000000 | tf_op jit(solution)/shard_map/pallas_call | solution.py:68
  18.1 1.5 %collective-permute-start.9 = (bf16[512,256]{1,0:T(8,128)(2,1)S(1)}, bf16[512,256]{1,0:T(8,128)(2,1)S(1)}, u32[]{:S(2)}, u32[]{:S(2)}) collective-permute-start(bf16[512,256]{1,0:T(8,128)(2,1)S(1)} %get-tuple-element.55), channel_id=1, source_target_pairs={{0,2},{1,3},{2,0},{3,1},{4,6},{5,7},{6,4},{7,5},{8,10},{9,11},{10,... | collective-permute-start | bytes 786440 | tf_op jit(solution)/shard_map/ppermute | solution.py:549
  19.6 0.9 %shard_map.78 = (f32[4,14,64,128]{3,2,1,0:T(8,128)S(1)}, f32[4,4,2,64,128]{4,3,2,1,0:T(8,128)S(1)}) custom-call(f32[3,4,15,31]{3,2,1,0:T(8,128)S(1)} %copy.8.table_ref), custom_call_target="tpu_custom_call" | custom-call | flops 18350080 | bytes 1835008 | tf_op jit(solution)/shard_map/pallas_call | solution.py:68
  21.5 1.5 %collective-permute-done.3.even_ref = bf16[2,256,256]{2,1,0:T(8,128)(2,1)S(1)} collective-permute-done((bf16[2,256,256]{2,1,0:T(8,128)(2,1)S(1)}, bf16[2,256,256]{2,1,0:T(8,128)(2,1)S(1)}, u32[]{:S(2)}, u32[]{:S(2)}) %collective-permute-start.3) | collective-permute-done | bytes 262176 | tf_op jit(solution)/shard_map/ppermute | solution.py:544
  23.0 0.7 halo.4.own_ref.refs_0_
  23.7 1.3 %collective-permute-start.6 = (bf16[256,256]{1,0:T(8,128)(2,1)S(1)}, bf16[256,256]{1,0:T(8,128)(2,1)S(1)}, u32[]{:S(2)}, u32[]{:S(2)}) collective-permute-start(bf16[256,256]{1,0:T(8,128)(2,1)S(1)} %halo.4.own_ref.refs_0_), channel_id=1, source_target_pairs={{0,2},{1,3},{2,0},{3,1},{4,6},{5,7},{6,4},{7,5},{8,10},{9,11},{10,... | collective-permute-start | bytes 393224 | tf_op jit(solution)/shard_map/ppermute | solution.py:549
  25.2 1.3 %collective-permute-start.10 = (bf16[512,128]{1,0:T(8,128)(2,1)S(1)}, bf16[512,128]{1,0:T(8,128)(2,1)S(1)}, u32[]{:S(2)}, u32[]{:S(2)}) collective-permute-start(bf16[512,128]{1,0:T(8,128)(2,1)S(1)} %get-tuple-element.56), channel_id=1, source_target_pairs={{0,2},{1,3},{2,0},{3,1},{4,6},{5,7},{6,4},{7,5},{8,10},{9,11},{10,... | collective-permute-start | bytes 393224 | tf_op jit(solution)/shard_map/ppermute | solution.py:549
  26.5 1.2 %collective-permute-start.12 = (bf16[512,256]{1,0:T(8,128)(2,1)S(1)}, bf16[512,256]{1,0:T(8,128)(2,1)S(1)}, u32[]{:S(2)}, u32[]{:S(2)}) collective-permute-start(bf16[512,256]{1,0:T(8,128)(2,1)S(1)} %collective-permute-done.9.refs_1_), channel_id=1, source_target_pairs={{0,16},{16,0},{1,17},{17,1},{2,18},{18,2},{3,19},{19,3},{4,20},{20... | collective-permute-start | bytes 786440 | tf_op jit(solution)/shard_map/ppermute | solution.py:549
  27.7 2.0 %collective-permute-start.5 = (bf16[256,256]{1,0:T(8,128)(2,1)S(1)}, bf16[256,256]{1,0:T(8,128)(2,1)S(1)}, u32[]{:S(2)}, u32[]{:S(2)}) collective-permute-start(bf16[256,256]{1,0:T(8,128)(2,1)S(1)} %halo.4.own_ref.refs_0_), channel_id=1, source_target_pairs={{0,1},{1,0},{2,3},{3,2},{4,5},{5,4},{6,7},{7,6},{8,9},{9,8},{10,11... | collective-permute-start | bytes 393224 | tf_op jit(solution)/shard_map/ppermute | solution.py:549
  29.7 1.2 %collective-permute-start.7 = (bf16[256,256]{1,0:T(8,128)(2,1)S(1)}, bf16[256,256]{1,0:T(8,128)(2,1)S(1)}, u32[]{:S(2)}, u32[]{:S(2)}) collective-permute-start(bf16[256,256]{1,0:T(8,128)(2,1)S(1)} %collective-permute-done.6.across_ref.refs_0_), channel_id=1, source_target_pairs={{0,1},{1,0},{2,3},{3,2},{4,5},{5,4},{6,7},{7,6},{8,9},{9,8},{10,11... | collective-permute-start | bytes 393224 | tf_op jit(solution)/shard_map/ppermute | solution.py:549
  30.9 1.5 %collective-permute-start.11 = (bf16[512,128]{1,0:T(8,128)(2,1)S(1)}, bf16[512,128]{1,0:T(8,128)(2,1)S(1)}, u32[]{:S(2)}, u32[]{:S(2)}) collective-permute-start(bf16[512,128]{1,0:T(8,128)(2,1)S(1)} %collective-permute-done.8.refs_0_), channel_id=1, source_target_pairs={{0,16},{16,0},{1,17},{17,1},{2,18},{18,2},{3,19},{19,3},{4,20},{20... | collective-permute-start | bytes 393224 | tf_op jit(solution)/shard_map/ppermute | solution.py:549
  32.4 1.3 %collective-permute-done.10.refs_2_ = bf16[512,128]{1,0:T(8,128)(2,1)S(1)} collective-permute-done((bf16[512,128]{1,0:T(8,128)(2,1)S(1)}, bf16[512,128]{1,0:T(8,128)(2,1)S(1)}, u32[]{:S(2)}, u32[]{:S(2)}) %collective-permute-start.10) | collective-permute-done | bytes 131104 | tf_op jit(solution)/shard_map/ppermute | solution.py:549
  33.7 1.5 %collective-permute-start.13 = (bf16[512,128]{1,0:T(8,128)(2,1)S(1)}, bf16[512,128]{1,0:T(8,128)(2,1)S(1)}, u32[]{:S(2)}, u32[]{:S(2)}) collective-permute-start(bf16[512,128]{1,0:T(8,128)(2,1)S(1)} %collective-permute-done.10.refs_2_), channel_id=1, source_target_pairs={{0,16},{16,0},{1,17},{17,1},{2,18},{18,2},{3,19},{19,3},{4,20},{20... | collective-permute-start | bytes 393224 | tf_op jit(solution)/shard_map/ppermute | solution.py:549
  36.2 1.9 %collective-permute-start.15 = (bf16[256,512]{1,0:T(8,128)(2,1)S(1)}, bf16[256,512]{1,0:T(8,128)(2,1)S(1)}, u32[]{:S(2)}, u32[]{:S(2)}) collective-permute-start(bf16[256,512]{1,0:T(8,128)(2,1)S(1)} %shard_map.84.refs_0_.refs_2_), channel_id=1, source_target_pairs={{0,1},{1,0},{2,3},{3,2},{4,5},{5,4},{6,7},{7,6},{8,9},{9,8},{10,11... | collective-permute-start | bytes 786440 | tf_op jit(solution)/shard_map/ppermute | solution.py:549
  38.1 0.8 collective-permute-done.13.refs_5_
  39.4 2.3 %collective-permute-start.14 = (bf16[256,512]{1,0:T(8,128)(2,1)S(1)}, bf16[256,512]{1,0:T(8,128)(2,1)S(1)}, u32[]{:S(2)}, u32[]{:S(2)}) collective-permute-start(bf16[256,512]{1,0:T(8,128)(2,1)S(1)} %lent.2.refs_1_.base_ref), channel_id=1, source_target_pairs={{0,1},{1,0},{2,3},{3,2},{4,5},{5,4},{6,7},{7,6},{8,9},{9,8},{10,11... | collective-permute-start | bytes 786440 | tf_op jit(solution)/shard_map/ppermute | solution.py:549
  43.2 2.4 %collective-permute-start.16 = (bf16[2,256,256]{2,1,0:T(8,128)(2,1)S(1)}, bf16[2,256,256]{2,1,0:T(8,128)(2,1)S(1)}, u32[]{:S(2)}, u32[]{:S(2)}) collective-permute-start(bf16[2,256,256]{2,1,0:T(8,128)(2,1)S(1)} %shard_map.88.pair_ref), channel_id=1, source_target_pairs={{0,4},{1,5},{2,6},{3,7},{4,0},{5,1},{6,2},{7,3},{8,12},{9,13},{10,... | collective-permute-start | bytes 786440 | tf_op jit(solution)/shard_map/ppermute | solution.py:544
  45.6 0.7 collective-permute-start.17
  46.2 1.2 %collective-permute-start.21 = (bf16[512,256]{1,0:T(8,128)(2,1)S(1)}, bf16[512,256]{1,0:T(8,128)(2,1)S(1)}, u32[]{:S(2)}, u32[]{:S(2)}) collective-permute-start(bf16[512,256]{1,0:T(8,128)(2,1)S(1)} %get-tuple-element.65), channel_id=1, source_target_pairs={{0,2},{1,3},{2,0},{3,1},{4,6},{5,7},{6,4},{7,5},{8,10},{9,11},{10,... | collective-permute-start | bytes 786440 | tf_op jit(solution)/shard_map/ppermute | solution.py:549
  47.7 0.9 %shard_map.89 = (f32[4,14,64,128]{3,2,1,0:T(8,128)S(1)}, f32[4,4,2,64,128]{4,3,2,1,0:T(8,128)S(1)}) custom-call(f32[3,4,15,31]{3,2,1,0:T(8,128)S(1)} %copy.8.table_ref), custom_call_target="tpu_custom_call" | custom-call | flops 18350080 | bytes 1835008 | tf_op jit(solution)/shard_map/pallas_call | solution.py:68
  49.6 2.3 %collective-permute-done.16.even_ref = bf16[2,256,256]{2,1,0:T(8,128)(2,1)S(1)} collective-permute-done((bf16[2,256,256]{2,1,0:T(8,128)(2,1)S(1)}, bf16[2,256,256]{2,1,0:T(8,128)(2,1)S(1)}, u32[]{:S(2)}, u32[]{:S(2)}) %collective-permute-start.16) | collective-permute-done | bytes 262176 | tf_op jit(solution)/shard_map/ppermute | solution.py:544
  51.9 0.7 halo.5.own_ref.refs_0_
  52.6 1.3 %collective-permute-start.19 = (bf16[256,256]{1,0:T(8,128)(2,1)S(1)}, bf16[256,256]{1,0:T(8,128)(2,1)S(1)}, u32[]{:S(2)}, u32[]{:S(2)}) collective-permute-start(bf16[256,256]{1,0:T(8,128)(2,1)S(1)} %halo.5.own_ref.refs_0_), channel_id=1, source_target_pairs={{0,2},{1,3},{2,0},{3,1},{4,6},{5,7},{6,4},{7,5},{8,10},{9,11},{10,... | collective-permute-start | bytes 393224 | tf_op jit(solution)/shard_map/ppermute | solution.py:549
  54.1 1.3 %collective-permute-start.23 = (bf16[512,256]{1,0:T(8,128)(2,1)S(1)}, bf16[512,256]{1,0:T(8,128)(2,1)S(1)}, u32[]{:S(2)}, u32[]{:S(2)}) collective-permute-start(bf16[512,256]{1,0:T(8,128)(2,1)S(1)} %collective-permute-done.21.refs_0_), channel_id=1, source_target_pairs={{0,16},{16,0},{1,17},{17,1},{2,18},{18,2},{3,19},{19,3},{4,20},{20... | collective-permute-start | bytes 786440 | tf_op jit(solution)/shard_map/ppermute | solution.py:549
  55.4 4.4 %collective-permute-done.22.refs_1_ = bf16[512,256]{1,0:T(8,128)(2,1)S(1)} collective-permute-done((bf16[512,256]{1,0:T(8,128)(2,1)S(1)}, bf16[512,256]{1,0:T(8,128)(2,1)S(1)}, u32[]{:S(2)}, u32[]{:S(2)}) %collective-permute-start.22) | collective-permute-done | bytes 262176 | tf_op jit(solution)/shard_map/ppermute | solution.py:549
  59.7 1.3 %collective-permute-start.24 = (bf16[512,256]{1,0:T(8,128)(2,1)S(1)}, bf16[512,256]{1,0:T(8,128)(2,1)S(1)}, u32[]{:S(2)}, u32[]{:S(2)}) collective-permute-start(bf16[512,256]{1,0:T(8,128)(2,1)S(1)} %collective-permute-done.22.refs_1_), channel_id=1, source_target_pairs={{0,16},{16,0},{1,17},{17,1},{2,18},{18,2},{3,19},{19,3},{4,20},{20... | collective-permute-start | bytes 786440 | tf_op jit(solution)/shard_map/ppermute | solution.py:549
  61.0 1.6 %collective-permute-start.18 = (bf16[256,256]{1,0:T(8,128)(2,1)S(1)}, bf16[256,256]{1,0:T(8,128)(2,1)S(1)}, u32[]{:S(2)}, u32[]{:S(2)}) collective-permute-start(bf16[256,256]{1,0:T(8,128)(2,1)S(1)} %halo.5.own_ref.refs_0_), channel_id=1, source_target_pairs={{0,1},{1,0},{2,3},{3,2},{4,5},{5,4},{6,7},{7,6},{8,9},{9,8},{10,11... | collective-permute-start | bytes 393224 | tf_op jit(solution)/shard_map/ppermute | solution.py:549
  62.6 0.8 collective-permute-start.20
  65.0 1.2 %collective-permute-done.24.refs_3_ = bf16[512,256]{1,0:T(8,128)(2,1)S(1)} collective-permute-done((bf16[512,256]{1,0:T(8,128)(2,1)S(1)}, bf16[512,256]{1,0:T(8,128)(2,1)S(1)}, u32[]{:S(2)}, u32[]{:S(2)}) %collective-permute-start.24) | collective-permute-done | bytes 262176 | tf_op jit(solution)/shard_map/ppermute | solution.py:549
  66.7 2.2 %collective-permute-start.25 = (bf16[256,512]{1,0:T(8,128)(2,1)S(1)}, bf16[256,512]{1,0:T(8,128)(2,1)S(1)}, u32[]{:S(2)}, u32[]{:S(2)}) collective-permute-start(bf16[256,512]{1,0:T(8,128)(2,1)S(1)} %lent.3.refs_1_), channel_id=1, source_target_pairs={{0,1},{1,0},{2,3},{3,2},{4,5},{5,4},{6,7},{7,6},{8,9},{9,8},{10,11... | collective-permute-start | bytes 786440 | tf_op jit(solution)/shard_map/ppermute | solution.py:549
  70.5 1.1 %collective-permute-start.32 = (bf16[2,256,128]{2,1,0:T(8,128)(2,1)S(1)}, bf16[2,256,128]{2,1,0:T(8,128)(2,1)S(1)}, u32[]{:S(2)}, u32[]{:S(2)}) collective-permute-start(bf16[2,256,128]{2,1,0:T(8,128)(2,1)S(1)} %get-tuple-element.78.pair_ref), channel_id=1, source_target_pairs={{0,4},{1,5},{2,6},{3,7},{4,0},{5,1},{6,2},{7,3},{8,12},{9,13},{10,... | collective-permute-start | bytes 393224 | tf_op jit(solution)/shard_map/ppermute | solution.py:544
  72.2 0.9 collective-permute-start.27
  73.1 1.2 %collective-permute-start.28 = (bf16[2,256,128]{2,1,0:T(8,128)(2,1)S(1)}, bf16[2,256,128]{2,1,0:T(8,128)(2,1)S(1)}, u32[]{:S(2)}, u32[]{:S(2)}) collective-permute-start(bf16[2,256,128]{2,1,0:T(8,128)(2,1)S(1)} %get-tuple-element.72.pair_ref), channel_id=1, source_target_pairs={{0,1},{1,0},{2,3},{3,2},{4,8},{5,9},{6,10},{7,11},{8,4},{9,5},{10,... | collective-permute-start | bytes 393224 | tf_op jit(solution)/shard_map/ppermute | solution.py:544
  74.3 0.9 %shard_map.99 = (f32[4,14,64,128]{3,2,1,0:T(8,128)S(1)}, f32[4,4,2,64,128]{4,3,2,1,0:T(8,128)S(1)}) custom-call(f32[3,4,15,31]{3,2,1,0:T(8,128)S(1)} %copy.8.table_ref), custom_call_target="tpu_custom_call" | custom-call | flops 18350080 | bytes 1835008 | tf_op jit(solution)/shard_map/pallas_call | solution.py:68
  76.6 1.1 %collective-permute-start.34 = (bf16[256,128]{1,0:T(8,128)(2,1)S(1)}, bf16[256,128]{1,0:T(8,128)(2,1)S(1)}, u32[]{:S(2)}, u32[]{:S(2)}) collective-permute-start(bf16[256,128]{1,0:T(8,128)(2,1)S(1)} %halo.7.refs_0_), channel_id=1, source_target_pairs={{0,2},{1,3},{2,0},{3,1},{4,6},{5,7},{6,4},{7,5},{8,10},{9,11},{10,... | collective-permute-start | bytes 196616 | tf_op jit(solution)/shard_map/ppermute | solution.py:549
  78.8 1.1 %collective-permute-start.29 = (bf16[256,128]{1,0:T(8,128)(2,1)S(1)}, bf16[256,128]{1,0:T(8,128)(2,1)S(1)}, u32[]{:S(2)}, u32[]{:S(2)}) collective-permute-start(bf16[256,128]{1,0:T(8,128)(2,1)S(1)} %halo.6.refs_0_), channel_id=1, source_target_pairs={{0,2},{1,3},{2,0},{3,1},{4,6},{5,7},{6,4},{7,5},{8,10},{9,11},{10,... | collective-permute-start | bytes 196616 | tf_op jit(solution)/shard_map/ppermute | solution.py:549
  79.8 1.5 %collective-permute-start.36 = (bf16[256,128]{1,0:T(8,128)(2,1)S(1)}, bf16[256,128]{1,0:T(8,128)(2,1)S(1)}, u32[]{:S(2)}, u32[]{:S(2)}) collective-permute-start(bf16[256,128]{1,0:T(8,128)(2,1)S(1)} %halo.7.refs_0_), channel_id=1, source_target_pairs={{0,1},{1,0},{2,3},{3,2},{4,5},{5,4},{6,7},{7,6},{8,9},{9,8},{10,11... | collective-permute-start | bytes 196616 | tf_op jit(solution)/shard_map/ppermute | solution.py:549
  81.4 1.0 %collective-permute-start.35 = (bf16[256,128]{1,0:T(8,128)(2,1)S(1)}, bf16[256,128]{1,0:T(8,128)(2,1)S(1)}, u32[]{:S(2)}, u32[]{:S(2)}) collective-permute-start(bf16[256,128]{1,0:T(8,128)(2,1)S(1)} %collective-permute-done.34.refs_0_), channel_id=1, source_target_pairs={{0,1},{1,0},{2,3},{3,2},{4,5},{5,4},{6,7},{7,6},{8,9},{9,8},{10,11... | collective-permute-start | bytes 196616 | tf_op jit(solution)/shard_map/ppermute | solution.py:549
  82.3 2.4 %collective-permute-start.30 = (bf16[256,128]{1,0:T(8,128)(2,1)S(1)}, bf16[256,128]{1,0:T(8,128)(2,1)S(1)}, u32[]{:S(2)}, u32[]{:S(2)}) collective-permute-start(bf16[256,128]{1,0:T(8,128)(2,1)S(1)} %collective-permute-done.29.refs_0_), channel_id=1, source_target_pairs={{0,1},{1,0},{2,3},{3,2},{4,5},{5,4},{6,7},{7,6},{8,9},{9,8},{10,11... | collective-permute-start | bytes 196616 | tf_op jit(solution)/shard_map/ppermute | solution.py:549
  86.4 0.9 %shard_map.109 = bf16[256,512]{1,0:T(8,128)(2,1)} custom-call(bf16[256,128]{1,0:T(8,128)(2,1)S(1)} %collective-permute-done.30.refs_0_, bf16[3,1024,512]{2,1,0:T(8,128)(2,1)S(1)} %copy-done, f32[256,512]{1,0:T(8,128)S(1)} %shard_map.108.refs_2_), custom_call_target="tpu_custom_call" | custom-call | flops 33554432 | bytes 1000000 | tf_op jit(solution)/shard_map/pallas_call | solution.py:68
  (88 shorter events, 15.2 us)
Async XLA Ops:
  0.0 8.2 %collective-permute-start = (bf16[256,512]{1,0:T(8,128)(2,1)}, bf16[256,512]{1,0:T(8,128)(2,1)S(1)}, u32[]{:S(2)}, u32[]{:S(2)}) collective-permute-start(bf16[256,512]{1,0:T(8,128)(2,1)} %refs_2_.13), channel_id=1, source_target_pairs={{0,2},{1,3},{2,0},{3,1},{4,6},{5,7},{6,4},{7,5},{8,10},{9,11},{10,... | collective-permute-start | bytes 786440 | tf_op jit(solution)/shard_map/ppermute | solution.py:549
  2.0 11.4 %collective-permute-start.2 = (bf16[256,512]{1,0:T(8,128)(2,1)}, bf16[256,512]{1,0:T(8,128)(2,1)S(1)}, u32[]{:S(2)}, u32[]{:S(2)}) collective-permute-start(bf16[256,512]{1,0:T(8,128)(2,1)} %refs_2_.13), channel_id=1, source_target_pairs={{0,1},{1,0},{2,3},{3,2},{4,5},{5,4},{6,7},{7,6},{8,9},{9,8},{10,11... | collective-permute-start | bytes 786440 | tf_op jit(solution)/shard_map/ppermute | solution.py:549
  8.2 6.2 %collective-permute-start.1 = (bf16[256,512]{1,0:T(8,128)(2,1)S(1)}, bf16[256,512]{1,0:T(8,128)(2,1)S(1)}, u32[]{:S(2)}, u32[]{:S(2)}) collective-permute-start(bf16[256,512]{1,0:T(8,128)(2,1)S(1)} %collective-permute-done.refs_0_.base_ref), channel_id=1, source_target_pairs={{0,1},{1,0},{2,3},{3,2},{4,5},{5,4},{6,7},{7,6},{8,9},{9,8},{10,11... | collective-permute-start | bytes 786440 | tf_op jit(solution)/shard_map/ppermute | solution.py:549
  9.5 0.8 copy-start.4
  10.3 0.9 %copy-start.6 = (bf16[256,512]{1,0:T(8,128)(2,1)S(1)}, bf16[256,512]{1,0:T(8,128)(2,1)}, u32[]{:S(2)}) copy-start(bf16[256,512]{1,0:T(8,128)(2,1)} %refs_2_.13) | copy-start | bytes 786436
  11.2 2.3 %copy-start.5 = (f32[3,2048]{1,0:T(4,128)S(1)}, f32[3,2048]{1,0:T(4,128)}, u32[]{:S(2)}) copy-start(f32[3,2048]{1,0:T(4,128)} %refs_1_.45) | copy-start | bytes 73732
  14.0 6.6 %copy-start.3 = (bf16[3,256,2048]{2,1,0:T(8,128)(2,1)S(1)}, bf16[3,256,2048]{2,1,0:T(8,128)(2,1)}, u32[]{:S(2)}) copy-start(bf16[3,256,2048]{2,1,0:T(8,128)(2,1)} %refs_4_.19) | copy-start | bytes 9437188
  14.5 5.1 %copy-start.8 = (f32[3,4,15,31]{3,1,2,0:T(4,128)S(1)}, f32[3,4,15,31]{3,1,2,0:T(4,128)}, u32[]{:S(2)}) copy-start(f32[3,4,15,31]{3,1,2,0:T(4,128)} %param.13) | copy-start | bytes 66964
  14.5 6.1 %copy-start.1 = (bf16[3,256,2048]{2,1,0:T(8,128)(2,1)S(1)}, bf16[3,256,2048]{2,1,0:T(8,128)(2,1)}, u32[]{:S(2)}) copy-start(bf16[3,256,2048]{2,1,0:T(8,128)(2,1)} %refs_2_.21) | copy-start | bytes 9437188
  14.5 6.1 %copy-start.2 = (bf16[3,256,2048]{2,1,0:T(8,128)(2,1)S(1)}, bf16[3,256,2048]{2,1,0:T(8,128)(2,1)}, u32[]{:S(2)}) copy-start(bf16[3,256,2048]{2,1,0:T(8,128)(2,1)} %refs_3_.19) | copy-start | bytes 9437188
  14.9 8.1 %collective-permute-start.3 = (bf16[2,256,256]{2,1,0:T(8,128)(2,1)S(1)}, bf16[2,256,256]{2,1,0:T(8,128)(2,1)S(1)}, u32[]{:S(2)}, u32[]{:S(2)}) collective-permute-start(bf16[2,256,256]{2,1,0:T(8,128)(2,1)S(1)} %shard_map.77.pair_ref), channel_id=1, source_target_pairs={{0,4},{1,5},{2,6},{3,7},{4,0},{5,1},{6,2},{7,3},{8,12},{9,13},{10,... | collective-permute-start | bytes 786440 | tf_op jit(solution)/shard_map/ppermute | solution.py:544
  16.5 6.5 %collective-permute-start.4 = (bf16[2,256,256]{2,1,0:T(8,128)(2,1)S(1)}, bf16[2,256,256]{2,1,0:T(8,128)(2,1)S(1)}, u32[]{:S(2)}, u32[]{:S(2)}) collective-permute-start(bf16[2,256,256]{2,1,0:T(8,128)(2,1)S(1)} %shard_map.77.pair_ref), channel_id=1, source_target_pairs={{0,1},{1,0},{2,3},{3,2},{4,8},{5,9},{6,10},{7,11},{8,4},{9,5},{10,... | collective-permute-start | bytes 786440 | tf_op jit(solution)/shard_map/ppermute | solution.py:544
  18.1 8.4 %collective-permute-start.9 = (bf16[512,256]{1,0:T(8,128)(2,1)S(1)}, bf16[512,256]{1,0:T(8,128)(2,1)S(1)}, u32[]{:S(2)}, u32[]{:S(2)}) collective-permute-start(bf16[512,256]{1,0:T(8,128)(2,1)S(1)} %get-tuple-element.55), channel_id=1, source_target_pairs={{0,2},{1,3},{2,0},{3,1},{4,6},{5,7},{6,4},{7,5},{8,10},{9,11},{10,... | collective-permute-start | bytes 786440 | tf_op jit(solution)/shard_map/ppermute | solution.py:549
  20.9 14.3 %copy-start = (bf16[3,1024,512]{2,1,0:T(8,128)(2,1)S(1)}, bf16[3,1024,512]{2,1,0:T(8,128)(2,1)}, u32[]{:S(2)}) copy-start(bf16[3,1024,512]{2,1,0:T(8,128)(2,1)} %refs_1_.53) | copy-start | bytes 9437188
  20.9 14.3 %copy-start.7 = (bf16[256,512]{1,0:T(8,128)(2,1)S(1)}, bf16[256,512]{1,0:T(8,128)(2,1)}, u32[]{:S(2)}) copy-start(bf16[256,512]{1,0:T(8,128)(2,1)} %refs_2_.13) | copy-start | bytes 786436
  23.7 6.0 %collective-permute-start.6 = (bf16[256,256]{1,0:T(8,128)(2,1)S(1)}, bf16[256,256]{1,0:T(8,128)(2,1)S(1)}, u32[]{:S(2)}, u32[]{:S(2)}) collective-permute-start(bf16[256,256]{1,0:T(8,128)(2,1)S(1)} %halo.4.own_ref.refs_0_), channel_id=1, source_target_pairs={{0,2},{1,3},{2,0},{3,1},{4,6},{5,7},{6,4},{7,5},{8,10},{9,11},{10,... | collective-permute-start | bytes 393224 | tf_op jit(solution)/shard_map/ppermute | solution.py:549
  25.0 5.9 %collective-permute-start.8 = (bf16[512,128]{1,0:T(8,128)(2,1)S(1)}, bf16[512,128]{1,0:T(8,128)(2,1)S(1)}, u32[]{:S(2)}, u32[]{:S(2)}) collective-permute-start(bf16[512,128]{1,0:T(8,128)(2,1)S(1)} %get-tuple-element.54), channel_id=1, source_target_pairs={{0,2},{1,3},{2,0},{3,1},{4,6},{5,7},{6,4},{7,5},{8,10},{9,11},{10,... | collective-permute-start | bytes 393224 | tf_op jit(solution)/shard_map/ppermute | solution.py:549
  25.2 8.4 %collective-permute-start.10 = (bf16[512,128]{1,0:T(8,128)(2,1)S(1)}, bf16[512,128]{1,0:T(8,128)(2,1)S(1)}, u32[]{:S(2)}, u32[]{:S(2)}) collective-permute-start(bf16[512,128]{1,0:T(8,128)(2,1)S(1)} %get-tuple-element.56), channel_id=1, source_target_pairs={{0,2},{1,3},{2,0},{3,1},{4,6},{5,7},{6,4},{7,5},{8,10},{9,11},{10,... | collective-permute-start | bytes 393224 | tf_op jit(solution)/shard_map/ppermute | solution.py:549
  26.5 12.4 %collective-permute-start.12 = (bf16[512,256]{1,0:T(8,128)(2,1)S(1)}, bf16[512,256]{1,0:T(8,128)(2,1)S(1)}, u32[]{:S(2)}, u32[]{:S(2)}) collective-permute-start(bf16[512,256]{1,0:T(8,128)(2,1)S(1)} %collective-permute-done.9.refs_1_), channel_id=1, source_target_pairs={{0,16},{16,0},{1,17},{17,1},{2,18},{18,2},{3,19},{19,3},{4,20},{20... | collective-permute-start | bytes 786440 | tf_op jit(solution)/shard_map/ppermute | solution.py:549
  27.7 7.7 %collective-permute-start.5 = (bf16[256,256]{1,0:T(8,128)(2,1)S(1)}, bf16[256,256]{1,0:T(8,128)(2,1)S(1)}, u32[]{:S(2)}, u32[]{:S(2)}) collective-permute-start(bf16[256,256]{1,0:T(8,128)(2,1)S(1)} %halo.4.own_ref.refs_0_), channel_id=1, source_target_pairs={{0,1},{1,0},{2,3},{3,2},{4,5},{5,4},{6,7},{7,6},{8,9},{9,8},{10,11... | collective-permute-start | bytes 393224 | tf_op jit(solution)/shard_map/ppermute | solution.py:549
  29.7 6.2 %collective-permute-start.7 = (bf16[256,256]{1,0:T(8,128)(2,1)S(1)}, bf16[256,256]{1,0:T(8,128)(2,1)S(1)}, u32[]{:S(2)}, u32[]{:S(2)}) collective-permute-start(bf16[256,256]{1,0:T(8,128)(2,1)S(1)} %collective-permute-done.6.across_ref.refs_0_), channel_id=1, source_target_pairs={{0,1},{1,0},{2,3},{3,2},{4,5},{5,4},{6,7},{7,6},{8,9},{9,8},{10,11... | collective-permute-start | bytes 393224 | tf_op jit(solution)/shard_map/ppermute | solution.py:549
  30.9 7.2 %collective-permute-start.11 = (bf16[512,128]{1,0:T(8,128)(2,1)S(1)}, bf16[512,128]{1,0:T(8,128)(2,1)S(1)}, u32[]{:S(2)}, u32[]{:S(2)}) collective-permute-start(bf16[512,128]{1,0:T(8,128)(2,1)S(1)} %collective-permute-done.8.refs_0_), channel_id=1, source_target_pairs={{0,16},{16,0},{1,17},{17,1},{2,18},{18,2},{3,19},{19,3},{4,20},{20... | collective-permute-start | bytes 393224 | tf_op jit(solution)/shard_map/ppermute | solution.py:549
  33.7 5.2 %collective-permute-start.13 = (bf16[512,128]{1,0:T(8,128)(2,1)S(1)}, bf16[512,128]{1,0:T(8,128)(2,1)S(1)}, u32[]{:S(2)}, u32[]{:S(2)}) collective-permute-start(bf16[512,128]{1,0:T(8,128)(2,1)S(1)} %collective-permute-done.10.refs_2_), channel_id=1, source_target_pairs={{0,16},{16,0},{1,17},{17,1},{2,18},{18,2},{3,19},{19,3},{4,20},{20... | collective-permute-start | bytes 393224 | tf_op jit(solution)/shard_map/ppermute | solution.py:549
  36.2 6.2 %collective-permute-start.15 = (bf16[256,512]{1,0:T(8,128)(2,1)S(1)}, bf16[256,512]{1,0:T(8,128)(2,1)S(1)}, u32[]{:S(2)}, u32[]{:S(2)}) collective-permute-start(bf16[256,512]{1,0:T(8,128)(2,1)S(1)} %shard_map.84.refs_0_.refs_2_), channel_id=1, source_target_pairs={{0,1},{1,0},{2,3},{3,2},{4,5},{5,4},{6,7},{7,6},{8,9},{9,8},{10,11... | collective-permute-start | bytes 786440 | tf_op jit(solution)/shard_map/ppermute | solution.py:549
  39.4 3.4 %collective-permute-start.14 = (bf16[256,512]{1,0:T(8,128)(2,1)S(1)}, bf16[256,512]{1,0:T(8,128)(2,1)S(1)}, u32[]{:S(2)}, u32[]{:S(2)}) collective-permute-start(bf16[256,512]{1,0:T(8,128)(2,1)S(1)} %lent.2.refs_1_.base_ref), channel_id=1, source_target_pairs={{0,1},{1,0},{2,3},{3,2},{4,5},{5,4},{6,7},{7,6},{8,9},{9,8},{10,11... | collective-permute-start | bytes 786440 | tf_op jit(solution)/shard_map/ppermute | solution.py:549
  43.2 8.7 %collective-permute-start.16 = (bf16[2,256,256]{2,1,0:T(8,128)(2,1)S(1)}, bf16[2,256,256]{2,1,0:T(8,128)(2,1)S(1)}, u32[]{:S(2)}, u32[]{:S(2)}) collective-permute-start(bf16[2,256,256]{2,1,0:T(8,128)(2,1)S(1)} %shard_map.88.pair_ref), channel_id=1, source_target_pairs={{0,4},{1,5},{2,6},{3,7},{4,0},{5,1},{6,2},{7,3},{8,12},{9,13},{10,... | collective-permute-start | bytes 786440 | tf_op jit(solution)/shard_map/ppermute | solution.py:544
  45.6 6.3 %collective-permute-start.17 = (bf16[2,256,256]{2,1,0:T(8,128)(2,1)S(1)}, bf16[2,256,256]{2,1,0:T(8,128)(2,1)S(1)}, u32[]{:S(2)}, u32[]{:S(2)}) collective-permute-start(bf16[2,256,256]{2,1,0:T(8,128)(2,1)S(1)} %shard_map.88.pair_ref), channel_id=1, source_target_pairs={{0,1},{1,0},{2,3},{3,2},{4,8},{5,9},{6,10},{7,11},{8,4},{9,5},{10,... | collective-permute-start | bytes 786440 | tf_op jit(solution)/shard_map/ppermute | solution.py:544
  46.2 7.9 %collective-permute-start.21 = (bf16[512,256]{1,0:T(8,128)(2,1)S(1)}, bf16[512,256]{1,0:T(8,128)(2,1)S(1)}, u32[]{:S(2)}, u32[]{:S(2)}) collective-permute-start(bf16[512,256]{1,0:T(8,128)(2,1)S(1)} %get-tuple-element.65), channel_id=1, source_target_pairs={{0,2},{1,3},{2,0},{3,1},{4,6},{5,7},{6,4},{7,5},{8,10},{9,11},{10,... | collective-permute-start | bytes 786440 | tf_op jit(solution)/shard_map/ppermute | solution.py:549
  47.5 12.2 %collective-permute-start.22 = (bf16[512,256]{1,0:T(8,128)(2,1)S(1)}, bf16[512,256]{1,0:T(8,128)(2,1)S(1)}, u32[]{:S(2)}, u32[]{:S(2)}) collective-permute-start(bf16[512,256]{1,0:T(8,128)(2,1)S(1)} %get-tuple-element.66), channel_id=1, source_target_pairs={{0,2},{1,3},{2,0},{3,1},{4,6},{5,7},{6,4},{7,5},{8,10},{9,11},{10,... | collective-permute-start | bytes 786440 | tf_op jit(solution)/shard_map/ppermute | solution.py:549
  52.6 10.0 %collective-permute-start.19 = (bf16[256,256]{1,0:T(8,128)(2,1)S(1)}, bf16[256,256]{1,0:T(8,128)(2,1)S(1)}, u32[]{:S(2)}, u32[]{:S(2)}) collective-permute-start(bf16[256,256]{1,0:T(8,128)(2,1)S(1)} %halo.5.own_ref.refs_0_), channel_id=1, source_target_pairs={{0,2},{1,3},{2,0},{3,1},{4,6},{5,7},{6,4},{7,5},{8,10},{9,11},{10,... | collective-permute-start | bytes 393224 | tf_op jit(solution)/shard_map/ppermute | solution.py:549
  54.1 10.9 %collective-permute-start.23 = (bf16[512,256]{1,0:T(8,128)(2,1)S(1)}, bf16[512,256]{1,0:T(8,128)(2,1)S(1)}, u32[]{:S(2)}, u32[]{:S(2)}) collective-permute-start(bf16[512,256]{1,0:T(8,128)(2,1)S(1)} %collective-permute-done.21.refs_0_), channel_id=1, source_target_pairs={{0,16},{16,0},{1,17},{17,1},{2,18},{18,2},{3,19},{19,3},{4,20},{20... | collective-permute-start | bytes 786440 | tf_op jit(solution)/shard_map/ppermute | solution.py:549
  59.7 6.5 %collective-permute-start.24 = (bf16[512,256]{1,0:T(8,128)(2,1)S(1)}, bf16[512,256]{1,0:T(8,128)(2,1)S(1)}, u32[]{:S(2)}, u32[]{:S(2)}) collective-permute-start(bf16[512,256]{1,0:T(8,128)(2,1)S(1)} %collective-permute-done.22.refs_1_), channel_id=1, source_target_pairs={{0,16},{16,0},{1,17},{17,1},{2,18},{18,2},{3,19},{19,3},{4,20},{20... | collective-permute-start | bytes 786440 | tf_op jit(solution)/shard_map/ppermute | solution.py:549
  61.0 2.6 %collective-permute-start.18 = (bf16[256,256]{1,0:T(8,128)(2,1)S(1)}, bf16[256,256]{1,0:T(8,128)(2,1)S(1)}, u32[]{:S(2)}, u32[]{:S(2)}) collective-permute-start(bf16[256,256]{1,0:T(8,128)(2,1)S(1)} %halo.5.own_ref.refs_0_), channel_id=1, source_target_pairs={{0,1},{1,0},{2,3},{3,2},{4,5},{5,4},{6,7},{7,6},{8,9},{9,8},{10,11... | collective-permute-start | bytes 393224 | tf_op jit(solution)/shard_map/ppermute | solution.py:549
  62.6 1.8 %collective-permute-start.20 = (bf16[256,256]{1,0:T(8,128)(2,1)S(1)}, bf16[256,256]{1,0:T(8,128)(2,1)S(1)}, u32[]{:S(2)}, u32[]{:S(2)}) collective-permute-start(bf16[256,256]{1,0:T(8,128)(2,1)S(1)} %collective-permute-done.19.across_ref.refs_0_), channel_id=1, source_target_pairs={{0,1},{1,0},{2,3},{3,2},{4,5},{5,4},{6,7},{7,6},{8,9},{9,8},{10,11... | collective-permute-start | bytes 393224 | tf_op jit(solution)/shard_map/ppermute | solution.py:549
  64.6 5.0 %collective-permute-start.26 = (bf16[256,512]{1,0:T(8,128)(2,1)S(1)}, bf16[256,512]{1,0:T(8,128)(2,1)S(1)}, u32[]{:S(2)}, u32[]{:S(2)}) collective-permute-start(bf16[256,512]{1,0:T(8,128)(2,1)S(1)} %shard_map.94.refs_0_.refs_2_), channel_id=1, source_target_pairs={{0,1},{1,0},{2,3},{3,2},{4,5},{5,4},{6,7},{7,6},{8,9},{9,8},{10,11... | collective-permute-start | bytes 786440 | tf_op jit(solution)/shard_map/ppermute | solution.py:549
  66.7 3.4 %collective-permute-start.25 = (bf16[256,512]{1,0:T(8,128)(2,1)S(1)}, bf16[256,512]{1,0:T(8,128)(2,1)S(1)}, u32[]{:S(2)}, u32[]{:S(2)}) collective-permute-start(bf16[256,512]{1,0:T(8,128)(2,1)S(1)} %lent.3.refs_1_), channel_id=1, source_target_pairs={{0,1},{1,0},{2,3},{3,2},{4,5},{5,4},{6,7},{7,6},{8,9},{9,8},{10,11... | collective-permute-start | bytes 786440 | tf_op jit(solution)/shard_map/ppermute | solution.py:549
  70.5 5.6 %collective-permute-start.32 = (bf16[2,256,128]{2,1,0:T(8,128)(2,1)S(1)}, bf16[2,256,128]{2,1,0:T(8,128)(2,1)S(1)}, u32[]{:S(2)}, u32[]{:S(2)}) collective-permute-start(bf16[2,256,128]{2,1,0:T(8,128)(2,1)S(1)} %get-tuple-element.78.pair_ref), channel_id=1, source_target_pairs={{0,4},{1,5},{2,6},{3,7},{4,0},{5,1},{6,2},{7,3},{8,12},{9,13},{10,... | collective-permute-start | bytes 393224 | tf_op jit(solution)/shard_map/ppermute | solution.py:544
  71.6 4.5 %collective-permute-start.33 = (bf16[2,256,128]{2,1,0:T(8,128)(2,1)S(1)}, bf16[2,256,128]{2,1,0:T(8,128)(2,1)S(1)}, u32[]{:S(2)}, u32[]{:S(2)}) collective-permute-start(bf16[2,256,128]{2,1,0:T(8,128)(2,1)S(1)} %get-tuple-element.78.pair_ref), channel_id=1, source_target_pairs={{0,1},{1,0},{2,3},{3,2},{4,8},{5,9},{6,10},{7,11},{8,4},{9,5},{10,... | collective-permute-start | bytes 393224 | tf_op jit(solution)/shard_map/ppermute | solution.py:544
  72.2 6.0 %collective-permute-start.27 = (bf16[2,256,128]{2,1,0:T(8,128)(2,1)S(1)}, bf16[2,256,128]{2,1,0:T(8,128)(2,1)S(1)}, u32[]{:S(2)}, u32[]{:S(2)}) collective-permute-start(bf16[2,256,128]{2,1,0:T(8,128)(2,1)S(1)} %get-tuple-element.72.pair_ref), channel_id=1, source_target_pairs={{0,4},{1,5},{2,6},{3,7},{4,0},{5,1},{6,2},{7,3},{8,12},{9,13},{10,... | collective-permute-start | bytes 393224 | tf_op jit(solution)/shard_map/ppermute | solution.py:544
  73.1 5.1 %collective-permute-start.28 = (bf16[2,256,128]{2,1,0:T(8,128)(2,1)S(1)}, bf16[2,256,128]{2,1,0:T(8,128)(2,1)S(1)}, u32[]{:S(2)}, u32[]{:S(2)}) collective-permute-start(bf16[2,256,128]{2,1,0:T(8,128)(2,1)S(1)} %get-tuple-element.72.pair_ref), channel_id=1, source_target_pairs={{0,1},{1,0},{2,3},{3,2},{4,8},{5,9},{6,10},{7,11},{8,4},{9,5},{10,... | collective-permute-start | bytes 393224 | tf_op jit(solution)/shard_map/ppermute | solution.py:544
  76.6 4.7 %collective-permute-start.34 = (bf16[256,128]{1,0:T(8,128)(2,1)S(1)}, bf16[256,128]{1,0:T(8,128)(2,1)S(1)}, u32[]{:S(2)}, u32[]{:S(2)}) collective-permute-start(bf16[256,128]{1,0:T(8,128)(2,1)S(1)} %halo.7.refs_0_), channel_id=1, source_target_pairs={{0,2},{1,3},{2,0},{3,1},{4,6},{5,7},{6,4},{7,5},{8,10},{9,11},{10,... | collective-permute-start | bytes 196616 | tf_op jit(solution)/shard_map/ppermute | solution.py:549
  78.8 3.6 %collective-permute-start.29 = (bf16[256,128]{1,0:T(8,128)(2,1)S(1)}, bf16[256,128]{1,0:T(8,128)(2,1)S(1)}, u32[]{:S(2)}, u32[]{:S(2)}) collective-permute-start(bf16[256,128]{1,0:T(8,128)(2,1)S(1)} %halo.6.refs_0_), channel_id=1, source_target_pairs={{0,2},{1,3},{2,0},{3,1},{4,6},{5,7},{6,4},{7,5},{8,10},{9,11},{10,... | collective-permute-start | bytes 196616 | tf_op jit(solution)/shard_map/ppermute | solution.py:549
  79.8 5.1 %collective-permute-start.36 = (bf16[256,128]{1,0:T(8,128)(2,1)S(1)}, bf16[256,128]{1,0:T(8,128)(2,1)S(1)}, u32[]{:S(2)}, u32[]{:S(2)}) collective-permute-start(bf16[256,128]{1,0:T(8,128)(2,1)S(1)} %halo.7.refs_0_), channel_id=1, source_target_pairs={{0,1},{1,0},{2,3},{3,2},{4,5},{5,4},{6,7},{7,6},{8,9},{9,8},{10,11... | collective-permute-start | bytes 196616 | tf_op jit(solution)/shard_map/ppermute | solution.py:549
  81.4 4.1 %collective-permute-start.35 = (bf16[256,128]{1,0:T(8,128)(2,1)S(1)}, bf16[256,128]{1,0:T(8,128)(2,1)S(1)}, u32[]{:S(2)}, u32[]{:S(2)}) collective-permute-start(bf16[256,128]{1,0:T(8,128)(2,1)S(1)} %collective-permute-done.34.refs_0_), channel_id=1, source_target_pairs={{0,1},{1,0},{2,3},{3,2},{4,5},{5,4},{6,7},{7,6},{8,9},{9,8},{10,11... | collective-permute-start | bytes 196616 | tf_op jit(solution)/shard_map/ppermute | solution.py:549
  82.3 3.6 %collective-permute-start.31 = (bf16[256,128]{1,0:T(8,128)(2,1)S(1)}, bf16[256,128]{1,0:T(8,128)(2,1)S(1)}, u32[]{:S(2)}, u32[]{:S(2)}) collective-permute-start(bf16[256,128]{1,0:T(8,128)(2,1)S(1)} %halo.6.refs_0_), channel_id=1, source_target_pairs={{0,1},{1,0},{2,3},{3,2},{4,5},{5,4},{6,7},{7,6},{8,9},{9,8},{10,11... | collective-permute-start | bytes 196616 | tf_op jit(solution)/shard_map/ppermute | solution.py:549
  82.3 4.0 %collective-permute-start.30 = (bf16[256,128]{1,0:T(8,128)(2,1)S(1)}, bf16[256,128]{1,0:T(8,128)(2,1)S(1)}, u32[]{:S(2)}, u32[]{:S(2)}) collective-permute-start(bf16[256,128]{1,0:T(8,128)(2,1)S(1)} %collective-permute-done.29.refs_0_), channel_id=1, source_target_pairs={{0,1},{1,0},{2,3},{3,2},{4,5},{5,4},{6,7},{7,6},{8,9},{9,8},{10,11... | collective-permute-start | bytes 196616 | tf_op jit(solution)/shard_map/ppermute | solution.py:549

commit v6 on v3

--- a/solution.py
+++ b/solution.py
@@ -14,6 +14,7 @@
 COL_SPAN = 16
 LAYERS = 3
 HALF = ROW_SPAN // 2
+PARTS = ((2, 1, 1), (2, 2))
 
 EPS = 1e-06
 NEG = -1e30
@@ -146,6 +147,7 @@
         scratch_shapes=scratch,
         cost_estimate=cost(flops, parts_n * width * (channels * 6 + tok * 2) + 4 * tok * channels),
         compiler_params=PARAMS,
+        name="project",
     )(*operands)
 
 
@@ -187,6 +189,7 @@
             2 * tok * width * cols * parts_n, parts_n * width * (cols + tok) * 2 + tok * cols * 6
         ),
         compiler_params=PARAMS,
+        name="emit",
     )(*parts, weight if first else in_vmem(weight), base if first else in_vmem(base))
 
 
@@ -214,29 +217,27 @@
     )(*arrays)
 
 
-def load_weights(weights, layer):
-    _, channels, full = weights[0].shape
-
-    def pick(sources, targets):
-        return [(source.at[layer], targets[0].at[kind]) for kind, source in enumerate(sources)]
-
-    return fetch(weights, [(3, channels, full)], pick, 3)[0]
-
-
-def cut_weight(weight, layer):
+def cut_weight(weight):
     _, rows, cols = weight.shape
-    half = rows // 2
-    widths = (cols // 2, cols // 4, cols // 4)
+    half, unit = rows // 2, cols // 4
+    slabs = []
+    for layer, parts in enumerate(PARTS):
+        first = 0
+        for part in parts:
+            slabs.append((layer, first * unit, part * unit))
+            first += part
 
     def pick(sources, targets):
         here = pl.ds(pl.multiple_of(lax.axis_index("grp") * half, half), half)
-        firsts = (0, cols // 2, 3 * cols // 4)
         return [
             (sources[0].at[layer, here, pl.ds(first, width)], target)
-            for first, width, target in zip(firsts, widths, targets)
+            for (layer, first, width), target in zip(slabs, targets)
         ]
 
-    return fetch([weight], [(half, width) for width in widths], pick, 3)
+    cuts = fetch([weight], [(half, width) for _, _, width in slabs], pick, len(slabs))
+    return [
+        [cut for cut, slab in zip(cuts, slabs) if slab[0] == layer] for layer in range(len(PARTS))
+    ]
 
 
 def far_kernel(pieces, own_ref, beside_ref, across_ref, corner_ref, base_ref, *refs):
@@ -323,7 +324,7 @@
         scratch_shapes=[pltpu.VMEM((heads_n, 2 * ROW_SPAN, LANES), F32)],
         cost_estimate=cost(heads_n * spans * GRID_W * LANES * 40, heads_n * spans * GRID_W * LANES * 4),
         compiler_params=PARAMS,
-        name="expand_bias",
+        name="bias",
     )(table)
 
 
@@ -336,7 +337,18 @@
     )
 
 
-def own_kernel(rows_dev, query_ref, pair_ref, bias_ref, mixed_ref, peak_ref):
+def own_kernel(rows_dev, layer, query_ref, pair_ref, bias_ref, *refs):
+    if layer is None:
+        mixed_ref, peak_ref = refs
+        copies = []
+    else:
+        *stored, mixed_ref, peak_ref, held_ref, sems = refs
+        copies = [
+            pltpu.make_async_copy(source.at[layer], held_ref.at[kind], sems.at[kind])
+            for kind, source in enumerate(stored)
+        ]
+    for copy in copies:
+        copy.start()
     channels = query_ref.shape[2]
     group = min(LANES, channels)
     heads_in = group // HEAD_DIM
@@ -371,24 +383,34 @@
             lifted = jnp.concatenate([jnp.exp(piece - peak).astype(BF16) for piece in pieces], axis=1)
             mixed_ref[pair, here, :] = jnp.dot(lifted, values, preferred_element_type=F32)
             peak_ref[pair, here, :] = jnp.broadcast_to(peak, (stack, LANES))
-
-
-def attend_own(query, pair, bias, rows_dev):
+    for copy in copies:
+        copy.wait()
+
+
+def attend_own(query, pair, bias, rows_dev, weights, layer):
     _, tok, channels = query.shape
     group = min(LANES, channels)
     pairs, rows = channels // group, tok * (group // HEAD_DIM)
-    return pl.pallas_call(
-        partial(own_kernel, rows_dev),
-        out_shape=[
-            pltpu.VMEM((pairs, rows, group + LANES), F32),
-            pltpu.VMEM((pairs, rows, LANES), F32),
-        ],
-        in_specs=[VMEM] * 3,
-        out_specs=[VMEM] * 2,
+    out_shape = [
+        pltpu.VMEM((pairs, rows, group + LANES), F32),
+        pltpu.VMEM((pairs, rows, LANES), F32),
+    ]
+    scratch = []
+    if layer is not None:
+        out_shape.append(pltpu.VMEM((3, *weights[0].shape[1:]), BF16))
+        scratch.append(pltpu.SemaphoreType.DMA((3,)))
+    else:
+        weights = []
+    return pl.pallas_call(
+        partial(own_kernel, rows_dev, layer),
+        out_shape=out_shape,
+        in_specs=[VMEM] * 3 + [HBM] * len(weights),
+        out_specs=[VMEM] * len(out_shape),
+        scratch_shapes=scratch,
         cost_estimate=cost(pairs * rows * tok * 800, bias.size * 4, pairs * rows * tok),
         compiler_params=PARAMS,
-        name="attend_own",
-    )(*map(in_vmem, (query, pair, bias)))
+        name="own",
+    )(*map(in_vmem, (query, pair, bias)), *weights)
 
 
 def halo_kernel(
@@ -449,7 +471,7 @@
         scratch_shapes=[pltpu.VMEM((ROW_SPAN * GRID_W, channels), BF16)] * 2,
         cost_estimate=cost(scores * HEAD_DIM * 6, bias.size * 4 + tok * channels * 16, scores),
         compiler_params=PARAMS,
-        name="attend_halo",
+        name="halo",
     )(*map(in_vmem, (query, even, odd, bias, mixed, peak)))
 
 
@@ -539,10 +561,9 @@
     return lax.ppermute(block, axis, [(at, at ^ bit) for at in range(count)])
 
 
-def send_weight(weight, layer):
-    cuts = cut_weight(weight, layer)
+def send_weight(cuts, layer):
     near = []
-    for cut in cuts:
+    for cut in cuts[layer]:
         near.append(flip(cut, "tp", 2))
     return near
 
@@ -559,12 +580,12 @@
     even_pairs = [(at, at + 1) for at in range(0, sp - 1, 2)]
     odd_pairs = [(at, at + 1) for at in range(1, sp - 1, 2)]
     stream = hidden_in
-    lend = split and tp == 4 and lax.axis_size("grp") == 2
+    lend = split and tp == 4 and lax.axis_size("grp") == 2 and len(PARTS) == LAYERS - 1
     carry = None
     for layer in range(LAYERS):
         step = partial(project, layer=layer, gain=norm_gain)
         if carry is not None:
-            parts, base, held = carry
+            parts, base, last_lent, held = carry
             beside = flip(stream, "tp", 1)
             across = emit_far(parts, base, *last_lent)
             corner = flip(across, "tp", 1)
@@ -587,7 +608,8 @@
             query, pair = carried[0][:1], carried[0][1:]
         if lend and layer < LAYERS - 1:
             if layer == 0:
-                near = send_weight(output_weight, layer)
+                cuts = cut_weight(output_weight)
+                near = send_weight(cuts, layer)
             side = []
             for piece in near:
                 side.append(flip(piece, "grp", 1))
@@ -604,7 +626,9 @@
         odd = exchange(to_odd, odd_pairs)
         bias, *halo_bias = expand_bias(offset_bias, layer, rows_dev if split else 0)
         if split:
-            mixed, peak = attend_own(query, pair, bias, rows_dev)
+            mixed, peak, *held_next = attend_own(
+                query, pair, bias, rows_dev, weights, layer + 1 if lent else None
+            )
             attended = attend_halo(
                 query, even, odd, halo_bias[0], mixed, peak, rows_dev
             )
@@ -612,22 +636,19 @@
             attended = attend(query, pair, even, odd, bias, rows_dev)
         step = partial(emit, layer=layer)
         carry = None
-        if lent:
-            last_lent = lent
-            carry = load_weights(weights, layer + 1)
         if tp == 4:
             across = flip(attended, "tp", 2)
             beside = flip(attended, "tp", 1)
             corner = flip(across, "tp", 1)
             if lent and layer + 1 < LAYERS - 1:
-                near = send_weight(output_weight, layer + 1)
+                near = send_weight(cuts, layer + 1)
             partly, held = step([attended], (0,), output_weight, stream, F32, True)
             (partly,) = step([beside], (1,), held, partly, F32, False)
             (partly,) = step([across], (2,), held, partly, F32, False)
             old = across_stream
             (stream,) = step([corner], (3,), held, partly, BF16, False)
-            if carry is not None:
-                carry = ([attended, beside, across, corner], old, carry)
+            if lent:
+                carry = ([attended, beside, across, corner], old, lent, held_next[0])
         else:
             gathered = lax.all_gather(attended, "tp", axis=1, tiled=True)
             stream, _ = step([gathered], (None,), output_weight, stream, BF16, True)

time: 94.3 us -> 88.2 us (0.935)
  starting transfers between devices: 38.5 us -> 36.2 us
  waiting for transfers between devices: 23.6 us -> 21.5 us
  Pallas kernels: 28.6 us -> 27 us
    pallas_call x4 -> x1, Pallas kernels: 5.91 us -> 1.28 us  [fetch(): pl.pallas_call(partial(fetch_kernel, pick, len(arrays)), out_shape=[pltpu...]
    ppermute x6, waiting for transfers between devices: 13.6 us -> 9.22 us  [exchange(): return lax.ppermute(block, ('sp', 'tp'), moves)]
    pallas_call x3, Pallas kernels: 1.87 us -> 5.24 us  [attend_own(): pl.pallas_call(partial(own_kernel, rows_dev, layer), out_shape=out_shape,...]
    ppermute x28 -> x26, starting transfers between devices: 35.3 us -> 32.3 us  [flip(): return lax.ppermute(block, axis, [(at, at ^ bit) for at in range(count)])]
    ppermute x28 -> x26, waiting for transfers between devices: 9.98 us -> 12.3 us  [flip(): return lax.ppermute(block, axis, [(at, at ^ bit) for at in range(count)])]
  transfers between devices with their start and end apart: 34 -> 32, of which waited for: 10 -> 11; matrix products, arithmetic and copies ran while one was open for 0% -> 0% of each run, Pallas kernels for 28% -> 28%
where the time goes in v6:
time: 88.2 us; the launch traced here: 86.8 us
  starting transfers between devices  36.2 us (41%)
  Pallas kernels  27 us (31%)
  waiting for transfers between devices  21.5 us (24%)
  local copies, waits for them, and re-layouts  1.73 us (2%)
    ppermute x26, starting transfers between devices, flip(): return lax.ppermute(block, axis, [(at, at ^ bit) for at in range(count)])  32.3 us
    ppermute x26, waiting for transfers between devices, flip(): return lax.ppermute(block, axis, [(at, at ^ bit) for at in range(count)])  12.3 us
    ppermute x6, waiting for transfers between devices, exchange(): return lax.ppermute(block, ('sp', 'tp'), moves)  9.22 us
    pallas_call x13, Pallas kernels, project(): pl.pallas_call(partial(project_kernel, bits, load, first, kinds, layer),...  7.36 us
    pallas_call x12, Pallas kernels, emit(): pl.pallas_call(partial(emit_kernel, bits, first, layer), out_shape=out_sh...  7.19 us
    pallas_call x3, Pallas kernels, attend_own(): pl.pallas_call(partial(own_kernel, rows_dev, layer), out_shape=out_shape,...  5.24 us
    ppermute x6, starting transfers between devices, exchange(): return lax.ppermute(block, ('sp', 'tp'), moves)  3.93 us
    pallas_call x3, Pallas kernels, expand_bias(): pl.pallas_call(partial(bias_kernel, layer, lax.axis_size('sp')), out_shap...  2.82 us
  transfers between devices with their start and end apart: 32, of which 11 were waited for; matrix products, arithmetic and copies ran while one was open for 0% of the time, Pallas kernels for 28%

profile of v6, /device:TPU:19, one launch (start us, length us, event | category | flops | bytes accessed | tf_op | source)
XLA Modules:
  0.0 86.8 jit_solution(7254552246661547296)
XLA Ops:
  0.3 1.0 %collective-permute-start.2 = (bf16[256,512]{1,0:T(8,128)(2,1)}, bf16[256,512]{1,0:T(8,128)(2,1)S(1)}, u32[]{:S(2)}, u32[]{:S(2)}) collective-permute-start(bf16[256,512]{1,0:T(8,128)(2,1)} %refs_2_.8), channel_id=1, source_target_pairs={{0,1},{1,0},{2,3},{3,2},{4,5},{5,4},{6,7},{7,6},{8,9},{9,8},{10,11... | collective-permute-start | bytes 786440 | tf_op jit(solution)/shard_map/ppermute | solution.py:561
  1.2 6.2 %collective-permute-done.refs_0_.base_ref = bf16[256,512]{1,0:T(8,128)(2,1)S(1)} collective-permute-done((bf16[256,512]{1,0:T(8,128)(2,1)}, bf16[256,512]{1,0:T(8,128)(2,1)S(1)}, u32[]{:S(2)}, u32[]{:S(2)}) %collective-permute-start) | collective-permute-done | bytes 262176 | tf_op jit(solution)/shard_map/ppermute | solution.py:561
  7.4 1.5 %collective-permute-start.1 = (bf16[256,512]{1,0:T(8,128)(2,1)S(1)}, bf16[256,512]{1,0:T(8,128)(2,1)S(1)}, u32[]{:S(2)}, u32[]{:S(2)}) collective-permute-start(bf16[256,512]{1,0:T(8,128)(2,1)S(1)} %collective-permute-done.refs_0_.base_ref), channel_id=1, source_target_pairs={{0,1},{1,0},{2,3},{3,2},{4,5},{5,4},{6,7},{7,6},{8,9},{9,8},{10,11... | collective-permute-start | bytes 786440 | tf_op jit(solution)/shard_map/ppermute | solution.py:561
  8.9 0.8 copy-done
  9.7 0.9 %copy-done.2 = bf16[256,512]{1,0:T(8,128)(2,1)S(1)} copy-done((bf16[256,512]{1,0:T(8,128)(2,1)S(1)}, bf16[256,512]{1,0:T(8,128)(2,1)}, u32[]{:S(2)}) %copy-start.2) | copy-done | bytes 262168
  10.6 2.2 %project.13 = (f32[3,256,256]{2,1,0:T(8,128)S(1)}, f32[256,128]{1,0:T(8,128)S(1)}, bf16[3,256,2048]{2,1,0:T(8,128)(2,1)S(1)}) custom-call(bf16[256,512]{1,0:T(8,128)(2,1)S(1)} %copy-done.2, f32[3,2048]{1,0:T(4,128)S(1)} %copy-done, bf16[3,256,2048]{2,1,0:T(8,128)(2,1)} %refs_0_.7, bf16[3,256,2048]{2,1,0:T(8,128)(2,1)} %refs_1_.26, bf16[3,256,2048]{2,1,0:T(8,128)(2,1)} %refs_2_.10), custom_call_target="tpu_custom_call" | custom-call | flops 201326592 | bytes 1310720 | tf_op jit(solution)/shard_map/project/pallas_call | solution.py:142
  14.3 1.4 %collective-permute-start.3 = (bf16[2,256,256]{2,1,0:T(8,128)(2,1)S(1)}, bf16[2,256,256]{2,1,0:T(8,128)(2,1)S(1)}, u32[]{:S(2)}, u32[]{:S(2)}) collective-permute-start(bf16[2,256,256]{2,1,0:T(8,128)(2,1)S(1)} %project.17.pair_ref), channel_id=1, source_target_pairs={{0,4},{1,5},{2,6},{3,7},{4,0},{5,1},{6,2},{7,3},{8,12},{9,13},{10,... | collective-permute-start | bytes 786440 | tf_op jit(solution)/shard_map/ppermute | solution.py:556
  15.6 1.3 %shard_map.73 = (bf16[512,256]{1,0:T(8,128)(2,1)S(1)}, bf16[512,128]{1,0:T(8,128)(2,1)S(1)}, bf16[512,128]{1,0:T(8,128)(2,1)S(1)}, bf16[512,256]{1,0:T(8,128)(2,1)S(1)}, bf16[512,256]{1,0:T(8,128)(2,1)S(1)}) custom-call(bf16[3,1024,512]{2,1,0:T(8,128)(2,1)} %refs_1_.31), custom_call_target="tpu_custom_call" | custom-call | flops 1000000 | bytes 1000000 | tf_op jit(solution)/shard_map/pallas_call | solution.py:209
  17.3 0.9 %bias.3 = (f32[4,14,64,128]{3,2,1,0:T(8,128)S(1)}, f32[4,4,2,64,128]{4,3,2,1,0:T(8,128)S(1)}) custom-call(f32[3,4,15,31]{3,2,1,0:T(8,128)S(1)} %copy.8.table_ref), custom_call_target="tpu_custom_call" | custom-call | flops 18350080 | bytes 1835008 | tf_op jit(solution)/shard_map/bias/pallas_call | solution.py:319
  18.5 2.3 %own.3 = (f32[2,512,256]{2,1,0:T(8,128)S(1)}, f32[2,512,128]{2,1,0:T(8,128)S(1)}, bf16[3,256,2048]{2,1,0:T(8,128)(2,1)S(1)}) custom-call(bf16[1,256,256]{2,1,0:T(8,128)(2,1)S(1)} %project.16.query_ref, bf16[2,256,256]{2,1,0:T(8,128)(2,1)S(1)} %project.17.pair_ref, f32[4,14,64,128]{3,2,1,0:T(8,128)S(1)} %get-tuple-element.53.bias_ref, ...), custom_call_target="tpu_custom_call" | custom-call | flops 209715200 | bytes 1835008 | tf_op jit(solution)/shard_map/own/pallas_call | solution.py:404
  20.8 1.3 %collective-permute-done.3.even_ref = bf16[2,256,256]{2,1,0:T(8,128)(2,1)S(1)} collective-permute-done((bf16[2,256,256]{2,1,0:T(8,128)(2,1)S(1)}, bf16[2,256,256]{2,1,0:T(8,128)(2,1)S(1)}, u32[]{:S(2)}, u32[]{:S(2)}) %collective-permute-start.3) | collective-permute-done | bytes 262176 | tf_op jit(solution)/shard_map/ppermute | solution.py:556
  22.2 1.0 %collective-permute-done.4.odd_ref = bf16[2,256,256]{2,1,0:T(8,128)(2,1)S(1)} collective-permute-done((bf16[2,256,256]{2,1,0:T(8,128)(2,1)S(1)}, bf16[2,256,256]{2,1,0:T(8,128)(2,1)S(1)}, u32[]{:S(2)}, u32[]{:S(2)}) %collective-permute-start.4) | collective-permute-done | bytes 262176 | tf_op jit(solution)/shard_map/ppermute | solution.py:556
  23.2 0.7 halo.3.own_ref.refs_0_
  24.2 1.2 %collective-permute-start.9 = (bf16[512,128]{1,0:T(8,128)(2,1)S(1)}, bf16[512,128]{1,0:T(8,128)(2,1)S(1)}, u32[]{:S(2)}, u32[]{:S(2)}) collective-permute-start(bf16[512,128]{1,0:T(8,128)(2,1)S(1)} %get-tuple-element.57), channel_id=1, source_target_pairs={{0,2},{1,3},{2,0},{3,1},{4,6},{5,7},{6,4},{7,5},{8,10},{9,11},{10,... | collective-permute-start | bytes 393224 | tf_op jit(solution)/shard_map/ppermute | solution.py:561
  25.7 1.2 %collective-permute-start.11 = (bf16[512,256]{1,0:T(8,128)(2,1)S(1)}, bf16[512,256]{1,0:T(8,128)(2,1)S(1)}, u32[]{:S(2)}, u32[]{:S(2)}) collective-permute-start(bf16[512,256]{1,0:T(8,128)(2,1)S(1)} %collective-permute-done.8.refs_0_), channel_id=1, source_target_pairs={{0,16},{16,0},{1,17},{17,1},{2,18},{18,2},{3,19},{19,3},{4,20},{20... | collective-permute-start | bytes 786440 | tf_op jit(solution)/shard_map/ppermute | solution.py:561
  26.9 2.3 %collective-permute-start.5 = (bf16[256,256]{1,0:T(8,128)(2,1)S(1)}, bf16[256,256]{1,0:T(8,128)(2,1)S(1)}, u32[]{:S(2)}, u32[]{:S(2)}) collective-permute-start(bf16[256,256]{1,0:T(8,128)(2,1)S(1)} %halo.3.own_ref.refs_0_), channel_id=1, source_target_pairs={{0,1},{1,0},{2,3},{3,2},{4,5},{5,4},{6,7},{7,6},{8,9},{9,8},{10,11... | collective-permute-start | bytes 393224 | tf_op jit(solution)/shard_map/ppermute | solution.py:561
  29.2 2.3 %collective-permute-start.7 = (bf16[256,256]{1,0:T(8,128)(2,1)S(1)}, bf16[256,256]{1,0:T(8,128)(2,1)S(1)}, u32[]{:S(2)}, u32[]{:S(2)}) collective-permute-start(bf16[256,256]{1,0:T(8,128)(2,1)S(1)} %collective-permute-done.6.across_ref.refs_0_), channel_id=1, source_target_pairs={{0,1},{1,0},{2,3},{3,2},{4,5},{5,4},{6,7},{7,6},{8,9},{9,8},{10,11... | collective-permute-start | bytes 393224 | tf_op jit(solution)/shard_map/ppermute | solution.py:561
  31.5 1.2 %collective-permute-start.12 = (bf16[512,128]{1,0:T(8,128)(2,1)S(1)}, bf16[512,128]{1,0:T(8,128)(2,1)S(1)}, u32[]{:S(2)}, u32[]{:S(2)}) collective-permute-start(bf16[512,128]{1,0:T(8,128)(2,1)S(1)} %collective-permute-done.9.refs_1_), channel_id=1, source_target_pairs={{0,16},{16,0},{1,17},{17,1},{2,18},{18,2},{3,19},{19,3},{4,20},{20... | collective-permute-start | bytes 393224 | tf_op jit(solution)/shard_map/ppermute | solution.py:561
  32.7 0.8 collective-permute-done.10.refs_2_
  33.5 1.2 %collective-permute-start.13 = (bf16[512,128]{1,0:T(8,128)(2,1)S(1)}, bf16[512,128]{1,0:T(8,128)(2,1)S(1)}, u32[]{:S(2)}, u32[]{:S(2)}) collective-permute-start(bf16[512,128]{1,0:T(8,128)(2,1)S(1)} %collective-permute-done.10.refs_2_), channel_id=1, source_target_pairs={{0,16},{16,0},{1,17},{17,1},{2,18},{18,2},{3,19},{19,3},{4,20},{20... | collective-permute-start | bytes 393224 | tf_op jit(solution)/shard_map/ppermute | solution.py:561
  34.7 1.5 %emit.12 = (f32[256,512]{1,0:T(8,128)S(1)}, bf16[1024,512]{1,0:T(8,128)(2,1)S(1)}) custom-call(bf16[256,256]{1,0:T(8,128)(2,1)S(1)} %halo.3.own_ref.refs_0_, bf16[3,1024,512]{2,1,0:T(8,128)(2,1)} %refs_1_.31, bf16[256,512]{1,0:T(8,128)(2,1)S(1)} %copy-done.3), custom_call_target="tpu_custom_call" | custom-call | flops 67108864 | bytes 1179648 | tf_op jit(solution)/shard_map/emit/pallas_call | solution.py:182
  36.9 2.3 %collective-permute-start.15 = (bf16[256,512]{1,0:T(8,128)(2,1)S(1)}, bf16[256,512]{1,0:T(8,128)(2,1)S(1)}, u32[]{:S(2)}, u32[]{:S(2)}) collective-permute-start(bf16[256,512]{1,0:T(8,128)(2,1)S(1)} %emit.15.refs_0_.refs_2_), channel_id=1, source_target_pairs={{0,1},{1,0},{2,3},{3,2},{4,5},{5,4},{6,7},{7,6},{8,9},{9,8},{10,11... | collective-permute-start | bytes 786440 | tf_op jit(solution)/shard_map/ppermute | solution.py:561
  39.9 1.6 %collective-permute-start.14 = (bf16[256,512]{1,0:T(8,128)(2,1)S(1)}, bf16[256,512]{1,0:T(8,128)(2,1)S(1)}, u32[]{:S(2)}, u32[]{:S(2)}) collective-permute-start(bf16[256,512]{1,0:T(8,128)(2,1)S(1)} %lent.2.refs_1_.base_ref), channel_id=1, source_target_pairs={{0,1},{1,0},{2,3},{3,2},{4,5},{5,4},{6,7},{7,6},{8,9},{9,8},{10,11... | collective-permute-start | bytes 786440 | tf_op jit(solution)/shard_map/ppermute | solution.py:561
  41.5 0.6 project.18
  43.0 0.6 collective-permute-start.16
  43.9 1.3 %collective-permute-start.22 = (bf16[512,256]{1,0:T(8,128)(2,1)S(1)}, bf16[512,256]{1,0:T(8,128)(2,1)S(1)}, u32[]{:S(2)}, u32[]{:S(2)}) collective-permute-start(bf16[512,256]{1,0:T(8,128)(2,1)S(1)} %get-tuple-element.71), channel_id=1, source_target_pairs={{0,2},{1,3},{2,0},{3,1},{4,6},{5,7},{6,4},{7,5},{8,10},{9,11},{10,... | collective-permute-start | bytes 786440 | tf_op jit(solution)/shard_map/ppermute | solution.py:561
  45.2 0.9 %bias.4 = (f32[4,14,64,128]{3,2,1,0:T(8,128)S(1)}, f32[4,4,2,64,128]{4,3,2,1,0:T(8,128)S(1)}) custom-call(f32[3,4,15,31]{3,2,1,0:T(8,128)S(1)} %copy.8.table_ref), custom_call_target="tpu_custom_call" | custom-call | flops 18350080 | bytes 1835008 | tf_op jit(solution)/shard_map/bias/pallas_call | solution.py:319
  46.4 2.3 %own.4 = (f32[2,512,256]{2,1,0:T(8,128)S(1)}, f32[2,512,128]{2,1,0:T(8,128)S(1)}, bf16[3,256,2048]{2,1,0:T(8,128)(2,1)S(1)}) custom-call(bf16[1,256,256]{2,1,0:T(8,128)(2,1)S(1)} %project.20.query_ref, bf16[2,256,256]{2,1,0:T(8,128)(2,1)S(1)} %project.21.pair_ref, f32[4,14,64,128]{3,2,1,0:T(8,128)S(1)} %get-tuple-element.67.bias_ref, ...), custom_call_target="tpu_custom_call" | custom-call | flops 209715200 | bytes 1835008 | tf_op jit(solution)/shard_map/own/pallas_call | solution.py:404
  48.7 1.8 %collective-permute-done.16.even_ref = bf16[2,256,256]{2,1,0:T(8,128)(2,1)S(1)} collective-permute-done((bf16[2,256,256]{2,1,0:T(8,128)(2,1)S(1)}, bf16[2,256,256]{2,1,0:T(8,128)(2,1)S(1)}, u32[]{:S(2)}, u32[]{:S(2)}) %collective-permute-start.16) | collective-permute-done | bytes 262176 | tf_op jit(solution)/shard_map/ppermute | solution.py:556
  50.8 0.7 halo.4.own_ref.refs_0_
  51.8 1.2 %collective-permute-start.23 = (bf16[512,256]{1,0:T(8,128)(2,1)S(1)}, bf16[512,256]{1,0:T(8,128)(2,1)S(1)}, u32[]{:S(2)}, u32[]{:S(2)}) collective-permute-start(bf16[512,256]{1,0:T(8,128)(2,1)S(1)} %collective-permute-done.21.refs_0_), channel_id=1, source_target_pairs={{0,16},{16,0},{1,17},{17,1},{2,18},{18,2},{3,19},{19,3},{4,20},{20... | collective-permute-start | bytes 786440 | tf_op jit(solution)/shard_map/ppermute | solution.py:561
  53.0 3.5 %collective-permute-done.22.refs_1_ = bf16[512,256]{1,0:T(8,128)(2,1)S(1)} collective-permute-done((bf16[512,256]{1,0:T(8,128)(2,1)S(1)}, bf16[512,256]{1,0:T(8,128)(2,1)S(1)}, u32[]{:S(2)}, u32[]{:S(2)}) %collective-permute-start.22) | collective-permute-done | bytes 262176 | tf_op jit(solution)/shard_map/ppermute | solution.py:561
  56.5 1.2 %collective-permute-start.24 = (bf16[512,256]{1,0:T(8,128)(2,1)S(1)}, bf16[512,256]{1,0:T(8,128)(2,1)S(1)}, u32[]{:S(2)}, u32[]{:S(2)}) collective-permute-start(bf16[512,256]{1,0:T(8,128)(2,1)S(1)} %collective-permute-done.22.refs_1_), channel_id=1, source_target_pairs={{0,16},{16,0},{1,17},{17,1},{2,18},{18,2},{3,19},{19,3},{4,20},{20... | collective-permute-start | bytes 786440 | tf_op jit(solution)/shard_map/ppermute | solution.py:561
  57.7 2.9 %collective-permute-start.18 = (bf16[256,256]{1,0:T(8,128)(2,1)S(1)}, bf16[256,256]{1,0:T(8,128)(2,1)S(1)}, u32[]{:S(2)}, u32[]{:S(2)}) collective-permute-start(bf16[256,256]{1,0:T(8,128)(2,1)S(1)} %halo.4.own_ref.refs_0_), channel_id=1, source_target_pairs={{0,1},{1,0},{2,3},{3,2},{4,5},{5,4},{6,7},{7,6},{8,9},{9,8},{10,11... | collective-permute-start | bytes 393224 | tf_op jit(solution)/shard_map/ppermute | solution.py:561
  60.8 1.5 %emit.16 = (f32[256,512]{1,0:T(8,128)S(1)}, bf16[1024,512]{1,0:T(8,128)(2,1)S(1)}) custom-call(bf16[256,256]{1,0:T(8,128)(2,1)S(1)} %halo.4.own_ref.refs_0_, bf16[3,1024,512]{2,1,0:T(8,128)(2,1)} %refs_1_.31, bf16[256,512]{1,0:T(8,128)(2,1)S(1)} %emit.15.refs_0_.refs_2_), custom_call_target="tpu_custom_call" | custom-call | flops 67108864 | bytes 1179648 | tf_op jit(solution)/shard_map/emit/pallas_call | solution.py:182
  64.0 2.7 %collective-permute-start.25 = (bf16[256,512]{1,0:T(8,128)(2,1)S(1)}, bf16[256,512]{1,0:T(8,128)(2,1)S(1)}, u32[]{:S(2)}, u32[]{:S(2)}) collective-permute-start(bf16[256,512]{1,0:T(8,128)(2,1)S(1)} %lent.3.refs_1_), channel_id=1, source_target_pairs={{0,1},{1,0},{2,3},{3,2},{4,5},{5,4},{6,7},{7,6},{8,9},{9,8},{10,11... | collective-permute-start | bytes 786440 | tf_op jit(solution)/shard_map/ppermute | solution.py:561
  66.7 0.6 project.22
  68.2 1.3 %collective-permute-start.27 = (bf16[2,256,256]{2,1,0:T(8,128)(2,1)S(1)}, bf16[2,256,256]{2,1,0:T(8,128)(2,1)S(1)}, u32[]{:S(2)}, u32[]{:S(2)}) collective-permute-start(bf16[2,256,256]{2,1,0:T(8,128)(2,1)S(1)} %project.25.pair_ref), channel_id=1, source_target_pairs={{0,4},{1,5},{2,6},{3,7},{4,0},{5,1},{6,2},{7,3},{8,12},{9,13},{10,... | collective-permute-start | bytes 786440 | tf_op jit(solution)/shard_map/ppermute | solution.py:556
  70.0 0.9 %bias.5 = (f32[4,14,64,128]{3,2,1,0:T(8,128)S(1)}, f32[4,4,2,64,128]{4,3,2,1,0:T(8,128)S(1)}) custom-call(f32[3,4,15,31]{3,2,1,0:T(8,128)S(1)} %copy.8.table_ref), custom_call_target="tpu_custom_call" | custom-call | flops 18350080 | bytes 1835008 | tf_op jit(solution)/shard_map/bias/pallas_call | solution.py:319
  71.3 0.6 own.5
  71.9 3.8 %collective-permute-done.27.even_ref = bf16[2,256,256]{2,1,0:T(8,128)(2,1)S(1)} collective-permute-done((bf16[2,256,256]{2,1,0:T(8,128)(2,1)S(1)}, bf16[2,256,256]{2,1,0:T(8,128)(2,1)S(1)}, u32[]{:S(2)}, u32[]{:S(2)}) %collective-permute-start.27) | collective-permute-done | bytes 262176 | tf_op jit(solution)/shard_map/ppermute | solution.py:556
  75.7 1.0 %collective-permute-done.28.odd_ref = bf16[2,256,256]{2,1,0:T(8,128)(2,1)S(1)} collective-permute-done((bf16[2,256,256]{2,1,0:T(8,128)(2,1)S(1)}, bf16[2,256,256]{2,1,0:T(8,128)(2,1)S(1)}, u32[]{:S(2)}, u32[]{:S(2)}) %collective-permute-start.28) | collective-permute-done | bytes 262176 | tf_op jit(solution)/shard_map/ppermute | solution.py:556
  76.7 0.7 halo.5.refs_0_
  77.9 1.8 %collective-permute-start.31 = (bf16[256,256]{1,0:T(8,128)(2,1)S(1)}, bf16[256,256]{1,0:T(8,128)(2,1)S(1)}, u32[]{:S(2)}, u32[]{:S(2)}) collective-permute-start(bf16[256,256]{1,0:T(8,128)(2,1)S(1)} %halo.5.refs_0_), channel_id=1, source_target_pairs={{0,1},{1,0},{2,3},{3,2},{4,5},{5,4},{6,7},{7,6},{8,9},{9,8},{10,11... | collective-permute-start | bytes 393224 | tf_op jit(solution)/shard_map/ppermute | solution.py:561
  79.7 1.6 %collective-permute-done.29.refs_0_ = bf16[256,256]{1,0:T(8,128)(2,1)S(1)} collective-permute-done((bf16[256,256]{1,0:T(8,128)(2,1)S(1)}, bf16[256,256]{1,0:T(8,128)(2,1)S(1)}, u32[]{:S(2)}, u32[]{:S(2)}) %collective-permute-start.29) | collective-permute-done | bytes 131104 | tf_op jit(solution)/shard_map/ppermute | solution.py:561
  81.3 2.7 %collective-permute-start.30 = (bf16[256,256]{1,0:T(8,128)(2,1)S(1)}, bf16[256,256]{1,0:T(8,128)(2,1)S(1)}, u32[]{:S(2)}, u32[]{:S(2)}) collective-permute-start(bf16[256,256]{1,0:T(8,128)(2,1)S(1)} %collective-permute-done.29.refs_0_), channel_id=1, source_target_pairs={{0,1},{1,0},{2,3},{3,2},{4,5},{5,4},{6,7},{7,6},{8,9},{9,8},{10,11... | collective-permute-start | bytes 393224 | tf_op jit(solution)/shard_map/ppermute | solution.py:561
  83.9 1.5 %emit.20 = (f32[256,512]{1,0:T(8,128)S(1)}, bf16[1024,512]{1,0:T(8,128)(2,1)S(1)}) custom-call(bf16[256,256]{1,0:T(8,128)(2,1)S(1)} %halo.5.refs_0_, bf16[3,1024,512]{2,1,0:T(8,128)(2,1)} %refs_1_.31, bf16[256,512]{1,0:T(8,128)(2,1)S(1)} %emit.19.refs_0_.refs_2_), custom_call_target="tpu_custom_call" | custom-call | flops 67108864 | bytes 1179648 | tf_op jit(solution)/shard_map/emit/pallas_call | solution.py:182
  85.9 0.9 %emit.23 = bf16[256,512]{1,0:T(8,128)(2,1)} custom-call(bf16[256,256]{1,0:T(8,128)(2,1)S(1)} %collective-permute-done.30.refs_0_, bf16[1024,512]{1,0:T(8,128)(2,1)S(1)} %get-tuple-element.83.refs_1_, f32[256,512]{1,0:T(8,128)S(1)} %emit.22.refs_2_), custom_call_target="tpu_custom_call" | custom-call | flops 67108864 | bytes 1179648 | tf_op jit(solution)/shard_map/emit/pallas_call | solution.py:182
  (64 shorter events, 10.5 us)
Async XLA Ops:
  0.0 7.4 %collective-permute-start = (bf16[256,512]{1,0:T(8,128)(2,1)}, bf16[256,512]{1,0:T(8,128)(2,1)S(1)}, u32[]{:S(2)}, u32[]{:S(2)}) collective-permute-start(bf16[256,512]{1,0:T(8,128)(2,1)} %refs_2_.8), channel_id=1, source_target_pairs={{0,2},{1,3},{2,0},{3,1},{4,6},{5,7},{6,4},{7,5},{8,10},{9,11},{10,... | collective-permute-start | bytes 786440 | tf_op jit(solution)/shard_map/ppermute | solution.py:561
  0.3 12.6 %collective-permute-start.2 = (bf16[256,512]{1,0:T(8,128)(2,1)}, bf16[256,512]{1,0:T(8,128)(2,1)S(1)}, u32[]{:S(2)}, u32[]{:S(2)}) collective-permute-start(bf16[256,512]{1,0:T(8,128)(2,1)} %refs_2_.8), channel_id=1, source_target_pairs={{0,1},{1,0},{2,3},{3,2},{4,5},{5,4},{6,7},{7,6},{8,9},{9,8},{10,11... | collective-permute-start | bytes 786440 | tf_op jit(solution)/shard_map/ppermute | solution.py:561
  7.4 6.5 %collective-permute-start.1 = (bf16[256,512]{1,0:T(8,128)(2,1)S(1)}, bf16[256,512]{1,0:T(8,128)(2,1)S(1)}, u32[]{:S(2)}, u32[]{:S(2)}) collective-permute-start(bf16[256,512]{1,0:T(8,128)(2,1)S(1)} %collective-permute-done.refs_0_.base_ref), channel_id=1, source_target_pairs={{0,1},{1,0},{2,3},{3,2},{4,5},{5,4},{6,7},{7,6},{8,9},{9,8},{10,11... | collective-permute-start | bytes 786440 | tf_op jit(solution)/shard_map/ppermute | solution.py:561
  8.9 0.8 copy-start
  9.7 0.9 %copy-start.2 = (bf16[256,512]{1,0:T(8,128)(2,1)S(1)}, bf16[256,512]{1,0:T(8,128)(2,1)}, u32[]{:S(2)}) copy-start(bf16[256,512]{1,0:T(8,128)(2,1)} %refs_2_.8) | copy-start | bytes 786436
  10.6 2.3 %copy-start.1 = (f32[3,2048]{1,0:T(4,128)S(1)}, f32[3,2048]{1,0:T(4,128)}, u32[]{:S(2)}) copy-start(f32[3,2048]{1,0:T(4,128)} %refs_1_.30) | copy-start | bytes 73732
  13.9 3.4 %copy-start.4 = (f32[3,4,15,31]{3,1,2,0:T(4,128)S(1)}, f32[3,4,15,31]{3,1,2,0:T(4,128)}, u32[]{:S(2)}) copy-start(f32[3,4,15,31]{3,1,2,0:T(4,128)} %param.13) | copy-start | bytes 66964
  14.3 7.9 %collective-permute-start.3 = (bf16[2,256,256]{2,1,0:T(8,128)(2,1)S(1)}, bf16[2,256,256]{2,1,0:T(8,128)(2,1)S(1)}, u32[]{:S(2)}, u32[]{:S(2)}) collective-permute-start(bf16[2,256,256]{2,1,0:T(8,128)(2,1)S(1)} %project.17.pair_ref), channel_id=1, source_target_pairs={{0,4},{1,5},{2,6},{3,7},{4,0},{5,1},{6,2},{7,3},{8,12},{9,13},{10,... | collective-permute-start | bytes 786440 | tf_op jit(solution)/shard_map/ppermute | solution.py:556
  15.6 7.6 %collective-permute-start.4 = (bf16[2,256,256]{2,1,0:T(8,128)(2,1)S(1)}, bf16[2,256,256]{2,1,0:T(8,128)(2,1)S(1)}, u32[]{:S(2)}, u32[]{:S(2)}) collective-permute-start(bf16[2,256,256]{2,1,0:T(8,128)(2,1)S(1)} %project.17.pair_ref), channel_id=1, source_target_pairs={{0,1},{1,0},{2,3},{3,2},{4,8},{5,9},{6,10},{7,11},{8,4},{9,5},{10,... | collective-permute-start | bytes 786440 | tf_op jit(solution)/shard_map/ppermute | solution.py:556
  16.9 8.7 %collective-permute-start.8 = (bf16[512,256]{1,0:T(8,128)(2,1)S(1)}, bf16[512,256]{1,0:T(8,128)(2,1)S(1)}, u32[]{:S(2)}, u32[]{:S(2)}) collective-permute-start(bf16[512,256]{1,0:T(8,128)(2,1)S(1)} %get-tuple-element.56), channel_id=1, source_target_pairs={{0,2},{1,3},{2,0},{3,1},{4,6},{5,7},{6,4},{7,5},{8,10},{9,11},{10,... | collective-permute-start | bytes 786440 | tf_op jit(solution)/shard_map/ppermute | solution.py:561
  20.8 13.9 %copy-start.3 = (bf16[256,512]{1,0:T(8,128)(2,1)S(1)}, bf16[256,512]{1,0:T(8,128)(2,1)}, u32[]{:S(2)}) copy-start(bf16[256,512]{1,0:T(8,128)(2,1)} %refs_2_.8) | copy-start | bytes 786436
  23.9 5.3 %collective-permute-start.6 = (bf16[256,256]{1,0:T(8,128)(2,1)S(1)}, bf16[256,256]{1,0:T(8,128)(2,1)S(1)}, u32[]{:S(2)}, u32[]{:S(2)}) collective-permute-start(bf16[256,256]{1,0:T(8,128)(2,1)S(1)} %halo.3.own_ref.refs_0_), channel_id=1, source_target_pairs={{0,2},{1,3},{2,0},{3,1},{4,6},{5,7},{6,4},{7,5},{8,10},{9,11},{10,... | collective-permute-start | bytes 393224 | tf_op jit(solution)/shard_map/ppermute | solution.py:561
  24.2 7.3 %collective-permute-start.9 = (bf16[512,128]{1,0:T(8,128)(2,1)S(1)}, bf16[512,128]{1,0:T(8,128)(2,1)S(1)}, u32[]{:S(2)}, u32[]{:S(2)}) collective-permute-start(bf16[512,128]{1,0:T(8,128)(2,1)S(1)} %get-tuple-element.57), channel_id=1, source_target_pairs={{0,2},{1,3},{2,0},{3,1},{4,6},{5,7},{6,4},{7,5},{8,10},{9,11},{10,... | collective-permute-start | bytes 393224 | tf_op jit(solution)/shard_map/ppermute | solution.py:561
  25.4 8.1 %collective-permute-start.10 = (bf16[512,128]{1,0:T(8,128)(2,1)S(1)}, bf16[512,128]{1,0:T(8,128)(2,1)S(1)}, u32[]{:S(2)}, u32[]{:S(2)}) collective-permute-start(bf16[512,128]{1,0:T(8,128)(2,1)S(1)} %get-tuple-element.58), channel_id=1, source_target_pairs={{0,2},{1,3},{2,0},{3,1},{4,6},{5,7},{6,4},{7,5},{8,10},{9,11},{10,... | collective-permute-start | bytes 393224 | tf_op jit(solution)/shard_map/ppermute | solution.py:561
  25.7 13.6 %collective-permute-start.11 = (bf16[512,256]{1,0:T(8,128)(2,1)S(1)}, bf16[512,256]{1,0:T(8,128)(2,1)S(1)}, u32[]{:S(2)}, u32[]{:S(2)}) collective-permute-start(bf16[512,256]{1,0:T(8,128)(2,1)S(1)} %collective-permute-done.8.refs_0_), channel_id=1, source_target_pairs={{0,16},{16,0},{1,17},{17,1},{2,18},{18,2},{3,19},{19,3},{4,20},{20... | collective-permute-start | bytes 786440 | tf_op jit(solution)/shard_map/ppermute | solution.py:561
  26.9 9.3 %collective-permute-start.5 = (bf16[256,256]{1,0:T(8,128)(2,1)S(1)}, bf16[256,256]{1,0:T(8,128)(2,1)S(1)}, u32[]{:S(2)}, u32[]{:S(2)}) collective-permute-start(bf16[256,256]{1,0:T(8,128)(2,1)S(1)} %halo.3.own_ref.refs_0_), channel_id=1, source_target_pairs={{0,1},{1,0},{2,3},{3,2},{4,5},{5,4},{6,7},{7,6},{8,9},{9,8},{10,11... | collective-permute-start | bytes 393224 | tf_op jit(solution)/shard_map/ppermute | solution.py:561
  29.2 7.5 %collective-permute-start.7 = (bf16[256,256]{1,0:T(8,128)(2,1)S(1)}, bf16[256,256]{1,0:T(8,128)(2,1)S(1)}, u32[]{:S(2)}, u32[]{:S(2)}) collective-permute-start(bf16[256,256]{1,0:T(8,128)(2,1)S(1)} %collective-permute-done.6.across_ref.refs_0_), channel_id=1, source_target_pairs={{0,1},{1,0},{2,3},{3,2},{4,5},{5,4},{6,7},{7,6},{8,9},{9,8},{10,11... | collective-permute-start | bytes 393224 | tf_op jit(solution)/shard_map/ppermute | solution.py:561
  31.5 7.8 %collective-permute-start.12 = (bf16[512,128]{1,0:T(8,128)(2,1)S(1)}, bf16[512,128]{1,0:T(8,128)(2,1)S(1)}, u32[]{:S(2)}, u32[]{:S(2)}) collective-permute-start(bf16[512,128]{1,0:T(8,128)(2,1)S(1)} %collective-permute-done.9.refs_1_), channel_id=1, source_target_pairs={{0,16},{16,0},{1,17},{17,1},{2,18},{18,2},{3,19},{19,3},{4,20},{20... | collective-permute-start | bytes 393224 | tf_op jit(solution)/shard_map/ppermute | solution.py:561
  33.5 5.8 %collective-permute-start.13 = (bf16[512,128]{1,0:T(8,128)(2,1)S(1)}, bf16[512,128]{1,0:T(8,128)(2,1)S(1)}, u32[]{:S(2)}, u32[]{:S(2)}) collective-permute-start(bf16[512,128]{1,0:T(8,128)(2,1)S(1)} %collective-permute-done.10.refs_2_), channel_id=1, source_target_pairs={{0,16},{16,0},{1,17},{17,1},{2,18},{18,2},{3,19},{19,3},{4,20},{20... | collective-permute-start | bytes 393224 | tf_op jit(solution)/shard_map/ppermute | solution.py:561
  36.9 5.2 %collective-permute-start.15 = (bf16[256,512]{1,0:T(8,128)(2,1)S(1)}, bf16[256,512]{1,0:T(8,128)(2,1)S(1)}, u32[]{:S(2)}, u32[]{:S(2)}) collective-permute-start(bf16[256,512]{1,0:T(8,128)(2,1)S(1)} %emit.15.refs_0_.refs_2_), channel_id=1, source_target_pairs={{0,1},{1,0},{2,3},{3,2},{4,5},{5,4},{6,7},{7,6},{8,9},{9,8},{10,11... | collective-permute-start | bytes 786440 | tf_op jit(solution)/shard_map/ppermute | solution.py:561
  39.9 2.8 %collective-permute-start.14 = (bf16[256,512]{1,0:T(8,128)(2,1)S(1)}, bf16[256,512]{1,0:T(8,128)(2,1)S(1)}, u32[]{:S(2)}, u32[]{:S(2)}) collective-permute-start(bf16[256,512]{1,0:T(8,128)(2,1)S(1)} %lent.2.refs_1_.base_ref), channel_id=1, source_target_pairs={{0,1},{1,0},{2,3},{3,2},{4,5},{5,4},{6,7},{7,6},{8,9},{9,8},{10,11... | collective-permute-start | bytes 786440 | tf_op jit(solution)/shard_map/ppermute | solution.py:561
  43.0 7.5 %collective-permute-start.16 = (bf16[2,256,256]{2,1,0:T(8,128)(2,1)S(1)}, bf16[2,256,256]{2,1,0:T(8,128)(2,1)S(1)}, u32[]{:S(2)}, u32[]{:S(2)}) collective-permute-start(bf16[2,256,256]{2,1,0:T(8,128)(2,1)S(1)} %project.21.pair_ref), channel_id=1, source_target_pairs={{0,4},{1,5},{2,6},{3,7},{4,0},{5,1},{6,2},{7,3},{8,12},{9,13},{10,... | collective-permute-start | bytes 786440 | tf_op jit(solution)/shard_map/ppermute | solution.py:556
  43.6 7.2 %collective-permute-start.17 = (bf16[2,256,256]{2,1,0:T(8,128)(2,1)S(1)}, bf16[2,256,256]{2,1,0:T(8,128)(2,1)S(1)}, u32[]{:S(2)}, u32[]{:S(2)}) collective-permute-start(bf16[2,256,256]{2,1,0:T(8,128)(2,1)S(1)} %project.21.pair_ref), channel_id=1, source_target_pairs={{0,1},{1,0},{2,3},{3,2},{4,8},{5,9},{6,10},{7,11},{8,4},{9,5},{10,... | collective-permute-start | bytes 786440 | tf_op jit(solution)/shard_map/ppermute | solution.py:556
  43.7 8.1 %collective-permute-start.21 = (bf16[512,256]{1,0:T(8,128)(2,1)S(1)}, bf16[512,256]{1,0:T(8,128)(2,1)S(1)}, u32[]{:S(2)}, u32[]{:S(2)}) collective-permute-start(bf16[512,256]{1,0:T(8,128)(2,1)S(1)} %get-tuple-element.70), channel_id=1, source_target_pairs={{0,2},{1,3},{2,0},{3,1},{4,6},{5,7},{6,4},{7,5},{8,10},{9,11},{10,... | collective-permute-start | bytes 786440 | tf_op jit(solution)/shard_map/ppermute | solution.py:561
  43.9 12.6 %collective-permute-start.22 = (bf16[512,256]{1,0:T(8,128)(2,1)S(1)}, bf16[512,256]{1,0:T(8,128)(2,1)S(1)}, u32[]{:S(2)}, u32[]{:S(2)}) collective-permute-start(bf16[512,256]{1,0:T(8,128)(2,1)S(1)} %get-tuple-element.71), channel_id=1, source_target_pairs={{0,2},{1,3},{2,0},{3,1},{4,6},{5,7},{6,4},{7,5},{8,10},{9,11},{10,... | collective-permute-start | bytes 786440 | tf_op jit(solution)/shard_map/ppermute | solution.py:561
  51.5 9.1 %collective-permute-start.19 = (bf16[256,256]{1,0:T(8,128)(2,1)S(1)}, bf16[256,256]{1,0:T(8,128)(2,1)S(1)}, u32[]{:S(2)}, u32[]{:S(2)}) collective-permute-start(bf16[256,256]{1,0:T(8,128)(2,1)S(1)} %halo.4.own_ref.refs_0_), channel_id=1, source_target_pairs={{0,2},{1,3},{2,0},{3,1},{4,6},{5,7},{6,4},{7,5},{8,10},{9,11},{10,... | collective-permute-start | bytes 393224 | tf_op jit(solution)/shard_map/ppermute | solution.py:561
  51.8 11.7 %collective-permute-start.23 = (bf16[512,256]{1,0:T(8,128)(2,1)S(1)}, bf16[512,256]{1,0:T(8,128)(2,1)S(1)}, u32[]{:S(2)}, u32[]{:S(2)}) collective-permute-start(bf16[512,256]{1,0:T(8,128)(2,1)S(1)} %collective-permute-done.21.refs_0_), channel_id=1, source_target_pairs={{0,16},{16,0},{1,17},{17,1},{2,18},{18,2},{3,19},{19,3},{4,20},{20... | collective-permute-start | bytes 786440 | tf_op jit(solution)/shard_map/ppermute | solution.py:561
  56.5 7.0 %collective-permute-start.24 = (bf16[512,256]{1,0:T(8,128)(2,1)S(1)}, bf16[512,256]{1,0:T(8,128)(2,1)S(1)}, u32[]{:S(2)}, u32[]{:S(2)}) collective-permute-start(bf16[512,256]{1,0:T(8,128)(2,1)S(1)} %collective-permute-done.22.refs_1_), channel_id=1, source_target_pairs={{0,16},{16,0},{1,17},{17,1},{2,18},{18,2},{3,19},{19,3},{4,20},{20... | collective-permute-start | bytes 786440 | tf_op jit(solution)/shard_map/ppermute | solution.py:561
  57.7 4.6 %collective-permute-start.18 = (bf16[256,256]{1,0:T(8,128)(2,1)S(1)}, bf16[256,256]{1,0:T(8,128)(2,1)S(1)}, u32[]{:S(2)}, u32[]{:S(2)}) collective-permute-start(bf16[256,256]{1,0:T(8,128)(2,1)S(1)} %halo.4.own_ref.refs_0_), channel_id=1, source_target_pairs={{0,1},{1,0},{2,3},{3,2},{4,5},{5,4},{6,7},{7,6},{8,9},{9,8},{10,11... | collective-permute-start | bytes 393224 | tf_op jit(solution)/shard_map/ppermute | solution.py:561
  60.7 2.1 %collective-permute-start.20 = (bf16[256,256]{1,0:T(8,128)(2,1)S(1)}, bf16[256,256]{1,0:T(8,128)(2,1)S(1)}, u32[]{:S(2)}, u32[]{:S(2)}) collective-permute-start(bf16[256,256]{1,0:T(8,128)(2,1)S(1)} %collective-permute-done.19.across_ref.refs_0_), channel_id=1, source_target_pairs={{0,1},{1,0},{2,3},{3,2},{4,5},{5,4},{6,7},{7,6},{8,9},{9,8},{10,11... | collective-permute-start | bytes 393224 | tf_op jit(solution)/shard_map/ppermute | solution.py:561
  63.1 4.2 %collective-permute-start.26 = (bf16[256,512]{1,0:T(8,128)(2,1)S(1)}, bf16[256,512]{1,0:T(8,128)(2,1)S(1)}, u32[]{:S(2)}, u32[]{:S(2)}) collective-permute-start(bf16[256,512]{1,0:T(8,128)(2,1)S(1)} %emit.19.refs_0_.refs_2_), channel_id=1, source_target_pairs={{0,1},{1,0},{2,3},{3,2},{4,5},{5,4},{6,7},{7,6},{8,9},{9,8},{10,11... | collective-permute-start | bytes 786440 | tf_op jit(solution)/shard_map/ppermute | solution.py:561
  64.0 3.8 %collective-permute-start.25 = (bf16[256,512]{1,0:T(8,128)(2,1)S(1)}, bf16[256,512]{1,0:T(8,128)(2,1)S(1)}, u32[]{:S(2)}, u32[]{:S(2)}) collective-permute-start(bf16[256,512]{1,0:T(8,128)(2,1)S(1)} %lent.3.refs_1_), channel_id=1, source_target_pairs={{0,1},{1,0},{2,3},{3,2},{4,5},{5,4},{6,7},{7,6},{8,9},{9,8},{10,11... | collective-permute-start | bytes 786440 | tf_op jit(solution)/shard_map/ppermute | solution.py:561
  68.2 7.6 %collective-permute-start.27 = (bf16[2,256,256]{2,1,0:T(8,128)(2,1)S(1)}, bf16[2,256,256]{2,1,0:T(8,128)(2,1)S(1)}, u32[]{:S(2)}, u32[]{:S(2)}) collective-permute-start(bf16[2,256,256]{2,1,0:T(8,128)(2,1)S(1)} %project.25.pair_ref), channel_id=1, source_target_pairs={{0,4},{1,5},{2,6},{3,7},{4,0},{5,1},{6,2},{7,3},{8,12},{9,13},{10,... | collective-permute-start | bytes 786440 | tf_op jit(solution)/shard_map/ppermute | solution.py:556
  69.5 7.2 %collective-permute-start.28 = (bf16[2,256,256]{2,1,0:T(8,128)(2,1)S(1)}, bf16[2,256,256]{2,1,0:T(8,128)(2,1)S(1)}, u32[]{:S(2)}, u32[]{:S(2)}) collective-permute-start(bf16[2,256,256]{2,1,0:T(8,128)(2,1)S(1)} %project.25.pair_ref), channel_id=1, source_target_pairs={{0,1},{1,0},{2,3},{3,2},{4,8},{5,9},{6,10},{7,11},{8,4},{9,5},{10,... | collective-permute-start | bytes 786440 | tf_op jit(solution)/shard_map/ppermute | solution.py:556
  77.4 3.9 %collective-permute-start.29 = (bf16[256,256]{1,0:T(8,128)(2,1)S(1)}, bf16[256,256]{1,0:T(8,128)(2,1)S(1)}, u32[]{:S(2)}, u32[]{:S(2)}) collective-permute-start(bf16[256,256]{1,0:T(8,128)(2,1)S(1)} %halo.5.refs_0_), channel_id=1, source_target_pairs={{0,2},{1,3},{2,0},{3,1},{4,6},{5,7},{6,4},{7,5},{8,10},{9,11},{10,... | collective-permute-start | bytes 393224 | tf_op jit(solution)/shard_map/ppermute | solution.py:561
  77.9 7.6 %collective-permute-start.31 = (bf16[256,256]{1,0:T(8,128)(2,1)S(1)}, bf16[256,256]{1,0:T(8,128)(2,1)S(1)}, u32[]{:S(2)}, u32[]{:S(2)}) collective-permute-start(bf16[256,256]{1,0:T(8,128)(2,1)S(1)} %halo.5.refs_0_), channel_id=1, source_target_pairs={{0,1},{1,0},{2,3},{3,2},{4,5},{5,4},{6,7},{7,6},{8,9},{9,8},{10,11... | collective-permute-start | bytes 393224 | tf_op jit(solution)/shard_map/ppermute | solution.py:561
  81.3 4.6 %collective-permute-start.30 = (bf16[256,256]{1,0:T(8,128)(2,1)S(1)}, bf16[256,256]{1,0:T(8,128)(2,1)S(1)}, u32[]{:S(2)}, u32[]{:S(2)}) collective-permute-start(bf16[256,256]{1,0:T(8,128)(2,1)S(1)} %collective-permute-done.29.refs_0_), channel_id=1, source_target_pairs={{0,1},{1,0},{2,3},{3,2},{4,5},{5,4},{6,7},{7,6},{8,9},{9,8},{10,11... | collective-permute-start | bytes 393224 | tf_op jit(solution)/shard_map/ppermute | solution.py:561

commit v7 on v5

--- a/solution.py
+++ b/solution.py
@@ -14,6 +14,7 @@
 COL_SPAN = 16
 LAYERS = 3
 HALF = ROW_SPAN // 2
+ALL, KEYED = (0, 1, 2), (1, 2)
 PARTS = ((1, 2, 1), (2, 2))
 
 EPS = 1e-06
@@ -97,7 +98,7 @@
     )
 
 
-def project_kernel(bits, load, shared, first, kinds, layer, *refs):
+def project_kernel(bits, load, shared, kinds, have, final, layer, *refs):
     sources, refs = refs[: len(bits)], refs[len(bits) :]
     gain_ref, refs = refs[0], refs[1:]
     if load:
@@ -113,7 +114,7 @@
         stored, refs = refs[:3], refs[3:]
     else:
         held_ref, refs = refs[0], refs[1:]
-    if not first:
+    if have:
         (acc_in, sq_in), refs = refs[:2], refs[2:]
     full = gain_ref.shape[1]
     totals = [None, None, None]
@@ -125,17 +126,17 @@
         square = jnp.sum(wide * wide, axis=1, keepdims=True)
         squares = square if squares is None else squares + square
         scaled = (wide * gain_ref[layer : layer + 1, cols]).astype(BF16)
-        for kind in kinds or range(3):
+        for kind in kinds:
             if load and at == 0:
                 copies[kind].wait()
             held = stored[kind][layer, :, cols] if shared else held_ref[kind, :, cols]
             product = nt_dot(scaled, held)
             totals[kind] = product if totals[kind] is None else totals[kind] + product
-    if not first:
+    if have:
         squares = squares + sq_in[:, :1]
-        for kind in kinds or range(3):
-            totals[kind] = totals[kind] + acc_in[kind]
-    if kinds:
+        for kind in kinds:
+            totals[kind] = totals[kind] + acc_in[have.index(kind)]
+    if final:
         row_scale = lax.rsqrt(squares * (1.0 / full) + EPS)
         for at, kind in enumerate(kinds):
             scale = row_scale * HEAD_DIM ** (-0.5) if kind == 0 else row_scale
@@ -145,15 +146,14 @@
                 out_ref[at] = made[:, group * width : (group + 1) * width]
     else:
         acc_out, sq_out = refs
-        for kind in range(3):
-            acc_out[kind] = totals[kind]
+        for at, kind in enumerate(kinds):
+            acc_out[at] = totals[kind]
         sq_out[...] = jnp.broadcast_to(squares, sq_out.shape)
 
 
-def project(parts, bits, weights, carried, kinds, layer, gain, groups=1):
+def project(parts, bits, weights, carried, kinds, have, final, layer, gain, groups=1):
     tok, width = parts[0].shape
     parts_n = len(parts)
-    first = carried is None
     operands = [*parts, gain]
     specs = [VMEM] * (parts_n + 1)
     load, shared = isinstance(weights, list), isinstance(weights, tuple)
@@ -169,20 +169,20 @@
         _, channels, full = weights.shape
         operands.append(in_vmem(weights))
         specs.append(VMEM)
-    if not first:
+    if have:
         operands += map(in_vmem, carried)
         specs += [VMEM] * 2
-    if kinds:
+    if final:
         out_shape = [pltpu.VMEM((len(kinds), tok, channels // groups), BF16)] * groups
     else:
-        out_shape = [pltpu.VMEM((3, tok, channels), F32), pltpu.VMEM((tok, LANES), F32)]
+        out_shape = [pltpu.VMEM((len(kinds), tok, channels), F32), pltpu.VMEM((tok, LANES), F32)]
     scratch = []
     if load:
         out_shape.append(pltpu.VMEM((3, channels, full), BF16))
         scratch.append(pltpu.SemaphoreType.DMA((3,)))
-    flops = 2 * tok * width * channels * len(kinds or range(3)) * parts_n
+    flops = 2 * tok * width * channels * len(kinds) * parts_n
     return call(
-        partial(project_kernel, bits, load, shared, first, kinds, layer),
+        partial(project_kernel, bits, load, shared, kinds, have, final, layer),
         operands,
         specs,
         out_shape,
@@ -576,23 +576,25 @@
             beside = flip(stream, "tp", 1)
             across = emit_far(parts, base, near[layer - 1], side)
             corner = flip(across, "tp", 1)
-            carried = step([stream, across], (0, 2), held, None, None)
-            carried = step([beside], (1,), held, carried, None)
+            carried = step([stream, across], (0, 2), held, None, KEYED, (), False)
+            carried = step([beside], (1,), held, carried, KEYED, KEYED, False)
         elif tp == 4:
             across = flip(stream, "tp", 2)
             beside = flip(stream, "tp", 1)
             corner = flip(across, "tp", 1)
-            *carried, held = step([stream], (0,), weights, None, None)
-            carried = step([beside], (1,), held, carried, None)
+            *carried, held = step([stream], (0,), weights, None, ALL, (), False)
+            carried = step([beside], (1,), held, carried, ALL, ALL, False)
             if lend:
                 cuts = cut_weight(in_hbm(output_weight))
                 send(cuts, layer, 0, len(cuts[layer]))
-            carried = step([across], (2,), held, carried, None)
+            carried = step([across], (2,), held, carried, ALL, ALL, False)
         groups = query_weight.shape[1] // LANES
+        if tp == 4:
+            sources = [stream, across, beside, corner]
         if lend and layer == LAYERS - 1 and groups == 2:
             pairs, queries, swaps, attended = [], [], [], []
-            pairs = step([corner], (3,), held, carried, (1, 2), groups=groups)
-            queries = step([corner], (3,), held, carried, (0,), groups=groups)
+            pairs = step([corner], (3,), held, carried, KEYED, KEYED, True, groups=groups)
+            queries = step(sources, (0, 2, 1, 3), held, None, (0,), (), True, groups=groups)
             for pair in pairs:
                 swaps.append(exchange(pair, even_pairs))
                 swaps.append(exchange(pair, odd_pairs))
@@ -625,11 +627,15 @@
             return stream
         if tp == 4:
             old = across
-            (pair,) = step([corner], (3,), held, carried, (1, 2))
-            (query,) = step([corner], (3,), shared if lend else held, carried, (0,))
+            (pair,) = step([corner], (3,), held, carried, KEYED, KEYED if layer and lend else ALL, True)
+            if layer and lend:
+                (query,) = step(sources, (0, 2, 1, 3), held, None, (0,), (), True)
+            else:
+                keep = shared if lend else held
+                (query,) = step([corner], (3,), keep, carried, (0,), ALL, True)
         else:
             gathered = lax.all_gather(stream, "tp", axis=1, tiled=True)
-            *carried, held = step([gathered], (None,), weights, None, (0, 1, 2))
+            *carried, held = step([gathered], (None,), weights, None, ALL, (), True)
             query, pair = carried[0][:1], carried[0][1:]
         if split:
             to_even = to_odd = pair

time: 87.5 us -> 87.5 us (level)
  transfers between devices with their start and end apart: 37 -> 37, of which waited for: 9 -> 12; matrix products, arithmetic and copies ran while one was open for 0% -> 0% of each run, Pallas kernels for 22% -> 22%
where the time goes in v7:
time: 87.5 us; the launch traced here: 87.3 us
  starting transfers between devices  46 us (53%)
  Pallas kernels  21.5 us (25%)
  waiting for transfers between devices  17.5 us (20%)
  local copies, waits for them, and re-layouts  1.76 us (2%)
    ppermute x29, starting transfers between devices, flip(): return lax.ppermute(block, axis, [(at, at ^ bit) for at in range(count)])  37.2 us
    pallas_call x37, Pallas kernels, call(): pl.pallas_call(carrying if rider else kernel, out_shape=[*out_shape, *(pl...  18 us
    ppermute x29, waiting for transfers between devices, flip(): return lax.ppermute(block, axis, [(at, at ^ bit) for at in range(count)])  14.1 us
    ppermute x8, starting transfers between devices, exchange(): return lax.ppermute(block, ('sp', 'tp'), moves)  8.76 us
    ppermute x8, waiting for transfers between devices, exchange(): return lax.ppermute(block, ('sp', 'tp'), moves)  3.47 us
    pallas_call x4, Pallas kernels, attend_halo(): pl.pallas_call(partial(halo_kernel, rows_dev, lax.axis_size('sp'), head0)...  2.43 us
    unnamed x19, local copies, waits for them, and re-layouts  1.76 us
  transfers between devices with their start and end apart: 37, of which 12 were waited for; matrix products, arithmetic and copies ran while one was open for 0% of the time, Pallas kernels for 22%

profile of v7, /device:TPU:1, one launch (start us, length us, event | category | flops | bytes accessed | tf_op | source)
XLA Modules:
  0.0 87.3 jit_solution(1357564010441786418)
XLA Ops:
  0.0 2.0 %collective-permute-start = (bf16[256,512]{1,0:T(8,128)(2,1)}, bf16[256,512]{1,0:T(8,128)(2,1)S(1)}, u32[]{:S(2)}, u32[]{:S(2)}) collective-permute-start(bf16[256,512]{1,0:T(8,128)(2,1)} %refs_2_.11), channel_id=1, source_target_pairs={{0,2},{1,3},{2,0},{3,1},{4,6},{5,7},{6,4},{7,5},{8,10},{9,11},{10,... | collective-permute-start | bytes 786440 | tf_op jit(solution)/shard_map/ppermute | solution.py:549
  2.0 1.0 %collective-permute-start.2 = (bf16[256,512]{1,0:T(8,128)(2,1)}, bf16[256,512]{1,0:T(8,128)(2,1)S(1)}, u32[]{:S(2)}, u32[]{:S(2)}) collective-permute-start(bf16[256,512]{1,0:T(8,128)(2,1)} %refs_2_.11), channel_id=1, source_target_pairs={{0,1},{1,0},{2,3},{3,2},{4,5},{5,4},{6,7},{7,6},{8,9},{9,8},{10,11... | collective-permute-start | bytes 786440 | tf_op jit(solution)/shard_map/ppermute | solution.py:549
  3.0 5.3 %collective-permute-done.refs_0_.base_ref = bf16[256,512]{1,0:T(8,128)(2,1)S(1)} collective-permute-done((bf16[256,512]{1,0:T(8,128)(2,1)}, bf16[256,512]{1,0:T(8,128)(2,1)S(1)}, u32[]{:S(2)}, u32[]{:S(2)}) %collective-permute-start) | collective-permute-done | bytes 262176 | tf_op jit(solution)/shard_map/ppermute | solution.py:549
  8.2 1.3 %collective-permute-start.1 = (bf16[256,512]{1,0:T(8,128)(2,1)S(1)}, bf16[256,512]{1,0:T(8,128)(2,1)S(1)}, u32[]{:S(2)}, u32[]{:S(2)}) collective-permute-start(bf16[256,512]{1,0:T(8,128)(2,1)S(1)} %collective-permute-done.refs_0_.base_ref), channel_id=1, source_target_pairs={{0,1},{1,0},{2,3},{3,2},{4,5},{5,4},{6,7},{7,6},{8,9},{9,8},{10,11... | collective-permute-start | bytes 786440 | tf_op jit(solution)/shard_map/ppermute | solution.py:549
  9.5 0.8 copy-done.4
  10.3 0.9 %copy-done.6 = bf16[256,512]{1,0:T(8,128)(2,1)S(1)} copy-done((bf16[256,512]{1,0:T(8,128)(2,1)S(1)}, bf16[256,512]{1,0:T(8,128)(2,1)}, u32[]{:S(2)}) %copy-start.6) | copy-done | bytes 262168
  11.2 2.2 %shard_map.73 = (f32[3,256,256]{2,1,0:T(8,128)S(1)}, f32[256,128]{1,0:T(8,128)S(1)}, bf16[3,256,2048]{2,1,0:T(8,128)(2,1)S(1)}) custom-call(bf16[256,512]{1,0:T(8,128)(2,1)S(1)} %copy-done.6, f32[3,2048]{1,0:T(4,128)S(1)} %copy-done.4, bf16[3,256,2048]{2,1,0:T(8,128)(2,1)} %refs_2_.17, bf16[3,256,2048]{2,1,0:T(8,128)(2,1)} %refs_3_.15, ...), custom_call_target="tpu_custom_call" | custom-call | flops 201326592 | bytes 1310720 | tf_op jit(solution)/shard_map/pallas_call | solution.py:69
  14.9 1.6 %collective-permute-start.3 = (bf16[2,256,256]{2,1,0:T(8,128)(2,1)S(1)}, bf16[2,256,256]{2,1,0:T(8,128)(2,1)S(1)}, u32[]{:S(2)}, u32[]{:S(2)}) collective-permute-start(bf16[2,256,256]{2,1,0:T(8,128)(2,1)S(1)} %shard_map.77.pair_ref), channel_id=1, source_target_pairs={{0,4},{1,5},{2,6},{3,7},{4,0},{5,1},{6,2},{7,3},{8,12},{9,13},{10,... | collective-permute-start | bytes 786440 | tf_op jit(solution)/shard_map/ppermute | solution.py:544
  16.8 1.3 %shard_map.84 = (bf16[512,128]{1,0:T(8,128)(2,1)S(1)}, bf16[512,256]{1,0:T(8,128)(2,1)S(1)}, bf16[512,128]{1,0:T(8,128)(2,1)S(1)}, bf16[512,256]{1,0:T(8,128)(2,1)S(1)}, bf16[512,256]{1,0:T(8,128)(2,1)S(1)}) custom-call(bf16[3,1024,512]{2,1,0:T(8,128)(2,1)} %refs_1_.49), custom_call_target="tpu_custom_call" | custom-call | flops 1000000 | bytes 1000000 | tf_op jit(solution)/shard_map/pallas_call | solution.py:69
  18.1 1.5 %collective-permute-start.9 = (bf16[512,256]{1,0:T(8,128)(2,1)S(1)}, bf16[512,256]{1,0:T(8,128)(2,1)S(1)}, u32[]{:S(2)}, u32[]{:S(2)}) collective-permute-start(bf16[512,256]{1,0:T(8,128)(2,1)S(1)} %get-tuple-element.55), channel_id=1, source_target_pairs={{0,2},{1,3},{2,0},{3,1},{4,6},{5,7},{6,4},{7,5},{8,10},{9,11},{10,... | collective-permute-start | bytes 786440 | tf_op jit(solution)/shard_map/ppermute | solution.py:549
  19.6 0.9 %shard_map.78 = (f32[4,14,64,128]{3,2,1,0:T(8,128)S(1)}, f32[4,4,2,64,128]{4,3,2,1,0:T(8,128)S(1)}) custom-call(f32[3,4,15,31]{3,2,1,0:T(8,128)S(1)} %copy.8.table_ref), custom_call_target="tpu_custom_call" | custom-call | flops 18350080 | bytes 1835008 | tf_op jit(solution)/shard_map/pallas_call | solution.py:69
  21.5 1.5 %collective-permute-done.3.even_ref = bf16[2,256,256]{2,1,0:T(8,128)(2,1)S(1)} collective-permute-done((bf16[2,256,256]{2,1,0:T(8,128)(2,1)S(1)}, bf16[2,256,256]{2,1,0:T(8,128)(2,1)S(1)}, u32[]{:S(2)}, u32[]{:S(2)}) %collective-permute-start.3) | collective-permute-done | bytes 262176 | tf_op jit(solution)/shard_map/ppermute | solution.py:544
  23.0 0.7 halo.4.refs_0_.own_ref
  23.7 1.3 %collective-permute-start.5 = (bf16[256,256]{1,0:T(8,128)(2,1)S(1)}, bf16[256,256]{1,0:T(8,128)(2,1)S(1)}, u32[]{:S(2)}, u32[]{:S(2)}) collective-permute-start(bf16[256,256]{1,0:T(8,128)(2,1)S(1)} %halo.4.refs_0_.own_ref), channel_id=1, source_target_pairs={{0,2},{1,3},{2,0},{3,1},{4,6},{5,7},{6,4},{7,5},{8,10},{9,11},{10,... | collective-permute-start | bytes 393224 | tf_op jit(solution)/shard_map/ppermute | solution.py:549
  25.2 1.3 %collective-permute-start.10 = (bf16[512,128]{1,0:T(8,128)(2,1)S(1)}, bf16[512,128]{1,0:T(8,128)(2,1)S(1)}, u32[]{:S(2)}, u32[]{:S(2)}) collective-permute-start(bf16[512,128]{1,0:T(8,128)(2,1)S(1)} %get-tuple-element.56), channel_id=1, source_target_pairs={{0,2},{1,3},{2,0},{3,1},{4,6},{5,7},{6,4},{7,5},{8,10},{9,11},{10,... | collective-permute-start | bytes 393224 | tf_op jit(solution)/shard_map/ppermute | solution.py:549
  26.5 1.2 %collective-permute-start.12 = (bf16[512,256]{1,0:T(8,128)(2,1)S(1)}, bf16[512,256]{1,0:T(8,128)(2,1)S(1)}, u32[]{:S(2)}, u32[]{:S(2)}) collective-permute-start(bf16[512,256]{1,0:T(8,128)(2,1)S(1)} %collective-permute-done.9.refs_1_), channel_id=1, source_target_pairs={{0,16},{16,0},{1,17},{17,1},{2,18},{18,2},{3,19},{19,3},{4,20},{20... | collective-permute-start | bytes 786440 | tf_op jit(solution)/shard_map/ppermute | solution.py:549
  27.7 2.0 %collective-permute-start.7 = (bf16[256,256]{1,0:T(8,128)(2,1)S(1)}, bf16[256,256]{1,0:T(8,128)(2,1)S(1)}, u32[]{:S(2)}, u32[]{:S(2)}) collective-permute-start(bf16[256,256]{1,0:T(8,128)(2,1)S(1)} %halo.4.refs_0_.own_ref), channel_id=1, source_target_pairs={{0,1},{1,0},{2,3},{3,2},{4,5},{5,4},{6,7},{7,6},{8,9},{9,8},{10,11... | collective-permute-start | bytes 393224 | tf_op jit(solution)/shard_map/ppermute | solution.py:549
  29.7 1.2 %collective-permute-start.6 = (bf16[256,256]{1,0:T(8,128)(2,1)S(1)}, bf16[256,256]{1,0:T(8,128)(2,1)S(1)}, u32[]{:S(2)}, u32[]{:S(2)}) collective-permute-start(bf16[256,256]{1,0:T(8,128)(2,1)S(1)} %collective-permute-done.5.refs_0_.across_ref), channel_id=1, source_target_pairs={{0,1},{1,0},{2,3},{3,2},{4,5},{5,4},{6,7},{7,6},{8,9},{9,8},{10,11... | collective-permute-start | bytes 393224 | tf_op jit(solution)/shard_map/ppermute | solution.py:549
  30.9 1.5 %collective-permute-start.11 = (bf16[512,128]{1,0:T(8,128)(2,1)S(1)}, bf16[512,128]{1,0:T(8,128)(2,1)S(1)}, u32[]{:S(2)}, u32[]{:S(2)}) collective-permute-start(bf16[512,128]{1,0:T(8,128)(2,1)S(1)} %collective-permute-done.8.refs_0_), channel_id=1, source_target_pairs={{0,16},{16,0},{1,17},{17,1},{2,18},{18,2},{3,19},{19,3},{4,20},{20... | collective-permute-start | bytes 393224 | tf_op jit(solution)/shard_map/ppermute | solution.py:549
  32.4 1.3 %collective-permute-done.10.refs_2_ = bf16[512,128]{1,0:T(8,128)(2,1)S(1)} collective-permute-done((bf16[512,128]{1,0:T(8,128)(2,1)S(1)}, bf16[512,128]{1,0:T(8,128)(2,1)S(1)}, u32[]{:S(2)}, u32[]{:S(2)}) %collective-permute-start.10) | collective-permute-done | bytes 131104 | tf_op jit(solution)/shard_map/ppermute | solution.py:549
  33.7 1.5 %collective-permute-start.13 = (bf16[512,128]{1,0:T(8,128)(2,1)S(1)}, bf16[512,128]{1,0:T(8,128)(2,1)S(1)}, u32[]{:S(2)}, u32[]{:S(2)}) collective-permute-start(bf16[512,128]{1,0:T(8,128)(2,1)S(1)} %collective-permute-done.10.refs_2_), channel_id=1, source_target_pairs={{0,16},{16,0},{1,17},{17,1},{2,18},{18,2},{3,19},{19,3},{4,20},{20... | collective-permute-start | bytes 393224 | tf_op jit(solution)/shard_map/ppermute | solution.py:549
  36.2 1.9 %collective-permute-start.14 = (bf16[256,512]{1,0:T(8,128)(2,1)S(1)}, bf16[256,512]{1,0:T(8,128)(2,1)S(1)}, u32[]{:S(2)}, u32[]{:S(2)}) collective-permute-start(bf16[256,512]{1,0:T(8,128)(2,1)S(1)} %shard_map.83.refs_0_.refs_2_), channel_id=1, source_target_pairs={{0,1},{1,0},{2,3},{3,2},{4,5},{5,4},{6,7},{7,6},{8,9},{9,8},{10,11... | collective-permute-start | bytes 786440 | tf_op jit(solution)/shard_map/ppermute | solution.py:549
  38.1 0.8 collective-permute-done.13.refs_5_
  39.4 2.3 %collective-permute-start.15 = (bf16[256,512]{1,0:T(8,128)(2,1)S(1)}, bf16[256,512]{1,0:T(8,128)(2,1)S(1)}, u32[]{:S(2)}, u32[]{:S(2)}) collective-permute-start(bf16[256,512]{1,0:T(8,128)(2,1)S(1)} %lent.2.refs_1_.base_ref), channel_id=1, source_target_pairs={{0,1},{1,0},{2,3},{3,2},{4,5},{5,4},{6,7},{7,6},{8,9},{9,8},{10,11... | collective-permute-start | bytes 786440 | tf_op jit(solution)/shard_map/ppermute | solution.py:549
  43.2 2.4 %collective-permute-start.16 = (bf16[2,256,256]{2,1,0:T(8,128)(2,1)S(1)}, bf16[2,256,256]{2,1,0:T(8,128)(2,1)S(1)}, u32[]{:S(2)}, u32[]{:S(2)}) collective-permute-start(bf16[2,256,256]{2,1,0:T(8,128)(2,1)S(1)} %shard_map.88.pair_ref), channel_id=1, source_target_pairs={{0,4},{1,5},{2,6},{3,7},{4,0},{5,1},{6,2},{7,3},{8,12},{9,13},{10,... | collective-permute-start | bytes 786440 | tf_op jit(solution)/shard_map/ppermute | solution.py:544
  45.6 0.7 collective-permute-start.17
  46.2 1.2 %collective-permute-start.21 = (bf16[512,256]{1,0:T(8,128)(2,1)S(1)}, bf16[512,256]{1,0:T(8,128)(2,1)S(1)}, u32[]{:S(2)}, u32[]{:S(2)}) collective-permute-start(bf16[512,256]{1,0:T(8,128)(2,1)S(1)} %get-tuple-element.65), channel_id=1, source_target_pairs={{0,2},{1,3},{2,0},{3,1},{4,6},{5,7},{6,4},{7,5},{8,10},{9,11},{10,... | collective-permute-start | bytes 786440 | tf_op jit(solution)/shard_map/ppermute | solution.py:549
  47.7 0.9 %shard_map.89 = (f32[4,14,64,128]{3,2,1,0:T(8,128)S(1)}, f32[4,4,2,64,128]{4,3,2,1,0:T(8,128)S(1)}) custom-call(f32[3,4,15,31]{3,2,1,0:T(8,128)S(1)} %copy.8.table_ref), custom_call_target="tpu_custom_call" | custom-call | flops 18350080 | bytes 1835008 | tf_op jit(solution)/shard_map/pallas_call | solution.py:69
  49.9 2.0 %collective-permute-done.16.even_ref = bf16[2,256,256]{2,1,0:T(8,128)(2,1)S(1)} collective-permute-done((bf16[2,256,256]{2,1,0:T(8,128)(2,1)S(1)}, bf16[2,256,256]{2,1,0:T(8,128)(2,1)S(1)}, u32[]{:S(2)}, u32[]{:S(2)}) %collective-permute-start.16) | collective-permute-done | bytes 262176 | tf_op jit(solution)/shard_map/ppermute | solution.py:544
  51.9 0.7 halo.5.refs_0_.own_ref
  52.6 1.3 %collective-permute-start.18 = (bf16[256,256]{1,0:T(8,128)(2,1)S(1)}, bf16[256,256]{1,0:T(8,128)(2,1)S(1)}, u32[]{:S(2)}, u32[]{:S(2)}) collective-permute-start(bf16[256,256]{1,0:T(8,128)(2,1)S(1)} %halo.5.refs_0_.own_ref), channel_id=1, source_target_pairs={{0,2},{1,3},{2,0},{3,1},{4,6},{5,7},{6,4},{7,5},{8,10},{9,11},{10,... | collective-permute-start | bytes 393224 | tf_op jit(solution)/shard_map/ppermute | solution.py:549
  54.1 1.3 %collective-permute-start.23 = (bf16[512,256]{1,0:T(8,128)(2,1)S(1)}, bf16[512,256]{1,0:T(8,128)(2,1)S(1)}, u32[]{:S(2)}, u32[]{:S(2)}) collective-permute-start(bf16[512,256]{1,0:T(8,128)(2,1)S(1)} %collective-permute-done.21.refs_0_), channel_id=1, source_target_pairs={{0,16},{16,0},{1,17},{17,1},{2,18},{18,2},{3,19},{19,3},{4,20},{20... | collective-permute-start | bytes 786440 | tf_op jit(solution)/shard_map/ppermute | solution.py:549
  55.4 4.4 %collective-permute-done.22.refs_1_ = bf16[512,256]{1,0:T(8,128)(2,1)S(1)} collective-permute-done((bf16[512,256]{1,0:T(8,128)(2,1)S(1)}, bf16[512,256]{1,0:T(8,128)(2,1)S(1)}, u32[]{:S(2)}, u32[]{:S(2)}) %collective-permute-start.22) | collective-permute-done | bytes 262176 | tf_op jit(solution)/shard_map/ppermute | solution.py:549
  59.7 1.3 %collective-permute-start.24 = (bf16[512,256]{1,0:T(8,128)(2,1)S(1)}, bf16[512,256]{1,0:T(8,128)(2,1)S(1)}, u32[]{:S(2)}, u32[]{:S(2)}) collective-permute-start(bf16[512,256]{1,0:T(8,128)(2,1)S(1)} %collective-permute-done.22.refs_1_), channel_id=1, source_target_pairs={{0,16},{16,0},{1,17},{17,1},{2,18},{18,2},{3,19},{19,3},{4,20},{20... | collective-permute-start | bytes 786440 | tf_op jit(solution)/shard_map/ppermute | solution.py:549
  61.0 1.6 %collective-permute-start.20 = (bf16[256,256]{1,0:T(8,128)(2,1)S(1)}, bf16[256,256]{1,0:T(8,128)(2,1)S(1)}, u32[]{:S(2)}, u32[]{:S(2)}) collective-permute-start(bf16[256,256]{1,0:T(8,128)(2,1)S(1)} %halo.5.refs_0_.own_ref), channel_id=1, source_target_pairs={{0,1},{1,0},{2,3},{3,2},{4,5},{5,4},{6,7},{7,6},{8,9},{9,8},{10,11... | collective-permute-start | bytes 393224 | tf_op jit(solution)/shard_map/ppermute | solution.py:549
  62.6 0.8 collective-permute-start.19
  65.0 1.2 %collective-permute-done.24.refs_3_ = bf16[512,256]{1,0:T(8,128)(2,1)S(1)} collective-permute-done((bf16[512,256]{1,0:T(8,128)(2,1)S(1)}, bf16[512,256]{1,0:T(8,128)(2,1)S(1)}, u32[]{:S(2)}, u32[]{:S(2)}) %collective-permute-start.24) | collective-permute-done | bytes 262176 | tf_op jit(solution)/shard_map/ppermute | solution.py:549
  66.7 2.2 %collective-permute-start.26 = (bf16[256,512]{1,0:T(8,128)(2,1)S(1)}, bf16[256,512]{1,0:T(8,128)(2,1)S(1)}, u32[]{:S(2)}, u32[]{:S(2)}) collective-permute-start(bf16[256,512]{1,0:T(8,128)(2,1)S(1)} %lent.3.refs_1_), channel_id=1, source_target_pairs={{0,1},{1,0},{2,3},{3,2},{4,5},{5,4},{6,7},{7,6},{8,9},{9,8},{10,11... | collective-permute-start | bytes 786440 | tf_op jit(solution)/shard_map/ppermute | solution.py:549
  70.5 1.1 %collective-permute-start.32 = (bf16[2,256,128]{2,1,0:T(8,128)(2,1)S(1)}, bf16[2,256,128]{2,1,0:T(8,128)(2,1)S(1)}, u32[]{:S(2)}, u32[]{:S(2)}) collective-permute-start(bf16[2,256,128]{2,1,0:T(8,128)(2,1)S(1)} %get-tuple-element.78.pair_ref), channel_id=1, source_target_pairs={{0,4},{1,5},{2,6},{3,7},{4,0},{5,1},{6,2},{7,3},{8,12},{9,13},{10,... | collective-permute-start | bytes 393224 | tf_op jit(solution)/shard_map/ppermute | solution.py:544
  72.2 0.9 collective-permute-start.27
  73.1 1.2 %collective-permute-start.28 = (bf16[2,256,128]{2,1,0:T(8,128)(2,1)S(1)}, bf16[2,256,128]{2,1,0:T(8,128)(2,1)S(1)}, u32[]{:S(2)}, u32[]{:S(2)}) collective-permute-start(bf16[2,256,128]{2,1,0:T(8,128)(2,1)S(1)} %get-tuple-element.72.pair_ref), channel_id=1, source_target_pairs={{0,1},{1,0},{2,3},{3,2},{4,8},{5,9},{6,10},{7,11},{8,4},{9,5},{10,... | collective-permute-start | bytes 393224 | tf_op jit(solution)/shard_map/ppermute | solution.py:544
  74.3 0.9 %shard_map.99 = (f32[4,14,64,128]{3,2,1,0:T(8,128)S(1)}, f32[4,4,2,64,128]{4,3,2,1,0:T(8,128)S(1)}) custom-call(f32[3,4,15,31]{3,2,1,0:T(8,128)S(1)} %copy.8.table_ref), custom_call_target="tpu_custom_call" | custom-call | flops 18350080 | bytes 1835008 | tf_op jit(solution)/shard_map/pallas_call | solution.py:69
  76.9 1.1 %collective-permute-start.34 = (bf16[256,128]{1,0:T(8,128)(2,1)S(1)}, bf16[256,128]{1,0:T(8,128)(2,1)S(1)}, u32[]{:S(2)}, u32[]{:S(2)}) collective-permute-start(bf16[256,128]{1,0:T(8,128)(2,1)S(1)} %halo.7.refs_0_), channel_id=1, source_target_pairs={{0,2},{1,3},{2,0},{3,1},{4,6},{5,7},{6,4},{7,5},{8,10},{9,11},{10,... | collective-permute-start | bytes 196616 | tf_op jit(solution)/shard_map/ppermute | solution.py:549
  79.1 0.8 collective-permute-start.29
  79.8 1.5 %collective-permute-start.36 = (bf16[256,128]{1,0:T(8,128)(2,1)S(1)}, bf16[256,128]{1,0:T(8,128)(2,1)S(1)}, u32[]{:S(2)}, u32[]{:S(2)}) collective-permute-start(bf16[256,128]{1,0:T(8,128)(2,1)S(1)} %halo.7.refs_0_), channel_id=1, source_target_pairs={{0,1},{1,0},{2,3},{3,2},{4,5},{5,4},{6,7},{7,6},{8,9},{9,8},{10,11... | collective-permute-start | bytes 196616 | tf_op jit(solution)/shard_map/ppermute | solution.py:549
  81.4 0.8 collective-permute-start.35
  82.2 2.5 %collective-permute-start.30 = (bf16[256,128]{1,0:T(8,128)(2,1)S(1)}, bf16[256,128]{1,0:T(8,128)(2,1)S(1)}, u32[]{:S(2)}, u32[]{:S(2)}) collective-permute-start(bf16[256,128]{1,0:T(8,128)(2,1)S(1)} %collective-permute-done.29.refs_0_), channel_id=1, source_target_pairs={{0,1},{1,0},{2,3},{3,2},{4,5},{5,4},{6,7},{7,6},{8,9},{9,8},{10,11... | collective-permute-start | bytes 196616 | tf_op jit(solution)/shard_map/ppermute | solution.py:549
  86.4 0.9 %shard_map.109 = bf16[256,512]{1,0:T(8,128)(2,1)} custom-call(bf16[256,128]{1,0:T(8,128)(2,1)S(1)} %collective-permute-done.30.refs_0_, bf16[3,1024,512]{2,1,0:T(8,128)(2,1)S(1)} %copy-done, f32[256,512]{1,0:T(8,128)S(1)} %shard_map.108.refs_2_), custom_call_target="tpu_custom_call" | custom-call | flops 33554432 | bytes 1000000 | tf_op jit(solution)/shard_map/pallas_call | solution.py:69
  (88 shorter events, 15.9 us)
Async XLA Ops:
  0.0 8.2 %collective-permute-start = (bf16[256,512]{1,0:T(8,128)(2,1)}, bf16[256,512]{1,0:T(8,128)(2,1)S(1)}, u32[]{:S(2)}, u32[]{:S(2)}) collective-permute-start(bf16[256,512]{1,0:T(8,128)(2,1)} %refs_2_.11), channel_id=1, source_target_pairs={{0,2},{1,3},{2,0},{3,1},{4,6},{5,7},{6,4},{7,5},{8,10},{9,11},{10,... | collective-permute-start | bytes 786440 | tf_op jit(solution)/shard_map/ppermute | solution.py:549
  2.0 11.4 %collective-permute-start.2 = (bf16[256,512]{1,0:T(8,128)(2,1)}, bf16[256,512]{1,0:T(8,128)(2,1)S(1)}, u32[]{:S(2)}, u32[]{:S(2)}) collective-permute-start(bf16[256,512]{1,0:T(8,128)(2,1)} %refs_2_.11), channel_id=1, source_target_pairs={{0,1},{1,0},{2,3},{3,2},{4,5},{5,4},{6,7},{7,6},{8,9},{9,8},{10,11... | collective-permute-start | bytes 786440 | tf_op jit(solution)/shard_map/ppermute | solution.py:549
  8.2 6.2 %collective-permute-start.1 = (bf16[256,512]{1,0:T(8,128)(2,1)S(1)}, bf16[256,512]{1,0:T(8,128)(2,1)S(1)}, u32[]{:S(2)}, u32[]{:S(2)}) collective-permute-start(bf16[256,512]{1,0:T(8,128)(2,1)S(1)} %collective-permute-done.refs_0_.base_ref), channel_id=1, source_target_pairs={{0,1},{1,0},{2,3},{3,2},{4,5},{5,4},{6,7},{7,6},{8,9},{9,8},{10,11... | collective-permute-start | bytes 786440 | tf_op jit(solution)/shard_map/ppermute | solution.py:549
  9.5 0.8 copy-start.4
  10.3 0.9 %copy-start.6 = (bf16[256,512]{1,0:T(8,128)(2,1)S(1)}, bf16[256,512]{1,0:T(8,128)(2,1)}, u32[]{:S(2)}) copy-start(bf16[256,512]{1,0:T(8,128)(2,1)} %refs_2_.11) | copy-start | bytes 786436
  11.2 2.3 %copy-start.5 = (f32[3,2048]{1,0:T(4,128)S(1)}, f32[3,2048]{1,0:T(4,128)}, u32[]{:S(2)}) copy-start(f32[3,2048]{1,0:T(4,128)} %refs_1_.41) | copy-start | bytes 73732
  14.0 6.6 %copy-start.3 = (bf16[3,256,2048]{2,1,0:T(8,128)(2,1)S(1)}, bf16[3,256,2048]{2,1,0:T(8,128)(2,1)}, u32[]{:S(2)}) copy-start(bf16[3,256,2048]{2,1,0:T(8,128)(2,1)} %refs_4_.19) | copy-start | bytes 9437188
  14.5 5.1 %copy-start.8 = (f32[3,4,15,31]{3,1,2,0:T(4,128)S(1)}, f32[3,4,15,31]{3,1,2,0:T(4,128)}, u32[]{:S(2)}) copy-start(f32[3,4,15,31]{3,1,2,0:T(4,128)} %param.13) | copy-start | bytes 66964
  14.5 6.1 %copy-start.1 = (bf16[3,256,2048]{2,1,0:T(8,128)(2,1)S(1)}, bf16[3,256,2048]{2,1,0:T(8,128)(2,1)}, u32[]{:S(2)}) copy-start(bf16[3,256,2048]{2,1,0:T(8,128)(2,1)} %refs_2_.17) | copy-start | bytes 9437188
  14.5 6.1 %copy-start.2 = (bf16[3,256,2048]{2,1,0:T(8,128)(2,1)S(1)}, bf16[3,256,2048]{2,1,0:T(8,128)(2,1)}, u32[]{:S(2)}) copy-start(bf16[3,256,2048]{2,1,0:T(8,128)(2,1)} %refs_3_.15) | copy-start | bytes 9437188
  14.9 8.1 %collective-permute-start.3 = (bf16[2,256,256]{2,1,0:T(8,128)(2,1)S(1)}, bf16[2,256,256]{2,1,0:T(8,128)(2,1)S(1)}, u32[]{:S(2)}, u32[]{:S(2)}) collective-permute-start(bf16[2,256,256]{2,1,0:T(8,128)(2,1)S(1)} %shard_map.77.pair_ref), channel_id=1, source_target_pairs={{0,4},{1,5},{2,6},{3,7},{4,0},{5,1},{6,2},{7,3},{8,12},{9,13},{10,... | collective-permute-start | bytes 786440 | tf_op jit(solution)/shard_map/ppermute | solution.py:544
  16.5 6.5 %collective-permute-start.4 = (bf16[2,256,256]{2,1,0:T(8,128)(2,1)S(1)}, bf16[2,256,256]{2,1,0:T(8,128)(2,1)S(1)}, u32[]{:S(2)}, u32[]{:S(2)}) collective-permute-start(bf16[2,256,256]{2,1,0:T(8,128)(2,1)S(1)} %shard_map.77.pair_ref), channel_id=1, source_target_pairs={{0,1},{1,0},{2,3},{3,2},{4,8},{5,9},{6,10},{7,11},{8,4},{9,5},{10,... | collective-permute-start | bytes 786440 | tf_op jit(solution)/shard_map/ppermute | solution.py:544
  18.1 8.4 %collective-permute-start.9 = (bf16[512,256]{1,0:T(8,128)(2,1)S(1)}, bf16[512,256]{1,0:T(8,128)(2,1)S(1)}, u32[]{:S(2)}, u32[]{:S(2)}) collective-permute-start(bf16[512,256]{1,0:T(8,128)(2,1)S(1)} %get-tuple-element.55), channel_id=1, source_target_pairs={{0,2},{1,3},{2,0},{3,1},{4,6},{5,7},{6,4},{7,5},{8,10},{9,11},{10,... | collective-permute-start | bytes 786440 | tf_op jit(solution)/shard_map/ppermute | solution.py:549
  20.9 14.3 %copy-start = (bf16[3,1024,512]{2,1,0:T(8,128)(2,1)S(1)}, bf16[3,1024,512]{2,1,0:T(8,128)(2,1)}, u32[]{:S(2)}) copy-start(bf16[3,1024,512]{2,1,0:T(8,128)(2,1)} %refs_1_.49) | copy-start | bytes 9437188
  20.9 14.3 %copy-start.7 = (bf16[256,512]{1,0:T(8,128)(2,1)S(1)}, bf16[256,512]{1,0:T(8,128)(2,1)}, u32[]{:S(2)}) copy-start(bf16[256,512]{1,0:T(8,128)(2,1)} %refs_2_.11) | copy-start | bytes 786436
  23.7 6.0 %collective-permute-start.5 = (bf16[256,256]{1,0:T(8,128)(2,1)S(1)}, bf16[256,256]{1,0:T(8,128)(2,1)S(1)}, u32[]{:S(2)}, u32[]{:S(2)}) collective-permute-start(bf16[256,256]{1,0:T(8,128)(2,1)S(1)} %halo.4.refs_0_.own_ref), channel_id=1, source_target_pairs={{0,2},{1,3},{2,0},{3,1},{4,6},{5,7},{6,4},{7,5},{8,10},{9,11},{10,... | collective-permute-start | bytes 393224 | tf_op jit(solution)/shard_map/ppermute | solution.py:549
  25.0 5.9 %collective-permute-start.8 = (bf16[512,128]{1,0:T(8,128)(2,1)S(1)}, bf16[512,128]{1,0:T(8,128)(2,1)S(1)}, u32[]{:S(2)}, u32[]{:S(2)}) collective-permute-start(bf16[512,128]{1,0:T(8,128)(2,1)S(1)} %get-tuple-element.54), channel_id=1, source_target_pairs={{0,2},{1,3},{2,0},{3,1},{4,6},{5,7},{6,4},{7,5},{8,10},{9,11},{10,... | collective-permute-start | bytes 393224 | tf_op jit(solution)/shard_map/ppermute | solution.py:549
  25.2 8.4 %collective-permute-start.10 = (bf16[512,128]{1,0:T(8,128)(2,1)S(1)}, bf16[512,128]{1,0:T(8,128)(2,1)S(1)}, u32[]{:S(2)}, u32[]{:S(2)}) collective-permute-start(bf16[512,128]{1,0:T(8,128)(2,1)S(1)} %get-tuple-element.56), channel_id=1, source_target_pairs={{0,2},{1,3},{2,0},{3,1},{4,6},{5,7},{6,4},{7,5},{8,10},{9,11},{10,... | collective-permute-start | bytes 393224 | tf_op jit(solution)/shard_map/ppermute | solution.py:549
  26.5 12.4 %collective-permute-start.12 = (bf16[512,256]{1,0:T(8,128)(2,1)S(1)}, bf16[512,256]{1,0:T(8,128)(2,1)S(1)}, u32[]{:S(2)}, u32[]{:S(2)}) collective-permute-start(bf16[512,256]{1,0:T(8,128)(2,1)S(1)} %collective-permute-done.9.refs_1_), channel_id=1, source_target_pairs={{0,16},{16,0},{1,17},{17,1},{2,18},{18,2},{3,19},{19,3},{4,20},{20... | collective-permute-start | bytes 786440 | tf_op jit(solution)/shard_map/ppermute | solution.py:549
  27.7 7.7 %collective-permute-start.7 = (bf16[256,256]{1,0:T(8,128)(2,1)S(1)}, bf16[256,256]{1,0:T(8,128)(2,1)S(1)}, u32[]{:S(2)}, u32[]{:S(2)}) collective-permute-start(bf16[256,256]{1,0:T(8,128)(2,1)S(1)} %halo.4.refs_0_.own_ref), channel_id=1, source_target_pairs={{0,1},{1,0},{2,3},{3,2},{4,5},{5,4},{6,7},{7,6},{8,9},{9,8},{10,11... | collective-permute-start | bytes 393224 | tf_op jit(solution)/shard_map/ppermute | solution.py:549
  29.7 6.2 %collective-permute-start.6 = (bf16[256,256]{1,0:T(8,128)(2,1)S(1)}, bf16[256,256]{1,0:T(8,128)(2,1)S(1)}, u32[]{:S(2)}, u32[]{:S(2)}) collective-permute-start(bf16[256,256]{1,0:T(8,128)(2,1)S(1)} %collective-permute-done.5.refs_0_.across_ref), channel_id=1, source_target_pairs={{0,1},{1,0},{2,3},{3,2},{4,5},{5,4},{6,7},{7,6},{8,9},{9,8},{10,11... | collective-permute-start | bytes 393224 | tf_op jit(solution)/shard_map/ppermute | solution.py:549
  30.9 7.2 %collective-permute-start.11 = (bf16[512,128]{1,0:T(8,128)(2,1)S(1)}, bf16[512,128]{1,0:T(8,128)(2,1)S(1)}, u32[]{:S(2)}, u32[]{:S(2)}) collective-permute-start(bf16[512,128]{1,0:T(8,128)(2,1)S(1)} %collective-permute-done.8.refs_0_), channel_id=1, source_target_pairs={{0,16},{16,0},{1,17},{17,1},{2,18},{18,2},{3,19},{19,3},{4,20},{20... | collective-permute-start | bytes 393224 | tf_op jit(solution)/shard_map/ppermute | solution.py:549
  33.7 5.2 %collective-permute-start.13 = (bf16[512,128]{1,0:T(8,128)(2,1)S(1)}, bf16[512,128]{1,0:T(8,128)(2,1)S(1)}, u32[]{:S(2)}, u32[]{:S(2)}) collective-permute-start(bf16[512,128]{1,0:T(8,128)(2,1)S(1)} %collective-permute-done.10.refs_2_), channel_id=1, source_target_pairs={{0,16},{16,0},{1,17},{17,1},{2,18},{18,2},{3,19},{19,3},{4,20},{20... | collective-permute-start | bytes 393224 | tf_op jit(solution)/shard_map/ppermute | solution.py:549
  36.2 6.0 %collective-permute-start.14 = (bf16[256,512]{1,0:T(8,128)(2,1)S(1)}, bf16[256,512]{1,0:T(8,128)(2,1)S(1)}, u32[]{:S(2)}, u32[]{:S(2)}) collective-permute-start(bf16[256,512]{1,0:T(8,128)(2,1)S(1)} %shard_map.83.refs_0_.refs_2_), channel_id=1, source_target_pairs={{0,1},{1,0},{2,3},{3,2},{4,5},{5,4},{6,7},{7,6},{8,9},{9,8},{10,11... | collective-permute-start | bytes 786440 | tf_op jit(solution)/shard_map/ppermute | solution.py:549
  39.4 3.4 %collective-permute-start.15 = (bf16[256,512]{1,0:T(8,128)(2,1)S(1)}, bf16[256,512]{1,0:T(8,128)(2,1)S(1)}, u32[]{:S(2)}, u32[]{:S(2)}) collective-permute-start(bf16[256,512]{1,0:T(8,128)(2,1)S(1)} %lent.2.refs_1_.base_ref), channel_id=1, source_target_pairs={{0,1},{1,0},{2,3},{3,2},{4,5},{5,4},{6,7},{7,6},{8,9},{9,8},{10,11... | collective-permute-start | bytes 786440 | tf_op jit(solution)/shard_map/ppermute | solution.py:549
  43.2 8.7 %collective-permute-start.16 = (bf16[2,256,256]{2,1,0:T(8,128)(2,1)S(1)}, bf16[2,256,256]{2,1,0:T(8,128)(2,1)S(1)}, u32[]{:S(2)}, u32[]{:S(2)}) collective-permute-start(bf16[2,256,256]{2,1,0:T(8,128)(2,1)S(1)} %shard_map.88.pair_ref), channel_id=1, source_target_pairs={{0,4},{1,5},{2,6},{3,7},{4,0},{5,1},{6,2},{7,3},{8,12},{9,13},{10,... | collective-permute-start | bytes 786440 | tf_op jit(solution)/shard_map/ppermute | solution.py:544
  45.6 6.3 %collective-permute-start.17 = (bf16[2,256,256]{2,1,0:T(8,128)(2,1)S(1)}, bf16[2,256,256]{2,1,0:T(8,128)(2,1)S(1)}, u32[]{:S(2)}, u32[]{:S(2)}) collective-permute-start(bf16[2,256,256]{2,1,0:T(8,128)(2,1)S(1)} %shard_map.88.pair_ref), channel_id=1, source_target_pairs={{0,1},{1,0},{2,3},{3,2},{4,8},{5,9},{6,10},{7,11},{8,4},{9,5},{10,... | collective-permute-start | bytes 786440 | tf_op jit(solution)/shard_map/ppermute | solution.py:544
  46.2 7.9 %collective-permute-start.21 = (bf16[512,256]{1,0:T(8,128)(2,1)S(1)}, bf16[512,256]{1,0:T(8,128)(2,1)S(1)}, u32[]{:S(2)}, u32[]{:S(2)}) collective-permute-start(bf16[512,256]{1,0:T(8,128)(2,1)S(1)} %get-tuple-element.65), channel_id=1, source_target_pairs={{0,2},{1,3},{2,0},{3,1},{4,6},{5,7},{6,4},{7,5},{8,10},{9,11},{10,... | collective-permute-start | bytes 786440 | tf_op jit(solution)/shard_map/ppermute | solution.py:549
  47.5 12.2 %collective-permute-start.22 = (bf16[512,256]{1,0:T(8,128)(2,1)S(1)}, bf16[512,256]{1,0:T(8,128)(2,1)S(1)}, u32[]{:S(2)}, u32[]{:S(2)}) collective-permute-start(bf16[512,256]{1,0:T(8,128)(2,1)S(1)} %get-tuple-element.66), channel_id=1, source_target_pairs={{0,2},{1,3},{2,0},{3,1},{4,6},{5,7},{6,4},{7,5},{8,10},{9,11},{10,... | collective-permute-start | bytes 786440 | tf_op jit(solution)/shard_map/ppermute | solution.py:549
  52.6 10.0 %collective-permute-start.18 = (bf16[256,256]{1,0:T(8,128)(2,1)S(1)}, bf16[256,256]{1,0:T(8,128)(2,1)S(1)}, u32[]{:S(2)}, u32[]{:S(2)}) collective-permute-start(bf16[256,256]{1,0:T(8,128)(2,1)S(1)} %halo.5.refs_0_.own_ref), channel_id=1, source_target_pairs={{0,2},{1,3},{2,0},{3,1},{4,6},{5,7},{6,4},{7,5},{8,10},{9,11},{10,... | collective-permute-start | bytes 393224 | tf_op jit(solution)/shard_map/ppermute | solution.py:549
  54.1 10.9 %collective-permute-start.23 = (bf16[512,256]{1,0:T(8,128)(2,1)S(1)}, bf16[512,256]{1,0:T(8,128)(2,1)S(1)}, u32[]{:S(2)}, u32[]{:S(2)}) collective-permute-start(bf16[512,256]{1,0:T(8,128)(2,1)S(1)} %collective-permute-done.21.refs_0_), channel_id=1, source_target_pairs={{0,16},{16,0},{1,17},{17,1},{2,18},{18,2},{3,19},{19,3},{4,20},{20... | collective-permute-start | bytes 786440 | tf_op jit(solution)/shard_map/ppermute | solution.py:549
  59.7 6.5 %collective-permute-start.24 = (bf16[512,256]{1,0:T(8,128)(2,1)S(1)}, bf16[512,256]{1,0:T(8,128)(2,1)S(1)}, u32[]{:S(2)}, u32[]{:S(2)}) collective-permute-start(bf16[512,256]{1,0:T(8,128)(2,1)S(1)} %collective-permute-done.22.refs_1_), channel_id=1, source_target_pairs={{0,16},{16,0},{1,17},{17,1},{2,18},{18,2},{3,19},{19,3},{4,20},{20... | collective-permute-start | bytes 786440 | tf_op jit(solution)/shard_map/ppermute | solution.py:549
  61.0 2.6 %collective-permute-start.20 = (bf16[256,256]{1,0:T(8,128)(2,1)S(1)}, bf16[256,256]{1,0:T(8,128)(2,1)S(1)}, u32[]{:S(2)}, u32[]{:S(2)}) collective-permute-start(bf16[256,256]{1,0:T(8,128)(2,1)S(1)} %halo.5.refs_0_.own_ref), channel_id=1, source_target_pairs={{0,1},{1,0},{2,3},{3,2},{4,5},{5,4},{6,7},{7,6},{8,9},{9,8},{10,11... | collective-permute-start | bytes 393224 | tf_op jit(solution)/shard_map/ppermute | solution.py:549
  62.6 1.8 %collective-permute-start.19 = (bf16[256,256]{1,0:T(8,128)(2,1)S(1)}, bf16[256,256]{1,0:T(8,128)(2,1)S(1)}, u32[]{:S(2)}, u32[]{:S(2)}) collective-permute-start(bf16[256,256]{1,0:T(8,128)(2,1)S(1)} %collective-permute-done.18.refs_0_.across_ref), channel_id=1, source_target_pairs={{0,1},{1,0},{2,3},{3,2},{4,5},{5,4},{6,7},{7,6},{8,9},{9,8},{10,11... | collective-permute-start | bytes 393224 | tf_op jit(solution)/shard_map/ppermute | solution.py:549
  64.6 4.9 %collective-permute-start.25 = (bf16[256,512]{1,0:T(8,128)(2,1)S(1)}, bf16[256,512]{1,0:T(8,128)(2,1)S(1)}, u32[]{:S(2)}, u32[]{:S(2)}) collective-permute-start(bf16[256,512]{1,0:T(8,128)(2,1)S(1)} %shard_map.94.refs_0_.refs_2_), channel_id=1, source_target_pairs={{0,1},{1,0},{2,3},{3,2},{4,5},{5,4},{6,7},{7,6},{8,9},{9,8},{10,11... | collective-permute-start | bytes 786440 | tf_op jit(solution)/shard_map/ppermute | solution.py:549
  66.7 3.4 %collective-permute-start.26 = (bf16[256,512]{1,0:T(8,128)(2,1)S(1)}, bf16[256,512]{1,0:T(8,128)(2,1)S(1)}, u32[]{:S(2)}, u32[]{:S(2)}) collective-permute-start(bf16[256,512]{1,0:T(8,128)(2,1)S(1)} %lent.3.refs_1_), channel_id=1, source_target_pairs={{0,1},{1,0},{2,3},{3,2},{4,5},{5,4},{6,7},{7,6},{8,9},{9,8},{10,11... | collective-permute-start | bytes 786440 | tf_op jit(solution)/shard_map/ppermute | solution.py:549
  70.5 5.9 %collective-permute-start.32 = (bf16[2,256,128]{2,1,0:T(8,128)(2,1)S(1)}, bf16[2,256,128]{2,1,0:T(8,128)(2,1)S(1)}, u32[]{:S(2)}, u32[]{:S(2)}) collective-permute-start(bf16[2,256,128]{2,1,0:T(8,128)(2,1)S(1)} %get-tuple-element.78.pair_ref), channel_id=1, source_target_pairs={{0,4},{1,5},{2,6},{3,7},{4,0},{5,1},{6,2},{7,3},{8,12},{9,13},{10,... | collective-permute-start | bytes 393224 | tf_op jit(solution)/shard_map/ppermute | solution.py:544
  71.6 4.8 %collective-permute-start.33 = (bf16[2,256,128]{2,1,0:T(8,128)(2,1)S(1)}, bf16[2,256,128]{2,1,0:T(8,128)(2,1)S(1)}, u32[]{:S(2)}, u32[]{:S(2)}) collective-permute-start(bf16[2,256,128]{2,1,0:T(8,128)(2,1)S(1)} %get-tuple-element.78.pair_ref), channel_id=1, source_target_pairs={{0,1},{1,0},{2,3},{3,2},{4,8},{5,9},{6,10},{7,11},{8,4},{9,5},{10,... | collective-permute-start | bytes 393224 | tf_op jit(solution)/shard_map/ppermute | solution.py:544
  72.2 6.3 %collective-permute-start.27 = (bf16[2,256,128]{2,1,0:T(8,128)(2,1)S(1)}, bf16[2,256,128]{2,1,0:T(8,128)(2,1)S(1)}, u32[]{:S(2)}, u32[]{:S(2)}) collective-permute-start(bf16[2,256,128]{2,1,0:T(8,128)(2,1)S(1)} %get-tuple-element.72.pair_ref), channel_id=1, source_target_pairs={{0,4},{1,5},{2,6},{3,7},{4,0},{5,1},{6,2},{7,3},{8,12},{9,13},{10,... | collective-permute-start | bytes 393224 | tf_op jit(solution)/shard_map/ppermute | solution.py:544
  73.1 5.4 %collective-permute-start.28 = (bf16[2,256,128]{2,1,0:T(8,128)(2,1)S(1)}, bf16[2,256,128]{2,1,0:T(8,128)(2,1)S(1)}, u32[]{:S(2)}, u32[]{:S(2)}) collective-permute-start(bf16[2,256,128]{2,1,0:T(8,128)(2,1)S(1)} %get-tuple-element.72.pair_ref), channel_id=1, source_target_pairs={{0,1},{1,0},{2,3},{3,2},{4,8},{5,9},{6,10},{7,11},{8,4},{9,5},{10,... | collective-permute-start | bytes 393224 | tf_op jit(solution)/shard_map/ppermute | solution.py:544
  76.9 4.5 %collective-permute-start.34 = (bf16[256,128]{1,0:T(8,128)(2,1)S(1)}, bf16[256,128]{1,0:T(8,128)(2,1)S(1)}, u32[]{:S(2)}, u32[]{:S(2)}) collective-permute-start(bf16[256,128]{1,0:T(8,128)(2,1)S(1)} %halo.7.refs_0_), channel_id=1, source_target_pairs={{0,2},{1,3},{2,0},{3,1},{4,6},{5,7},{6,4},{7,5},{8,10},{9,11},{10,... | collective-permute-start | bytes 196616 | tf_op jit(solution)/shard_map/ppermute | solution.py:549
  79.1 3.2 %collective-permute-start.29 = (bf16[256,128]{1,0:T(8,128)(2,1)S(1)}, bf16[256,128]{1,0:T(8,128)(2,1)S(1)}, u32[]{:S(2)}, u32[]{:S(2)}) collective-permute-start(bf16[256,128]{1,0:T(8,128)(2,1)S(1)} %halo.6.refs_0_), channel_id=1, source_target_pairs={{0,2},{1,3},{2,0},{3,1},{4,6},{5,7},{6,4},{7,5},{8,10},{9,11},{10,... | collective-permute-start | bytes 196616 | tf_op jit(solution)/shard_map/ppermute | solution.py:549
  79.8 5.1 %collective-permute-start.36 = (bf16[256,128]{1,0:T(8,128)(2,1)S(1)}, bf16[256,128]{1,0:T(8,128)(2,1)S(1)}, u32[]{:S(2)}, u32[]{:S(2)}) collective-permute-start(bf16[256,128]{1,0:T(8,128)(2,1)S(1)} %halo.7.refs_0_), channel_id=1, source_target_pairs={{0,1},{1,0},{2,3},{3,2},{4,5},{5,4},{6,7},{7,6},{8,9},{9,8},{10,11... | collective-permute-start | bytes 196616 | tf_op jit(solution)/shard_map/ppermute | solution.py:549
  81.4 4.1 %collective-permute-start.35 = (bf16[256,128]{1,0:T(8,128)(2,1)S(1)}, bf16[256,128]{1,0:T(8,128)(2,1)S(1)}, u32[]{:S(2)}, u32[]{:S(2)}) collective-permute-start(bf16[256,128]{1,0:T(8,128)(2,1)S(1)} %collective-permute-done.34.refs_0_), channel_id=1, source_target_pairs={{0,1},{1,0},{2,3},{3,2},{4,5},{5,4},{6,7},{7,6},{8,9},{9,8},{10,11... | collective-permute-start | bytes 196616 | tf_op jit(solution)/shard_map/ppermute | solution.py:549
  82.1 3.7 %collective-permute-start.31 = (bf16[256,128]{1,0:T(8,128)(2,1)S(1)}, bf16[256,128]{1,0:T(8,128)(2,1)S(1)}, u32[]{:S(2)}, u32[]{:S(2)}) collective-permute-start(bf16[256,128]{1,0:T(8,128)(2,1)S(1)} %halo.6.refs_0_), channel_id=1, source_target_pairs={{0,1},{1,0},{2,3},{3,2},{4,5},{5,4},{6,7},{7,6},{8,9},{9,8},{10,11... | collective-permute-start | bytes 196616 | tf_op jit(solution)/shard_map/ppermute | solution.py:549
  82.2 4.1 %collective-permute-start.30 = (bf16[256,128]{1,0:T(8,128)(2,1)S(1)}, bf16[256,128]{1,0:T(8,128)(2,1)S(1)}, u32[]{:S(2)}, u32[]{:S(2)}) collective-permute-start(bf16[256,128]{1,0:T(8,128)(2,1)S(1)} %collective-permute-done.29.refs_0_), channel_id=1, source_target_pairs={{0,1},{1,0},{2,3},{3,2},{4,5},{5,4},{6,7},{7,6},{8,9},{9,8},{10,11... | collective-permute-start | bytes 196616 | tf_op jit(solution)/shard_map/ppermute | solution.py:549
